TPU v7x, 256 devices: a whole 4x4x8 slice. The times are simulated.
256 devices in a mesh: ep: 64 (over z, y, core), tp: 4 (over x).
Axes of the slice: x: 4, y: 4, z: 8, core: 2. Of those that a mesh axis runs over, the one named last changes fastest.
Arguments:
- query: bfloat16 [8192, 1536], P('ep', 'tp'), may hold values from -136 to 136
- latent: bfloat16 [8192, 512], P(('ep', 'tp')), may hold values from -6 to 6
- rope_key: bfloat16 [8192, 32], P(('ep', 'tp')), may hold values from -6 to 6
- latent_gain: float32 [512], replicated, may hold values from 0.1 to 1.9
- key_up: bfloat16 [512, 1024], P(None, 'tp'), may hold values from -0.25 to 0.25
- value_up: bfloat16 [512, 1024], P(None, 'tp'), may hold values from -2 to 2
- out_proj: bfloat16 [1024, 2048], replicated, may hold values from -0.1875 to 0.1875
- tokens: bfloat16 [16384, 2048], P(('ep', 'tp')), may hold values from -6 to 6
- moe_gain: float32 [2048], replicated, may hold values from 0.1 to 1.9
- routes: int32 [16384, 2], P(('ep', 'tp')), may hold values from 0 to 63, all different within a row; in each aligned block of 64 rows (0 to 63, 64 to 127, ...) at most 4 rows name the same one
- group_prob: float32 [16384], P(('ep', 'tp')), may hold values from 0.25 to 1
- expert_prob: float32 [16384, 2], P(('ep', 'tp')), may hold values from 0.02 to 1
- w_gate: bfloat16 [64, 2048, 1024], P('ep', None, 'tp'), may hold values from -0.125 to 0.125
- w_up: bfloat16 [64, 2048, 1024], P('ep', None, 'tp'), may hold values from -0.125 to 0.125
- w_down: bfloat16 [64, 1024, 2048], P('ep', 'tp'), may hold values from -0.1875 to 0.1875
Outputs:
- mixed: bfloat16 [8192, 2048], P(('ep', 'tp'))
- moe_out: bfloat16 [16384, 2048], P(('ep', 'tp'))
Inputs may be any that keep to these rules, and one draw needn't show every extreme that they name: `routes`: each row names 2 different experts; within the rows of one device no expert is named more than 4 times.
All inputs are finite; a program needn't handle non-finite values.
Results may differ from a plain program's by a relative error of at most 0.025.
Values may be sent and summed in bfloat16 or wider, within the bound.
No kernel may reach another device: no remote copies, remote signals or barrier semaphores. Data moves between devices by JAX's collectives and lax.ppermute only.
A program may use at most 128 MiB of HBM per device.

v0:
```python
import math

import jax
import jax.numpy as jnp
from jax import lax
from jax.sharding import PartitionSpec as P

NOPE = 64
ROPE_DIM = 32
V_DIM = 64


epsilon = 1e-06
rope_base = 10000.0
masked_value = -1e30


def in_one_piece(arrays, axis, dim, along):
    both = jnp.concatenate(arrays, axis=along)
    out, at, done = (lax.all_gather(both, axis, axis=dim, tiled=True), 0, [])
    for a in arrays:
        done.append(lax.slice_in_dim(out, at, at + a.shape[along], axis=along))
        at += a.shape[along]
    return tuple(done)


def split_up(value, dim, devices):
    before, after = (value.shape[:dim], value.shape[dim + 1 :])
    return jnp.moveaxis(value.reshape(*before, devices, -1, *after), dim, 0)


def sent_and_summed(value, axis, dim):
    devices = lax.axis_size(axis)
    parts = lax.all_to_all(split_up(value, dim, devices), axis, 0, 0, tiled=True)
    return jnp.sum(parts.astype(jnp.float32), axis=0)


def rms_scale(values, gain):
    widened = values.astype(jnp.float32)
    return widened * lax.rsqrt(jnp.mean(widened * widened, axis=-1, keepdims=True) + epsilon) * gain


def tables(positions, rope_width):
    half_width = rope_width // 2
    inverse = rope_base ** (-2.0 * jnp.arange(half_width, dtype=jnp.float32) / rope_width)
    angles = positions.astype(jnp.float32)[:, None] * inverse[None, :]
    return (jnp.cos(angles), jnp.sin(angles))


def rotate(values, cosine, sine):
    half_width = values.shape[-1] // 2
    lower = values[..., :half_width]
    upper = values[..., half_width:]
    return jnp.concatenate([lower * cosine - upper * sine, lower * sine + upper * cosine], axis=-1)


def keep_state(state_in):
    return state_in


def attend_block(running, query_rot, query_pos, key_part, value_part, rope_part):
    amount = key_part.shape[0]
    span_rows = math.gcd(amount, 1024)
    head_count = query_rot.shape[1]
    scale_factor = query_rot.shape[2] ** (-0.5)
    last_query = query_pos[-1]

    def update(state, block_at):
        row_begin = block_at * span_rows
        keys_here = lax.dynamic_slice_in_dim(key_part, row_begin, span_rows, 0).reshape(
            span_rows, head_count, -1
        )
        values_here = lax.dynamic_slice_in_dim(value_part, row_begin, span_rows, 0).reshape(
            span_rows, head_count, -1
        )
        rope_here = lax.dynamic_slice_in_dim(rope_part, row_begin, span_rows, 0)
        key_pos = row_begin + jnp.arange(span_rows, dtype=jnp.int32)

        def advance(state_in):
            top_old, totals, weighted = state_in
            shared = jnp.broadcast_to(
                rope_here[:, None, :], (span_rows, head_count, rope_here.shape[1])
            )
            full_keys = jnp.concatenate([keys_here, shared], axis=-1)
            scores = (
                jnp.einsum("qhd,khd->hqk", query_rot, full_keys, preferred_element_type=jnp.float32)
                * scale_factor
            )
            allowed = key_pos[None, :] <= query_pos[:, None]
            scores = jnp.where(allowed[None], scores, masked_value)
            top_new = jnp.maximum(top_old, jnp.max(scores, axis=-1))
            raised = jnp.where(allowed[None], jnp.exp(scores - top_new[..., None]), 0.0)
            factor = jnp.exp(top_old - top_new)
            totals = totals * factor + jnp.sum(raised, axis=-1)
            weighted = weighted * factor[..., None] + jnp.einsum(
                "hqk,khd->hqd",
                raised.astype(jnp.bfloat16),
                values_here,
                preferred_element_type=jnp.float32,
            )
            return (top_new, totals, weighted)

        return (lax.cond(key_pos[0] <= last_query, advance, keep_state, state), None)

    running, _ = lax.scan(update, running, jnp.arange(amount // span_rows))
    return running


def mixer_half(query, latent, rope_key, latent_gain, key_up, value_up, out_proj):
    query_rows = query.shape[0]
    own_rows = latent.shape[0]
    query_start = lax.axis_index("ep") * query_rows
    key_start = query_start + lax.axis_index("tp") * own_rows
    head_count = query.shape[1] // (NOPE + ROPE_DIM)
    normed = rms_scale(latent, latent_gain).astype(jnp.bfloat16)
    key_cos, key_sin = tables(key_start + jnp.arange(own_rows, dtype=jnp.int32), ROPE_DIM)
    rotated_key = rotate(rope_key.astype(jnp.float32), key_cos, key_sin).astype(jnp.bfloat16)
    query_pos = query_start + jnp.arange(query_rows, dtype=jnp.int32)
    query_cos, query_sin = tables(query_pos, ROPE_DIM)
    query_heads = query.reshape(query_rows, head_count, NOPE + ROPE_DIM)
    turned = rotate(
        query_heads[..., NOPE:].astype(jnp.float32), query_cos[:, None, :], query_sin[:, None, :]
    ).astype(jnp.bfloat16)
    query_rot = jnp.concatenate([query_heads[..., :NOPE], turned], axis=-1)
    last_query = query_start + query_rows - 1
    initial = (
        jnp.full((head_count, query_rows), masked_value, jnp.float32),
        jnp.zeros((head_count, query_rows), jnp.float32),
        jnp.zeros((head_count, query_rows, V_DIM), jnp.float32),
    )
    group_latent, group_rope = in_one_piece((normed, rotated_key), "tp", 0, 1)
    key_part = jnp.dot(group_latent, key_up, preferred_element_type=jnp.float32).astype(
        jnp.bfloat16
    )
    value_part = jnp.dot(group_latent, value_up, preferred_element_type=jnp.float32).astype(
        jnp.bfloat16
    )
    shard_rows = in_one_piece((key_part, value_part, group_rope), "ep", 0, 1)

    def compute(state_in):
        return attend_block(
            state_in, query_rot, query_pos, shard_rows[0], shard_rows[1], shard_rows[2]
        )

    running = lax.cond(jnp.int32(0) <= last_query, compute, keep_state, initial)
    totals = running[1]
    weighted = running[2]
    attention = (
        (weighted / totals[..., None])
        .transpose(1, 0, 2)
        .reshape(query_rows, head_count * V_DIM)
        .astype(jnp.bfloat16)
    )
    own_attention = lax.all_to_all(attention, "tp", split_axis=0, concat_axis=1, tiled=True)
    return jnp.dot(own_attention, out_proj, preferred_element_type=jnp.float32).astype(jnp.bfloat16)


def expert_half(tokens, moe_gain, routes, group_prob, expert_prob, w_gate, w_up, w_down):
    row_count, model_width = tokens.shape
    top_count = routes.shape[1]
    expert_count = lax.axis_size("ep")
    capacity = 2 * top_count * row_count // expert_count
    normed = rms_scale(tokens, moe_gain).astype(jnp.bfloat16)
    flat_routes = routes.reshape(-1)
    onehot = (flat_routes[:, None] == jnp.arange(expert_count, dtype=jnp.int32)[None, :]).astype(
        jnp.int32
    )
    earlier = jnp.cumsum(onehot, axis=0) - onehot
    slot_index = jnp.sum(earlier * onehot, axis=1)
    target = flat_routes * capacity + slot_index
    owner = target[None, :] == jnp.arange(expert_count * capacity, dtype=jnp.int32)[:, None]
    dispatch_table = jnp.any(
        owner.reshape(expert_count * capacity, row_count, top_count), axis=2
    ).astype(jnp.bfloat16)
    outgoing = jnp.dot(dispatch_table, normed, preferred_element_type=jnp.float32).astype(
        jnp.bfloat16
    )
    outgoing = outgoing.reshape(expert_count, capacity, model_width)
    arrived = lax.all_to_all(outgoing, "ep", split_axis=0, concat_axis=0, tiled=True)
    sources, slots, _ = arrived.shape
    flat_rows = arrived.reshape(sources * slots, model_width)
    shard_rows = lax.all_gather(flat_rows, "tp", axis=0, tiled=True)
    gate_values = jnp.dot(shard_rows, w_gate[0], preferred_element_type=jnp.float32)
    up_values = jnp.dot(shard_rows, w_up[0], preferred_element_type=jnp.float32)
    hidden = (jax.nn.silu(gate_values) * up_values).astype(jnp.bfloat16)

    def lower(offset, amount):
        return jnp.dot(hidden, w_down[0], preferred_element_type=jnp.float32)

    summed = sent_and_summed(
        lower(jnp.int32(0), sources * slots * lax.axis_size("tp")).astype(jnp.bfloat16), "tp", 0
    )
    result = summed.astype(jnp.bfloat16).reshape(sources, slots, model_width)
    returned = lax.all_to_all(result, "ep", split_axis=0, concat_axis=0, tiled=True)
    returned_flat = returned.reshape(expert_count * capacity, model_width)
    picked = returned_flat[target].reshape(row_count, top_count, model_width).astype(jnp.float32)
    shares = group_prob[:, None] * expert_prob / jnp.sum(expert_prob, axis=1, keepdims=True)
    return jnp.sum(shares[:, :, None] * picked, axis=1).astype(jnp.bfloat16)


def body(
    query,
    latent,
    rope_key,
    latent_gain,
    key_up,
    value_up,
    out_proj,
    tokens,
    moe_gain,
    routes,
    group_prob,
    expert_prob,
    w_gate,
    w_up,
    w_down,
):
    mixed = mixer_half(query, latent, rope_key, latent_gain, key_up, value_up, out_proj)
    moe_out = expert_half(tokens, moe_gain, routes, group_prob, expert_prob, w_gate, w_up, w_down)
    return (mixed, moe_out)


def solution(mesh):
    return jax.shard_map(
        body,
        mesh=mesh,
        in_specs=(
            P("ep", "tp"),
            P(("ep", "tp"), None),
            P(("ep", "tp"), None),
            P(),
            P(None, "tp"),
            P(None, "tp"),
            P(),
            P(("ep", "tp"), None),
            P(),
            P(("ep", "tp"), None),
            P(("ep", "tp")),
            P(("ep", "tp"), None),
            P("ep", None, "tp"),
            P("ep", None, "tp"),
            P("ep", "tp", None),
        ),
        out_specs=(P(("ep", "tp"), None), P(("ep", "tp"), None)),
        check_vma=False,
    )
```

profile of v0, /device:TPU:224, one launch (start us, length us, event | category | flops | bytes accessed | tf_op | source)
XLA Modules:
  0.0 333.0 jit_solution(12804921602035847933)
XLA Ops:
  7.2 0.8 copy.49
  9.0 1.1 fusion.27
  10.1 1.5 convolution_convert_fusion.1
  12.0 36.0 %all_to_all.31 = bf16[64,4,2048]{2,1,0:T(4,128)(2,1)S(1)} all-to-all(bf16[64,4,2048]{2,1,0:T(4,128)(2,1)S(1)} %reshape.209), channel_id=1, replica_groups=mesh['ep'=64,'tp'=4] {'ep'}, dimensions={0} | all-to-all | bytes 2097152 | tf_op jit(solution)/shard_map/all_to_all | solution.py:179
  48.1 1.1 reshape.210
  50.0 12.4 %all_gather.9 = bf16[128,544]{1,0:T(8,128)(2,1)S(1)} all-gather(bf16[32,544]{1,0:T(8,128)(2,1)S(1)} %pad_maximum_fusion.2), channel_id=1, replica_groups=mesh['ep'=64,'tp'=4] {'tp'}, dimensions={0}, use_global_device_ids=true | all-gather | bytes 174080 | tf_op jit(solution)/shard_map/all_gather | solution.py:20
  62.8 0.7 pad_maximum_fusion
  63.6 35.2 %all-gather.5.cloned.1.call-done = bf16[1024,2048]{1,0:T(8,128)(2,1)} async-done(((bf16[256,2048]{1,0:T(8,128)(2,1)}), bf16[1024,2048]{1,0:T(8,128)(2,1)}) %all-gather.5.cloned.1.call-update) | async-done | bytes 4194320 | tf_op jit(solution)/shard_map/all_gather | solution.py:182
  98.8 4.4 %fusion.20 = f32[1024,256]{1,0:T(8,128)} fusion(bf16[1024,2048]{1,0:T(8,128)(2,1)} %all-gather.5.cloned.1.call-done, bf16[1,2048,256]{2,1,0:T(8,128)(2,1)S(1)} %copy-done.9), kind=kOutput, calls=%fused_computation.36 | convolution fusion | flops 1073741824 | bytes 6291456 | tf_op jit(solution)/shard_map/dot_general | solution.py:183
  103.2 8.8 %convolution_convert_fusion = bf16[1024,2048]{1,0:T(8,128)(2,1)} fusion(bf16[1024,2048]{1,0:T(8,128)(2,1)} %all-gather.5.cloned.1.call-done, bf16[1,256,2048]{2,1,0:T(8,128)(2,1)S(1)} %copy-done, bf16[1,2048,256]{2,1,0:T(8,128)(2,1)S(1)} %copy-done.10, f32[1024,256]{1,0:T(8,128)} %fusion.20), kind=kOutput, calls=%fused_computation.27 | convolution fusion | flops 2151153664 | bytes 11534336 | tf_op jit(solution)/shard_map/dot_general | solution.py:188
  112.0 54.6 %all_to_all.32 = bf16[4,256,2048]{2,1,0:T(8,128)(2,1)} all-to-all(bf16[4,256,2048]{2,1,0:T(8,128)(2,1)} %bitcast.54), channel_id=1, replica_groups=mesh['ep'=64,'tp'=4] {'tp'}, dimensions={0} | all-to-all | bytes 8388608 | tf_op jit(solution)/shard_map/all_to_all | solution.py:34
  166.6 3.4 %reduce_sum.78 = bf16[256,2048]{1,0:T(8,128)(2,1)S(1)} reduce(bf16[4,256,2048]{2,1,0:T(8,128)(2,1)} %all_to_all.32, bf16[]{:T(256)} %constant.106.clone.1), dimensions={0}, to_apply=%region_14.15 | reduce | flops 1572864 | bytes 5242882 | tf_op jit(solution)/shard_map/reduce_sum | solution.py:35
  170.1 1.2 reshape.212
  171.3 10.0 %all-to-all-start.3 = ((bf16[64,4,2048]{2,1,0:T(4,128)(2,1)}), bf16[64,4,2048]{2,1,0:T(4,128)(2,1)S(1)}, u32[]{:S(2)}, u32[]{:S(2)}) async-start(bf16[64,4,2048]{2,1,0:T(4,128)(2,1)} %reshape.212), calls=%async_computation.3 | async-start | bytes 2097152 | tf_op jit(solution)/shard_map/all_to_all | solution.py:194
  181.9 26.5 %all-to-all-done.3 = bf16[64,4,2048]{2,1,0:T(4,128)(2,1)S(1)} async-done(((bf16[64,4,2048]{2,1,0:T(4,128)(2,1)}), bf16[64,4,2048]{2,1,0:T(4,128)(2,1)S(1)}, u32[]{:S(2)}, u32[]{:S(2)}) %all-to-all-start.3) | async-done | bytes 1048608 | tf_op jit(solution)/shard_map/all_to_all | solution.py:194
  208.7 0.9 gather_fusion
  209.7 0.7 reshape.214
  210.4 101.0 %conditional.2 = (f32[4,128]{1,0:T(4,128)}, f32[4,128,64]{1,2,0:T(8,128)}) conditional(s32[]{:T(128)} %convert_element_type.89, () %tuple.36, (bf16[8192,544]{1,0:T(8,128)(2,1)}, s32[]{:T(128)}, s32[128]{0:T(128)S(1)}, bf16[128,4,96]{0,2,1:T(8,128)(2,1)S(1)}) %tuple.37), branch_computations={%region_1.0_spmd, %region_2.9_spmd} | conditional | flops 176359552 | bytes 46872600 | solution.py:145
  210.4 12.9 %copy.45 = bf16[8192,544]{0,1:T(8,128)(2,1)} copy(bf16[8192,544]{1,0:T(8,128)(2,1)} %get-tuple-element.221) | data formatting | bytes 17825792 | tf_op jit(solution)/shard_map
  223.3 6.1 %fusion.53 = (bf16[8192,256]{0,1:T(8,128)(2,1)}, bf16[8192,256]{0,1:T(8,128)(2,1)}) fusion(bf16[8192,544]{0,1:T(8,128)(2,1)} %copy.45), kind=kLoop, calls=%fused_computation.97 | loop fusion | bytes 16777216 | tf_op jit(solution)/shard_map/slice | solution.py:22
  229.4 1.1 slice.53
  231.1 0.7 broadcast_in_dim.75
  232.3 79.0 %while.13 = (s32[]{:T(128)}, f32[4,128]{1,0:T(4,128)S(1)}, f32[4,128]{1,0:T(4,128)}, f32[4,128,64]{1,2,0:T(8,128)}, s32[8]{0:T(128)S(1)}, /*index=5*/s32[]{:T(12...) while((s32[]{:T(128)}, f32[4,128]{1,0:T(4,128)S(1)}, ...), condition=%wide.region_8.8_spmd, body=%wide.region_3.7_spmd.sunk | while | flops 176359424 | bytes 11084641 | solution.py:105
  235.2 7.0 %conditional.4 = ((f32[4,128]{1,0:T(4,128)S(1)}, f32[4,128]{1,0:T(4,128)}, f32[4,128,64]{1,2,0:T(8,128)})) conditional(s32[]{:T(128)} %convert_element_type.152, (f32[4,128]{1,0:T(4,128)S(1)}, f32[4,128]{1,0:T(4,128)}, f32[4,128,64]{1,2,0:T(8,128)}) %tuple.61, (s32[1024]{0:T(1024)S(1)}, s32[128]{0:T(128)S(1)}, s32[]{:T(128)}, ...), branch_computations={%region_4.3_spmd, %region_5.6_spmd} | conditional | flops 176358400 | bytes 11080266 | solution.py:103
  235.2 1.9 constant_dynamic-slice_fusion
  238.6 1.3 multiply_add_fusion
  239.9 2.3 convolution_add_fusion
  245.1 7.0 %conditional.4 = ((f32[4,128]{1,0:T(4,128)S(1)}, f32[4,128]{1,0:T(4,128)}, f32[4,128,64]{1,2,0:T(8,128)})) conditional(s32[]{:T(128)} %convert_element_type.152, (f32[4,128]{1,0:T(4,128)S(1)}, f32[4,128]{1,0:T(4,128)}, f32[4,128,64]{1,2,0:T(8,128)}) %tuple.61, (s32[1024]{0:T(1024)S(1)}, s32[128]{0:T(128)S(1)}, s32[]{:T(128)}, ...), branch_computations={%region_4.3_spmd, %region_5.6_spmd} | conditional | flops 176358400 | bytes 11080266 | solution.py:103
  245.1 1.9 constant_dynamic-slice_fusion
  247.3 0.6 fusion
  248.5 1.3 multiply_add_fusion
  249.8 2.3 convolution_add_fusion
  255.0 7.0 %conditional.4 = ((f32[4,128]{1,0:T(4,128)S(1)}, f32[4,128]{1,0:T(4,128)}, f32[4,128,64]{1,2,0:T(8,128)})) conditional(s32[]{:T(128)} %convert_element_type.152, (f32[4,128]{1,0:T(4,128)S(1)}, f32[4,128]{1,0:T(4,128)}, f32[4,128,64]{1,2,0:T(8,128)}) %tuple.61, (s32[1024]{0:T(1024)S(1)}, s32[128]{0:T(128)S(1)}, s32[]{:T(128)}, ...), branch_computations={%region_4.3_spmd, %region_5.6_spmd} | conditional | flops 176358400 | bytes 11080266 | solution.py:103
  255.0 1.9 constant_dynamic-slice_fusion
  258.4 1.3 multiply_add_fusion
  259.7 2.3 convolution_add_fusion
  264.9 7.0 %conditional.4 = ((f32[4,128]{1,0:T(4,128)S(1)}, f32[4,128]{1,0:T(4,128)}, f32[4,128,64]{1,2,0:T(8,128)})) conditional(s32[]{:T(128)} %convert_element_type.152, (f32[4,128]{1,0:T(4,128)S(1)}, f32[4,128]{1,0:T(4,128)}, f32[4,128,64]{1,2,0:T(8,128)}) %tuple.61, (s32[1024]{0:T(1024)S(1)}, s32[128]{0:T(128)S(1)}, s32[]{:T(128)}, ...), branch_computations={%region_4.3_spmd, %region_5.6_spmd} | conditional | flops 176358400 | bytes 11080266 | solution.py:103
  264.9 1.9 constant_dynamic-slice_fusion
  267.1 0.6 fusion
  268.3 1.3 multiply_add_fusion
  269.6 2.3 convolution_add_fusion
  274.8 7.0 %conditional.4 = ((f32[4,128]{1,0:T(4,128)S(1)}, f32[4,128]{1,0:T(4,128)}, f32[4,128,64]{1,2,0:T(8,128)})) conditional(s32[]{:T(128)} %convert_element_type.152, (f32[4,128]{1,0:T(4,128)S(1)}, f32[4,128]{1,0:T(4,128)}, f32[4,128,64]{1,2,0:T(8,128)}) %tuple.61, (s32[1024]{0:T(1024)S(1)}, s32[128]{0:T(128)S(1)}, s32[]{:T(128)}, ...), branch_computations={%region_4.3_spmd, %region_5.6_spmd} | conditional | flops 176358400 | bytes 11080266 | solution.py:103
  274.8 1.9 constant_dynamic-slice_fusion
  278.2 1.3 multiply_add_fusion
  279.4 2.3 convolution_add_fusion
  284.6 7.0 %conditional.4 = ((f32[4,128]{1,0:T(4,128)S(1)}, f32[4,128]{1,0:T(4,128)}, f32[4,128,64]{1,2,0:T(8,128)})) conditional(s32[]{:T(128)} %convert_element_type.152, (f32[4,128]{1,0:T(4,128)S(1)}, f32[4,128]{1,0:T(4,128)}, f32[4,128,64]{1,2,0:T(8,128)}) %tuple.61, (s32[1024]{0:T(1024)S(1)}, s32[128]{0:T(128)S(1)}, s32[]{:T(128)}, ...), branch_computations={%region_4.3_spmd, %region_5.6_spmd} | conditional | flops 176358400 | bytes 11080266 | solution.py:103
  284.7 1.9 constant_dynamic-slice_fusion
  286.9 0.6 fusion
  288.1 1.3 multiply_add_fusion
  289.3 2.3 convolution_add_fusion
  294.5 7.0 %conditional.4 = ((f32[4,128]{1,0:T(4,128)S(1)}, f32[4,128]{1,0:T(4,128)}, f32[4,128,64]{1,2,0:T(8,128)})) conditional(s32[]{:T(128)} %convert_element_type.152, (f32[4,128]{1,0:T(4,128)S(1)}, f32[4,128]{1,0:T(4,128)}, f32[4,128,64]{1,2,0:T(8,128)}) %tuple.61, (s32[1024]{0:T(1024)S(1)}, s32[128]{0:T(128)S(1)}, s32[]{:T(128)}, ...), branch_computations={%region_4.3_spmd, %region_5.6_spmd} | conditional | flops 176358400 | bytes 11080266 | solution.py:103
  294.5 1.9 constant_dynamic-slice_fusion
  297.9 1.3 multiply_add_fusion
  299.2 2.3 convolution_add_fusion
  304.4 6.9 %conditional.4 = ((f32[4,128]{1,0:T(4,128)S(1)}, f32[4,128]{1,0:T(4,128)}, f32[4,128,64]{1,2,0:T(8,128)})) conditional(s32[]{:T(128)} %convert_element_type.152, (f32[4,128]{1,0:T(4,128)S(1)}, f32[4,128]{1,0:T(4,128)}, f32[4,128,64]{1,2,0:T(8,128)}) %tuple.61, (s32[1024]{0:T(1024)S(1)}, s32[128]{0:T(128)S(1)}, s32[]{:T(128)}, ...), branch_computations={%region_4.3_spmd, %region_5.6_spmd} | conditional | flops 176358400 | bytes 11080266 | solution.py:103
  304.4 1.8 constant_dynamic-slice_fusion
  307.8 1.3 multiply_add_fusion
  309.1 2.3 convolution_add_fusion
  311.3 0.9 fusion.41
  312.4 0.8 convert_element_type.100
  313.2 3.7 %all-to-all-start = ((bf16[4,32,256]{2,1,0:T(8,128)(2,1)}), bf16[4,32,256]{2,1,0:T(8,128)(2,1)S(1)}, u32[]{:S(2)}, u32[]{:S(2)}) async-start(bf16[4,32,256]{2,1,0:T(8,128)(2,1)} %convert_element_type.100), calls=%async_computation | async-start | bytes 131072 | tf_op jit(solution)/shard_map/all_to_all | solution.py:154
  316.9 2.2 multiply_reduce_fusion
  319.1 3.4 %all-to-all-done = bf16[4,32,256]{2,1,0:T(8,128)(2,1)S(1)} async-done(((bf16[4,32,256]{2,1,0:T(8,128)(2,1)}), bf16[4,32,256]{2,1,0:T(8,128)(2,1)S(1)}, u32[]{:S(2)}, u32[]{:S(2)}) %all-to-all-start) | async-done | bytes 65568 | tf_op jit(solution)/shard_map/all_to_all | solution.py:154
  322.5 3.7 %convolution_convert_fusion.2 = bf16[32,2048]{1,0:T(8,128)(2,1)} fusion(bf16[32,1024]{1,0:T(8,128)(2,1)S(1)} %bitcast.57, bf16[1024,2048]{1,0:T(8,128)(2,1)} %param.27), kind=kOutput, calls=%fused_computation.29 | convolution fusion | flops 134283264 | bytes 4390912 | tf_op jit(solution)/shard_map/dot_general | solution.py:155
  (150 shorter events, 23.5 us)
Async XLA Ops:
  7.2 96.0 %copy-start = (bf16[1,256,2048]{2,1,0:T(8,128)(2,1)S(1)}, bf16[1,256,2048]{2,1,0:T(8,128)(2,1)}, u32[]{:S(2)}) copy-start(bf16[1,256,2048]{2,1,0:T(8,128)(2,1)} %param.35) | copy-start | bytes 3145732
  7.2 91.6 %all-gather.5.cloned.1.call-start = ((), (), s32[]{:S(2)}) async-start(), calls=%async_computation.5 | async-start | bytes 5242880 | tf_op jit(solution)/shard_map/all_gather | solution.py:182
  48.0 1.3 copy-start.5
  48.0 1.7 copy-start.3
  48.0 1.8 copy-start.7
  48.1 14.4 %copy-start.1 = (bf16[512,256]{1,0:T(8,128)(2,1)S(1)}, bf16[512,256]{1,0:T(8,128)(2,1)}, u32[]{:S(2)}) copy-start(bf16[512,256]{1,0:T(8,128)(2,1)} %param.26) | copy-start | bytes 786436
  48.1 14.6 %copy-start.2 = (bf16[512,256]{1,0:T(8,128)(2,1)S(1)}, bf16[512,256]{1,0:T(8,128)(2,1)}, u32[]{:S(2)}) copy-start(bf16[512,256]{1,0:T(8,128)(2,1)} %param.25) | copy-start | bytes 786436
  49.2 49.6 %copy-start.9 = (bf16[1,2048,256]{2,1,0:T(8,128)(2,1)S(1)}, bf16[1,2048,256]{2,1,0:T(8,128)(2,1)}, u32[]{:S(2)}) copy-start(bf16[1,2048,256]{2,1,0:T(8,128)(2,1)} %param.33) | copy-start | bytes 3145732
  49.2 161.1 %all-gather.3.cloned.1.call-start = ((), (), s32[]{:S(2)}) async-start(), calls=%async_computation.4 | async-start | bytes 10649600 | tf_op jit(solution)/shard_map/all_gather | solution.py:20
  63.5 39.7 %copy-start.10 = (bf16[1,2048,256]{2,1,0:T(8,128)(2,1)S(1)}, bf16[1,2048,256]{2,1,0:T(8,128)(2,1)}, u32[]{:S(2)}) copy-start(bf16[1,2048,256]{2,1,0:T(8,128)(2,1)} %param.34) | copy-start | bytes 3145732
  170.0 11.3 %copy-start.4 = (bf16[128,384]{1,0:T(8,128)(2,1)S(1)}, bf16[128,384]{1,0:T(8,128)(2,1)}, u32[]{:S(2)}) copy-start(bf16[128,384]{1,0:T(8,128)(2,1)} %param.21) | copy-start | bytes 294916
  170.0 11.6 %copy-start.6 = (f32[64,2]{0,1:T(2,128)S(1)}, f32[64,2]{0,1:T(2,128)}, u32[]{:S(2)}) copy-start(f32[64,2]{0,1:T(2,128)} %param.32) | copy-start | bytes 1540
  170.0 11.6 %copy-start.8 = (f32[64]{0:T(128)S(1)}, f32[64]{0:T(128)}, u32[]{:S(2)}) copy-start(f32[64]{0:T(128)} %param.31) | copy-start | bytes 772
  171.3 37.2 %all-to-all-start.3 = ((bf16[64,4,2048]{2,1,0:T(4,128)(2,1)}), bf16[64,4,2048]{2,1,0:T(4,128)(2,1)S(1)}, u32[]{:S(2)}, u32[]{:S(2)}) async-start(bf16[64,4,2048]{2,1,0:T(4,128)(2,1)} %reshape.212), calls=%async_computation.3 | async-start | bytes 2097152 | tf_op jit(solution)/shard_map/all_to_all | solution.py:194
  313.2 9.3 %all-to-all-start = ((bf16[4,32,256]{2,1,0:T(8,128)(2,1)}), bf16[4,32,256]{2,1,0:T(8,128)(2,1)S(1)}, u32[]{:S(2)}, u32[]{:S(2)}) async-start(bf16[4,32,256]{2,1,0:T(8,128)(2,1)} %convert_element_type.100), calls=%async_computation | async-start | bytes 131072 | tf_op jit(solution)/shard_map/all_to_all | solution.py:154
Sparse Core Ops, SparseCore 0:
  49.4 49.3 all-gather.4
  102.1 91.5 all-gather.2
where the time goes:
time: 335 us; the launch traced here: 333 us
  blocking collectives  103 us (31%)
  waiting for transfers between devices  65.2 us (19%)
  local copies, waits for them, and re-layouts  54 us (16%)
  matrix products  42 us (13%)
  other arithmetic  25.7 us (8%)
  loops' own time  15 us (4%)
  between operations  14.4 us (4%)
  starting transfers between devices  13.8 us (4%)
    all_to_all x1, blocking collectives, sent_and_summed(): lax.all_to_all(split_up(value, dim, devices), axis, 0, 0, tiled=True)  54.6 us
    all_to_all x1, blocking collectives, expert_half(): lax.all_to_all(outgoing, 'ep', split_axis=0, concat_axis=0, tiled=True)  36 us
    all_gather x1, waiting for transfers between devices, expert_half(): shard_rows = lax.all_gather(flat_rows, 'tp', axis=0, tiled=True)  35.2 us
    all_to_all x1, waiting for transfers between devices, expert_half(): lax.all_to_all(result, 'ep', split_axis=0, concat_axis=0, tiled=True)  26.5 us
    dot_general x8, matrix products, advance(): jnp.einsum('hqk,khd->hqd', raised.astype(jnp.bfloat16), values_here, pref...  18.2 us
    dynamic_slice x8, local copies, waits for them, and re-layouts, update(): lax.dynamic_slice_in_dim(value_part, row_begin, span_rows, 0)  15 us
    another operation x1, loops' own time, attend_block(): running, _ = lax.scan(update, running, jnp.arange(amount // span_rows))  14.5 us
    another operation x3, local copies, waits for them, and re-layouts  13.1 us
  transfers between devices with their start and end apart: 4, of which 3 were waited for; matrix products, arithmetic and copies ran while one was open for 7% of the time, Pallas kernels for 0%

commit v1 on v0

v1 whole, which is shorter than its diff:
```python
import functools

import jax
import jax.numpy as jnp
from jax import lax
from jax.experimental import pallas as pl
from jax.experimental.pallas import tpu as pltpu
from jax.sharding import Mesh, PartitionSpec as P

NOPE = 64
ROPE_DIM = 32
V_DIM = 64
QK_DIM = NOPE + ROPE_DIM
KV_ROWS = QK_DIM + V_DIM
CAP = 4
BF = jnp.bfloat16
F32 = jnp.float32

epsilon = 1e-06
rope_base = 10000.0
masked_value = -1e30
log2_e = 1.4426950408889634

SMEM_SPEC = pl.BlockSpec(memory_space=pltpu.SMEM)


def mm(a, b, dims=((1,), (0,))):
    return lax.dot_general(a, b, (dims, ((), ())), preferred_element_type=F32)


def shifted(value, axis, amount):
    n = lax.axis_size(axis)
    return lax.ppermute(value, axis, [(i, (i + amount) % n) for i in range(n)])


def trig(positions):
    half = ROPE_DIM // 2
    inverse = rope_base ** (-2.0 * jnp.arange(half, dtype=F32) / ROPE_DIM)
    angles = positions.astype(F32)[:, None] * inverse[None, :]
    return jnp.cos(angles), jnp.sin(angles)


def rms_scale(values, gain):
    widened = values.astype(F32)
    return widened * lax.rsqrt(jnp.mean(widened * widened, axis=-1, keepdims=True) + epsilon) * gain


def dispatch_kernel(tokens, gain, routes, group_prob, expert_prob, outgoing, shares_out):
    rows = tokens.shape[0]
    slots = outgoing.shape[0]
    normed = rms_scale(tokens[...], gain[...]).astype(BF)
    slot = lax.broadcasted_iota(jnp.int32, (rows, slots), 1)
    expert = slot // CAP
    first = routes[:, 0:1] == expert
    second = routes[:, 1:2] == expert
    named = (first | second).astype(BF)
    before = lax.broadcasted_iota(jnp.int32, (rows, rows), 1) < lax.broadcasted_iota(
        jnp.int32, (rows, rows), 0
    )
    prior = mm(before.astype(BF), named)
    mine = (first | second) & (prior == (slot % CAP).astype(F32))
    outgoing[...] = mm(mine.astype(BF), normed, ((0,), (0,))).astype(BF)
    probs = expert_prob[...]
    shares = group_prob[...] * probs / jnp.sum(probs, axis=1, keepdims=True)
    weights = jnp.where(first, shares[:, 0:1], shares[:, 1:2])
    weights = jnp.where(mine, weights, 0.0)
    high = weights.astype(BF)
    shares_out[0:rows, :] = high
    shares_out[rows : 2 * rows, :] = (weights - high.astype(F32)).astype(BF)


def dispatch(tokens, gain, routes, group_prob, expert_prob, slots):
    rows, width = tokens.shape
    return pl.pallas_call(
        dispatch_kernel,
        out_shape=(
            jax.ShapeDtypeStruct((slots, width), BF),
            jax.ShapeDtypeStruct((2 * rows, slots), BF),
        ),
        name="dispatch",
    )(tokens, gain[None, :], routes, group_prob[:, None], expert_prob)


def hidden_kernel(rows, w_gate, w_up, out):
    gate = mm(rows[...], w_gate[...])
    up = mm(rows[...], w_up[...])
    out[...] = (gate / (1.0 + jnp.exp(-gate)) * up).astype(BF)


def hidden_of(rows, w_gate, w_up, name):
    return pl.pallas_call(
        hidden_kernel,
        out_shape=jax.ShapeDtypeStruct((rows.shape[0], w_gate.shape[1]), BF),
        name=name,
    )(rows, w_gate, w_up)


def down_kernel(h0, h1, h2, h3, w0, w1, w2a, w2b, w3, out):
    half = w2a.shape[0]
    total = mm(h0[...], w0[...]) + mm(h1[...], w1[...]) + mm(h3[...], w3[...])
    total = total + mm(h2[:, :half], w2a[...]) + mm(h2[:, half:], w2b[...])
    out[...] = total.astype(BF)


def combine_kernel(returned, shares, out):
    rows = out.shape[0]
    both = mm(shares[...], returned[...])
    out[...] = (both[:rows] + both[rows:]).astype(BF)


def ring_gathered(value):
    half = value.shape[0] // 2
    left = shifted(value, "x", 1)
    right = shifted(value, "x", -1)
    far_a = shifted(left[:half], "x", 1)
    far_b = shifted(right[half:], "x", -1)
    return left, right, far_a, far_b


def expert_half(tokens, moe_gain, routes, group_prob, expert_prob, w_gate, w_up, w_down):
    ep_axes = ("z", "y", "c")
    experts = lax.axis_size(ep_axes)
    rows, width = tokens.shape
    slots = experts * CAP
    w_gate, w_up, w_down = w_gate[0], w_up[0], w_down[0]
    down_left, down_right, down_far_a, down_far_b = ring_gathered(w_down)
    outgoing, shares = dispatch(tokens, moe_gain, routes, group_prob, expert_prob, slots)
    arrived = lax.all_to_all(
        outgoing.reshape(experts, CAP, width), ep_axes, split_axis=0, concat_axis=0, tiled=True
    ).reshape(slots, width)
    left, right, far_a, far_b = ring_gathered(arrived)
    own_hidden = hidden_of(arrived, w_gate, w_up, "hidden_own")
    left_hidden = hidden_of(left, w_gate, w_up, "hidden_left")
    right_hidden = hidden_of(right, w_gate, w_up, "hidden_right")
    far_hidden = hidden_of(jnp.concatenate([far_a, far_b], axis=0), w_gate, w_up, "hidden_far")
    from_right = shifted(left_hidden, "x", -1)
    from_left = shifted(right_hidden, "x", 1)
    from_far = shifted(far_hidden, "x", 2)
    result = pl.pallas_call(
        down_kernel, out_shape=jax.ShapeDtypeStruct((slots, width), BF), name="down"
    )(
        own_hidden,
        from_right,
        from_far,
        from_left,
        w_down,
        down_right,
        down_far_a,
        down_far_b,
        down_left,
    )
    returned = lax.all_to_all(
        result.reshape(experts, CAP, width), ep_axes, split_axis=0, concat_axis=0, tiled=True
    ).reshape(slots, width)
    return pl.pallas_call(
        combine_kernel, out_shape=jax.ShapeDtypeStruct((rows, width), BF), name="combine"
    )(returned, shares)


def query_kernel(where, query, cosine, sine, o0, o1, o2, o3, heads):
    count = heads.shape[0]
    turned = query[...].astype(F32).T
    for h in range(count):
        at = h * QK_DIM
        half = ROPE_DIM // 2
        a = turned[at + NOPE : at + NOPE + half]
        b = turned[at + NOPE + half : at + QK_DIM]
        heads[h, :NOPE, :] = turned[at : at + NOPE].astype(BF)
        heads[h, NOPE : NOPE + half, :] = (a * cosine[...] - b * sine[...]).astype(BF)
        heads[h, NOPE + half :, :] = (a * sine[...] + b * cosine[...]).astype(BF)
    for k, out in enumerate((o0, o1, o2, o3)):
        out[...] = heads[lax.rem(where[1] + k, 4)]


def keys_kernel(where, l0, l1, l2, l3, key_up, value_up, out, keys, values):
    latent = key_up.shape[0]
    strip = l0.shape[0]
    eye = (
        lax.broadcasted_iota(jnp.int32, (ROPE_DIM, ROPE_DIM), 0)
        == lax.broadcasted_iota(jnp.int32, (ROPE_DIM, ROPE_DIM), 1)
    ).astype(BF)
    for j, block in enumerate((l0, l1, l2, l3)):
        cols = slice(j * strip, (j + 1) * strip)
        got = block[:, :latent]
        keys[:, :, cols] = (
            mm(key_up[...], got, ((0,), (1,))).astype(BF).reshape(keys.shape[0], NOPE, strip)
        )
        values[:, :, cols] = (
            mm(value_up[...], got, ((0,), (1,))).astype(BF).reshape(values.shape[0], V_DIM, strip)
        )
        out[NOPE:QK_DIM, cols] = mm(eye, block[:, latent:], ((1,), (1,))).astype(BF)
    out[:NOPE, :] = keys[where[1]]
    out[QK_DIM:, :] = values[where[1]]


def attend_kernel(where, q0, q1, q2, q3, kv, o0, o1, o2, o3, q_s, top_s, acc_s):
    step = pl.program_id(0)
    z, y, c, x = where[0], where[1], where[2], where[3]
    strip = q0.shape[1]
    span = kv.shape[2]
    factor = QK_DIM ** (-0.5) * log2_e

    @pl.when(step == 0)
    def _():
        for j, q in enumerate((q0, q1, q2, q3)):
            q_s[j] = q[...].astype(F32).T.astype(BF)
        top_s[...] = jnp.full(top_s.shape, masked_value, F32)
        acc_s[...] = jnp.zeros(acc_s.shape, F32)

    def advance(masked):
        ones = jnp.ones((V_DIM, span), BF)
        extended = [jnp.concatenate([kv[p, QK_DIM:, :], ones], axis=0) for p in range(2)]
        if masked:
            col = lax.broadcasted_iota(jnp.int32, (1, span), 1)
            col_y = (y - col // strip + 4) % 4
            col_x = (x - (col // 32) % 4 + 4) % 4
            key_at = [(col_y * 2 + p) * strip + col_x * 32 + col % 32 for p in range(2)]
            row = lax.broadcasted_iota(jnp.int32, (strip, 1), 0)
        for j in range(4):
            q = q_s[j]
            scores = [mm(q, kv[p, :QK_DIM, :]) for p in range(2)]
            if masked:
                query_at = (lax.rem(y - j + 4, 4) * 2 + c) * strip + row
                scores = [
                    jnp.where(key_at[p] <= query_at, scores[p], masked_value) for p in range(2)
                ]
            old = top_s[j]
            peak = jnp.maximum(
                jnp.max(scores[0], axis=1, keepdims=True),
                jnp.max(scores[1], axis=1, keepdims=True),
            )
            new = jnp.maximum(old, peak)
            top_s[j] = new
            base = new[:, :1]
            total = acc_s[j] * jnp.exp2((old - new) * factor)
            for p in range(2):
                raised = jnp.exp2((scores[p] - base) * factor).astype(BF)
                total = total + mm(raised, extended[p], ((1,), (1,)))
            acc_s[j] = total

    pl.when(step < z)(functools.partial(advance, False))
    pl.when(step == z)(functools.partial(advance, True))

    @pl.when(step == pl.num_programs(0) - 1)
    def _():
        for j, out in enumerate((o0, o1, o2, o3)):
            total = acc_s[j]
            out[...] = (total[:, :V_DIM] / total[:, V_DIM:]).astype(BF)


def attend(where, queries, kv):
    blocks, rows, span = kv.shape
    strip = queries[0].shape[1]
    steps = blocks // 2
    whole = pl.BlockSpec((QK_DIM, strip), lambda s, w: (0, 0))
    return pl.pallas_call(
        attend_kernel,
        grid_spec=pltpu.PrefetchScalarGridSpec(
            num_scalar_prefetch=1,
            grid=(steps,),
            in_specs=[whole] * 4
            + [pl.BlockSpec((2, rows, span), lambda s, w: (jnp.minimum(s, w[0]), 0, 0))],
            out_specs=[pl.BlockSpec((strip, V_DIM), lambda s, w: (0, 0))] * 4,
            scratch_shapes=[
                pltpu.VMEM((4, strip, QK_DIM), BF),
                pltpu.VMEM((4, strip, 128), F32),
                pltpu.VMEM((4, strip, 128), F32),
            ],
        ),
        out_shape=[jax.ShapeDtypeStruct((strip, V_DIM), BF)] * 4,
        name="attend",
    )(where, *queries, kv)


def spread_kernel(where, a0, a1, a2, a3, o0, o1, o2, o3, heads, parts):
    for j, a in enumerate((a0, a1, a2, a3)):
        heads[lax.rem(where[1] + j, 4)] = a[...]
    beside = jnp.concatenate([heads[h] for h in range(4)], axis=1)
    parts[...] = beside.reshape(parts.shape)
    for k, out in enumerate((o0, o1, o2, o3)):
        out[...] = parts[lax.rem(where[3] + k, 4)]


def project_kernel(where, a0, a1, a2, a3, out_proj, out, parts):
    width = a0.shape[1]
    for k, a in enumerate((a0, a1, a2, a3)):
        parts[lax.rem(where[3] - k + 4, 4)] = a[...]
    total = mm(parts[0], out_proj[:width, :])
    for h in range(1, 4):
        total = total + mm(parts[h], out_proj[h * width : (h + 1) * width, :])
    out[...] = total.astype(BF)


def mixer_half(where, query, latent, rope_key, latent_gain, key_up, value_up, out_proj):
    strip = query.shape[0]
    own = latent.shape[0]
    query_start = ((where[0] * 4 + where[1]) * 2 + where[2]) * strip
    vmem = pl.BlockSpec(memory_space=pltpu.VMEM)

    cosine, sine = trig(query_start + jnp.arange(strip, dtype=jnp.int32))
    shape = jax.ShapeDtypeStruct((QK_DIM, strip), BF)
    blocks = pl.pallas_call(
        query_kernel,
        in_specs=[SMEM_SPEC, vmem, vmem, vmem],
        out_shape=[shape] * 4,
        scratch_shapes=[pltpu.VMEM((4, QK_DIM, strip), BF)],
        name="queries",
    )(where, query, cosine.T, sine.T)
    queries = [blocks[0]] + [shifted(blocks[k], "y", k) for k in range(1, 4)]

    normed = rms_scale(latent, latent_gain).astype(BF)
    key_cos, key_sin = trig(query_start + where[3] * own + jnp.arange(own, dtype=jnp.int32))
    half = ROPE_DIM // 2
    a = rope_key[:, :half].astype(F32)
    b = rope_key[:, half:].astype(F32)
    both = jnp.concatenate(
        [
            normed,
            (a * key_cos - b * key_sin).astype(BF),
            (a * key_sin + b * key_cos).astype(BF),
        ],
        axis=1,
    )
    near = jnp.concatenate([both] + [shifted(both, "x", k) for k in range(1, 4)], axis=0)
    latents = [near] + [shifted(near, "y", k) for k in range(1, 4)]
    kv = pl.pallas_call(
        keys_kernel,
        in_specs=[SMEM_SPEC] + [vmem] * 6,
        out_shape=jax.ShapeDtypeStruct((KV_ROWS, 4 * strip), BF),
        scratch_shapes=[
            pltpu.VMEM((4, NOPE, 4 * strip), BF),
            pltpu.VMEM((4, V_DIM, 4 * strip), BF),
        ],
        name="keys",
    )(where, *latents, key_up, value_up)
    gathered = lax.all_gather(kv, ("z", "c"), axis=0, tiled=False)

    parts = attend(where, queries, gathered)
    parts = [parts[0]] + [shifted(parts[j], "y", -j) for j in range(1, 4)]
    shape = jax.ShapeDtypeStruct((own, 4 * V_DIM), BF)
    parts = pl.pallas_call(
        spread_kernel,
        in_specs=[SMEM_SPEC] + [vmem] * 4,
        out_shape=[shape] * 4,
        scratch_shapes=[
            pltpu.VMEM((4, strip, V_DIM), BF),
            pltpu.VMEM((4, own, 4 * V_DIM), BF),
        ],
        name="spread",
    )(where, *parts)
    parts = [parts[0]] + [shifted(parts[k], "x", k) for k in range(1, 4)]
    return pl.pallas_call(
        project_kernel,
        in_specs=[SMEM_SPEC] + [vmem] * 5,
        out_shape=jax.ShapeDtypeStruct((own, out_proj.shape[1]), BF),
        scratch_shapes=[pltpu.VMEM((4, own, 4 * V_DIM), BF)],
        name="project",
    )(where, *parts, out_proj)


def body(
    query,
    latent,
    rope_key,
    latent_gain,
    key_up,
    value_up,
    out_proj,
    tokens,
    moe_gain,
    routes,
    group_prob,
    expert_prob,
    w_gate,
    w_up,
    w_down,
):
    where = jnp.stack([lax.axis_index(n) for n in ("z", "y", "c", "x")]).astype(jnp.int32)
    mixed = mixer_half(where, query, latent, rope_key, latent_gain, key_up, value_up, out_proj)
    moe_out = expert_half(tokens, moe_gain, routes, group_prob, expert_prob, w_gate, w_up, w_down)
    return (mixed, moe_out)


def solution(mesh):
    ep = ("z", "y", "c")
    every = ("z", "y", "c", "x")
    split = Mesh(mesh.devices.reshape(8, 4, 2, 4), every)
    return jax.shard_map(
        body,
        mesh=split,
        in_specs=(
            P(ep, "x"),
            P(every, None),
            P(every, None),
            P(),
            P(None, "x"),
            P(None, "x"),
            P(),
            P(every, None),
            P(),
            P(every, None),
            P(every),
            P(every, None),
            P(ep, None, "x"),
            P(ep, None, "x"),
            P(ep, "x", None),
        ),
        out_specs=(P(every, None), P(every, None)),
        check_vma=False,
    )
```

time: 335 us -> 208 us (0.62)
  blocking collectives: 103 us -> 0 us
  Pallas kernels: 0 us -> 46.2 us
  matrix products: 42 us -> 0 us
  starting transfers between devices: 13.8 us -> 53.5 us
  local copies, waits for them, and re-layouts: 54 us -> 16.8 us
  other arithmetic: 25.7 us -> 4.08 us
  loops' own time: 15 us -> 0 us
  waiting for transfers between devices: 65.2 us -> 72.4 us
    all_to_all x2 -> x0, blocking collectives: 90.6 us -> none  [the longest x1 54.6 us: sent_and_summed(): lax.all_to_all(split_up(value, dim, devices), axis, 0, 0, tiled=True)]
    ppermute x0 -> x26, waiting for transfers between devices: none -> 72.4 us  [shifted(): return lax.ppermute(value, axis, [(i, (i + amount) % n) for i in range(n)])]
    pallas_call x0 -> x12, Pallas kernels: none -> 46.2 us  [the longest x1 13.5 us: attend(): pl.pallas_call(attend_kernel, grid_spec=pltpu.PrefetchScalarGridSpec(num_...]
    dot_general x22 -> x0, matrix products: 42 us -> none  [the longest x8 18.2 us: advance(): jnp.einsum('hqk,khd->hqd', raised.astype(jnp.bfloat16), values_here, pref...]
    ppermute x0 -> x26, starting transfers between devices: none -> 35.7 us  [shifted(): return lax.ppermute(value, axis, [(i, (i + amount) % n) for i in range(n)])]
    all_gather x2 -> x1, waiting for transfers between devices: 35.2 us -> 0.01 us  [mixer_half(): gathered = lax.all_gather(kv, ('z', 'c'), axis=0, tiled=False)]
    all_to_all x2, waiting for transfers between devices: 29.9 us -> 0.01 us  [the longest x1 0.01 us: expert_half(): lax.all_to_all(outgoing.reshape(experts, CAP, width), ep_axes, split_axis...]
    dynamic_slice x24 -> x0, local copies, waits for them, and re-layouts: 20.4 us -> none  [the longest x8 15 us: update(): lax.dynamic_slice_in_dim(value_part, row_begin, span_rows, 0)]
  transfers between devices with their start and end apart: 4 -> 29, of which waited for: 3 -> 16; matrix products, arithmetic and copies ran while one was open for 7% -> 5% of each run, Pallas kernels for 0% -> 20%
where the time goes in v1:
time: 208 us; the launch traced here: 207 us
  waiting for transfers between devices  72.4 us (35%)
  starting transfers between devices  53.5 us (26%)
  Pallas kernels  46.2 us (22%)
  local copies, waits for them, and re-layouts  16.8 us (8%)
  between operations  14.3 us (7%)
  other arithmetic  4.08 us (2%)
    ppermute x26, waiting for transfers between devices, shifted(): return lax.ppermute(value, axis, [(i, (i + amount) % n) for i in range(n)])  72.4 us
    ppermute x26, starting transfers between devices, shifted(): return lax.ppermute(value, axis, [(i, (i + amount) % n) for i in range(n)])  35.7 us
    pallas_call x1, Pallas kernels, attend(): pl.pallas_call(attend_kernel, grid_spec=pltpu.PrefetchScalarGridSpec(num_...  13.5 us
    pallas_call x4, Pallas kernels, hidden_of(): pl.pallas_call(hidden_kernel, out_shape=jax.ShapeDtypeStruct((rows.shape[...  13 us
    all_to_all x1, starting transfers between devices, expert_half(): lax.all_to_all(outgoing.reshape(experts, CAP, width), ep_axes, split_axis...  9.3 us
    all_to_all x1, starting transfers between devices, expert_half(): lax.all_to_all(result.reshape(experts, CAP, width), ep_axes, split_axis=0...  8.42 us
    unnamed x55, local copies, waits for them, and re-layouts  6.7 us
    pallas_call x1, Pallas kernels, expert_half(): pl.pallas_call(down_kernel, out_shape=jax.ShapeDtypeStruct((slots, width)...  4.92 us
  transfers between devices with their start and end apart: 29, of which 16 were waited for; matrix products, arithmetic and copies ran while one was open for 5% of the time, Pallas kernels for 20%

profile of v1, /device:TPU:224, one launch (start us, length us, event | category | flops | bytes accessed | tf_op | source)
XLA Modules:
  0.0 207.3 jit_solution(3519659654647757992)
XLA Ops:
  7.2 1.4 copy.23.routes
  8.5 1.4 copy.24.group_prob
  9.9 1.4 copy.25.expert_prob
  11.3 2.7 %dispatch.1 = (bf16[256,2048]{1,0:T(8,128)(2,1)}, bf16[128,256]{1,0:T(8,128)(2,1)}) custom-call(bf16[64,2048]{1,0:T(8,128)(2,1)} %tokens.1, f32[1,2048]{1,0:T(1,128)} %bitcast.24, s32[64,2]{1,0:T(8,128)} %copy.23.routes, f32[64,1]{1,0:T(8,128)} %copy.24.group_prob, f32[64,2]{1,0:T(8,128)} %copy.25.expert_prob), custom_call_target="tpu_custom_call" | custom-call | tf_op jit(solution)/shard_map/dispatch/pallas_call | solution.py:74
  14.0 2.3 %reshape.40 = bf16[64,4,2048]{2,1,0:T(4,128)(2,1)} reshape(bf16[256,2048]{1,0:T(8,128)(2,1)} %get-tuple-element.28) | data formatting | bytes 2097152 | tf_op jit(solution)/shard_map/reshape | solution.py:129
  16.3 9.3 %all-to-all-start = ((bf16[64,4,2048]{2,1,0:T(4,128)(2,1)}), bf16[64,4,2048]{2,1,0:T(4,128)(2,1)S(1)}, u32[]{:S(2)}, u32[]{:S(2)}) async-start(bf16[64,4,2048]{2,1,0:T(4,128)(2,1)} %reshape.40), calls=%async_computation | async-start | bytes 2097152 | tf_op jit(solution)/shard_map/all_to_all | solution.py:128
  26.3 2.8 %collective-permute-start.5 = (bf16[32,544]{1,0:T(8,128)(2,1)S(1)}, bf16[32,544]{1,0:T(8,128)(2,1)S(1)}, u32[]{:S(2)}, u32[]{:S(2)}) collective-permute-start(bf16[32,544]{1,0:T(8,128)(2,1)S(1)} %pad_maximum_fusion.2), channel_id=1, source_target_pairs={{0,3},{1,0},{2,1},{3,2},{4,7},{5,4},{6,5},{7,6},{8,11},{9,8},{10,9... | collective-permute-start | bytes 104456 | tf_op jit(solution)/shard_map/ppermute | solution.py:33
  29.1 0.8 collective-permute-start.4
  29.9 0.9 collective-permute-start.3
  31.1 3.5 %collective-permute-done.4 = bf16[32,544]{1,0:T(8,128)(2,1)S(1)} collective-permute-done((bf16[32,544]{1,0:T(8,128)(2,1)S(1)}, bf16[32,544]{1,0:T(8,128)(2,1)S(1)}, u32[]{:S(2)}, u32[]{:S(2)}) %collective-permute-start.4) | collective-permute-done | bytes 34848 | tf_op jit(solution)/shard_map/ppermute | solution.py:33
  35.2 2.7 %collective-permute-start.8 = (bf16[128,544]{1,0:T(8,128)(2,1)S(1)}, bf16[128,544]{1,0:T(8,128)(2,1)S(1)}, u32[]{:S(2)}, u32[]{:S(2)}) collective-permute-start(bf16[128,544]{1,0:T(8,128)(2,1)S(1)} %pad_maximum_fusion.1.l0), channel_id=1, source_target_pairs={{0,24},{8,0},{16,8},{24,16},{1,25},{9,1},{17,9},{25,17},{2,26},{10... | collective-permute-start | bytes 417800 | tf_op jit(solution)/shard_map/ppermute | solution.py:33
  37.9 0.8 collective-permute-start.7
  38.8 0.9 collective-permute-start.6
  39.6 0.6 pad_add_fusion.where
  40.2 5.1 %collective-permute-done.8.l3 = bf16[128,544]{1,0:T(8,128)(2,1)S(1)} collective-permute-done((bf16[128,544]{1,0:T(8,128)(2,1)S(1)}, bf16[128,544]{1,0:T(8,128)(2,1)S(1)}, u32[]{:S(2)}, u32[]{:S(2)}) %collective-permute-start.8) | collective-permute-done | bytes 139296 | tf_op jit(solution)/shard_map/ppermute | solution.py:33
  45.3 3.8 %collective-permute-done.7.l2 = bf16[128,544]{1,0:T(8,128)(2,1)S(1)} collective-permute-done((bf16[128,544]{1,0:T(8,128)(2,1)S(1)}, bf16[128,544]{1,0:T(8,128)(2,1)S(1)}, u32[]{:S(2)}, u32[]{:S(2)}) %collective-permute-start.7) | collective-permute-done | bytes 139296 | tf_op jit(solution)/shard_map/ppermute | solution.py:33
  49.2 3.2 %collective-permute-done.6.l1 = bf16[128,544]{1,0:T(8,128)(2,1)S(1)} collective-permute-done((bf16[128,544]{1,0:T(8,128)(2,1)S(1)}, bf16[128,544]{1,0:T(8,128)(2,1)S(1)}, u32[]{:S(2)}, u32[]{:S(2)}) %collective-permute-start.6) | collective-permute-done | bytes 139296 | tf_op jit(solution)/shard_map/ppermute | solution.py:33
  52.4 0.7 copy-done.10
  53.1 2.8 %keys.1 = bf16[160,512]{1,0:T(8,128)(2,1)} custom-call(s32[4]{0:T(128)} %pad_add_fusion.where, bf16[128,544]{1,0:T(8,128)(2,1)} %copy-done.6, bf16[128,544]{1,0:T(8,128)(2,1)} %copy-done.10, bf16[128,544]{1,0:T(8,128)(2,1)} %copy-done.9, bf16[128,544]{1,0:T(8,128)(2,1)} %copy-done.8, bf16[512,256]{1,0:T(8,128)(2,1)} %key_up.1, bf16[512,256]{1,0:T(8,128)(2,1)} %value_up.1), custom_call_target="tpu_custom_call" | custom-call | tf_op jit(solution)/shard_map/keys/pallas_call | solution.py:326
  56.2 1.1 collective-permute-start.18
  57.4 1.0 collective-permute-start.15
  58.4 3.1 %collective-permute-start.22 = (bf16[256,2048]{1,0:T(8,128)(2,1)S(1)}, bf16[256,2048]{1,0:T(8,128)(2,1)S(1)}, u32[]{:S(2)}, u32[]{:S(2)}) collective-permute-start(bf16[256,2048]{1,0:T(8,128)(2,1)S(1)} %bitcast.22), channel_id=1, source_target_pairs={{0,3},{1,0},{2,1},{3,2},{4,7},{5,4},{6,5},{7,6},{8,11},{9,8},{10,9... | collective-permute-start | bytes 3145736 | tf_op jit(solution)/shard_map/ppermute | solution.py:33
  61.6 20.8 %collective-permute-done.18.rows = bf16[256,2048]{1,0:T(8,128)(2,1)S(1)} collective-permute-done((bf16[256,2048]{1,0:T(8,128)(2,1)S(1)}, bf16[256,2048]{1,0:T(8,128)(2,1)S(1)}, u32[]{:S(2)}, u32[]{:S(2)}) %collective-permute-start.18) | collective-permute-done | bytes 1048608 | tf_op jit(solution)/shard_map/ppermute | solution.py:33
  82.3 0.9 slice.25
  83.2 2.3 %collective-permute-start.19 = (bf16[128,2048]{1,0:T(8,128)(2,1)}, bf16[128,2048]{1,0:T(8,128)(2,1)}, u32[]{:S(2)}, u32[]{:S(2)}) collective-permute-start(bf16[128,2048]{1,0:T(8,128)(2,1)} %slice.25), channel_id=1, source_target_pairs={{0,3},{1,0},{2,1},{3,2},{4,7},{5,4},{6,5},{7,6},{8,11},{9,8},{10,9... | collective-permute-start | bytes 1572872 | tf_op jit(solution)/shard_map/ppermute | solution.py:33
  85.5 0.9 slice.24
  86.4 20.7 %collective-permute-done.23.w3 = bf16[256,2048]{1,0:T(8,128)(2,1)S(1)} collective-permute-done((bf16[256,2048]{1,0:T(8,128)(2,1)S(1)}, bf16[256,2048]{1,0:T(8,128)(2,1)S(1)}, u32[]{:S(2)}, u32[]{:S(2)}) %collective-permute-start.23) | collective-permute-done | bytes 1048608 | tf_op jit(solution)/shard_map/ppermute | solution.py:33
  107.1 0.9 slice.26
  108.1 3.3 %collective-permute-start.25 = (bf16[128,2048]{1,0:T(8,128)(2,1)S(1)}, bf16[128,2048]{1,0:T(8,128)(2,1)S(1)}, u32[]{:S(2)}, u32[]{:S(2)}) collective-permute-start(bf16[128,2048]{1,0:T(8,128)(2,1)S(1)} %slice.27), channel_id=1, source_target_pairs={{0,3},{1,0},{2,1},{3,2},{4,7},{5,4},{6,5},{7,6},{8,11},{9,8},{10,9... | collective-permute-start | bytes 1572872 | tf_op jit(solution)/shard_map/ppermute | solution.py:33
  111.4 3.2 %hidden_right.1 = bf16[256,256]{1,0:T(8,128)(2,1)} custom-call(bf16[256,2048]{1,0:T(8,128)(2,1)} %copy-done.2, bf16[2048,256]{1,0:T(8,128)(2,1)} %bitcast.11, bf16[2048,256]{1,0:T(8,128)(2,1)} %bitcast.15), custom_call_target="tpu_custom_call" | custom-call | tf_op jit(solution)/shard_map/hidden_right/pallas_call | solution.py:91
  114.6 3.2 %hidden_left.1 = bf16[256,256]{1,0:T(8,128)(2,1)} custom-call(bf16[256,2048]{1,0:T(8,128)(2,1)} %copy-done.1, bf16[2048,256]{1,0:T(8,128)(2,1)} %bitcast.12, bf16[2048,256]{1,0:T(8,128)(2,1)} %bitcast.16), custom_call_target="tpu_custom_call" | custom-call | tf_op jit(solution)/shard_map/hidden_left/pallas_call | solution.py:91
  117.9 3.2 %collective-permute-start.16 = (bf16[256,256]{1,0:T(8,128)(2,1)}, bf16[256,256]{1,0:T(8,128)(2,1)S(1)}, u32[]{:S(2)}, u32[]{:S(2)}) collective-permute-start(bf16[256,256]{1,0:T(8,128)(2,1)} %hidden_left.1), channel_id=1, source_target_pairs={{0,3},{1,0},{2,1},{3,2},{4,7},{5,4},{6,5},{7,6},{8,11},{9,8},{10,9... | collective-permute-start | bytes 393224 | tf_op jit(solution)/shard_map/ppermute | solution.py:33
  121.1 2.3 %pad_maximum_fusion.rows = bf16[256,2048]{1,0:T(8,128)(2,1)} fusion(bf16[128,2048]{1,0:T(8,128)(2,1)} %collective-permute-done.19, bf16[128,2048]{1,0:T(8,128)(2,1)} %collective-permute-done.17), kind=kLoop, calls=%fused_computation | loop fusion | flops 2097152 | bytes 2097152 | tf_op jit(solution)/shard_map/concatenate | solution.py:135
  123.4 3.2 %hidden_far.1 = bf16[256,256]{1,0:T(8,128)(2,1)} custom-call(bf16[256,2048]{1,0:T(8,128)(2,1)} %pad_maximum_fusion.rows, bf16[2048,256]{1,0:T(8,128)(2,1)} %bitcast.13, bf16[2048,256]{1,0:T(8,128)(2,1)} %bitcast.17), custom_call_target="tpu_custom_call" | custom-call | tf_op jit(solution)/shard_map/hidden_far/pallas_call | solution.py:91
  126.6 3.2 %hidden_own.1.h0 = bf16[256,256]{1,0:T(8,128)(2,1)} custom-call(bf16[256,2048]{1,0:T(8,128)(2,1)} %copy-done, bf16[2048,256]{1,0:T(8,128)(2,1)} %bitcast.14, bf16[2048,256]{1,0:T(8,128)(2,1)} %bitcast.18), custom_call_target="tpu_custom_call" | custom-call | tf_op jit(solution)/shard_map/hidden_own/pallas_call | solution.py:91
  129.8 4.1 %collective-permute-done.21.h3 = bf16[256,256]{1,0:T(8,128)(2,1)S(1)} collective-permute-done((bf16[256,256]{1,0:T(8,128)(2,1)}, bf16[256,256]{1,0:T(8,128)(2,1)S(1)}, u32[]{:S(2)}, u32[]{:S(2)}) %collective-permute-start.21) | collective-permute-done | bytes 131104 | tf_op jit(solution)/shard_map/ppermute | solution.py:33
  133.9 0.6 copy-done.11
  134.6 0.6 copy-done.13
  135.3 4.9 %down.1 = bf16[256,2048]{1,0:T(8,128)(2,1)} custom-call(bf16[256,256]{1,0:T(8,128)(2,1)} %hidden_own.1.h0, bf16[256,256]{1,0:T(8,128)(2,1)} %copy-done.12, bf16[256,256]{1,0:T(8,128)(2,1)} %copy-done.13, bf16[256,256]{1,0:T(8,128)(2,1)} %copy-done.11, bf16[256,2048]{1,0:T(8,128)(2,1)} %bitcast.20, bf16[256,2048]{1,0:T(8,128)(2,1)} %copy-done.4, ...), custom_call_target="tpu_custom_call" | custom-call | tf_op jit(solution)/shard_map/down/pallas_call | solution.py:139
  140.2 2.2 %reshape.42 = bf16[64,4,2048]{2,1,0:T(4,128)(2,1)} reshape(bf16[256,2048]{1,0:T(8,128)(2,1)} %down.1) | data formatting | bytes 2097152 | tf_op jit(solution)/shard_map/reshape | solution.py:153
  142.4 8.4 %all-to-all-start.1 = ((bf16[64,4,2048]{2,1,0:T(4,128)(2,1)}), bf16[64,4,2048]{2,1,0:T(4,128)(2,1)S(1)}, u32[]{:S(2)}, u32[]{:S(2)}) async-start(bf16[64,4,2048]{2,1,0:T(4,128)(2,1)} %reshape.42), calls=%async_computation.1 | async-start | bytes 2097152 | tf_op jit(solution)/shard_map/all_to_all | solution.py:152
  150.9 0.7 multiply_sine_fusion.1
  151.6 1.7 queries.1
  153.3 1.5 collective-permute-start
  154.7 2.7 %collective-permute-start.1 = (bf16[96,128]{1,0:T(8,128)(2,1)}, bf16[96,128]{1,0:T(8,128)(2,1)S(1)}, u32[]{:S(2)}, u32[]{:S(2)}) collective-permute-start(bf16[96,128]{1,0:T(8,128)(2,1)} %get-tuple-element.18), channel_id=1, source_target_pairs={{0,16},{8,24},{16,0},{24,8},{1,17},{9,25},{17,1},{25,9},{2,18},{10... | collective-permute-start | bytes 73736 | tf_op jit(solution)/shard_map/ppermute | solution.py:33
  157.5 1.4 collective-permute-start.2
  158.9 1.7 collective-permute-done.1.q2
  160.6 0.9 collective-permute-done.2.q3
  161.5 0.6 copy-done.21
  162.1 13.5 %attend.1 = (bf16[128,64]{1,0:T(8,128)(2,1)}, bf16[128,64]{1,0:T(8,128)(2,1)}, bf16[128,64]{1,0:T(8,128)(2,1)}, bf16[128,64]{1,0:T(8,128)(2,1)}) custom-call(s32[4]{0:T(128)} %pad_add_fusion.where, bf16[96,128]{1,0:T(8,128)(2,1)} %get-tuple-element.16.q0, bf16[96,128]{1,0:T(8,128)(2,1)} %copy-done.19, bf16[96,128]{1,0:T(8,128)(2,1)} %copy-done.20, ...), custom_call_target="tpu_custom_call" | custom-call | tf_op jit(solution)/shard_map/attend/pallas_call | solution.py:256
  175.7 2.9 %collective-permute-start.9 = (bf16[128,64]{1,0:T(8,128)(2,1)}, bf16[128,64]{1,0:T(8,128)(2,1)S(1)}, u32[]{:S(2)}, u32[]{:S(2)}) collective-permute-start(bf16[128,64]{1,0:T(8,128)(2,1)} %get-tuple-element.21), channel_id=1, source_target_pairs={{0,24},{8,0},{16,8},{24,16},{1,25},{9,1},{17,9},{25,17},{2,26},{10... | collective-permute-start | bytes 49160 | tf_op jit(solution)/shard_map/ppermute | solution.py:33
  178.6 0.9 collective-permute-start.11
  179.5 1.0 collective-permute-done.9.a1
  180.4 3.8 %collective-permute-done.10.a2 = bf16[128,64]{1,0:T(8,128)(2,1)S(1)} collective-permute-done((bf16[128,64]{1,0:T(8,128)(2,1)}, bf16[128,64]{1,0:T(8,128)(2,1)S(1)}, u32[]{:S(2)}, u32[]{:S(2)}) %collective-permute-start.10) | collective-permute-done | bytes 16416 | tf_op jit(solution)/shard_map/ppermute | solution.py:33
  184.3 0.6 copy-done.17
  184.9 1.6 spread.1
  186.5 1.7 collective-permute-start.13
  188.2 1.5 collective-permute-start.14
  189.7 1.9 collective-permute-done.12.a1
  192.0 0.7 collective-permute-done.14.a3
  192.7 0.6 copy-done.24
  193.3 3.8 %project.1 = bf16[32,2048]{1,0:T(8,128)(2,1)} custom-call(s32[4]{0:T(128)} %pad_add_fusion.where, bf16[32,256]{1,0:T(8,128)(2,1)} %get-tuple-element.24.a0, bf16[32,256]{1,0:T(8,128)(2,1)} %copy-done.22, bf16[32,256]{1,0:T(8,128)(2,1)} %copy-done.23, bf16[32,256]{1,0:T(8,128)(2,1)} %copy-done.24, bf16[1024,2048]{1,0:T(8,128)(2,1)} %out_proj.1), custom_call_target="tpu_custom_call" | custom-call | tf_op jit(solution)/shard_map/project/pallas_call | solution.py:352
  197.0 1.2 reshape.43.returned
  198.2 2.2 %combine.1 = bf16[64,2048]{1,0:T(8,128)(2,1)} custom-call(bf16[256,2048]{1,0:T(8,128)(2,1)} %reshape.43.returned, bf16[128,256]{1,0:T(8,128)(2,1)} %get-tuple-element.29.shares), custom_call_target="tpu_custom_call" | custom-call | tf_op jit(solution)/shard_map/combine/pallas_call | solution.py:155
  (84 shorter events, 2.6 us)
Async XLA Ops:
  14.0 11.7 %copy-start.14 = (bf16[32,512]{1,0:T(8,128)(2,1)S(1)}, bf16[32,512]{1,0:T(8,128)(2,1)}, u32[]{:S(2)}) copy-start(bf16[32,512]{1,0:T(8,128)(2,1)} %param.16) | copy-start | bytes 98308
  14.0 11.8 %copy-start.15 = (bf16[32,32]{1,0:T(8,128)(2,1)S(1)}, bf16[32,32]{1,0:T(8,128)(2,1)}, u32[]{:S(2)}) copy-start(bf16[32,32]{1,0:T(8,128)(2,1)} %param.17) | copy-start | bytes 6148
  14.0 12.2 %copy-start.25 = (f32[512]{0:T(512)S(1)}, f32[512]{0:T(512)}, u32[]{:S(2)}) copy-start(f32[512]{0:T(512)} %param.18) | copy-start | bytes 6148
  16.3 39.6 %all-to-all-start = ((bf16[64,4,2048]{2,1,0:T(4,128)(2,1)}), bf16[64,4,2048]{2,1,0:T(4,128)(2,1)S(1)}, u32[]{:S(2)}, u32[]{:S(2)}) async-start(bf16[64,4,2048]{2,1,0:T(4,128)(2,1)} %reshape.40), calls=%async_computation | async-start | bytes 2097152 | tf_op jit(solution)/shard_map/all_to_all | solution.py:128
  25.6 135.9 %all-gather.3.cloned.1.call-start = ((), (), s32[]{:S(2)}) async-start(), calls=%async_computation.2 | async-start | bytes 2785280 | tf_op jit(solution)/shard_map/all_gather | solution.py:336
  25.8 32.5 %copy-start.5 = (bf16[1,256,2048]{2,1,0:T(8,128)(2,1)S(1)}, bf16[1,256,2048]{2,1,0:T(8,128)(2,1)}, u32[]{:S(2)}) copy-start(bf16[1,256,2048]{2,1,0:T(8,128)(2,1)} %param.29) | copy-start | bytes 3145732
  26.3 4.8 %collective-permute-start.5 = (bf16[32,544]{1,0:T(8,128)(2,1)S(1)}, bf16[32,544]{1,0:T(8,128)(2,1)S(1)}, u32[]{:S(2)}, u32[]{:S(2)}) collective-permute-start(bf16[32,544]{1,0:T(8,128)(2,1)S(1)} %pad_maximum_fusion.2), channel_id=1, source_target_pairs={{0,3},{1,0},{2,1},{3,2},{4,7},{5,4},{6,5},{7,6},{8,11},{9,8},{10,9... | collective-permute-start | bytes 104456 | tf_op jit(solution)/shard_map/ppermute | solution.py:33
  29.1 5.5 %collective-permute-start.4 = (bf16[32,544]{1,0:T(8,128)(2,1)S(1)}, bf16[32,544]{1,0:T(8,128)(2,1)S(1)}, u32[]{:S(2)}, u32[]{:S(2)}) collective-permute-start(bf16[32,544]{1,0:T(8,128)(2,1)S(1)} %pad_maximum_fusion.2), channel_id=1, source_target_pairs={{0,2},{1,3},{2,0},{3,1},{4,6},{5,7},{6,4},{7,5},{8,10},{9,11},{10,... | collective-permute-start | bytes 104456 | tf_op jit(solution)/shard_map/ppermute | solution.py:33
  29.9 5.2 %collective-permute-start.3 = (bf16[32,544]{1,0:T(8,128)(2,1)S(1)}, bf16[32,544]{1,0:T(8,128)(2,1)S(1)}, u32[]{:S(2)}, u32[]{:S(2)}) collective-permute-start(bf16[32,544]{1,0:T(8,128)(2,1)S(1)} %pad_maximum_fusion.2), channel_id=1, source_target_pairs={{0,1},{1,2},{2,3},{3,0},{4,5},{5,6},{6,7},{7,4},{8,9},{9,10},{10,1... | collective-permute-start | bytes 104456 | tf_op jit(solution)/shard_map/ppermute | solution.py:33
  35.2 17.2 %copy-start.6 = (bf16[128,544]{1,0:T(8,128)(2,1)}, bf16[128,544]{1,0:T(8,128)(2,1)S(1)}, u32[]{:S(2)}) copy-start(bf16[128,544]{1,0:T(8,128)(2,1)S(1)} %pad_maximum_fusion.1.l0) | copy-start | bytes 417796
  35.2 10.1 %collective-permute-start.8 = (bf16[128,544]{1,0:T(8,128)(2,1)S(1)}, bf16[128,544]{1,0:T(8,128)(2,1)S(1)}, u32[]{:S(2)}, u32[]{:S(2)}) collective-permute-start(bf16[128,544]{1,0:T(8,128)(2,1)S(1)} %pad_maximum_fusion.1.l0), channel_id=1, source_target_pairs={{0,24},{8,0},{16,8},{24,16},{1,25},{9,1},{17,9},{25,17},{2,26},{10... | collective-permute-start | bytes 417800 | tf_op jit(solution)/shard_map/ppermute | solution.py:33
  37.9 11.2 %collective-permute-start.7 = (bf16[128,544]{1,0:T(8,128)(2,1)S(1)}, bf16[128,544]{1,0:T(8,128)(2,1)S(1)}, u32[]{:S(2)}, u32[]{:S(2)}) collective-permute-start(bf16[128,544]{1,0:T(8,128)(2,1)S(1)} %pad_maximum_fusion.1.l0), channel_id=1, source_target_pairs={{0,16},{8,24},{16,0},{24,8},{1,17},{9,25},{17,1},{25,9},{2,18},{10... | collective-permute-start | bytes 417800 | tf_op jit(solution)/shard_map/ppermute | solution.py:33
  38.8 13.6 %collective-permute-start.6 = (bf16[128,544]{1,0:T(8,128)(2,1)S(1)}, bf16[128,544]{1,0:T(8,128)(2,1)S(1)}, u32[]{:S(2)}, u32[]{:S(2)}) collective-permute-start(bf16[128,544]{1,0:T(8,128)(2,1)S(1)} %pad_maximum_fusion.1.l0), channel_id=1, source_target_pairs={{0,8},{8,16},{16,24},{24,0},{1,9},{9,17},{17,25},{25,1},{2,10},{10... | collective-permute-start | bytes 417800 | tf_op jit(solution)/shard_map/ppermute | solution.py:33
  45.3 7.1 %copy-start.8 = (bf16[128,544]{1,0:T(8,128)(2,1)}, bf16[128,544]{1,0:T(8,128)(2,1)S(1)}, u32[]{:S(2)}) copy-start(bf16[128,544]{1,0:T(8,128)(2,1)S(1)} %collective-permute-done.8.l3) | copy-start | bytes 417796
  49.2 3.2 %copy-start.9 = (bf16[128,544]{1,0:T(8,128)(2,1)}, bf16[128,544]{1,0:T(8,128)(2,1)S(1)}, u32[]{:S(2)}) copy-start(bf16[128,544]{1,0:T(8,128)(2,1)S(1)} %collective-permute-done.7.l2) | copy-start | bytes 417796
  52.4 0.7 copy-start.10
  56.2 51.8 %copy-start = (bf16[256,2048]{1,0:T(8,128)(2,1)}, bf16[256,2048]{1,0:T(8,128)(2,1)S(1)}, u32[]{:S(2)}) copy-start(bf16[256,2048]{1,0:T(8,128)(2,1)S(1)} %reshape.41.rows) | copy-start | bytes 3145732
  56.2 26.1 %collective-permute-start.18 = (bf16[256,2048]{1,0:T(8,128)(2,1)S(1)}, bf16[256,2048]{1,0:T(8,128)(2,1)S(1)}, u32[]{:S(2)}, u32[]{:S(2)}) collective-permute-start(bf16[256,2048]{1,0:T(8,128)(2,1)S(1)} %reshape.41.rows), channel_id=1, source_target_pairs={{0,3},{1,0},{2,1},{3,2},{4,7},{5,4},{6,5},{7,6},{8,11},{9,8},{10,9... | collective-permute-start | bytes 3145736 | tf_op jit(solution)/shard_map/ppermute | solution.py:33
  57.4 28.1 %collective-permute-start.15 = (bf16[256,2048]{1,0:T(8,128)(2,1)S(1)}, bf16[256,2048]{1,0:T(8,128)(2,1)S(1)}, u32[]{:S(2)}, u32[]{:S(2)}) collective-permute-start(bf16[256,2048]{1,0:T(8,128)(2,1)S(1)} %reshape.41.rows), channel_id=1, source_target_pairs={{0,1},{1,2},{2,3},{3,0},{4,5},{5,6},{6,7},{7,4},{8,9},{9,10},{10,1... | collective-permute-start | bytes 3145736 | tf_op jit(solution)/shard_map/ppermute | solution.py:33
  58.3 48.7 %collective-permute-start.23 = (bf16[256,2048]{1,0:T(8,128)(2,1)S(1)}, bf16[256,2048]{1,0:T(8,128)(2,1)S(1)}, u32[]{:S(2)}, u32[]{:S(2)}) collective-permute-start(bf16[256,2048]{1,0:T(8,128)(2,1)S(1)} %bitcast.21), channel_id=1, source_target_pairs={{0,1},{1,2},{2,3},{3,0},{4,5},{5,6},{6,7},{7,4},{8,9},{9,10},{10,1... | collective-permute-start | bytes 3145736 | tf_op jit(solution)/shard_map/ppermute | solution.py:33
  58.4 49.6 %collective-permute-start.22 = (bf16[256,2048]{1,0:T(8,128)(2,1)S(1)}, bf16[256,2048]{1,0:T(8,128)(2,1)S(1)}, u32[]{:S(2)}, u32[]{:S(2)}) collective-permute-start(bf16[256,2048]{1,0:T(8,128)(2,1)S(1)} %bitcast.22), channel_id=1, source_target_pairs={{0,3},{1,0},{2,1},{3,2},{4,7},{5,4},{6,5},{7,6},{8,11},{9,8},{10,9... | collective-permute-start | bytes 3145736 | tf_op jit(solution)/shard_map/ppermute | solution.py:33
  82.3 25.7 %copy-start.2 = (bf16[256,2048]{1,0:T(8,128)(2,1)}, bf16[256,2048]{1,0:T(8,128)(2,1)S(1)}, u32[]{:S(2)}) copy-start(bf16[256,2048]{1,0:T(8,128)(2,1)S(1)} %collective-permute-done.18.rows) | copy-start | bytes 3145732
  83.2 34.6 %collective-permute-start.19 = (bf16[128,2048]{1,0:T(8,128)(2,1)}, bf16[128,2048]{1,0:T(8,128)(2,1)}, u32[]{:S(2)}, u32[]{:S(2)}) collective-permute-start(bf16[128,2048]{1,0:T(8,128)(2,1)} %slice.25), channel_id=1, source_target_pairs={{0,3},{1,0},{2,1},{3,2},{4,7},{5,4},{6,5},{7,6},{8,11},{9,8},{10,9... | collective-permute-start | bytes 1572872 | tf_op jit(solution)/shard_map/ppermute | solution.py:33
  85.5 29.1 %copy-start.1 = (bf16[256,2048]{1,0:T(8,128)(2,1)}, bf16[256,2048]{1,0:T(8,128)(2,1)S(1)}, u32[]{:S(2)}) copy-start(bf16[256,2048]{1,0:T(8,128)(2,1)S(1)} %collective-permute-done.15.rows) | copy-start | bytes 3145732
  86.4 34.7 %collective-permute-start.17 = (bf16[128,2048]{1,0:T(8,128)(2,1)}, bf16[128,2048]{1,0:T(8,128)(2,1)}, u32[]{:S(2)}, u32[]{:S(2)}) collective-permute-start(bf16[128,2048]{1,0:T(8,128)(2,1)} %slice.24), channel_id=1, source_target_pairs={{0,1},{1,2},{2,3},{3,0},{4,5},{5,6},{6,7},{7,4},{8,9},{9,10},{10,1... | collective-permute-start | bytes 1572872 | tf_op jit(solution)/shard_map/ppermute | solution.py:33
  107.1 4.3 %copy-start.3 = (bf16[256,2048]{1,0:T(8,128)(2,1)}, bf16[256,2048]{1,0:T(8,128)(2,1)S(1)}, u32[]{:S(2)}) copy-start(bf16[256,2048]{1,0:T(8,128)(2,1)S(1)} %collective-permute-done.23.w3) | copy-start | bytes 3145732
  108.0 21.9 %collective-permute-start.24 = (bf16[128,2048]{1,0:T(8,128)(2,1)}, bf16[128,2048]{1,0:T(8,128)(2,1)}, u32[]{:S(2)}, u32[]{:S(2)}) collective-permute-start(bf16[128,2048]{1,0:T(8,128)(2,1)} %slice.26), channel_id=1, source_target_pairs={{0,1},{1,2},{2,3},{3,0},{4,5},{5,6},{6,7},{7,4},{8,9},{9,10},{10,1... | collective-permute-start | bytes 1572872 | tf_op jit(solution)/shard_map/ppermute | solution.py:33
  108.0 3.4 %copy-start.4 = (bf16[256,2048]{1,0:T(8,128)(2,1)}, bf16[256,2048]{1,0:T(8,128)(2,1)S(1)}, u32[]{:S(2)}) copy-start(bf16[256,2048]{1,0:T(8,128)(2,1)S(1)} %collective-permute-done.22.w1) | copy-start | bytes 3145732
  108.1 21.8 %collective-permute-start.25 = (bf16[128,2048]{1,0:T(8,128)(2,1)S(1)}, bf16[128,2048]{1,0:T(8,128)(2,1)S(1)}, u32[]{:S(2)}, u32[]{:S(2)}) collective-permute-start(bf16[128,2048]{1,0:T(8,128)(2,1)S(1)} %slice.27), channel_id=1, source_target_pairs={{0,3},{1,0},{2,1},{3,2},{4,7},{5,4},{6,5},{7,6},{8,11},{9,8},{10,9... | collective-permute-start | bytes 1572872 | tf_op jit(solution)/shard_map/ppermute | solution.py:33
  114.6 19.3 %collective-permute-start.21 = (bf16[256,256]{1,0:T(8,128)(2,1)}, bf16[256,256]{1,0:T(8,128)(2,1)S(1)}, u32[]{:S(2)}, u32[]{:S(2)}) collective-permute-start(bf16[256,256]{1,0:T(8,128)(2,1)} %hidden_right.1), channel_id=1, source_target_pairs={{0,1},{1,2},{2,3},{3,0},{4,5},{5,6},{6,7},{7,4},{8,9},{9,10},{10,1... | collective-permute-start | bytes 393224 | tf_op jit(solution)/shard_map/ppermute | solution.py:33
  117.9 16.1 %collective-permute-start.16 = (bf16[256,256]{1,0:T(8,128)(2,1)}, bf16[256,256]{1,0:T(8,128)(2,1)S(1)}, u32[]{:S(2)}, u32[]{:S(2)}) collective-permute-start(bf16[256,256]{1,0:T(8,128)(2,1)} %hidden_left.1), channel_id=1, source_target_pairs={{0,3},{1,0},{2,1},{3,2},{4,7},{5,4},{6,5},{7,6},{8,11},{9,8},{10,9... | collective-permute-start | bytes 393224 | tf_op jit(solution)/shard_map/ppermute | solution.py:33
  126.6 7.3 %collective-permute-start.20 = (bf16[256,256]{1,0:T(8,128)(2,1)}, bf16[256,256]{1,0:T(8,128)(2,1)S(1)}, u32[]{:S(2)}, u32[]{:S(2)}) collective-permute-start(bf16[256,256]{1,0:T(8,128)(2,1)} %hidden_far.1), channel_id=1, source_target_pairs={{0,2},{1,3},{2,0},{3,1},{4,6},{5,7},{6,4},{7,5},{8,10},{9,11},{10,... | collective-permute-start | bytes 393224 | tf_op jit(solution)/shard_map/ppermute | solution.py:33
  129.8 4.1 %copy-start.7 = (bf16[128,2048]{1,0:T(8,128)(2,1)}, bf16[128,2048]{1,0:T(8,128)(2,1)S(1)}, u32[]{:S(2)}) copy-start(bf16[128,2048]{1,0:T(8,128)(2,1)S(1)} %collective-permute-done.25.w2b) | copy-start | bytes 1572868
  133.9 0.7 copy-start.11
  133.9 0.7 copy-start.12
  134.6 0.6 copy-start.13
  142.4 54.6 %all-to-all-start.1 = ((bf16[64,4,2048]{2,1,0:T(4,128)(2,1)}), bf16[64,4,2048]{2,1,0:T(4,128)(2,1)S(1)}, u32[]{:S(2)}, u32[]{:S(2)}) async-start(bf16[64,4,2048]{2,1,0:T(4,128)(2,1)} %reshape.42), calls=%async_computation.1 | async-start | bytes 2097152 | tf_op jit(solution)/shard_map/all_to_all | solution.py:152
  153.3 5.6 %collective-permute-start = (bf16[96,128]{1,0:T(8,128)(2,1)}, bf16[96,128]{1,0:T(8,128)(2,1)S(1)}, u32[]{:S(2)}, u32[]{:S(2)}) collective-permute-start(bf16[96,128]{1,0:T(8,128)(2,1)} %get-tuple-element.17), channel_id=1, source_target_pairs={{0,8},{8,16},{16,24},{24,0},{1,9},{9,17},{17,25},{25,1},{2,10},{10... | collective-permute-start | bytes 73736 | tf_op jit(solution)/shard_map/ppermute | solution.py:33
  154.7 5.9 %collective-permute-start.1 = (bf16[96,128]{1,0:T(8,128)(2,1)}, bf16[96,128]{1,0:T(8,128)(2,1)S(1)}, u32[]{:S(2)}, u32[]{:S(2)}) collective-permute-start(bf16[96,128]{1,0:T(8,128)(2,1)} %get-tuple-element.18), channel_id=1, source_target_pairs={{0,16},{8,24},{16,0},{24,8},{1,17},{9,25},{17,1},{25,9},{2,18},{10... | collective-permute-start | bytes 73736 | tf_op jit(solution)/shard_map/ppermute | solution.py:33
  157.5 4.1 %collective-permute-start.2 = (bf16[96,128]{1,0:T(8,128)(2,1)}, bf16[96,128]{1,0:T(8,128)(2,1)S(1)}, u32[]{:S(2)}, u32[]{:S(2)}) collective-permute-start(bf16[96,128]{1,0:T(8,128)(2,1)} %get-tuple-element.19), channel_id=1, source_target_pairs={{0,24},{8,0},{16,8},{24,16},{1,25},{9,1},{17,9},{25,17},{2,26},{10... | collective-permute-start | bytes 73736 | tf_op jit(solution)/shard_map/ppermute | solution.py:33
  158.9 2.6 %copy-start.19 = (bf16[96,128]{1,0:T(8,128)(2,1)}, bf16[96,128]{1,0:T(8,128)(2,1)S(1)}, u32[]{:S(2)}) copy-start(bf16[96,128]{1,0:T(8,128)(2,1)S(1)} %collective-permute-done.q1) | copy-start | bytes 73732
  160.6 0.9 copy-start.20
  161.5 0.6 copy-start.21
  175.7 4.8 %collective-permute-start.9 = (bf16[128,64]{1,0:T(8,128)(2,1)}, bf16[128,64]{1,0:T(8,128)(2,1)S(1)}, u32[]{:S(2)}, u32[]{:S(2)}) collective-permute-start(bf16[128,64]{1,0:T(8,128)(2,1)} %get-tuple-element.21), channel_id=1, source_target_pairs={{0,24},{8,0},{16,8},{24,16},{1,25},{9,1},{17,9},{25,17},{2,26},{10... | collective-permute-start | bytes 49160 | tf_op jit(solution)/shard_map/ppermute | solution.py:33
  178.5 5.7 %collective-permute-start.10 = (bf16[128,64]{1,0:T(8,128)(2,1)}, bf16[128,64]{1,0:T(8,128)(2,1)S(1)}, u32[]{:S(2)}, u32[]{:S(2)}) collective-permute-start(bf16[128,64]{1,0:T(8,128)(2,1)} %get-tuple-element.22), channel_id=1, source_target_pairs={{0,16},{8,24},{16,0},{24,8},{1,17},{9,25},{17,1},{25,9},{2,18},{10... | collective-permute-start | bytes 49160 | tf_op jit(solution)/shard_map/ppermute | solution.py:33
  178.6 5.7 %collective-permute-start.11 = (bf16[128,64]{1,0:T(8,128)(2,1)}, bf16[128,64]{1,0:T(8,128)(2,1)S(1)}, u32[]{:S(2)}, u32[]{:S(2)}) collective-permute-start(bf16[128,64]{1,0:T(8,128)(2,1)} %get-tuple-element.23), channel_id=1, source_target_pairs={{0,8},{8,16},{16,24},{24,0},{1,9},{9,17},{17,25},{25,1},{2,10},{10... | collective-permute-start | bytes 49160 | tf_op jit(solution)/shard_map/ppermute | solution.py:33
  180.4 3.8 %copy-start.16 = (bf16[128,64]{1,0:T(8,128)(2,1)}, bf16[128,64]{1,0:T(8,128)(2,1)S(1)}, u32[]{:S(2)}) copy-start(bf16[128,64]{1,0:T(8,128)(2,1)S(1)} %collective-permute-done.9.a1) | copy-start | bytes 49156
  184.3 0.6 copy-start.17
  184.3 0.6 copy-start.18
  186.5 5.2 %collective-permute-start.12 = (bf16[32,256]{1,0:T(8,128)(2,1)}, bf16[32,256]{1,0:T(8,128)(2,1)S(1)}, u32[]{:S(2)}, u32[]{:S(2)}) collective-permute-start(bf16[32,256]{1,0:T(8,128)(2,1)} %get-tuple-element.25), channel_id=1, source_target_pairs={{0,1},{1,2},{2,3},{3,0},{4,5},{5,6},{6,7},{7,4},{8,9},{9,10},{10,1... | collective-permute-start | bytes 49160 | tf_op jit(solution)/shard_map/ppermute | solution.py:33
  186.5 5.5 %collective-permute-start.13 = (bf16[32,256]{1,0:T(8,128)(2,1)}, bf16[32,256]{1,0:T(8,128)(2,1)S(1)}, u32[]{:S(2)}, u32[]{:S(2)}) collective-permute-start(bf16[32,256]{1,0:T(8,128)(2,1)} %get-tuple-element.26), channel_id=1, source_target_pairs={{0,2},{1,3},{2,0},{3,1},{4,6},{5,7},{6,4},{7,5},{8,10},{9,11},{10,... | collective-permute-start | bytes 49160 | tf_op jit(solution)/shard_map/ppermute | solution.py:33
  188.2 4.5 %collective-permute-start.14 = (bf16[32,256]{1,0:T(8,128)(2,1)}, bf16[32,256]{1,0:T(8,128)(2,1)S(1)}, u32[]{:S(2)}, u32[]{:S(2)}) collective-permute-start(bf16[32,256]{1,0:T(8,128)(2,1)} %get-tuple-element.27), channel_id=1, source_target_pairs={{0,3},{1,0},{2,1},{3,2},{4,7},{5,4},{6,5},{7,6},{8,11},{9,8},{10,9... | collective-permute-start | bytes 49160 | tf_op jit(solution)/shard_map/ppermute | solution.py:33
  191.6 1.0 copy-start.22
  192.0 0.7 copy-start.23
  192.7 0.6 copy-start.24
Sparse Core Ops, SparseCore 0:
  56.0 36.7 all-gather.2

commit v2 on v1

v2 whole, which is shorter than its diff:
```python
import jax
import jax.numpy as jnp
from jax import lax
from jax.experimental import pallas as pl
from jax.experimental.pallas import tpu as pltpu
from jax.sharding import Mesh, PartitionSpec as P

NOPE = 64
ROPE_DIM = 32
V_DIM = 64
QK_DIM = NOPE + ROPE_DIM
KV_ROWS = QK_DIM + V_DIM
CAP = 4
BF = jnp.bfloat16
F32 = jnp.float32

epsilon = 1e-06
rope_base = 10000.0
masked_value = -1e30
log2_e = 1.4426950408889634

AXES = ("zh", "zl", "y", "c", "x")
EP = AXES[:4]

SMEM_SPEC = pl.BlockSpec(memory_space=pltpu.SMEM)
VMEM_SPEC = pl.BlockSpec(memory_space=pltpu.VMEM)


def call(kernel, out_shape, name, arrays, where=None, scratch=(), limit=16 << 20):
    arrays = [pltpu.with_memory_space_constraint(a, pltpu.VMEM) for a in arrays]
    specs = [VMEM_SPEC] * len(arrays)
    if where is not None:
        arrays, specs = [where] + arrays, [SMEM_SPEC] + specs
    single = not isinstance(out_shape, (list, tuple))
    return pl.pallas_call(
        kernel,
        in_specs=specs,
        out_specs=VMEM_SPEC if single else [VMEM_SPEC] * len(out_shape),
        out_shape=out_shape,
        scratch_shapes=list(scratch),
        compiler_params=pltpu.CompilerParams(vmem_limit_bytes=limit),
        name=name,
    )(*arrays)


def mm(a, b, dims=((1,), (0,))):
    return lax.dot_general(a, b, (dims, ((), ())), preferred_element_type=F32)


def shifted(value, axis, amount):
    n = lax.axis_size(axis)
    return lax.ppermute(value, axis, [(i, (i + amount) % n) for i in range(n)])


def trig(positions):
    half = ROPE_DIM // 2
    inverse = rope_base ** (-2.0 * jnp.arange(half, dtype=F32) / ROPE_DIM)
    angles = positions.astype(F32)[:, None] * inverse[None, :]
    return jnp.cos(angles), jnp.sin(angles)


def rms_scale(values, gain):
    widened = values.astype(F32)
    return widened * lax.rsqrt(jnp.mean(widened * widened, axis=-1, keepdims=True) + epsilon) * gain


def dispatch_kernel(tokens, gain, routes, group_prob, expert_prob, outgoing, shares_out):
    rows = tokens.shape[0]
    experts, cap, width = outgoing.shape
    slots = experts * cap
    normed = rms_scale(tokens[...], gain[...]).astype(BF)
    slot = lax.broadcasted_iota(jnp.int32, (slots, rows), 0)
    expert = slot // cap
    first = routes[0:1, :] == expert
    second = routes[1:2, :] == expert
    named = (first | second).astype(BF)
    before = lax.broadcasted_iota(jnp.int32, (rows, rows), 0) < lax.broadcasted_iota(
        jnp.int32, (rows, rows), 1
    )
    prior = mm(named, before.astype(BF))
    mine = (first | second) & (prior == (slot % cap).astype(F32))
    outgoing[...] = mm(mine.astype(BF), normed).reshape(experts, cap, width).astype(BF)
    probs = expert_prob[...]
    shares = group_prob[...] * probs / jnp.sum(probs, axis=0, keepdims=True)
    weights = jnp.where(first, shares[0:1, :], shares[1:2, :])
    weights = jnp.where(mine, weights, 0.0)
    high = weights.astype(BF)
    shares_out[:, 0:rows] = high
    shares_out[:, rows : 2 * rows] = (weights - high.astype(F32)).astype(BF)


def dispatch(tokens, gain, routes, group_prob, expert_prob, experts):
    rows, width = tokens.shape
    return call(
        dispatch_kernel,
        (
            jax.ShapeDtypeStruct((experts, CAP, width), BF),
            jax.ShapeDtypeStruct((experts * CAP, 2 * rows), BF),
        ),
        "dispatch",
        [tokens, gain[None, :], routes.T, group_prob[None, :], expert_prob.T],
    )


def hidden_kernel(rows_a, rows_b, w_gate, w_up, out):
    half = out.shape[0] // 2
    for at, rows in ((0, rows_a), (half, rows_b)):
        got = rows[...].reshape(half, w_gate.shape[0])
        gate = mm(got, w_gate[...])
        up = mm(got, w_up[...])
        out[at : at + half, :] = (gate / (1.0 + jnp.exp(-gate)) * up).astype(BF)


def hidden_of(rows_a, rows_b, w_gate, w_up, name):
    shape = jax.ShapeDtypeStruct((2 * rows_a.shape[0] * CAP, w_gate.shape[1]), BF)
    return call(hidden_kernel, shape, name, [rows_a, rows_b, w_gate, w_up])


def down_kernel(h0, h1, h2, h3, w0, w1, w2, w3, out):
    total = mm(h0[...], w0[...]) + mm(h1[...], w1[...])
    total = total + mm(h2[...], w2[...]) + mm(h3[...], w3[...])
    out[...] = total.reshape(out.shape).astype(BF)


def combine_kernel(returned, shares, out):
    rows = out.shape[0]
    got = returned[...].reshape(shares.shape[0], out.shape[1])
    both = mm(shares[...], got, ((0,), (0,)))
    out[...] = (both[:rows] + both[rows:]).astype(BF)


def both_halves(
    where,
    query,
    latent,
    rope_key,
    latent_gain,
    key_up,
    value_up,
    out_proj,
    tokens,
    moe_gain,
    routes,
    group_prob,
    expert_prob,
    w_gate,
    w_up,
    w_down,
):
    experts = lax.axis_size(EP)
    rows, width = tokens.shape
    w_gate, w_up, w_down = w_gate[0], w_up[0], w_down[0]
    down = [shifted(w_down, "x", k) for k in (-1, 2, 1)]
    outgoing, shares = dispatch(tokens, moe_gain, routes, group_prob, expert_prob, experts)
    arrived = lax.all_to_all(outgoing, EP, split_axis=0, concat_axis=0, tiled=True)
    queries, pair = query_and_pair(where, query, latent, rope_key, latent_gain, key_up, value_up)
    arrived, pair, down = lax.optimization_barrier((arrived, pair, down))
    down = [w_down] + down
    half = experts // 2
    a, b = arrived[:half], arrived[half:]
    left_a, right_b = shifted(a, "x", 1), shifted(b, "x", -1)
    left_b, right_a = shifted(b, "x", 1), shifted(a, "x", -1)
    far_a, far_b = shifted(left_a, "x", 1), shifted(right_b, "x", -1)
    parts = attend(where, queries, pair)
    left_b, right_a, parts = lax.optimization_barrier((left_b, right_a, parts))
    hidden = [
        hidden_of(a, b, w_gate, w_up, "hidden_own"),
        shifted(hidden_of(left_a, left_b, w_gate, w_up, "hidden_left"), "x", -1),
        shifted(hidden_of(far_a, far_b, w_gate, w_up, "hidden_far"), "x", 2),
        shifted(hidden_of(right_a, right_b, w_gate, w_up, "hidden_right"), "x", 1),
    ]
    shape = jax.ShapeDtypeStruct((experts, CAP, width), BF)
    result = call(down_kernel, shape, "down", hidden + down)
    returned = lax.all_to_all(result, EP, split_axis=0, concat_axis=0, tiled=True)
    mixed = project(where, parts, out_proj, latent.shape[0])
    shape = jax.ShapeDtypeStruct((rows, width), BF)
    return mixed, call(combine_kernel, shape, "combine", [returned, shares])


def heads_kernel(
    where, l0, l1, l2, l3, key_up, value_up, query, cosine, sine, o0, o1, o2, o3, strip_s, heads
):
    latent = key_up.shape[0]
    own, strip = l0.shape[0], query.shape[0]
    count = heads.shape[0]
    half = ROPE_DIM // 2
    turned = query[...].astype(F32).T
    for h in range(count):
        at = h * QK_DIM
        a = turned[at + NOPE : at + NOPE + half]
        b = turned[at + NOPE + half : at + QK_DIM]
        heads[h, :NOPE, :] = turned[at : at + NOPE].astype(BF)
        heads[h, NOPE : NOPE + half, :] = (a * cosine[...] - b * sine[...]).astype(BF)
        heads[h, NOPE + half : QK_DIM, :] = (a * sine[...] + b * cosine[...]).astype(BF)
    for k, block in enumerate((l0, l1, l2, l3)):
        strip_s[k * own : (k + 1) * own, :] = block[...]
    got = strip_s[:, :latent]
    keys = mm(key_up[...], got, ((0,), (1,))).astype(BF)
    values = mm(value_up[...], got, ((0,), (1,))).astype(BF)
    eye = (
        lax.broadcasted_iota(jnp.int32, (ROPE_DIM, ROPE_DIM), 0)
        == lax.broadcasted_iota(jnp.int32, (ROPE_DIM, ROPE_DIM), 1)
    ).astype(BF)
    rope = mm(eye, strip_s[:, latent:], ((1,), (1,))).astype(BF)
    for h in range(count):
        heads[h, QK_DIM : QK_DIM + NOPE, :] = keys[h * NOPE : (h + 1) * NOPE]
        heads[h, QK_DIM + NOPE : 2 * QK_DIM, :] = rope
        heads[h, 2 * QK_DIM :, :] = values[h * V_DIM : (h + 1) * V_DIM]
    for k, out in enumerate((o0, o1, o2, o3)):
        out[...] = heads[lax.rem(where[0] + k, 4)]


def attend_kernel(where, q0, q1, q2, q3, *refs):
    blocks, (o0, o1, o2, o3, q_s, top_s, acc_s) = refs[:8], refs[8:]
    zh, zl, y, c, x = (where[i] for i in range(5))
    strip = q0.shape[1]
    span = blocks[0].shape[2]
    factor = QK_DIM ** (-0.5) * log2_e
    for j, q in enumerate((q0, q1, q2, q3)):
        at = pl.multiple_of(lax.rem(zh - j + 4, 4) * strip, strip)
        q_s[pl.ds(at, strip), :] = q[:QK_DIM, :].astype(F32).T.astype(BF)
    top_s[...] = jnp.full(top_s.shape, masked_value, F32)
    acc_s[...] = jnp.zeros(acc_s.shape, F32)

    col = lax.broadcasted_iota(jnp.int32, (1, span), 1)
    col_zl = jnp.bitwise_xor(zl, col // strip)
    within = col % strip
    col_x = ((x - within // 32 + 4) % 4) * 32 + within % 32
    query_at = (zl * 8 + y * 2 + c) * strip + lax.broadcasted_iota(jnp.int32, (strip, 1), 0)
    ones = jnp.ones((V_DIM, span), BF)

    def advance(rows, parts, masks):
        q = q_s[rows, :]
        old = top_s[rows, :]
        scores = [mm(q, part[:QK_DIM, :]) for part in parts]
        if masks is not None:
            scores = [jnp.where(m, s, masked_value) for m, s in zip(masks, scores)]
        peak = scores[0]
        for s in scores[1:]:
            peak = jnp.maximum(peak, s)
        new = jnp.maximum(old, jnp.max(peak, axis=1, keepdims=True))
        top_s[rows, :] = new
        base = new[:, :1]
        total = acc_s[rows, :] * jnp.exp2((old - new) * factor)
        for s, part in zip(scores, parts):
            raised = jnp.exp2((s - base) * factor).astype(BF)
            extended = jnp.concatenate([part[QK_DIM:, :], ones], axis=0)
            total = total + mm(raised, extended, ((1,), (1,)))
        acc_s[rows, :] = total

    for m in range(2):
        group = blocks[4 * m : 4 * m + 4]
        masks = []
        for k in range(4):
            key_y = lax.rem(y - k + 4, 4)
            key_at = (col_zl * 8 + key_y * 2 + jnp.bitwise_xor(c, m)) * strip + col_x
            masks.append(key_at <= query_at)
        for g in range(4):
            from_zh = lax.rem(zh - g + 4, 4)
            parts = [block[from_zh] for block in group]
            advance(slice(g * strip, (g + 1) * strip), parts, masks)
            if g < 3:
                advance(slice((g + 1) * strip, 4 * strip), parts, None)
    for j, out in enumerate((o0, o1, o2, o3)):
        at = pl.multiple_of(lax.rem(zh - j + 4, 4) * strip, strip)
        total = acc_s[pl.ds(at, strip), :]
        out[...] = (total[:, :V_DIM] / total[:, V_DIM:]).astype(BF)


def spread_kernel(where, a0, a1, a2, a3, o0, o1, o2, o3, heads, parts):
    for j, a in enumerate((a0, a1, a2, a3)):
        heads[lax.rem(where[0] + j, 4)] = a[...]
    beside = jnp.concatenate([heads[h] for h in range(4)], axis=1)
    parts[...] = beside.reshape(parts.shape)
    for k, out in enumerate((o0, o1, o2, o3)):
        out[...] = parts[lax.rem(where[4] + k, 4)]


def project_kernel(where, a0, a1, a2, a3, out_proj, out, parts):
    width = a0.shape[1]
    for k, a in enumerate((a0, a1, a2, a3)):
        parts[lax.rem(where[4] - k + 4, 4)] = a[...]
    total = mm(parts[0], out_proj[:width, :])
    for h in range(1, 4):
        total = total + mm(parts[h], out_proj[h * width : (h + 1) * width, :])
    out[...] = total.astype(BF)


def query_and_pair(where, query, latent, rope_key, latent_gain, key_up, value_up):
    strip = query.shape[0]
    own = latent.shape[0]
    query_start = (((where[0] * 2 + where[1]) * 4 + where[2]) * 2 + where[3]) * strip

    normed = rms_scale(latent, latent_gain).astype(BF)
    key_cos, key_sin = trig(query_start + where[4] * own + jnp.arange(own, dtype=jnp.int32))
    half = ROPE_DIM // 2
    a = rope_key[:, :half].astype(F32)
    b = rope_key[:, half:].astype(F32)
    both = jnp.concatenate(
        [
            normed,
            (a * key_cos - b * key_sin).astype(BF),
            (a * key_sin + b * key_cos).astype(BF),
        ],
        axis=1,
    )
    near = [both] + [shifted(both, "x", k) for k in range(1, 4)]
    cosine, sine = trig(query_start + jnp.arange(strip, dtype=jnp.int32))
    blocks = call(
        heads_kernel,
        [jax.ShapeDtypeStruct((QK_DIM + KV_ROWS, strip), BF)] * 4,
        "heads",
        near + [key_up, value_up, query, cosine.T, sine.T],
        where,
        [
            pltpu.VMEM((strip, both.shape[1]), BF),
            pltpu.VMEM((4, QK_DIM + KV_ROWS, strip), BF),
        ],
    )
    blocks = [blocks[0]] + [shifted(blocks[k], "zh", k) for k in range(1, 4)]
    mine = jnp.stack([block[QK_DIM:] for block in blocks])
    return blocks, jnp.concatenate([mine, shifted(mine, "zl", 1)], axis=2)


def attend(where, blocks, pair):
    strip = blocks[0].shape[1]
    column = [pair] + [shifted(pair, "y", k) for k in range(1, 4)]
    column = column + [shifted(part, "c", 1) for part in column]
    return call(
        attend_kernel,
        [jax.ShapeDtypeStruct((strip, V_DIM), BF)] * 4,
        "attend",
        blocks + column,
        where,
        [
            pltpu.VMEM((4 * strip, QK_DIM), BF),
            pltpu.VMEM((4 * strip, 128), F32),
            pltpu.VMEM((4 * strip, 128), F32),
        ],
    )


def project(where, parts, out_proj, own):
    strip = parts[0].shape[0]
    parts = [parts[0]] + [shifted(parts[j], "zh", -j) for j in range(1, 4)]
    parts = call(
        spread_kernel,
        [jax.ShapeDtypeStruct((own, 4 * V_DIM), BF)] * 4,
        "spread",
        parts,
        where,
        [pltpu.VMEM((4, strip, V_DIM), BF), pltpu.VMEM((4, own, 4 * V_DIM), BF)],
    )
    parts = [parts[0]] + [shifted(parts[k], "x", k) for k in range(1, 4)]
    return call(
        project_kernel,
        jax.ShapeDtypeStruct((own, out_proj.shape[1]), BF),
        "project",
        parts + [out_proj],
        where,
        [pltpu.VMEM((4, own, 4 * V_DIM), BF)],
    )


def body(
    query,
    latent,
    rope_key,
    latent_gain,
    key_up,
    value_up,
    out_proj,
    tokens,
    moe_gain,
    routes,
    group_prob,
    expert_prob,
    w_gate,
    w_up,
    w_down,
):
    where = jnp.stack([lax.axis_index(n) for n in AXES]).astype(jnp.int32)
    return both_halves(
        where,
        query,
        latent,
        rope_key,
        latent_gain,
        key_up,
        value_up,
        out_proj,
        tokens,
        moe_gain,
        routes,
        group_prob,
        expert_prob,
        w_gate,
        w_up,
        w_down,
    )


def solution(mesh):
    ep, every = EP, AXES
    split = Mesh(mesh.devices.reshape(4, 2, 4, 2, 4), AXES)
    return jax.shard_map(
        body,
        mesh=split,
        in_specs=(
            P(ep, "x"),
            P(every, None),
            P(every, None),
            P(),
            P(None, "x"),
            P(None, "x"),
            P(),
            P(every, None),
            P(),
            P(every, None),
            P(every),
            P(every, None),
            P(ep, None, "x"),
            P(ep, None, "x"),
            P(ep, "x", None),
        ),
        out_specs=(P(every, None), P(every, None)),
        check_vma=False,
    )
```

time: 208 us -> 191 us (0.918)
  the two profiles are of different devices: /device:TPU:224 before, /device:TPU:8 now
where the time goes in v2:
time: 191 us; the launch traced here: 190 us
  waiting for transfers between devices  78.2 us (41%)
  starting transfers between devices  73.6 us (39%)
  Pallas kernels  18.7 us (10%)
  local copies, waits for them, and re-layouts  16.1 us (8%)
  other arithmetic  2.85 us (1%)
    ppermute x32, waiting for transfers between devices, shifted(): return lax.ppermute(value, axis, [(i, (i + amount) % n) for i in range(n)])  78.2 us
    ppermute x32, starting transfers between devices, shifted(): return lax.ppermute(value, axis, [(i, (i + amount) % n) for i in range(n)])  51.7 us
    pallas_call x11, Pallas kernels, call(): pl.pallas_call(kernel, in_specs=specs, out_specs=VMEM_SPEC if single else...  18.7 us
    unnamed x61, local copies, waits for them, and re-layouts  14.2 us
    all_to_all x1, starting transfers between devices, both_halves(): lax.all_to_all(outgoing, EP, split_axis=0, concat_axis=0, tiled=True)  12.3 us
    all_to_all x1, starting transfers between devices, both_halves(): lax.all_to_all(result, EP, split_axis=0, concat_axis=0, tiled=True)  9.57 us
  transfers between devices with their start and end apart: 34, of which 16 were waited for; matrix products, arithmetic and copies ran while one was open for 3% of the time, Pallas kernels for 7%

profile of v2, /device:TPU:8, one launch (start us, length us, event | category | flops | bytes accessed | tf_op | source)
XLA Modules:
  0.0 190.5 jit_solution(17766340016835701987)
XLA Ops:
  0.6 0.9 copy-done.6
  1.6 0.7 copy-done.20
  2.3 0.7 copy-done.21
  3.0 0.7 copy-done.22
  3.6 0.7 copy-done.23
  4.3 1.6 dispatch.1
  6.6 12.3 %all-to-all-start = ((bf16[64,4,2048]{2,1,0:T(4,128)(2,1)}), bf16[64,4,2048]{2,1,0:T(4,128)(2,1)}, u32[]{:S(2)}, u32[]{:S(2)}) async-start(bf16[64,4,2048]{2,1,0:T(4,128)(2,1)} %get-tuple-element.27), calls=%async_computation | async-start | bytes 2097152 | tf_op jit(solution)/shard_map/all_to_all | solution.py:155
  18.9 0.9 copy.20
  19.9 0.9 fusion
  20.8 0.8 fusion.8
  21.7 0.8 fusion.2
  22.6 1.5 collective-permute-start
  24.1 2.7 %collective-permute-start.1 = (bf16[32,544]{1,0:T(8,128)(2,1)S(1)}, bf16[32,544]{1,0:T(8,128)(2,1)S(1)}, u32[]{:S(2)}, u32[]{:S(2)}) collective-permute-start(bf16[32,544]{1,0:T(8,128)(2,1)S(1)} %pad_maximum_fusion.2.l0), channel_id=1, source_target_pairs={{0,2},{1,3},{2,0},{3,1},{4,6},{5,7},{6,4},{7,5},{8,10},{9,11},{10,... | collective-permute-start | bytes 104456 | tf_op jit(solution)/shard_map/ppermute | solution.py:52
  26.8 1.4 collective-permute-start.2
  28.3 2.6 %collective-permute-start.8 = (bf16[256,2048]{1,0:T(8,128)(2,1)}, bf16[256,2048]{1,0:T(8,128)(2,1)}, u32[]{:S(2)}, u32[]{:S(2)}) collective-permute-start(bf16[256,2048]{1,0:T(8,128)(2,1)} %bitcast.30), channel_id=1, source_target_pairs={{0,2},{1,3},{2,0},{3,1},{4,6},{5,7},{6,4},{7,5},{8,10},{9,11},{10,... | collective-permute-start | bytes 3145736 | tf_op jit(solution)/shard_map/ppermute | solution.py:52
  31.3 0.9 copy-done.7
  32.2 0.9 copy-done.8
  33.2 0.9 copy-done.15
  34.0 0.9 heads.1
  34.9 3.9 %collective-permute-start.5 = (bf16[256,128]{1,0:T(8,128)(2,1)S(1)}, bf16[256,128]{1,0:T(8,128)(2,1)S(1)}, u32[]{:S(2)}, u32[]{:S(2)}) collective-permute-start(bf16[256,128]{1,0:T(8,128)(2,1)S(1)} %get-tuple-element.31), channel_id=1, source_target_pairs={{0,192},{64,0},{128,64},{192,128},{1,193},{65,1},{129,65},{193,129... | collective-permute-start | bytes 196616 | tf_op jit(solution)/shard_map/ppermute | solution.py:52
  38.8 2.1 %collective-permute-start.4 = (bf16[256,128]{1,0:T(8,128)(2,1)S(1)}, bf16[256,128]{1,0:T(8,128)(2,1)S(1)}, u32[]{:S(2)}, u32[]{:S(2)}) collective-permute-start(bf16[256,128]{1,0:T(8,128)(2,1)S(1)} %get-tuple-element.30), channel_id=1, source_target_pairs={{0,128},{64,192},{128,0},{192,64},{1,129},{65,193},{129,1},{193,65... | collective-permute-start | bytes 196616 | tf_op jit(solution)/shard_map/ppermute | solution.py:52
  41.0 6.6 %collective-permute-done.5.q3 = bf16[256,128]{1,0:T(8,128)(2,1)S(1)} collective-permute-done((bf16[256,128]{1,0:T(8,128)(2,1)S(1)}, bf16[256,128]{1,0:T(8,128)(2,1)S(1)}, u32[]{:S(2)}, u32[]{:S(2)}) %collective-permute-start.5) | collective-permute-done | bytes 65568 | tf_op jit(solution)/shard_map/ppermute | solution.py:52
  47.6 5.5 %collective-permute-start.3 = (bf16[256,128]{1,0:T(8,128)(2,1)S(1)}, bf16[256,128]{1,0:T(8,128)(2,1)S(1)}, u32[]{:S(2)}, u32[]{:S(2)}) collective-permute-start(bf16[256,128]{1,0:T(8,128)(2,1)S(1)} %get-tuple-element.29), channel_id=1, source_target_pairs={{0,64},{64,128},{128,192},{192,0},{1,65},{65,129},{129,193},{193,1... | collective-permute-start | bytes 196616 | tf_op jit(solution)/shard_map/ppermute | solution.py:52
  53.1 2.5 %collective-permute-done.3.q1 = bf16[256,128]{1,0:T(8,128)(2,1)S(1)} collective-permute-done((bf16[256,128]{1,0:T(8,128)(2,1)S(1)}, bf16[256,128]{1,0:T(8,128)(2,1)S(1)}, u32[]{:S(2)}, u32[]{:S(2)}) %collective-permute-start.3) | collective-permute-done | bytes 65568 | tf_op jit(solution)/shard_map/ppermute | solution.py:52
  56.2 4.8 %collective-permute-done.6 = bf16[4,160,128]{2,1,0:T(8,128)(2,1)S(1)} collective-permute-done((bf16[4,160,128]{2,1,0:T(8,128)(2,1)S(1)}, bf16[4,160,128]{2,1,0:T(8,128)(2,1)S(1)}, u32[]{:S(2)}, u32[]{:S(2)}) %collective-permute-start.6) | collective-permute-done | bytes 163872 | tf_op jit(solution)/shard_map/ppermute | solution.py:52
  61.1 15.7 %collective-permute-done.9.w3 = bf16[256,2048]{1,0:T(8,128)(2,1)S(1)} collective-permute-done((bf16[256,2048]{1,0:T(8,128)(2,1)}, bf16[256,2048]{1,0:T(8,128)(2,1)S(1)}, u32[]{:S(2)}, u32[]{:S(2)}) %collective-permute-start.9) | collective-permute-done | bytes 1048608 | tf_op jit(solution)/shard_map/ppermute | solution.py:52
  76.8 1.0 copy-done.4
  77.8 1.5 collective-permute-start.12
  79.2 1.0 collective-permute-start.13
  80.2 1.7 fusion.11
  81.9 1.8 collective-permute-start.28
  84.0 2.2 %collective-permute-start.14 = (bf16[4,160,256]{2,1,0:T(8,128)(2,1)S(1)}, bf16[4,160,256]{2,1,0:T(8,128)(2,1)S(1)}, u32[]{:S(2)}, u32[]{:S(2)}) collective-permute-start(bf16[4,160,256]{2,1,0:T(8,128)(2,1)S(1)} %pad_maximum_fusion.refs_0_), channel_id=1, source_target_pairs={{0,24},{8,0},{16,8},{24,16},{1,25},{9,1},{17,9},{25,17},{2,26},{10... | collective-permute-start | bytes 983048 | tf_op jit(solution)/shard_map/ppermute | solution.py:52
  86.3 2.1 %collective-permute-done.12.refs_1_ = bf16[4,160,256]{2,1,0:T(8,128)(2,1)S(1)} collective-permute-done((bf16[4,160,256]{2,1,0:T(8,128)(2,1)S(1)}, bf16[4,160,256]{2,1,0:T(8,128)(2,1)S(1)}, u32[]{:S(2)}, u32[]{:S(2)}) %collective-permute-start.12) | collective-permute-done | bytes 327712 | tf_op jit(solution)/shard_map/ppermute | solution.py:52
  88.4 3.0 %collective-permute-done.13.refs_2_ = bf16[4,160,256]{2,1,0:T(8,128)(2,1)S(1)} collective-permute-done((bf16[4,160,256]{2,1,0:T(8,128)(2,1)S(1)}, bf16[4,160,256]{2,1,0:T(8,128)(2,1)S(1)}, u32[]{:S(2)}, u32[]{:S(2)}) %collective-permute-start.13) | collective-permute-done | bytes 327712 | tf_op jit(solution)/shard_map/ppermute | solution.py:52
  91.4 5.7 %collective-permute-done.14.refs_3_ = bf16[4,160,256]{2,1,0:T(8,128)(2,1)S(1)} collective-permute-done((bf16[4,160,256]{2,1,0:T(8,128)(2,1)S(1)}, bf16[4,160,256]{2,1,0:T(8,128)(2,1)S(1)}, u32[]{:S(2)}, u32[]{:S(2)}) %collective-permute-start.14) | collective-permute-done | bytes 327712 | tf_op jit(solution)/shard_map/ppermute | solution.py:52
  97.1 3.2 %collective-permute-start.11 = (bf16[32,4,2048]{2,1,0:T(4,128)(2,1)S(1)}, bf16[32,4,2048]{2,1,0:T(4,128)(2,1)S(1)}, u32[]{:S(2)}, u32[]{:S(2)}) collective-permute-start(bf16[32,4,2048]{2,1,0:T(4,128)(2,1)S(1)} %get-tuple-element.52.rows_a), channel_id=1, source_target_pairs={{0,3},{1,0},{2,1},{3,2},{4,7},{5,4},{6,5},{7,6},{8,11},{9,8},{10,9... | collective-permute-start | bytes 1572872 | tf_op jit(solution)/shard_map/ppermute | solution.py:52
  100.4 3.2 %collective-permute-start.29 = (bf16[32,4,2048]{2,1,0:T(4,128)(2,1)S(1)}, bf16[32,4,2048]{2,1,0:T(4,128)(2,1)S(1)}, u32[]{:S(2)}, u32[]{:S(2)}) collective-permute-start(bf16[32,4,2048]{2,1,0:T(4,128)(2,1)S(1)} %collective-permute-done.28.rows_b), channel_id=1, source_target_pairs={{0,3},{1,0},{2,1},{3,2},{4,7},{5,4},{6,5},{7,6},{8,11},{9,8},{10,9... | collective-permute-start | bytes 1572872 | tf_op jit(solution)/shard_map/ppermute | solution.py:52
  103.6 1.6 collective-permute-done.18.refs_7_
  105.3 0.8 copy-done.10
  106.1 0.8 copy-done.12
  106.9 0.8 copy-done.14
  107.8 5.9 %attend.1 = (bf16[128,64]{1,0:T(8,128)(2,1)S(1)}, bf16[128,64]{1,0:T(8,128)(2,1)S(1)}, bf16[128,64]{1,0:T(8,128)(2,1)S(1)}, bf16[128,64]{1,0:T(8,128)(2,1)S(1)}) custom-call(s32[5]{0:T(128)S(1)} %stack.38.where, bf16[256,128]{1,0:T(8,128)(2,1)S(1)} %get-tuple-element.28.q0, bf16[256,128]{1,0:T(8,128)(2,1)S(1)} %copy-done.14, ...), custom_call_target="tpu_custom_call" | custom-call | tf_op jit(solution)/shard_map/attend/pallas_call | solution.py:35
  113.8 0.7 hidden_right.1
  114.9 0.7 hidden_left.1
  115.6 3.3 %collective-permute-start.26 = (bf16[256,256]{1,0:T(8,128)(2,1)S(1)}, bf16[256,256]{1,0:T(8,128)(2,1)S(1)}, u32[]{:S(2)}, u32[]{:S(2)}) collective-permute-start(bf16[256,256]{1,0:T(8,128)(2,1)S(1)} %hidden_left.1), channel_id=1, source_target_pairs={{0,3},{1,0},{2,1},{3,2},{4,7},{5,4},{6,5},{7,6},{8,11},{9,8},{10,9... | collective-permute-start | bytes 393224 | tf_op jit(solution)/shard_map/ppermute | solution.py:52
  118.9 5.5 %collective-permute-done.27.rows_a = bf16[32,4,2048]{2,1,0:T(4,128)(2,1)S(1)} collective-permute-done((bf16[32,4,2048]{2,1,0:T(4,128)(2,1)S(1)}, bf16[32,4,2048]{2,1,0:T(4,128)(2,1)S(1)}, u32[]{:S(2)}, u32[]{:S(2)}) %collective-permute-start.27) | collective-permute-done | bytes 524320 | tf_op jit(solution)/shard_map/ppermute | solution.py:52
  124.4 0.7 hidden_far.1
  125.1 1.6 collective-permute-start.30
  126.7 0.7 hidden_own.1.h0
  127.5 4.2 %collective-permute-done.30.h2 = bf16[256,256]{1,0:T(8,128)(2,1)S(1)} collective-permute-done((bf16[256,256]{1,0:T(8,128)(2,1)S(1)}, bf16[256,256]{1,0:T(8,128)(2,1)S(1)}, u32[]{:S(2)}, u32[]{:S(2)}) %collective-permute-start.30) | collective-permute-done | bytes 131104 | tf_op jit(solution)/shard_map/ppermute | solution.py:52
  131.7 3.6 %down.1 = bf16[64,4,2048]{2,1,0:T(4,128)(2,1)} custom-call(bf16[256,256]{1,0:T(8,128)(2,1)S(1)} %hidden_own.1.h0, bf16[256,256]{1,0:T(8,128)(2,1)S(1)} %collective-permute-done.26.h1, bf16[256,256]{1,0:T(8,128)(2,1)S(1)} %collective-permute-done.30.h2, bf16[256,256]{1,0:T(8,128)(2,1)S(1)} %collective-permute-done.31.h3, bf16[256,2048]{1,0:T(8,128)(2,1)S(1)} %bitcast.32, ...), custom_call_target="tpu_custom_call" | custom-call | tf_op jit(solution)/shard_map/down/pallas_call | solution.py:35
  135.3 9.6 %all-to-all-start.1 = ((bf16[64,4,2048]{2,1,0:T(4,128)(2,1)}), bf16[64,4,2048]{2,1,0:T(4,128)(2,1)S(1)}, u32[]{:S(2)}, u32[]{:S(2)}) async-start(bf16[64,4,2048]{2,1,0:T(4,128)(2,1)} %down.1), calls=%async_computation.1 | async-start | bytes 2097152 | tf_op jit(solution)/shard_map/all_to_all | solution.py:174
  144.8 3.9 %collective-permute-start.19 = (bf16[128,64]{1,0:T(8,128)(2,1)S(1)}, bf16[128,64]{1,0:T(8,128)(2,1)S(1)}, u32[]{:S(2)}, u32[]{:S(2)}) collective-permute-start(bf16[128,64]{1,0:T(8,128)(2,1)S(1)} %copy-done.29), channel_id=1, source_target_pairs={{0,192},{64,0},{128,64},{192,128},{1,193},{65,1},{129,65},{193,129... | collective-permute-start | bytes 49160 | tf_op jit(solution)/shard_map/ppermute | solution.py:52
  148.7 2.1 %collective-permute-start.20 = (bf16[128,64]{1,0:T(8,128)(2,1)S(1)}, bf16[128,64]{1,0:T(8,128)(2,1)S(1)}, u32[]{:S(2)}, u32[]{:S(2)}) collective-permute-start(bf16[128,64]{1,0:T(8,128)(2,1)S(1)} %copy-done.27), channel_id=1, source_target_pairs={{0,128},{64,192},{128,0},{192,64},{1,129},{65,193},{129,1},{193,65... | collective-permute-start | bytes 49160 | tf_op jit(solution)/shard_map/ppermute | solution.py:52
  150.9 2.5 %collective-permute-start.21 = (bf16[128,64]{1,0:T(8,128)(2,1)S(1)}, bf16[128,64]{1,0:T(8,128)(2,1)S(1)}, u32[]{:S(2)}, u32[]{:S(2)}) collective-permute-start(bf16[128,64]{1,0:T(8,128)(2,1)S(1)} %copy-done.25), channel_id=1, source_target_pairs={{0,64},{64,128},{128,192},{192,0},{1,65},{65,129},{129,193},{193,1... | collective-permute-start | bytes 49160 | tf_op jit(solution)/shard_map/ppermute | solution.py:52
  153.3 18.2 %collective-permute-done.19.a1 = bf16[128,64]{1,0:T(8,128)(2,1)S(1)} collective-permute-done((bf16[128,64]{1,0:T(8,128)(2,1)S(1)}, bf16[128,64]{1,0:T(8,128)(2,1)S(1)}, u32[]{:S(2)}, u32[]{:S(2)}) %collective-permute-start.19) | collective-permute-done | bytes 16416 | tf_op jit(solution)/shard_map/ppermute | solution.py:52
  171.5 4.5 %collective-permute-done.20.a2 = bf16[128,64]{1,0:T(8,128)(2,1)S(1)} collective-permute-done((bf16[128,64]{1,0:T(8,128)(2,1)S(1)}, bf16[128,64]{1,0:T(8,128)(2,1)S(1)}, u32[]{:S(2)}, u32[]{:S(2)}) %collective-permute-start.20) | collective-permute-done | bytes 16416 | tf_op jit(solution)/shard_map/ppermute | solution.py:52
  176.0 0.7 spread.1
  177.3 4.1 %collective-permute-start.23 = (bf16[32,256]{1,0:T(8,128)(2,1)S(1)}, bf16[32,256]{1,0:T(8,128)(2,1)S(1)}, u32[]{:S(2)}, u32[]{:S(2)}) collective-permute-start(bf16[32,256]{1,0:T(8,128)(2,1)S(1)} %get-tuple-element.44), channel_id=1, source_target_pairs={{0,2},{1,3},{2,0},{3,1},{4,6},{5,7},{6,4},{7,5},{8,10},{9,11},{10,... | collective-permute-start | bytes 49160 | tf_op jit(solution)/shard_map/ppermute | solution.py:52
  181.7 1.6 collective-permute-done.23.a2
  183.3 1.9 collective-permute-done.24.a3
  185.2 2.2 %copy-done.2 = bf16[1024,2048]{1,0:T(8,128)(2,1)S(1)} copy-done((bf16[1024,2048]{1,0:T(8,128)(2,1)S(1)}, bf16[1024,2048]{1,0:T(8,128)(2,1)}, u32[]{:S(2)}) %copy-start.2) | copy-done | bytes 4194328
  187.4 2.0 %project.1 = bf16[32,2048]{1,0:T(8,128)(2,1)} custom-call(s32[5]{0:T(128)S(1)} %stack.38.where, bf16[32,256]{1,0:T(8,128)(2,1)S(1)} %get-tuple-element.42.a0, bf16[32,256]{1,0:T(8,128)(2,1)S(1)} %collective-permute-done.22.a1, bf16[32,256]{1,0:T(8,128)(2,1)S(1)} %collective-permute-done.23.a2, bf16[32,256]{1,0:T(8,128)(2,1)S(1)} %collective-permute-done.24.a3, ...), custom_call_target="tpu_custom_call" | custom-call | tf_op jit(solution)/shard_map/project/pallas_call | solution.py:35
  189.4 1.0 combine.1
  (94 shorter events, 3.5 us)
Async XLA Ops:
  0.6 1.0 copy-start.6
  1.6 0.7 copy-start.20
  2.3 0.7 copy-start.21
  3.0 0.7 copy-start.22
  3.6 0.7 copy-start.23
  5.9 0.6 copy-start.16
  6.6 71.2 %all-to-all-start = ((bf16[64,4,2048]{2,1,0:T(4,128)(2,1)}), bf16[64,4,2048]{2,1,0:T(4,128)(2,1)}, u32[]{:S(2)}, u32[]{:S(2)}) async-start(bf16[64,4,2048]{2,1,0:T(4,128)(2,1)} %get-tuple-element.27), calls=%async_computation | async-start | bytes 2097152 | tf_op jit(solution)/shard_map/all_to_all | solution.py:155
  18.9 94.9 %copy-start = (bf16[1,2048,256]{2,1,0:T(8,128)(2,1)S(1)}, bf16[1,2048,256]{2,1,0:T(8,128)(2,1)}, u32[]{:S(2)}) copy-start(bf16[1,2048,256]{2,1,0:T(8,128)(2,1)} %param.27) | copy-start | bytes 3145732
  18.9 94.9 %copy-start.1 = (bf16[1,2048,256]{2,1,0:T(8,128)(2,1)S(1)}, bf16[1,2048,256]{2,1,0:T(8,128)(2,1)}, u32[]{:S(2)}) copy-start(bf16[1,2048,256]{2,1,0:T(8,128)(2,1)} %param.28) | copy-start | bytes 3145732
  22.6 8.5 %collective-permute-start = (bf16[32,544]{1,0:T(8,128)(2,1)S(1)}, bf16[32,544]{1,0:T(8,128)(2,1)S(1)}, u32[]{:S(2)}, u32[]{:S(2)}) collective-permute-start(bf16[32,544]{1,0:T(8,128)(2,1)S(1)} %pad_maximum_fusion.2.l0), channel_id=1, source_target_pairs={{0,1},{1,2},{2,3},{3,0},{4,5},{5,6},{6,7},{7,4},{8,9},{9,10},{10,1... | collective-permute-start | bytes 104456 | tf_op jit(solution)/shard_map/ppermute | solution.py:52
  24.1 7.1 %collective-permute-start.1 = (bf16[32,544]{1,0:T(8,128)(2,1)S(1)}, bf16[32,544]{1,0:T(8,128)(2,1)S(1)}, u32[]{:S(2)}, u32[]{:S(2)}) collective-permute-start(bf16[32,544]{1,0:T(8,128)(2,1)S(1)} %pad_maximum_fusion.2.l0), channel_id=1, source_target_pairs={{0,2},{1,3},{2,0},{3,1},{4,6},{5,7},{6,4},{7,5},{8,10},{9,11},{10,... | collective-permute-start | bytes 104456 | tf_op jit(solution)/shard_map/ppermute | solution.py:52
  26.8 4.4 %collective-permute-start.2 = (bf16[32,544]{1,0:T(8,128)(2,1)S(1)}, bf16[32,544]{1,0:T(8,128)(2,1)S(1)}, u32[]{:S(2)}, u32[]{:S(2)}) collective-permute-start(bf16[32,544]{1,0:T(8,128)(2,1)S(1)} %pad_maximum_fusion.2.l0), channel_id=1, source_target_pairs={{0,3},{1,0},{2,1},{3,2},{4,7},{5,4},{6,5},{7,6},{8,11},{9,8},{10,9... | collective-permute-start | bytes 104456 | tf_op jit(solution)/shard_map/ppermute | solution.py:52
  28.2 32.8 %collective-permute-start.7 = (bf16[256,2048]{1,0:T(8,128)(2,1)}, bf16[256,2048]{1,0:T(8,128)(2,1)S(1)}, u32[]{:S(2)}, u32[]{:S(2)}) collective-permute-start(bf16[256,2048]{1,0:T(8,128)(2,1)} %bitcast.29), channel_id=1, source_target_pairs={{0,3},{1,0},{2,1},{3,2},{4,7},{5,4},{6,5},{7,6},{8,11},{9,8},{10,9... | collective-permute-start | bytes 3145736 | tf_op jit(solution)/shard_map/ppermute | solution.py:52
  28.3 32.8 %collective-permute-start.8 = (bf16[256,2048]{1,0:T(8,128)(2,1)}, bf16[256,2048]{1,0:T(8,128)(2,1)}, u32[]{:S(2)}, u32[]{:S(2)}) collective-permute-start(bf16[256,2048]{1,0:T(8,128)(2,1)} %bitcast.30), channel_id=1, source_target_pairs={{0,2},{1,3},{2,0},{3,1},{4,6},{5,7},{6,4},{7,5},{8,10},{9,11},{10,... | collective-permute-start | bytes 3145736 | tf_op jit(solution)/shard_map/ppermute | solution.py:52
  31.1 45.7 %collective-permute-start.9 = (bf16[256,2048]{1,0:T(8,128)(2,1)}, bf16[256,2048]{1,0:T(8,128)(2,1)S(1)}, u32[]{:S(2)}, u32[]{:S(2)}) collective-permute-start(bf16[256,2048]{1,0:T(8,128)(2,1)} %bitcast.31), channel_id=1, source_target_pairs={{0,1},{1,2},{2,3},{3,0},{4,5},{5,6},{6,7},{7,4},{8,9},{9,10},{10,1... | collective-permute-start | bytes 3145736 | tf_op jit(solution)/shard_map/ppermute | solution.py:52
  31.2 1.0 copy-start.7
  32.2 0.9 copy-start.8
  33.2 0.9 copy-start.15
  34.9 12.6 %collective-permute-start.5 = (bf16[256,128]{1,0:T(8,128)(2,1)S(1)}, bf16[256,128]{1,0:T(8,128)(2,1)S(1)}, u32[]{:S(2)}, u32[]{:S(2)}) collective-permute-start(bf16[256,128]{1,0:T(8,128)(2,1)S(1)} %get-tuple-element.31), channel_id=1, source_target_pairs={{0,192},{64,0},{128,64},{192,128},{1,193},{65,1},{129,65},{193,129... | collective-permute-start | bytes 196616 | tf_op jit(solution)/shard_map/ppermute | solution.py:52
  38.8 14.3 %collective-permute-start.4 = (bf16[256,128]{1,0:T(8,128)(2,1)S(1)}, bf16[256,128]{1,0:T(8,128)(2,1)S(1)}, u32[]{:S(2)}, u32[]{:S(2)}) collective-permute-start(bf16[256,128]{1,0:T(8,128)(2,1)S(1)} %get-tuple-element.30), channel_id=1, source_target_pairs={{0,128},{64,192},{128,0},{192,64},{1,129},{65,193},{129,1},{193,65... | collective-permute-start | bytes 196616 | tf_op jit(solution)/shard_map/ppermute | solution.py:52
  47.6 8.2 %copy-start.9 = (bf16[256,128]{1,0:T(8,128)(2,1)}, bf16[256,128]{1,0:T(8,128)(2,1)S(1)}, u32[]{:S(2)}) copy-start(bf16[256,128]{1,0:T(8,128)(2,1)S(1)} %collective-permute-done.5.q3) | copy-start | bytes 196612
  47.6 8.0 %collective-permute-start.3 = (bf16[256,128]{1,0:T(8,128)(2,1)S(1)}, bf16[256,128]{1,0:T(8,128)(2,1)S(1)}, u32[]{:S(2)}, u32[]{:S(2)}) collective-permute-start(bf16[256,128]{1,0:T(8,128)(2,1)S(1)} %get-tuple-element.29), channel_id=1, source_target_pairs={{0,64},{64,128},{128,192},{192,0},{1,65},{65,129},{129,193},{193,1... | collective-permute-start | bytes 196616 | tf_op jit(solution)/shard_map/ppermute | solution.py:52
  53.1 2.6 %copy-start.11 = (bf16[256,128]{1,0:T(8,128)(2,1)}, bf16[256,128]{1,0:T(8,128)(2,1)S(1)}, u32[]{:S(2)}) copy-start(bf16[256,128]{1,0:T(8,128)(2,1)S(1)} %collective-permute-done.4.q2) | copy-start | bytes 196612
  55.6 0.6 copy-start.13
  55.6 5.4 %collective-permute-start.6 = (bf16[4,160,128]{2,1,0:T(8,128)(2,1)S(1)}, bf16[4,160,128]{2,1,0:T(8,128)(2,1)S(1)}, u32[]{:S(2)}, u32[]{:S(2)}) collective-permute-start(bf16[4,160,128]{2,1,0:T(8,128)(2,1)S(1)} %pad_maximum_fusion.1), channel_id=1, source_target_pairs={{0,32},{32,0},{1,33},{33,1},{2,34},{34,2},{3,35},{35,3},{4,36},{36... | collective-permute-start | bytes 491528 | tf_op jit(solution)/shard_map/ppermute | solution.py:52
  76.8 1.0 copy-start.4
  77.8 10.6 %collective-permute-start.12 = (bf16[4,160,256]{2,1,0:T(8,128)(2,1)S(1)}, bf16[4,160,256]{2,1,0:T(8,128)(2,1)S(1)}, u32[]{:S(2)}, u32[]{:S(2)}) collective-permute-start(bf16[4,160,256]{2,1,0:T(8,128)(2,1)S(1)} %pad_maximum_fusion.refs_0_), channel_id=1, source_target_pairs={{0,8},{8,16},{16,24},{24,0},{1,9},{9,17},{17,25},{25,1},{2,10},{10... | collective-permute-start | bytes 983048 | tf_op jit(solution)/shard_map/ppermute | solution.py:52
  79.2 12.1 %collective-permute-start.13 = (bf16[4,160,256]{2,1,0:T(8,128)(2,1)S(1)}, bf16[4,160,256]{2,1,0:T(8,128)(2,1)S(1)}, u32[]{:S(2)}, u32[]{:S(2)}) collective-permute-start(bf16[4,160,256]{2,1,0:T(8,128)(2,1)S(1)} %pad_maximum_fusion.refs_0_), channel_id=1, source_target_pairs={{0,16},{8,24},{16,0},{24,8},{1,17},{9,25},{17,1},{25,9},{2,18},{10... | collective-permute-start | bytes 983048 | tf_op jit(solution)/shard_map/ppermute | solution.py:52
  81.9 15.2 %collective-permute-start.28 = (bf16[32,4,2048]{2,1,0:T(4,128)(2,1)S(1)}, bf16[32,4,2048]{2,1,0:T(4,128)(2,1)S(1)}, u32[]{:S(2)}, u32[]{:S(2)}) collective-permute-start(bf16[32,4,2048]{2,1,0:T(4,128)(2,1)S(1)} %get-tuple-element.53.rows_b), channel_id=1, source_target_pairs={{0,3},{1,0},{2,1},{3,2},{4,7},{5,4},{6,5},{7,6},{8,11},{9,8},{10,9... | collective-permute-start | bytes 1572872 | tf_op jit(solution)/shard_map/ppermute | solution.py:52
  83.7 16.7 %collective-permute-start.25 = (bf16[32,4,2048]{2,1,0:T(4,128)(2,1)S(1)}, bf16[32,4,2048]{2,1,0:T(4,128)(2,1)S(1)}, u32[]{:S(2)}, u32[]{:S(2)}) collective-permute-start(bf16[32,4,2048]{2,1,0:T(4,128)(2,1)S(1)} %get-tuple-element.52.rows_a), channel_id=1, source_target_pairs={{0,1},{1,2},{2,3},{3,0},{4,5},{5,6},{6,7},{7,4},{8,9},{9,10},{10,1... | collective-permute-start | bytes 1572872 | tf_op jit(solution)/shard_map/ppermute | solution.py:52
  84.0 13.1 %collective-permute-start.14 = (bf16[4,160,256]{2,1,0:T(8,128)(2,1)S(1)}, bf16[4,160,256]{2,1,0:T(8,128)(2,1)S(1)}, u32[]{:S(2)}, u32[]{:S(2)}) collective-permute-start(bf16[4,160,256]{2,1,0:T(8,128)(2,1)S(1)} %pad_maximum_fusion.refs_0_), channel_id=1, source_target_pairs={{0,24},{8,0},{16,8},{24,16},{1,25},{9,1},{17,9},{25,17},{2,26},{10... | collective-permute-start | bytes 983048 | tf_op jit(solution)/shard_map/ppermute | solution.py:52
  88.3 8.8 %collective-permute-start.15 = (bf16[4,160,256]{2,1,0:T(8,128)(2,1)S(1)}, bf16[4,160,256]{2,1,0:T(8,128)(2,1)S(1)}, u32[]{:S(2)}, u32[]{:S(2)}) collective-permute-start(bf16[4,160,256]{2,1,0:T(8,128)(2,1)S(1)} %pad_maximum_fusion.refs_0_), channel_id=1, source_target_pairs={{0,4},{4,0},{1,5},{5,1},{2,6},{6,2},{3,7},{7,3},{8,12},{12,8},{9,1... | collective-permute-start | bytes 983048 | tf_op jit(solution)/shard_map/ppermute | solution.py:52
  91.4 9.0 %collective-permute-start.16 = (bf16[4,160,256]{2,1,0:T(8,128)(2,1)S(1)}, bf16[4,160,256]{2,1,0:T(8,128)(2,1)S(1)}, u32[]{:S(2)}, u32[]{:S(2)}) collective-permute-start(bf16[4,160,256]{2,1,0:T(8,128)(2,1)S(1)} %collective-permute-done.12.refs_1_), channel_id=1, source_target_pairs={{0,4},{4,0},{1,5},{5,1},{2,6},{6,2},{3,7},{7,3},{8,12},{12,8},{9,1... | collective-permute-start | bytes 983048 | tf_op jit(solution)/shard_map/ppermute | solution.py:52
  97.1 6.5 %collective-permute-start.17 = (bf16[4,160,256]{2,1,0:T(8,128)(2,1)S(1)}, bf16[4,160,256]{2,1,0:T(8,128)(2,1)S(1)}, u32[]{:S(2)}, u32[]{:S(2)}) collective-permute-start(bf16[4,160,256]{2,1,0:T(8,128)(2,1)S(1)} %collective-permute-done.13.refs_2_), channel_id=1, source_target_pairs={{0,4},{4,0},{1,5},{5,1},{2,6},{6,2},{3,7},{7,3},{8,12},{12,8},{9,1... | collective-permute-start | bytes 983048 | tf_op jit(solution)/shard_map/ppermute | solution.py:52
  97.1 16.6 %collective-permute-start.10 = (bf16[32,4,2048]{2,1,0:T(4,128)(2,1)S(1)}, bf16[32,4,2048]{2,1,0:T(4,128)(2,1)S(1)}, u32[]{:S(2)}, u32[]{:S(2)}) collective-permute-start(bf16[32,4,2048]{2,1,0:T(4,128)(2,1)S(1)} %get-tuple-element.53.rows_b), channel_id=1, source_target_pairs={{0,1},{1,2},{2,3},{3,0},{4,5},{5,6},{6,7},{7,4},{8,9},{9,10},{10,1... | collective-permute-start | bytes 1572872 | tf_op jit(solution)/shard_map/ppermute | solution.py:52
  97.1 16.6 %collective-permute-start.11 = (bf16[32,4,2048]{2,1,0:T(4,128)(2,1)S(1)}, bf16[32,4,2048]{2,1,0:T(4,128)(2,1)S(1)}, u32[]{:S(2)}, u32[]{:S(2)}) collective-permute-start(bf16[32,4,2048]{2,1,0:T(4,128)(2,1)S(1)} %get-tuple-element.52.rows_a), channel_id=1, source_target_pairs={{0,3},{1,0},{2,1},{3,2},{4,7},{5,4},{6,5},{7,6},{8,11},{9,8},{10,9... | collective-permute-start | bytes 1572872 | tf_op jit(solution)/shard_map/ppermute | solution.py:52
  100.4 24.0 %collective-permute-start.27 = (bf16[32,4,2048]{2,1,0:T(4,128)(2,1)S(1)}, bf16[32,4,2048]{2,1,0:T(4,128)(2,1)S(1)}, u32[]{:S(2)}, u32[]{:S(2)}) collective-permute-start(bf16[32,4,2048]{2,1,0:T(4,128)(2,1)S(1)} %collective-permute-done.25.rows_a), channel_id=1, source_target_pairs={{0,1},{1,2},{2,3},{3,0},{4,5},{5,6},{6,7},{7,4},{8,9},{9,10},{10,1... | collective-permute-start | bytes 1572872 | tf_op jit(solution)/shard_map/ppermute | solution.py:52
  100.4 24.0 %collective-permute-start.29 = (bf16[32,4,2048]{2,1,0:T(4,128)(2,1)S(1)}, bf16[32,4,2048]{2,1,0:T(4,128)(2,1)S(1)}, u32[]{:S(2)}, u32[]{:S(2)}) collective-permute-start(bf16[32,4,2048]{2,1,0:T(4,128)(2,1)S(1)} %collective-permute-done.28.rows_b), channel_id=1, source_target_pairs={{0,3},{1,0},{2,1},{3,2},{4,7},{5,4},{6,5},{7,6},{8,11},{9,8},{10,9... | collective-permute-start | bytes 1572872 | tf_op jit(solution)/shard_map/ppermute | solution.py:52
  103.6 1.6 collective-permute-start.18
  105.2 0.8 copy-start.10
  106.1 0.8 copy-start.12
  106.9 0.8 copy-start.14
  113.7 0.8 copy-start.18
  113.7 0.8 copy-start.24
  113.7 11.4 %copy-start.26 = (bf16[128,64]{1,0:T(8,128)(2,1)}, bf16[128,64]{1,0:T(8,128)(2,1)S(1)}, u32[]{:S(2)}) copy-start(bf16[128,64]{1,0:T(8,128)(2,1)S(1)} %get-tuple-element.40) | copy-start | bytes 49156
  113.7 11.4 %copy-start.28 = (bf16[128,64]{1,0:T(8,128)(2,1)}, bf16[128,64]{1,0:T(8,128)(2,1)S(1)}, u32[]{:S(2)}) copy-start(bf16[128,64]{1,0:T(8,128)(2,1)S(1)} %get-tuple-element.39) | copy-start | bytes 49156
  114.5 17.2 %copy-start.3 = (bf16[1,256,2048]{2,1,0:T(8,128)(2,1)S(1)}, bf16[1,256,2048]{2,1,0:T(8,128)(2,1)}, u32[]{:S(2)}) copy-start(bf16[1,256,2048]{2,1,0:T(8,128)(2,1)} %param.29) | copy-start | bytes 3145732
  114.5 17.2 %copy-start.5 = (bf16[256,2048]{1,0:T(8,128)(2,1)S(1)}, bf16[256,2048]{1,0:T(8,128)(2,1)}, u32[]{:S(2)}) copy-start(bf16[256,2048]{1,0:T(8,128)(2,1)} %copy-done.4) | copy-start | bytes 3145732
  114.5 12.9 %collective-permute-start.31 = (bf16[256,256]{1,0:T(8,128)(2,1)S(1)}, bf16[256,256]{1,0:T(8,128)(2,1)S(1)}, u32[]{:S(2)}, u32[]{:S(2)}) collective-permute-start(bf16[256,256]{1,0:T(8,128)(2,1)S(1)} %hidden_right.1), channel_id=1, source_target_pairs={{0,1},{1,2},{2,3},{3,0},{4,5},{5,6},{6,7},{7,4},{8,9},{9,10},{10,1... | collective-permute-start | bytes 393224 | tf_op jit(solution)/shard_map/ppermute | solution.py:52
  115.6 11.9 %collective-permute-start.26 = (bf16[256,256]{1,0:T(8,128)(2,1)S(1)}, bf16[256,256]{1,0:T(8,128)(2,1)S(1)}, u32[]{:S(2)}, u32[]{:S(2)}) collective-permute-start(bf16[256,256]{1,0:T(8,128)(2,1)S(1)} %hidden_left.1), channel_id=1, source_target_pairs={{0,3},{1,0},{2,1},{3,2},{4,7},{5,4},{6,5},{7,6},{8,11},{9,8},{10,9... | collective-permute-start | bytes 393224 | tf_op jit(solution)/shard_map/ppermute | solution.py:52
  125.1 6.6 %collective-permute-start.30 = (bf16[256,256]{1,0:T(8,128)(2,1)S(1)}, bf16[256,256]{1,0:T(8,128)(2,1)S(1)}, u32[]{:S(2)}, u32[]{:S(2)}) collective-permute-start(bf16[256,256]{1,0:T(8,128)(2,1)S(1)} %hidden_far.1), channel_id=1, source_target_pairs={{0,2},{1,3},{2,0},{3,1},{4,6},{5,7},{6,4},{7,5},{8,10},{9,11},{10,... | collective-permute-start | bytes 393224 | tf_op jit(solution)/shard_map/ppermute | solution.py:52
  127.4 17.4 %copy-start.29 = (bf16[128,64]{1,0:T(8,128)(2,1)S(1)}, bf16[128,64]{1,0:T(8,128)(2,1)}, u32[]{:S(2)}) copy-start(bf16[128,64]{1,0:T(8,128)(2,1)} %copy-done.28) | copy-start | bytes 49156
  127.4 21.3 %copy-start.27 = (bf16[128,64]{1,0:T(8,128)(2,1)S(1)}, bf16[128,64]{1,0:T(8,128)(2,1)}, u32[]{:S(2)}) copy-start(bf16[128,64]{1,0:T(8,128)(2,1)} %copy-done.26) | copy-start | bytes 49156
  127.5 23.4 %copy-start.25 = (bf16[128,64]{1,0:T(8,128)(2,1)S(1)}, bf16[128,64]{1,0:T(8,128)(2,1)}, u32[]{:S(2)}) copy-start(bf16[128,64]{1,0:T(8,128)(2,1)} %copy-done.24) | copy-start | bytes 49156
  127.5 48.6 %copy-start.19 = (bf16[128,64]{1,0:T(8,128)(2,1)S(1)}, bf16[128,64]{1,0:T(8,128)(2,1)}, u32[]{:S(2)}) copy-start(bf16[128,64]{1,0:T(8,128)(2,1)} %copy-done.18) | copy-start | bytes 49156
  135.3 54.2 %copy-start.17 = (bf16[256,128]{1,0:T(8,128)(2,1)S(1)}, bf16[256,128]{1,0:T(8,128)(2,1)}, u32[]{:S(2)}) copy-start(bf16[256,128]{1,0:T(8,128)(2,1)} %copy-done.16) | copy-start | bytes 196612
  135.3 54.2 %all-to-all-start.1 = ((bf16[64,4,2048]{2,1,0:T(4,128)(2,1)}), bf16[64,4,2048]{2,1,0:T(4,128)(2,1)S(1)}, u32[]{:S(2)}, u32[]{:S(2)}) async-start(bf16[64,4,2048]{2,1,0:T(4,128)(2,1)} %down.1), calls=%async_computation.1 | async-start | bytes 2097152 | tf_op jit(solution)/shard_map/all_to_all | solution.py:174
  144.8 26.7 %collective-permute-start.19 = (bf16[128,64]{1,0:T(8,128)(2,1)S(1)}, bf16[128,64]{1,0:T(8,128)(2,1)S(1)}, u32[]{:S(2)}, u32[]{:S(2)}) collective-permute-start(bf16[128,64]{1,0:T(8,128)(2,1)S(1)} %copy-done.29), channel_id=1, source_target_pairs={{0,192},{64,0},{128,64},{192,128},{1,193},{65,1},{129,65},{193,129... | collective-permute-start | bytes 49160 | tf_op jit(solution)/shard_map/ppermute | solution.py:52
  148.7 27.3 %collective-permute-start.20 = (bf16[128,64]{1,0:T(8,128)(2,1)S(1)}, bf16[128,64]{1,0:T(8,128)(2,1)S(1)}, u32[]{:S(2)}, u32[]{:S(2)}) collective-permute-start(bf16[128,64]{1,0:T(8,128)(2,1)S(1)} %copy-done.27), channel_id=1, source_target_pairs={{0,128},{64,192},{128,0},{192,64},{1,129},{65,193},{129,1},{193,65... | collective-permute-start | bytes 49160 | tf_op jit(solution)/shard_map/ppermute | solution.py:52
  150.9 25.1 %collective-permute-start.21 = (bf16[128,64]{1,0:T(8,128)(2,1)S(1)}, bf16[128,64]{1,0:T(8,128)(2,1)S(1)}, u32[]{:S(2)}, u32[]{:S(2)}) collective-permute-start(bf16[128,64]{1,0:T(8,128)(2,1)S(1)} %copy-done.25), channel_id=1, source_target_pairs={{0,64},{64,128},{128,192},{192,0},{1,65},{65,129},{129,193},{193,1... | collective-permute-start | bytes 49160 | tf_op jit(solution)/shard_map/ppermute | solution.py:52
  176.7 5.0 %collective-permute-start.22 = (bf16[32,256]{1,0:T(8,128)(2,1)S(1)}, bf16[32,256]{1,0:T(8,128)(2,1)S(1)}, u32[]{:S(2)}, u32[]{:S(2)}) collective-permute-start(bf16[32,256]{1,0:T(8,128)(2,1)S(1)} %get-tuple-element.43), channel_id=1, source_target_pairs={{0,1},{1,2},{2,3},{3,0},{4,5},{5,6},{6,7},{7,4},{8,9},{9,10},{10,1... | collective-permute-start | bytes 49160 | tf_op jit(solution)/shard_map/ppermute | solution.py:52
  177.3 6.0 %collective-permute-start.23 = (bf16[32,256]{1,0:T(8,128)(2,1)S(1)}, bf16[32,256]{1,0:T(8,128)(2,1)S(1)}, u32[]{:S(2)}, u32[]{:S(2)}) collective-permute-start(bf16[32,256]{1,0:T(8,128)(2,1)S(1)} %get-tuple-element.44), channel_id=1, source_target_pairs={{0,2},{1,3},{2,0},{3,1},{4,6},{5,7},{6,4},{7,5},{8,10},{9,11},{10,... | collective-permute-start | bytes 49160 | tf_op jit(solution)/shard_map/ppermute | solution.py:52
  181.4 3.7 %collective-permute-start.24 = (bf16[32,256]{1,0:T(8,128)(2,1)S(1)}, bf16[32,256]{1,0:T(8,128)(2,1)S(1)}, u32[]{:S(2)}, u32[]{:S(2)}) collective-permute-start(bf16[32,256]{1,0:T(8,128)(2,1)S(1)} %get-tuple-element.45), channel_id=1, source_target_pairs={{0,3},{1,0},{2,1},{3,2},{4,7},{5,4},{6,5},{7,6},{8,11},{9,8},{10,9... | collective-permute-start | bytes 49160 | tf_op jit(solution)/shard_map/ppermute | solution.py:52
  185.2 2.2 %copy-start.2 = (bf16[1024,2048]{1,0:T(8,128)(2,1)S(1)}, bf16[1024,2048]{1,0:T(8,128)(2,1)}, u32[]{:S(2)}) copy-start(bf16[1024,2048]{1,0:T(8,128)(2,1)} %out_proj.1) | copy-start | bytes 12582916

commit v3 on v2

--- a/solution.py
+++ b/solution.py
@@ -4,6 +4,7 @@
 from jax.experimental import pallas as pl
 from jax.experimental.pallas import tpu as pltpu
 from jax.sharding import Mesh, PartitionSpec as P
+
 
 NOPE = 64
 ROPE_DIM = 32
@@ -19,6 +20,7 @@
 masked_value = -1e30
 log2_e = 1.4426950408889634
 
+
 AXES = ("zh", "zl", "y", "c", "x")
 EP = AXES[:4]
 
@@ -26,8 +28,11 @@
 VMEM_SPEC = pl.BlockSpec(memory_space=pltpu.VMEM)
 
 
-def call(kernel, out_shape, name, arrays, where=None, scratch=(), limit=16 << 20):
-    arrays = [pltpu.with_memory_space_constraint(a, pltpu.VMEM) for a in arrays]
+def call(kernel, out_shape, arrays, where=None, scratch=(), limit=16 << 20, unplaced=()):
+    arrays = [
+        a if i in unplaced else pltpu.with_memory_space_constraint(a, pltpu.VMEM)
+        for i, a in enumerate(arrays)
+    ]
     specs = [VMEM_SPEC] * len(arrays)
     if where is not None:
         arrays, specs = [where] + arrays, [SMEM_SPEC] + specs
@@ -39,7 +44,6 @@
         out_shape=out_shape,
         scratch_shapes=list(scratch),
         compiler_params=pltpu.CompilerParams(vmem_limit_bytes=limit),
-        name=name,
     )(*arrays)
 
 
@@ -97,8 +101,8 @@
             jax.ShapeDtypeStruct((experts, CAP, width), BF),
             jax.ShapeDtypeStruct((experts * CAP, 2 * rows), BF),
         ),
-        "dispatch",
         [tokens, gain[None, :], routes.T, group_prob[None, :], expert_prob.T],
+        unplaced=range(5),
     )
 
 
@@ -111,9 +115,9 @@
         out[at : at + half, :] = (gate / (1.0 + jnp.exp(-gate)) * up).astype(BF)
 
 
-def hidden_of(rows_a, rows_b, w_gate, w_up, name):
+def hidden_of(rows_a, rows_b, w_gate, w_up):
     shape = jax.ShapeDtypeStruct((2 * rows_a.shape[0] * CAP, w_gate.shape[1]), BF)
-    return call(hidden_kernel, shape, name, [rows_a, rows_b, w_gate, w_up])
+    return call(hidden_kernel, shape, [rows_a, rows_b, w_gate, w_up])
 
 
 def down_kernel(h0, h1, h2, h3, w0, w1, w2, w3, out):
@@ -154,7 +158,6 @@
     outgoing, shares = dispatch(tokens, moe_gain, routes, group_prob, expert_prob, experts)
     arrived = lax.all_to_all(outgoing, EP, split_axis=0, concat_axis=0, tiled=True)
     queries, pair = query_and_pair(where, query, latent, rope_key, latent_gain, key_up, value_up)
-    arrived, pair, down = lax.optimization_barrier((arrived, pair, down))
     down = [w_down] + down
     half = experts // 2
     a, b = arrived[:half], arrived[half:]
@@ -162,26 +165,25 @@
     left_b, right_a = shifted(b, "x", 1), shifted(a, "x", -1)
     far_a, far_b = shifted(left_a, "x", 1), shifted(right_b, "x", -1)
     parts = attend(where, queries, pair)
-    left_b, right_a, parts = lax.optimization_barrier((left_b, right_a, parts))
     hidden = [
-        hidden_of(a, b, w_gate, w_up, "hidden_own"),
-        shifted(hidden_of(left_a, left_b, w_gate, w_up, "hidden_left"), "x", -1),
-        shifted(hidden_of(far_a, far_b, w_gate, w_up, "hidden_far"), "x", 2),
-        shifted(hidden_of(right_a, right_b, w_gate, w_up, "hidden_right"), "x", 1),
+        hidden_of(a, b, w_gate, w_up),
+        shifted(hidden_of(left_a, left_b, w_gate, w_up), "x", -1),
+        shifted(hidden_of(far_a, far_b, w_gate, w_up), "x", 2),
+        shifted(hidden_of(right_a, right_b, w_gate, w_up), "x", 1),
     ]
     shape = jax.ShapeDtypeStruct((experts, CAP, width), BF)
-    result = call(down_kernel, shape, "down", hidden + down)
+    result = call(down_kernel, shape, hidden + down)
     returned = lax.all_to_all(result, EP, split_axis=0, concat_axis=0, tiled=True)
     mixed = project(where, parts, out_proj, latent.shape[0])
     shape = jax.ShapeDtypeStruct((rows, width), BF)
-    return mixed, call(combine_kernel, shape, "combine", [returned, shares])
+    return mixed, call(combine_kernel, shape, [returned, shares])
 
 
 def heads_kernel(
     where, l0, l1, l2, l3, key_up, value_up, query, cosine, sine, o0, o1, o2, o3, strip_s, heads
 ):
     latent = key_up.shape[0]
-    own, strip = l0.shape[0], query.shape[0]
+    own = l0.shape[0]
     count = heads.shape[0]
     half = ROPE_DIM // 2
     turned = query[...].astype(F32).T
@@ -309,13 +311,13 @@
     blocks = call(
         heads_kernel,
         [jax.ShapeDtypeStruct((QK_DIM + KV_ROWS, strip), BF)] * 4,
-        "heads",
         near + [key_up, value_up, query, cosine.T, sine.T],
         where,
         [
             pltpu.VMEM((strip, both.shape[1]), BF),
             pltpu.VMEM((4, QK_DIM + KV_ROWS, strip), BF),
         ],
+        unplaced=range(4, 9),
     )
     blocks = [blocks[0]] + [shifted(blocks[k], "zh", k) for k in range(1, 4)]
     mine = jnp.stack([block[QK_DIM:] for block in blocks])
@@ -329,7 +331,6 @@
     return call(
         attend_kernel,
         [jax.ShapeDtypeStruct((strip, V_DIM), BF)] * 4,
-        "attend",
         blocks + column,
         where,
         [
@@ -346,7 +347,6 @@
     parts = call(
         spread_kernel,
         [jax.ShapeDtypeStruct((own, 4 * V_DIM), BF)] * 4,
-        "spread",
         parts,
         where,
         [pltpu.VMEM((4, strip, V_DIM), BF), pltpu.VMEM((4, own, 4 * V_DIM), BF)],
@@ -355,7 +355,6 @@
     return call(
         project_kernel,
         jax.ShapeDtypeStruct((own, out_proj.shape[1]), BF),
-        "project",
         parts + [out_proj],
         where,
         [pltpu.VMEM((4, own, 4 * V_DIM), BF)],

time: 191 us -> 235 us (1.23)
  the two profiles are of different devices: /device:TPU:8 before, /device:TPU:224 now
where the time goes in v3:
time: 235 us; the launch traced here: 231 us
  waiting for transfers between devices  93.4 us (40%)
  starting transfers between devices  72.3 us (31%)
  blocking collectives  36 us (15%)
  Pallas kernels  20.6 us (9%)
  local copies, waits for them, and re-layouts  7.46 us (3%)
    ppermute x32, waiting for transfers between devices, shifted(): return lax.ppermute(value, axis, [(i, (i + amount) % n) for i in range(n)])  93.4 us
    ppermute x32, starting transfers between devices, shifted(): return lax.ppermute(value, axis, [(i, (i + amount) % n) for i in range(n)])  65.5 us
    all_to_all x1, blocking collectives, both_halves(): lax.all_to_all(outgoing, EP, split_axis=0, concat_axis=0, tiled=True)  36 us
    pallas_call x11, Pallas kernels, call(): pl.pallas_call(kernel, in_specs=specs, out_specs=VMEM_SPEC if single else...  20.6 us
    all_to_all x1, starting transfers between devices, both_halves(): lax.all_to_all(result, EP, split_axis=0, concat_axis=0, tiled=True)  6.81 us
    unnamed x37, local copies, waits for them, and re-layouts  6.79 us
  transfers between devices with their start and end apart: 33, of which 16 were waited for; matrix products, arithmetic and copies ran while one was open for 0% of the time, Pallas kernels for 8%

profile of v3, /device:TPU:224, one launch (start us, length us, event | category | flops | bytes accessed | tf_op | source)
XLA Modules:
  0.0 231.3 jit_solution(1240792825445422736)
XLA Ops:
  0.7 1.1 copy-done.7
  1.8 0.7 copy-done.11
  2.5 0.7 copy-done.12
  3.1 0.7 copy-done.13
  3.8 0.7 copy-done.14
  4.5 0.6 shard_map.162
  5.1 36.0 %all_to_all.10 = bf16[64,4,2048]{2,1,0:T(4,128)(2,1)S(1)} all-to-all(bf16[64,4,2048]{2,1,0:T(4,128)(2,1)S(1)} %get-tuple-element.28), channel_id=1, replica_groups=mesh['zh'=4,'zl'=2,'y'=4,'c'=2,'x'=4] {'zh','zl','y','c'}, dimensions={0} | all-to-all | bytes 2097152 | tf_op jit(solution)/shard_map/all_to_all | solution.py:159
  41.1 0.5 fusion.11
  41.6 1.6 collective-permute-start.20
  43.2 1.7 collective-permute-start.24
  44.9 0.3 collective-permute-start.21
  45.2 3.0 %collective-permute-start.27 = (bf16[32,4,2048]{2,1,0:T(4,128)(2,1)S(1)}, bf16[32,4,2048]{2,1,0:T(4,128)(2,1)}, u32[]{:S(2)}, u32[]{:S(2)}) collective-permute-start(bf16[32,4,2048]{2,1,0:T(4,128)(2,1)S(1)} %get-tuple-element.31.rows_a), channel_id=1, source_target_pairs={{0,3},{1,0},{2,1},{3,2},{4,7},{5,4},{6,5},{7,6},{8,11},{9,8},{10,9... | collective-permute-start | bytes 1572872 | tf_op jit(solution)/shard_map/ppermute | solution.py:56
  48.2 0.3 collective-permute-start.29
  48.6 9.1 %collective-permute-done.20.rows_a = bf16[32,4,2048]{2,1,0:T(4,128)(2,1)S(1)} collective-permute-done((bf16[32,4,2048]{2,1,0:T(4,128)(2,1)S(1)}, bf16[32,4,2048]{2,1,0:T(4,128)(2,1)S(1)}, u32[]{:S(2)}, u32[]{:S(2)}) %collective-permute-start.20) | collective-permute-done | bytes 524320 | tf_op jit(solution)/shard_map/ppermute | solution.py:56
  57.7 1.8 collective-permute-start.30
  59.5 0.8 copy-done.3
  60.3 0.6 collective-permute-start.31
  61.1 8.4 %collective-permute-done.21.rows_b = bf16[32,4,2048]{2,1,0:T(4,128)(2,1)} collective-permute-done((bf16[32,4,2048]{2,1,0:T(4,128)(2,1)S(1)}, bf16[32,4,2048]{2,1,0:T(4,128)(2,1)}, u32[]{:S(2)}, u32[]{:S(2)}) %collective-permute-start.21) | collective-permute-done | bytes 524320 | tf_op jit(solution)/shard_map/ppermute | solution.py:56
  69.5 20.6 %collective-permute-start.23 = (bf16[32,4,2048]{2,1,0:T(4,128)(2,1)}, bf16[32,4,2048]{2,1,0:T(4,128)(2,1)S(1)}, u32[]{:S(2)}, u32[]{:S(2)}) collective-permute-start(bf16[32,4,2048]{2,1,0:T(4,128)(2,1)} %copy-done.5), channel_id=1, source_target_pairs={{0,1},{1,2},{2,3},{3,0},{4,5},{5,6},{6,7},{7,4},{8,9},{9,10},{10,1... | collective-permute-start | bytes 1572872 | tf_op jit(solution)/shard_map/ppermute | solution.py:56
  90.4 1.0 copy-done.6
  91.5 1.8 shard_map.164
  93.3 1.0 copy-done.4
  94.3 1.8 shard_map.166
  96.1 28.3 %collective-permute-done.23.rows_a = bf16[32,4,2048]{2,1,0:T(4,128)(2,1)S(1)} collective-permute-done((bf16[32,4,2048]{2,1,0:T(4,128)(2,1)}, bf16[32,4,2048]{2,1,0:T(4,128)(2,1)S(1)}, u32[]{:S(2)}, u32[]{:S(2)}) %collective-permute-start.23) | collective-permute-done | bytes 524320 | tf_op jit(solution)/shard_map/ppermute | solution.py:56
  124.4 1.6 collective-permute-start.22
  126.0 0.4 collective-permute-start.28
  126.4 0.7 shard_map.165
  127.2 2.5 %collective-permute-start.26 = (bf16[256,256]{1,0:T(8,128)(2,1)S(1)}, bf16[256,256]{1,0:T(8,128)(2,1)S(1)}, u32[]{:S(2)}, u32[]{:S(2)}) collective-permute-start(bf16[256,256]{1,0:T(8,128)(2,1)S(1)} %shard_map.165), channel_id=1, source_target_pairs={{0,2},{1,3},{2,0},{3,1},{4,6},{5,7},{6,4},{7,5},{8,10},{9,11},{10,... | collective-permute-start | bytes 393224 | tf_op jit(solution)/shard_map/ppermute | solution.py:56
  129.7 0.7 shard_map.163.h0
  130.5 1.4 collective-permute-start
  131.9 1.2 collective-permute-start.1
  133.0 1.6 collective-permute-start.2
  134.6 0.6 collective-permute-done.28.h3
  135.3 4.5 %shard_map.167 = bf16[64,4,2048]{2,1,0:T(4,128)(2,1)} custom-call(bf16[256,256]{1,0:T(8,128)(2,1)S(1)} %shard_map.163.h0, bf16[256,256]{1,0:T(8,128)(2,1)S(1)} %collective-permute-done.22.h1, bf16[256,256]{1,0:T(8,128)(2,1)S(1)} %collective-permute-done.26.h2, bf16[256,256]{1,0:T(8,128)(2,1)S(1)} %collective-permute-done.28.h3, ...), custom_call_target="tpu_custom_call" | custom-call | tf_op jit(solution)/shard_map/pallas_call | solution.py:40
  139.7 6.8 %all-to-all-start.1 = ((bf16[64,4,2048]{2,1,0:T(4,128)(2,1)}), bf16[64,4,2048]{2,1,0:T(4,128)(2,1)S(1)}, u32[]{:S(2)}, u32[]{:S(2)}) async-start(bf16[64,4,2048]{2,1,0:T(4,128)(2,1)} %shard_map.167), calls=%async_computation.1 | async-start | bytes 2097152 | tf_op jit(solution)/shard_map/all_to_all | solution.py:176
  146.8 0.9 shard_map.158
  147.7 2.3 %collective-permute-start.5 = (bf16[256,128]{1,0:T(8,128)(2,1)S(1)}, bf16[256,128]{1,0:T(8,128)(2,1)S(1)}, u32[]{:S(2)}, u32[]{:S(2)}) collective-permute-start(bf16[256,128]{1,0:T(8,128)(2,1)S(1)} %get-tuple-element.19), channel_id=1, source_target_pairs={{0,192},{64,0},{128,64},{192,128},{1,193},{65,1},{129,65},{193,129... | collective-permute-start | bytes 196616 | tf_op jit(solution)/shard_map/ppermute | solution.py:56
  150.0 1.3 collective-permute-start.4
  151.4 3.6 %collective-permute-start.3 = (bf16[256,128]{1,0:T(8,128)(2,1)S(1)}, bf16[256,128]{1,0:T(8,128)(2,1)S(1)}, u32[]{:S(2)}, u32[]{:S(2)}) collective-permute-start(bf16[256,128]{1,0:T(8,128)(2,1)S(1)} %get-tuple-element.17), channel_id=1, source_target_pairs={{0,64},{64,128},{128,192},{192,0},{1,65},{65,129},{129,193},{193,1... | collective-permute-start | bytes 196616 | tf_op jit(solution)/shard_map/ppermute | solution.py:56
  155.0 19.6 %collective-permute-done.5.q3 = bf16[256,128]{1,0:T(8,128)(2,1)S(1)} collective-permute-done((bf16[256,128]{1,0:T(8,128)(2,1)S(1)}, bf16[256,128]{1,0:T(8,128)(2,1)S(1)}, u32[]{:S(2)}, u32[]{:S(2)}) %collective-permute-start.5) | collective-permute-done | bytes 65568 | tf_op jit(solution)/shard_map/ppermute | solution.py:56
  174.6 2.5 %collective-permute-done.4.q2 = bf16[256,128]{1,0:T(8,128)(2,1)S(1)} collective-permute-done((bf16[256,128]{1,0:T(8,128)(2,1)S(1)}, bf16[256,128]{1,0:T(8,128)(2,1)S(1)}, u32[]{:S(2)}, u32[]{:S(2)}) %collective-permute-start.4) | collective-permute-done | bytes 65568 | tf_op jit(solution)/shard_map/ppermute | solution.py:56
  177.1 2.1 collective-permute-start.6
  179.2 4.0 %collective-permute-done.6 = bf16[4,160,128]{2,1,0:T(8,128)(2,1)S(1)} collective-permute-done((bf16[4,160,128]{2,1,0:T(8,128)(2,1)S(1)}, bf16[4,160,128]{2,1,0:T(8,128)(2,1)S(1)}, u32[]{:S(2)}, u32[]{:S(2)}) %collective-permute-start.6) | collective-permute-done | bytes 163872 | tf_op jit(solution)/shard_map/ppermute | solution.py:56
  183.2 1.5 collective-permute-start.7
  184.8 2.9 %collective-permute-start.8 = (bf16[4,160,256]{2,1,0:T(8,128)(2,1)S(1)}, bf16[4,160,256]{2,1,0:T(8,128)(2,1)S(1)}, u32[]{:S(2)}, u32[]{:S(2)}) collective-permute-start(bf16[4,160,256]{2,1,0:T(8,128)(2,1)S(1)} %pad_maximum_fusion.refs_0_), channel_id=1, source_target_pairs={{0,16},{8,24},{16,0},{24,8},{1,17},{9,25},{17,1},{25,9},{2,18},{10... | collective-permute-start | bytes 983048 | tf_op jit(solution)/shard_map/ppermute | solution.py:56
  187.6 1.4 collective-permute-start.9
  189.1 4.8 %collective-permute-done.7.refs_1_ = bf16[4,160,256]{2,1,0:T(8,128)(2,1)S(1)} collective-permute-done((bf16[4,160,256]{2,1,0:T(8,128)(2,1)S(1)}, bf16[4,160,256]{2,1,0:T(8,128)(2,1)S(1)}, u32[]{:S(2)}, u32[]{:S(2)}) %collective-permute-start.7) | collective-permute-done | bytes 327712 | tf_op jit(solution)/shard_map/ppermute | solution.py:56
  193.8 7.6 %collective-permute-done.8.refs_2_ = bf16[4,160,256]{2,1,0:T(8,128)(2,1)S(1)} collective-permute-done((bf16[4,160,256]{2,1,0:T(8,128)(2,1)S(1)}, bf16[4,160,256]{2,1,0:T(8,128)(2,1)S(1)}, u32[]{:S(2)}, u32[]{:S(2)}) %collective-permute-start.8) | collective-permute-done | bytes 327712 | tf_op jit(solution)/shard_map/ppermute | solution.py:56
  201.4 0.5 collective-permute-start.13
  202.0 1.1 collective-permute-done.12.refs_6_
  203.1 0.5 collective-permute-done.13.refs_7_
  203.5 5.8 %shard_map.159 = (bf16[128,64]{1,0:T(8,128)(2,1)S(1)}, bf16[128,64]{1,0:T(8,128)(2,1)S(1)}, bf16[128,64]{1,0:T(8,128)(2,1)S(1)}, bf16[128,64]{1,0:T(8,128)(2,1)S(1)}) custom-call(s32[5]{0:T(128)S(1)} %stack.38.where, bf16[256,128]{1,0:T(8,128)(2,1)S(1)} %get-tuple-element.16.q0, bf16[256,128]{1,0:T(8,128)(2,1)S(1)} %collective-permute-done.3.q1, ...), custom_call_target="tpu_custom_call" | custom-call | tf_op jit(solution)/shard_map/pallas_call | solution.py:40
  209.5 5.8 %collective-permute-start.15 = (bf16[128,64]{1,0:T(8,128)(2,1)S(1)}, bf16[128,64]{1,0:T(8,128)(2,1)S(1)}, u32[]{:S(2)}, u32[]{:S(2)}) collective-permute-start(bf16[128,64]{1,0:T(8,128)(2,1)S(1)} %get-tuple-element.22), channel_id=1, source_target_pairs={{0,128},{64,192},{128,0},{192,64},{1,129},{65,193},{129,1},{193,65... | collective-permute-start | bytes 49160 | tf_op jit(solution)/shard_map/ppermute | solution.py:56
  215.2 1.1 collective-permute-start.16
  216.3 1.1 collective-permute-done.15.a2
  217.5 2.8 %collective-permute-done.16.a3 = bf16[128,64]{1,0:T(8,128)(2,1)S(1)} collective-permute-done((bf16[128,64]{1,0:T(8,128)(2,1)S(1)}, bf16[128,64]{1,0:T(8,128)(2,1)S(1)}, u32[]{:S(2)}, u32[]{:S(2)}) %collective-permute-start.16) | collective-permute-done | bytes 16416 | tf_op jit(solution)/shard_map/ppermute | solution.py:56
  220.3 0.7 shard_map.160
  221.0 3.4 %collective-permute-start.18 = (bf16[32,256]{1,0:T(8,128)(2,1)S(1)}, bf16[32,256]{1,0:T(8,128)(2,1)S(1)}, u32[]{:S(2)}, u32[]{:S(2)}) collective-permute-start(bf16[32,256]{1,0:T(8,128)(2,1)S(1)} %get-tuple-element.26), channel_id=1, source_target_pairs={{0,2},{1,3},{2,0},{3,1},{4,6},{5,7},{6,4},{7,5},{8,10},{9,11},{10,... | collective-permute-start | bytes 49160 | tf_op jit(solution)/shard_map/ppermute | solution.py:56
  224.5 0.8 collective-permute-start.19
  225.2 0.7 collective-permute-done.17.a1
  226.0 0.4 collective-permute-done.18.a2
  226.4 1.8 collective-permute-done.19.a3
  228.2 2.0 shard_map.161
  230.2 1.0 shard_map.168
  (69 shorter events, 1.2 us)
Async XLA Ops:
  0.6 89.8 %copy-start = (bf16[1,2048,256]{2,1,0:T(8,128)(2,1)S(1)}, bf16[1,2048,256]{2,1,0:T(8,128)(2,1)}, u32[]{:S(2)}) copy-start(bf16[1,2048,256]{2,1,0:T(8,128)(2,1)} %param.27) | copy-start | bytes 3145732
  0.6 89.8 %copy-start.1 = (bf16[1,2048,256]{2,1,0:T(8,128)(2,1)S(1)}, bf16[1,2048,256]{2,1,0:T(8,128)(2,1)}, u32[]{:S(2)}) copy-start(bf16[1,2048,256]{2,1,0:T(8,128)(2,1)} %param.28) | copy-start | bytes 3145732
  0.7 1.1 copy-start.7
  1.8 0.7 copy-start.11
  2.4 0.7 copy-start.12
  3.1 0.7 copy-start.13
  3.8 0.7 copy-start.14
  4.5 44.0 %copy-start.15 = (bf16[32,512]{1,0:T(8,128)(2,1)S(1)}, bf16[32,512]{1,0:T(8,128)(2,1)}, u32[]{:S(2)}) copy-start(bf16[32,512]{1,0:T(8,128)(2,1)} %param.16) | copy-start | bytes 98308
  4.5 56.5 %copy-start.16 = (bf16[32,32]{1,0:T(8,128)(2,1)S(1)}, bf16[32,32]{1,0:T(8,128)(2,1)}, u32[]{:S(2)}) copy-start(bf16[32,32]{1,0:T(8,128)(2,1)} %param.17) | copy-start | bytes 6148
  4.5 85.9 %copy-start.17 = (f32[512]{0:T(512)S(1)}, f32[512]{0:T(512)}, u32[]{:S(2)}) copy-start(f32[512]{0:T(512)} %param.18) | copy-start | bytes 6148
  41.6 16.1 %collective-permute-start.20 = (bf16[32,4,2048]{2,1,0:T(4,128)(2,1)S(1)}, bf16[32,4,2048]{2,1,0:T(4,128)(2,1)S(1)}, u32[]{:S(2)}, u32[]{:S(2)}) collective-permute-start(bf16[32,4,2048]{2,1,0:T(4,128)(2,1)S(1)} %get-tuple-element.31.rows_a), channel_id=1, source_target_pairs={{0,1},{1,2},{2,3},{3,0},{4,5},{5,6},{6,7},{7,4},{8,9},{9,10},{10,1... | collective-permute-start | bytes 1572872 | tf_op jit(solution)/shard_map/ppermute | solution.py:56
  43.2 16.3 %collective-permute-start.24 = (bf16[32,4,2048]{2,1,0:T(4,128)(2,1)S(1)}, bf16[32,4,2048]{2,1,0:T(4,128)(2,1)S(1)}, u32[]{:S(2)}, u32[]{:S(2)}) collective-permute-start(bf16[32,4,2048]{2,1,0:T(4,128)(2,1)S(1)} %get-tuple-element.30.rows_b), channel_id=1, source_target_pairs={{0,3},{1,0},{2,1},{3,2},{4,7},{5,4},{6,5},{7,6},{8,11},{9,8},{10,9... | collective-permute-start | bytes 1572872 | tf_op jit(solution)/shard_map/ppermute | solution.py:56
  44.9 24.6 %collective-permute-start.21 = (bf16[32,4,2048]{2,1,0:T(4,128)(2,1)S(1)}, bf16[32,4,2048]{2,1,0:T(4,128)(2,1)}, u32[]{:S(2)}, u32[]{:S(2)}) collective-permute-start(bf16[32,4,2048]{2,1,0:T(4,128)(2,1)S(1)} %get-tuple-element.30.rows_b), channel_id=1, source_target_pairs={{0,1},{1,2},{2,3},{3,0},{4,5},{5,6},{6,7},{7,4},{8,9},{9,10},{10,1... | collective-permute-start | bytes 1572872 | tf_op jit(solution)/shard_map/ppermute | solution.py:56
  45.2 45.0 %collective-permute-start.27 = (bf16[32,4,2048]{2,1,0:T(4,128)(2,1)S(1)}, bf16[32,4,2048]{2,1,0:T(4,128)(2,1)}, u32[]{:S(2)}, u32[]{:S(2)}) collective-permute-start(bf16[32,4,2048]{2,1,0:T(4,128)(2,1)S(1)} %get-tuple-element.31.rows_a), channel_id=1, source_target_pairs={{0,3},{1,0},{2,1},{3,2},{4,7},{5,4},{6,5},{7,6},{8,11},{9,8},{10,9... | collective-permute-start | bytes 1572872 | tf_op jit(solution)/shard_map/ppermute | solution.py:56
  48.2 79.0 %collective-permute-start.29 = (bf16[256,2048]{1,0:T(8,128)(2,1)}, bf16[256,2048]{1,0:T(8,128)(2,1)}, u32[]{:S(2)}, u32[]{:S(2)}) collective-permute-start(bf16[256,2048]{1,0:T(8,128)(2,1)} %bitcast.15.w0), channel_id=1, source_target_pairs={{0,3},{1,0},{2,1},{3,2},{4,7},{5,4},{6,5},{7,6},{8,11},{9,8},{10,9... | collective-permute-start | bytes 3145736 | tf_op jit(solution)/shard_map/ppermute | solution.py:56
  57.7 3.2 %copy-start.5 = (bf16[32,4,2048]{2,1,0:T(4,128)(2,1)}, bf16[32,4,2048]{2,1,0:T(4,128)(2,1)S(1)}, u32[]{:S(2)}) copy-start(bf16[32,4,2048]{2,1,0:T(4,128)(2,1)S(1)} %collective-permute-done.20.rows_a) | copy-start | bytes 1572868
  57.7 72.8 %collective-permute-start.30 = (bf16[256,2048]{1,0:T(8,128)(2,1)}, bf16[256,2048]{1,0:T(8,128)(2,1)}, u32[]{:S(2)}, u32[]{:S(2)}) collective-permute-start(bf16[256,2048]{1,0:T(8,128)(2,1)} %bitcast.15.w0), channel_id=1, source_target_pairs={{0,2},{1,3},{2,0},{3,1},{4,6},{5,7},{6,4},{7,5},{8,10},{9,11},{10,... | collective-permute-start | bytes 3145736 | tf_op jit(solution)/shard_map/ppermute | solution.py:56
  59.5 0.8 copy-start.3
  60.3 71.5 %collective-permute-start.31 = (bf16[256,2048]{1,0:T(8,128)(2,1)}, bf16[256,2048]{1,0:T(8,128)(2,1)}, u32[]{:S(2)}, u32[]{:S(2)}) collective-permute-start(bf16[256,2048]{1,0:T(8,128)(2,1)} %bitcast.15.w0), channel_id=1, source_target_pairs={{0,1},{1,2},{2,3},{3,0},{4,5},{5,6},{6,7},{7,4},{8,9},{9,10},{10,1... | collective-permute-start | bytes 3145736 | tf_op jit(solution)/shard_map/ppermute | solution.py:56
  69.5 54.8 %collective-permute-start.23 = (bf16[32,4,2048]{2,1,0:T(4,128)(2,1)}, bf16[32,4,2048]{2,1,0:T(4,128)(2,1)S(1)}, u32[]{:S(2)}, u32[]{:S(2)}) collective-permute-start(bf16[32,4,2048]{2,1,0:T(4,128)(2,1)} %copy-done.5), channel_id=1, source_target_pairs={{0,1},{1,2},{2,3},{3,0},{4,5},{5,6},{6,7},{7,4},{8,9},{9,10},{10,1... | collective-permute-start | bytes 1572872 | tf_op jit(solution)/shard_map/ppermute | solution.py:56
  90.2 35.8 %collective-permute-start.25 = (bf16[32,4,2048]{2,1,0:T(4,128)(2,1)}, bf16[32,4,2048]{2,1,0:T(4,128)(2,1)S(1)}, u32[]{:S(2)}, u32[]{:S(2)}) collective-permute-start(bf16[32,4,2048]{2,1,0:T(4,128)(2,1)} %copy-done.3), channel_id=1, source_target_pairs={{0,3},{1,0},{2,1},{3,2},{4,7},{5,4},{6,5},{7,6},{8,11},{9,8},{10,9... | collective-permute-start | bytes 1572872 | tf_op jit(solution)/shard_map/ppermute | solution.py:56
  90.4 1.0 copy-start.6
  93.3 1.0 copy-start.4
  124.4 8.7 %collective-permute-start.22 = (bf16[256,256]{1,0:T(8,128)(2,1)S(1)}, bf16[256,256]{1,0:T(8,128)(2,1)S(1)}, u32[]{:S(2)}, u32[]{:S(2)}) collective-permute-start(bf16[256,256]{1,0:T(8,128)(2,1)S(1)} %shard_map.164), channel_id=1, source_target_pairs={{0,3},{1,0},{2,1},{3,2},{4,7},{5,4},{6,5},{7,6},{8,11},{9,8},{10,9... | collective-permute-start | bytes 393224 | tf_op jit(solution)/shard_map/ppermute | solution.py:56
  126.0 9.3 %collective-permute-start.28 = (bf16[256,256]{1,0:T(8,128)(2,1)S(1)}, bf16[256,256]{1,0:T(8,128)(2,1)S(1)}, u32[]{:S(2)}, u32[]{:S(2)}) collective-permute-start(bf16[256,256]{1,0:T(8,128)(2,1)S(1)} %shard_map.166), channel_id=1, source_target_pairs={{0,1},{1,2},{2,3},{3,0},{4,5},{5,6},{6,7},{7,4},{8,9},{9,10},{10,1... | collective-permute-start | bytes 393224 | tf_op jit(solution)/shard_map/ppermute | solution.py:56
  127.2 8.1 %collective-permute-start.26 = (bf16[256,256]{1,0:T(8,128)(2,1)S(1)}, bf16[256,256]{1,0:T(8,128)(2,1)S(1)}, u32[]{:S(2)}, u32[]{:S(2)}) collective-permute-start(bf16[256,256]{1,0:T(8,128)(2,1)S(1)} %shard_map.165), channel_id=1, source_target_pairs={{0,2},{1,3},{2,0},{3,1},{4,6},{5,7},{6,4},{7,5},{8,10},{9,11},{10,... | collective-permute-start | bytes 393224 | tf_op jit(solution)/shard_map/ppermute | solution.py:56
  130.5 16.3 %copy-start.8 = (bf16[512,256]{1,0:T(8,128)(2,1)S(1)}, bf16[512,256]{1,0:T(8,128)(2,1)}, u32[]{:S(2)}) copy-start(bf16[512,256]{1,0:T(8,128)(2,1)} %key_up.1) | copy-start | bytes 786436
  130.5 16.3 %copy-start.9 = (bf16[512,256]{1,0:T(8,128)(2,1)S(1)}, bf16[512,256]{1,0:T(8,128)(2,1)}, u32[]{:S(2)}) copy-start(bf16[512,256]{1,0:T(8,128)(2,1)} %value_up.1) | copy-start | bytes 786436
  130.5 16.3 %copy-start.10 = (bf16[128,384]{1,0:T(8,128)(2,1)S(1)}, bf16[128,384]{1,0:T(8,128)(2,1)}, u32[]{:S(2)}) copy-start(bf16[128,384]{1,0:T(8,128)(2,1)} %query.1) | copy-start | bytes 294916
  130.5 16.3 %collective-permute-start = (bf16[32,544]{1,0:T(8,128)(2,1)S(1)}, bf16[32,544]{1,0:T(8,128)(2,1)S(1)}, u32[]{:S(2)}, u32[]{:S(2)}) collective-permute-start(bf16[32,544]{1,0:T(8,128)(2,1)S(1)} %pad_maximum_fusion.2.l0), channel_id=1, source_target_pairs={{0,1},{1,2},{2,3},{3,0},{4,5},{5,6},{6,7},{7,4},{8,9},{9,10},{10,1... | collective-permute-start | bytes 104456 | tf_op jit(solution)/shard_map/ppermute | solution.py:56
  131.9 14.9 %collective-permute-start.1 = (bf16[32,544]{1,0:T(8,128)(2,1)S(1)}, bf16[32,544]{1,0:T(8,128)(2,1)S(1)}, u32[]{:S(2)}, u32[]{:S(2)}) collective-permute-start(bf16[32,544]{1,0:T(8,128)(2,1)S(1)} %pad_maximum_fusion.2.l0), channel_id=1, source_target_pairs={{0,2},{1,3},{2,0},{3,1},{4,6},{5,7},{6,4},{7,5},{8,10},{9,11},{10,... | collective-permute-start | bytes 104456 | tf_op jit(solution)/shard_map/ppermute | solution.py:56
  133.0 13.7 %collective-permute-start.2 = (bf16[32,544]{1,0:T(8,128)(2,1)S(1)}, bf16[32,544]{1,0:T(8,128)(2,1)S(1)}, u32[]{:S(2)}, u32[]{:S(2)}) collective-permute-start(bf16[32,544]{1,0:T(8,128)(2,1)S(1)} %pad_maximum_fusion.2.l0), channel_id=1, source_target_pairs={{0,3},{1,0},{2,1},{3,2},{4,7},{5,4},{6,5},{7,6},{8,11},{9,8},{10,9... | collective-permute-start | bytes 104456 | tf_op jit(solution)/shard_map/ppermute | solution.py:56
  139.7 90.5 %all-to-all-start.1 = ((bf16[64,4,2048]{2,1,0:T(4,128)(2,1)}), bf16[64,4,2048]{2,1,0:T(4,128)(2,1)S(1)}, u32[]{:S(2)}, u32[]{:S(2)}) async-start(bf16[64,4,2048]{2,1,0:T(4,128)(2,1)} %shard_map.167), calls=%async_computation.1 | async-start | bytes 2097152 | tf_op jit(solution)/shard_map/all_to_all | solution.py:176
  146.8 81.4 %copy-start.2 = (bf16[1024,2048]{1,0:T(8,128)(2,1)S(1)}, bf16[1024,2048]{1,0:T(8,128)(2,1)}, u32[]{:S(2)}) copy-start(bf16[1024,2048]{1,0:T(8,128)(2,1)} %out_proj.1) | copy-start | bytes 12582916
  147.7 26.8 %collective-permute-start.5 = (bf16[256,128]{1,0:T(8,128)(2,1)S(1)}, bf16[256,128]{1,0:T(8,128)(2,1)S(1)}, u32[]{:S(2)}, u32[]{:S(2)}) collective-permute-start(bf16[256,128]{1,0:T(8,128)(2,1)S(1)} %get-tuple-element.19), channel_id=1, source_target_pairs={{0,192},{64,0},{128,64},{192,128},{1,193},{65,1},{129,65},{193,129... | collective-permute-start | bytes 196616 | tf_op jit(solution)/shard_map/ppermute | solution.py:56
  150.0 27.0 %collective-permute-start.4 = (bf16[256,128]{1,0:T(8,128)(2,1)S(1)}, bf16[256,128]{1,0:T(8,128)(2,1)S(1)}, u32[]{:S(2)}, u32[]{:S(2)}) collective-permute-start(bf16[256,128]{1,0:T(8,128)(2,1)S(1)} %get-tuple-element.18), channel_id=1, source_target_pairs={{0,128},{64,192},{128,0},{192,64},{1,129},{65,193},{129,1},{193,65... | collective-permute-start | bytes 196616 | tf_op jit(solution)/shard_map/ppermute | solution.py:56
  151.4 25.7 %collective-permute-start.3 = (bf16[256,128]{1,0:T(8,128)(2,1)S(1)}, bf16[256,128]{1,0:T(8,128)(2,1)S(1)}, u32[]{:S(2)}, u32[]{:S(2)}) collective-permute-start(bf16[256,128]{1,0:T(8,128)(2,1)S(1)} %get-tuple-element.17), channel_id=1, source_target_pairs={{0,64},{64,128},{128,192},{192,0},{1,65},{65,129},{129,193},{193,1... | collective-permute-start | bytes 196616 | tf_op jit(solution)/shard_map/ppermute | solution.py:56
  177.1 6.1 %collective-permute-start.6 = (bf16[4,160,128]{2,1,0:T(8,128)(2,1)S(1)}, bf16[4,160,128]{2,1,0:T(8,128)(2,1)S(1)}, u32[]{:S(2)}, u32[]{:S(2)}) collective-permute-start(bf16[4,160,128]{2,1,0:T(8,128)(2,1)S(1)} %pad_maximum_fusion.1), channel_id=1, source_target_pairs={{0,32},{32,0},{1,33},{33,1},{2,34},{34,2},{3,35},{35,3},{4,36},{36... | collective-permute-start | bytes 491528 | tf_op jit(solution)/shard_map/ppermute | solution.py:56
  183.2 10.6 %collective-permute-start.7 = (bf16[4,160,256]{2,1,0:T(8,128)(2,1)S(1)}, bf16[4,160,256]{2,1,0:T(8,128)(2,1)S(1)}, u32[]{:S(2)}, u32[]{:S(2)}) collective-permute-start(bf16[4,160,256]{2,1,0:T(8,128)(2,1)S(1)} %pad_maximum_fusion.refs_0_), channel_id=1, source_target_pairs={{0,8},{8,16},{16,24},{24,0},{1,9},{9,17},{17,25},{25,1},{2,10},{10... | collective-permute-start | bytes 983048 | tf_op jit(solution)/shard_map/ppermute | solution.py:56
  184.8 16.7 %collective-permute-start.8 = (bf16[4,160,256]{2,1,0:T(8,128)(2,1)S(1)}, bf16[4,160,256]{2,1,0:T(8,128)(2,1)S(1)}, u32[]{:S(2)}, u32[]{:S(2)}) collective-permute-start(bf16[4,160,256]{2,1,0:T(8,128)(2,1)S(1)} %pad_maximum_fusion.refs_0_), channel_id=1, source_target_pairs={{0,16},{8,24},{16,0},{24,8},{1,17},{9,25},{17,1},{25,9},{2,18},{10... | collective-permute-start | bytes 983048 | tf_op jit(solution)/shard_map/ppermute | solution.py:56
  187.6 13.8 %collective-permute-start.9 = (bf16[4,160,256]{2,1,0:T(8,128)(2,1)S(1)}, bf16[4,160,256]{2,1,0:T(8,128)(2,1)S(1)}, u32[]{:S(2)}, u32[]{:S(2)}) collective-permute-start(bf16[4,160,256]{2,1,0:T(8,128)(2,1)S(1)} %pad_maximum_fusion.refs_0_), channel_id=1, source_target_pairs={{0,24},{8,0},{16,8},{24,16},{1,25},{9,1},{17,9},{25,17},{2,26},{10... | collective-permute-start | bytes 983048 | tf_op jit(solution)/shard_map/ppermute | solution.py:56
  189.0 12.9 %collective-permute-start.10 = (bf16[4,160,256]{2,1,0:T(8,128)(2,1)S(1)}, bf16[4,160,256]{2,1,0:T(8,128)(2,1)S(1)}, u32[]{:S(2)}, u32[]{:S(2)}) collective-permute-start(bf16[4,160,256]{2,1,0:T(8,128)(2,1)S(1)} %pad_maximum_fusion.refs_0_), channel_id=1, source_target_pairs={{0,4},{4,0},{1,5},{5,1},{2,6},{6,2},{3,7},{7,3},{8,12},{12,8},{9,1... | collective-permute-start | bytes 983048 | tf_op jit(solution)/shard_map/ppermute | solution.py:56
  193.8 8.1 %collective-permute-start.11 = (bf16[4,160,256]{2,1,0:T(8,128)(2,1)S(1)}, bf16[4,160,256]{2,1,0:T(8,128)(2,1)S(1)}, u32[]{:S(2)}, u32[]{:S(2)}) collective-permute-start(bf16[4,160,256]{2,1,0:T(8,128)(2,1)S(1)} %collective-permute-done.7.refs_1_), channel_id=1, source_target_pairs={{0,4},{4,0},{1,5},{5,1},{2,6},{6,2},{3,7},{7,3},{8,12},{12,8},{9,1... | collective-permute-start | bytes 983048 | tf_op jit(solution)/shard_map/ppermute | solution.py:56
  201.4 1.6 collective-permute-start.12
  201.4 2.1 collective-permute-start.13
  209.4 7.0 %collective-permute-start.14 = (bf16[128,64]{1,0:T(8,128)(2,1)S(1)}, bf16[128,64]{1,0:T(8,128)(2,1)S(1)}, u32[]{:S(2)}, u32[]{:S(2)}) collective-permute-start(bf16[128,64]{1,0:T(8,128)(2,1)S(1)} %get-tuple-element.21), channel_id=1, source_target_pairs={{0,192},{64,0},{128,64},{192,128},{1,193},{65,1},{129,65},{193,129... | collective-permute-start | bytes 49160 | tf_op jit(solution)/shard_map/ppermute | solution.py:56
  209.5 8.0 %collective-permute-start.15 = (bf16[128,64]{1,0:T(8,128)(2,1)S(1)}, bf16[128,64]{1,0:T(8,128)(2,1)S(1)}, u32[]{:S(2)}, u32[]{:S(2)}) collective-permute-start(bf16[128,64]{1,0:T(8,128)(2,1)S(1)} %get-tuple-element.22), channel_id=1, source_target_pairs={{0,128},{64,192},{128,0},{192,64},{1,129},{65,193},{129,1},{193,65... | collective-permute-start | bytes 49160 | tf_op jit(solution)/shard_map/ppermute | solution.py:56
  215.2 5.0 %collective-permute-start.16 = (bf16[128,64]{1,0:T(8,128)(2,1)S(1)}, bf16[128,64]{1,0:T(8,128)(2,1)S(1)}, u32[]{:S(2)}, u32[]{:S(2)}) collective-permute-start(bf16[128,64]{1,0:T(8,128)(2,1)S(1)} %get-tuple-element.23), channel_id=1, source_target_pairs={{0,64},{64,128},{128,192},{192,0},{1,65},{65,129},{129,193},{193,1... | collective-permute-start | bytes 49160 | tf_op jit(solution)/shard_map/ppermute | solution.py:56
  220.9 5.0 %collective-permute-start.17 = (bf16[32,256]{1,0:T(8,128)(2,1)S(1)}, bf16[32,256]{1,0:T(8,128)(2,1)S(1)}, u32[]{:S(2)}, u32[]{:S(2)}) collective-permute-start(bf16[32,256]{1,0:T(8,128)(2,1)S(1)} %get-tuple-element.25), channel_id=1, source_target_pairs={{0,1},{1,2},{2,3},{3,0},{4,5},{5,6},{6,7},{7,4},{8,9},{9,10},{10,1... | collective-permute-start | bytes 49160 | tf_op jit(solution)/shard_map/ppermute | solution.py:56
  221.0 5.3 %collective-permute-start.18 = (bf16[32,256]{1,0:T(8,128)(2,1)S(1)}, bf16[32,256]{1,0:T(8,128)(2,1)S(1)}, u32[]{:S(2)}, u32[]{:S(2)}) collective-permute-start(bf16[32,256]{1,0:T(8,128)(2,1)S(1)} %get-tuple-element.26), channel_id=1, source_target_pairs={{0,2},{1,3},{2,0},{3,1},{4,6},{5,7},{6,4},{7,5},{8,10},{9,11},{10,... | collective-permute-start | bytes 49160 | tf_op jit(solution)/shard_map/ppermute | solution.py:56
  224.5 3.7 %collective-permute-start.19 = (bf16[32,256]{1,0:T(8,128)(2,1)S(1)}, bf16[32,256]{1,0:T(8,128)(2,1)S(1)}, u32[]{:S(2)}, u32[]{:S(2)}) collective-permute-start(bf16[32,256]{1,0:T(8,128)(2,1)S(1)} %get-tuple-element.27), channel_id=1, source_target_pairs={{0,3},{1,0},{2,1},{3,2},{4,7},{5,4},{6,5},{7,6},{8,11},{9,8},{10,9... | collective-permute-start | bytes 49160 | tf_op jit(solution)/shard_map/ppermute | solution.py:56

commit v4 on v3

--- a/solution.py
+++ b/solution.py
@@ -28,15 +28,20 @@
 VMEM_SPEC = pl.BlockSpec(memory_space=pltpu.VMEM)
 
 
-def call(kernel, out_shape, arrays, where=None, scratch=(), limit=16 << 20, unplaced=()):
+def call(kernel, out_shape, arrays, where=None, scratch=(), limit=16 << 20, unplaced=(), place=True):
     arrays = [
-        a if i in unplaced else pltpu.with_memory_space_constraint(a, pltpu.VMEM)
+        pltpu.with_memory_space_constraint(a, pltpu.HBM if i in unplaced else pltpu.VMEM)
         for i, a in enumerate(arrays)
     ]
     specs = [VMEM_SPEC] * len(arrays)
     if where is not None:
         arrays, specs = [where] + arrays, [SMEM_SPEC] + specs
     single = not isinstance(out_shape, (list, tuple))
+    if place:
+        if single:
+            out_shape = pltpu.VMEM(out_shape.shape, out_shape.dtype)
+        else:
+            out_shape = [pltpu.VMEM(s.shape, s.dtype) for s in out_shape]
     return pl.pallas_call(
         kernel,
         in_specs=specs,
@@ -120,9 +125,10 @@
     return call(hidden_kernel, shape, [rows_a, rows_b, w_gate, w_up])
 
 
-def down_kernel(h0, h1, h2, h3, w0, w1, w2, w3, out):
-    total = mm(h0[...], w0[...]) + mm(h1[...], w1[...])
-    total = total + mm(h2[...], w2[...]) + mm(h3[...], w3[...])
+def down_kernel(h0, h1, h2, h3, w0, w1, w2a, w2b, w3, out):
+    half = w2a.shape[0]
+    total = mm(h0[...], w0[...]) + mm(h1[...], w1[...]) + mm(h3[...], w3[...])
+    total = total + mm(h2[:, :half], w2a[...]) + mm(h2[:, half:], w2b[...])
     out[...] = total.reshape(out.shape).astype(BF)
 
 
@@ -154,11 +160,13 @@
     experts = lax.axis_size(EP)
     rows, width = tokens.shape
     w_gate, w_up, w_down = w_gate[0], w_up[0], w_down[0]
-    down = [shifted(w_down, "x", k) for k in (-1, 2, 1)]
+    down_left, down_right = shifted(w_down, "x", 1), shifted(w_down, "x", -1)
+    units = w_down.shape[0] // 2
+    cut_a, cut_b = down_left[:units], down_right[units:]
+    down_far = [shifted(cut_a, "x", 1), shifted(cut_b, "x", -1)]
     outgoing, shares = dispatch(tokens, moe_gain, routes, group_prob, expert_prob, experts)
     arrived = lax.all_to_all(outgoing, EP, split_axis=0, concat_axis=0, tiled=True)
     queries, pair = query_and_pair(where, query, latent, rope_key, latent_gain, key_up, value_up)
-    down = [w_down] + down
     half = experts // 2
     a, b = arrived[:half], arrived[half:]
     left_a, right_b = shifted(a, "x", 1), shifted(b, "x", -1)
@@ -172,11 +180,21 @@
         shifted(hidden_of(right_a, right_b, w_gate, w_up), "x", 1),
     ]
     shape = jax.ShapeDtypeStruct((experts, CAP, width), BF)
+    down = [w_down, down_right] + down_far + [down_left]
     result = call(down_kernel, shape, hidden + down)
     returned = lax.all_to_all(result, EP, split_axis=0, concat_axis=0, tiled=True)
-    mixed = project(where, parts, out_proj, latent.shape[0])
+    mixed = project(parts, out_proj)
     shape = jax.ShapeDtypeStruct((rows, width), BF)
-    return mixed, call(combine_kernel, shape, [returned, shares])
+    return mixed, call(combine_kernel, shape, [returned, shares], place=False)
+
+
+def latent_kernel(latent, gain, rope_key, cosine, sine, out):
+    width = latent.shape[1]
+    half = ROPE_DIM // 2
+    out[:, :width] = rms_scale(latent[...], gain[...]).astype(BF)
+    rope = rope_key[...].astype(F32)
+    crossed = jnp.concatenate([-rope[:, half:], rope[:, :half]], axis=1)
+    out[:, width:] = (rope * cosine[...] + crossed * sine[...]).astype(BF)
 
 
 def heads_kernel(
@@ -212,8 +230,13 @@
         out[...] = heads[lax.rem(where[0] + k, 4)]
 
 
+def stack_kernel(b0, b1, b2, b3, out):
+    for j, block in enumerate((b0, b1, b2, b3)):
+        out[j] = block[QK_DIM:, :]
+
+
 def attend_kernel(where, q0, q1, q2, q3, *refs):
-    blocks, (o0, o1, o2, o3, q_s, top_s, acc_s) = refs[:8], refs[8:]
+    blocks, (out, q_s, top_s, acc_s) = refs[:8], refs[8:]
     zh, zl, y, c, x = (where[i] for i in range(5))
     strip = q0.shape[1]
     span = blocks[0].shape[2]
@@ -263,29 +286,15 @@
             advance(slice(g * strip, (g + 1) * strip), parts, masks)
             if g < 3:
                 advance(slice((g + 1) * strip, 4 * strip), parts, None)
-    for j, out in enumerate((o0, o1, o2, o3)):
-        at = pl.multiple_of(lax.rem(zh - j + 4, 4) * strip, strip)
-        total = acc_s[pl.ds(at, strip), :]
-        out[...] = (total[:, :V_DIM] / total[:, V_DIM:]).astype(BF)
-
-
-def spread_kernel(where, a0, a1, a2, a3, o0, o1, o2, o3, heads, parts):
-    for j, a in enumerate((a0, a1, a2, a3)):
-        heads[lax.rem(where[0] + j, 4)] = a[...]
-    beside = jnp.concatenate([heads[h] for h in range(4)], axis=1)
-    parts[...] = beside.reshape(parts.shape)
-    for k, out in enumerate((o0, o1, o2, o3)):
-        out[...] = parts[lax.rem(where[4] + k, 4)]
-
-
-def project_kernel(where, a0, a1, a2, a3, out_proj, out, parts):
-    width = a0.shape[1]
-    for k, a in enumerate((a0, a1, a2, a3)):
-        parts[lax.rem(where[4] - k + 4, 4)] = a[...]
-    total = mm(parts[0], out_proj[:width, :])
-    for h in range(1, 4):
-        total = total + mm(parts[h], out_proj[h * width : (h + 1) * width, :])
-    out[...] = total.astype(BF)
+    total = acc_s[...]
+    divided = total / jnp.concatenate([total[:, V_DIM:], total[:, V_DIM:]], axis=1)
+    out[...] = divided.reshape(out.shape).astype(BF)
+
+
+def project_kernel(parts, out_proj, out):
+    order = [zh * 4 + x for x in range(4) for zh in range(4)]
+    beside = jnp.concatenate([parts[i, :, :V_DIM] for i in order], axis=1)
+    out[...] = mm(beside, out_proj[...]).astype(BF)
 
 
 def query_and_pair(where, query, latent, rope_key, latent_gain, key_up, value_up):
@@ -293,18 +302,18 @@
     own = latent.shape[0]
     query_start = (((where[0] * 2 + where[1]) * 4 + where[2]) * 2 + where[3]) * strip
 
-    normed = rms_scale(latent, latent_gain).astype(BF)
     key_cos, key_sin = trig(query_start + where[4] * own + jnp.arange(own, dtype=jnp.int32))
-    half = ROPE_DIM // 2
-    a = rope_key[:, :half].astype(F32)
-    b = rope_key[:, half:].astype(F32)
-    both = jnp.concatenate(
+    both = call(
+        latent_kernel,
+        jax.ShapeDtypeStruct((own, latent.shape[1] + ROPE_DIM), BF),
         [
-            normed,
-            (a * key_cos - b * key_sin).astype(BF),
-            (a * key_sin + b * key_cos).astype(BF),
+            latent,
+            latent_gain[None, :],
+            rope_key,
+            jnp.concatenate([key_cos, key_cos], axis=1),
+            jnp.concatenate([key_sin, key_sin], axis=1),
         ],
-        axis=1,
+        unplaced=range(3),
     )
     near = [both] + [shifted(both, "x", k) for k in range(1, 4)]
     cosine, sine = trig(query_start + jnp.arange(strip, dtype=jnp.int32))
@@ -313,14 +322,15 @@
         [jax.ShapeDtypeStruct((QK_DIM + KV_ROWS, strip), BF)] * 4,
         near + [key_up, value_up, query, cosine.T, sine.T],
         where,
-        [
+        scratch=[
             pltpu.VMEM((strip, both.shape[1]), BF),
             pltpu.VMEM((4, QK_DIM + KV_ROWS, strip), BF),
         ],
-        unplaced=range(4, 9),
+        unplaced=range(4, 7),
     )
     blocks = [blocks[0]] + [shifted(blocks[k], "zh", k) for k in range(1, 4)]
-    mine = jnp.stack([block[QK_DIM:] for block in blocks])
+    shape = jax.ShapeDtypeStruct((4, KV_ROWS, strip), BF)
+    mine = call(stack_kernel, shape, blocks)
     return blocks, jnp.concatenate([mine, shifted(mine, "zl", 1)], axis=2)
 
 
@@ -328,9 +338,9 @@
     strip = blocks[0].shape[1]
     column = [pair] + [shifted(pair, "y", k) for k in range(1, 4)]
     column = column + [shifted(part, "c", 1) for part in column]
-    return call(
+    parts = call(
         attend_kernel,
-        [jax.ShapeDtypeStruct((strip, V_DIM), BF)] * 4,
+        jax.ShapeDtypeStruct((16, strip // 4, 2 * V_DIM), BF),
         blocks + column,
         where,
         [
@@ -339,26 +349,12 @@
             pltpu.VMEM((4 * strip, 128), F32),
         ],
     )
-
-
-def project(where, parts, out_proj, own):
-    strip = parts[0].shape[0]
-    parts = [parts[0]] + [shifted(parts[j], "zh", -j) for j in range(1, 4)]
-    parts = call(
-        spread_kernel,
-        [jax.ShapeDtypeStruct((own, 4 * V_DIM), BF)] * 4,
-        parts,
-        where,
-        [pltpu.VMEM((4, strip, V_DIM), BF), pltpu.VMEM((4, own, 4 * V_DIM), BF)],
-    )
-    parts = [parts[0]] + [shifted(parts[k], "x", k) for k in range(1, 4)]
-    return call(
-        project_kernel,
-        jax.ShapeDtypeStruct((own, out_proj.shape[1]), BF),
-        parts + [out_proj],
-        where,
-        [pltpu.VMEM((4, own, 4 * V_DIM), BF)],
-    )
+    return lax.all_to_all(parts, ("zh", "x"), split_axis=0, concat_axis=0, tiled=True)
+
+
+def project(parts, out_proj):
+    shape = jax.ShapeDtypeStruct((parts.shape[1], out_proj.shape[1]), BF)
+    return call(project_kernel, shape, [parts, out_proj], place=False)
 
 
 def body(

time: 235 us -> 184 us (0.78)
  the two profiles are of different devices: /device:TPU:224 before, /device:TPU:6 now
where the time goes in v4:
time: 184 us
  waiting for transfers between devices  83.6 us (45%)
  starting transfers between devices  60.7 us (33%)
  Pallas kernels  25.7 us (14%)
  local copies, waits for them, and re-layouts  12.3 us (7%)
    ppermute x27, waiting for transfers between devices, shifted(): return lax.ppermute(value, axis, [(i, (i + amount) % n) for i in range(n)])  58.5 us
    ppermute x27, starting transfers between devices, shifted(): return lax.ppermute(value, axis, [(i, (i + amount) % n) for i in range(n)])  34.5 us
    pallas_call x12, Pallas kernels, call(): pl.pallas_call(kernel, in_specs=specs, out_specs=VMEM_SPEC if single else...  25.7 us
    all_to_all x1, waiting for transfers between devices, both_halves(): lax.all_to_all(result, EP, split_axis=0, concat_axis=0, tiled=True)  25.1 us
    all_to_all x1, starting transfers between devices, both_halves(): lax.all_to_all(outgoing, EP, split_axis=0, concat_axis=0, tiled=True)  12.4 us
    all_to_all x1, starting transfers between devices, both_halves(): lax.all_to_all(result, EP, split_axis=0, concat_axis=0, tiled=True)  7.84 us
    unnamed x38, local copies, waits for them, and re-layouts  6.87 us
    all_to_all x1, starting transfers between devices, attend(): lax.all_to_all(parts, ('zh', 'x'), split_axis=0, concat_axis=0, tiled=True)  5.95 us
  transfers between devices with their start and end apart: 30, of which 14 were waited for; matrix products, arithmetic and copies ran while one was open for 3% of the time, Pallas kernels for 12%

profile of v4, /device:TPU:6, one launch (start us, length us, event | category | flops | bytes accessed | tf_op | source)
XLA Modules:
  0.0 183.6 jit_solution(4949171957911719824)
XLA Ops:
  0.6 2.6 %shard_map.163 = (bf16[64,4,2048]{2,1,0:T(4,128)(2,1)}, bf16[256,128]{1,0:T(8,128)(2,1)S(1)}) custom-call(bf16[64,2048]{1,0:T(8,128)(2,1)} %tokens.1, f32[1,2048]{1,0:T(1,128)} %bitcast.24, s32[2,64]{1,0:T(2,128)} %bitcast.26, f32[1,64]{1,0:T(1,128)} %bitcast.28, f32[2,64]{1,0:T(2,128)} %bitcast.27), custom_call_target="tpu_custom_call" | custom-call | tf_op jit(solution)/shard_map/pallas_call | solution.py:45
  3.3 0.6 copy-done.17
  3.9 12.4 %all-to-all-start.1 = ((bf16[64,4,2048]{2,1,0:T(4,128)(2,1)}), bf16[64,4,2048]{2,1,0:T(4,128)(2,1)}, u32[]{:S(2)}, u32[]{:S(2)}) async-start(bf16[64,4,2048]{2,1,0:T(4,128)(2,1)} %get-tuple-element.12), calls=%async_computation.1 | async-start | bytes 2097152 | tf_op jit(solution)/shard_map/all_to_all | solution.py:168
  16.3 0.1 multiply_sine_fusion
  16.5 0.9 shard_map.158.l0
  17.4 0.5 collective-permute-start
  18.0 2.4 %collective-permute-start.1 = (bf16[32,544]{1,0:T(8,128)(2,1)S(1)}, bf16[32,544]{1,0:T(8,128)(2,1)S(1)}, u32[]{:S(2)}, u32[]{:S(2)}) collective-permute-start(bf16[32,544]{1,0:T(8,128)(2,1)S(1)} %shard_map.158.l0), channel_id=1, source_target_pairs={{0,2},{1,3},{2,0},{3,1},{4,6},{5,7},{6,4},{7,5},{8,10},{9,11},{10,... | collective-permute-start | bytes 104456 | tf_op jit(solution)/shard_map/ppermute | solution.py:61
  20.4 0.1 multiply_sine_fusion.1
  20.5 0.1 stack.23.where
  20.6 0.9 collective-permute-done.l1
  21.5 2.0 %collective-permute-done.1.l2 = bf16[32,544]{1,0:T(8,128)(2,1)S(1)} collective-permute-done((bf16[32,544]{1,0:T(8,128)(2,1)S(1)}, bf16[32,544]{1,0:T(8,128)(2,1)S(1)}, u32[]{:S(2)}, u32[]{:S(2)}) %collective-permute-start.1) | collective-permute-done | bytes 34848 | tf_op jit(solution)/shard_map/ppermute | solution.py:61
  23.5 2.1 %collective-permute-done.2.l3 = bf16[32,544]{1,0:T(8,128)(2,1)S(1)} collective-permute-done((bf16[32,544]{1,0:T(8,128)(2,1)S(1)}, bf16[32,544]{1,0:T(8,128)(2,1)S(1)}, u32[]{:S(2)}, u32[]{:S(2)}) %collective-permute-start.2) | collective-permute-done | bytes 34848 | tf_op jit(solution)/shard_map/ppermute | solution.py:61
  25.6 1.4 shard_map.159
  27.0 2.5 %collective-permute-start.3 = (bf16[256,128]{1,0:T(8,128)(2,1)S(1)}, bf16[256,128]{1,0:T(8,128)(2,1)S(1)}, u32[]{:S(2)}, u32[]{:S(2)}) collective-permute-start(bf16[256,128]{1,0:T(8,128)(2,1)S(1)} %get-tuple-element.9), channel_id=1, source_target_pairs={{0,64},{64,128},{128,192},{192,0},{1,65},{65,129},{129,193},{193,1... | collective-permute-start | bytes 196616 | tf_op jit(solution)/shard_map/ppermute | solution.py:61
  29.5 3.8 %collective-permute-start.4 = (bf16[256,128]{1,0:T(8,128)(2,1)S(1)}, bf16[256,128]{1,0:T(8,128)(2,1)S(1)}, u32[]{:S(2)}, u32[]{:S(2)}) collective-permute-start(bf16[256,128]{1,0:T(8,128)(2,1)S(1)} %get-tuple-element.10), channel_id=1, source_target_pairs={{0,128},{64,192},{128,0},{192,64},{1,129},{65,193},{129,1},{193,65... | collective-permute-start | bytes 196616 | tf_op jit(solution)/shard_map/ppermute | solution.py:61
  33.3 3.5 %collective-permute-start.5 = (bf16[256,128]{1,0:T(8,128)(2,1)S(1)}, bf16[256,128]{1,0:T(8,128)(2,1)S(1)}, u32[]{:S(2)}, u32[]{:S(2)}) collective-permute-start(bf16[256,128]{1,0:T(8,128)(2,1)S(1)} %get-tuple-element.11), channel_id=1, source_target_pairs={{0,192},{64,0},{128,64},{192,128},{1,193},{65,1},{129,65},{193,129... | collective-permute-start | bytes 196616 | tf_op jit(solution)/shard_map/ppermute | solution.py:61
  36.7 9.6 %collective-permute-done.3.b1.q1 = bf16[256,128]{1,0:T(8,128)(2,1)S(1)} collective-permute-done((bf16[256,128]{1,0:T(8,128)(2,1)S(1)}, bf16[256,128]{1,0:T(8,128)(2,1)S(1)}, u32[]{:S(2)}, u32[]{:S(2)}) %collective-permute-start.3) | collective-permute-done | bytes 65568 | tf_op jit(solution)/shard_map/ppermute | solution.py:61
  46.4 4.1 %collective-permute-done.4.b2.q2 = bf16[256,128]{1,0:T(8,128)(2,1)S(1)} collective-permute-done((bf16[256,128]{1,0:T(8,128)(2,1)S(1)}, bf16[256,128]{1,0:T(8,128)(2,1)S(1)}, u32[]{:S(2)}, u32[]{:S(2)}) %collective-permute-start.4) | collective-permute-done | bytes 65568 | tf_op jit(solution)/shard_map/ppermute | solution.py:61
  50.5 0.1 collective-permute-start.6
  50.6 5.3 %collective-permute-done.6 = bf16[4,160,128]{2,1,0:T(8,128)(2,1)S(1)} collective-permute-done((bf16[4,160,128]{2,1,0:T(8,128)(2,1)S(1)}, bf16[4,160,128]{2,1,0:T(8,128)(2,1)S(1)}, u32[]{:S(2)}, u32[]{:S(2)}) %collective-permute-start.6) | collective-permute-done | bytes 163872 | tf_op jit(solution)/shard_map/ppermute | solution.py:61
  56.0 1.6 collective-permute-start.7
  57.5 2.7 %collective-permute-start.8 = (bf16[4,160,256]{2,1,0:T(8,128)(2,1)S(1)}, bf16[4,160,256]{2,1,0:T(8,128)(2,1)}, u32[]{:S(2)}, u32[]{:S(2)}) collective-permute-start(bf16[4,160,256]{2,1,0:T(8,128)(2,1)S(1)} %pad_maximum_fusion.refs_0_), channel_id=1, source_target_pairs={{0,16},{8,24},{16,0},{24,8},{1,17},{9,25},{17,1},{25,9},{2,18},{10... | collective-permute-start | bytes 983048 | tf_op jit(solution)/shard_map/ppermute | solution.py:61
  60.2 1.4 collective-permute-start.9
  61.7 0.5 collective-permute-start.24
  62.2 1.6 collective-permute-start.23
  63.7 3.7 %collective-permute-done.7.refs_1_ = bf16[4,160,256]{2,1,0:T(8,128)(2,1)} collective-permute-done((bf16[4,160,256]{2,1,0:T(8,128)(2,1)S(1)}, bf16[4,160,256]{2,1,0:T(8,128)(2,1)}, u32[]{:S(2)}, u32[]{:S(2)}) %collective-permute-start.7) | collective-permute-done | bytes 327712 | tf_op jit(solution)/shard_map/ppermute | solution.py:61
  67.5 4.7 %collective-permute-done.8.refs_2_ = bf16[4,160,256]{2,1,0:T(8,128)(2,1)} collective-permute-done((bf16[4,160,256]{2,1,0:T(8,128)(2,1)S(1)}, bf16[4,160,256]{2,1,0:T(8,128)(2,1)}, u32[]{:S(2)}, u32[]{:S(2)}) %collective-permute-start.8) | collective-permute-done | bytes 327712 | tf_op jit(solution)/shard_map/ppermute | solution.py:61
  72.2 0.7 copy-done.9
  73.0 0.5 collective-permute-start.12
  73.5 2.7 %fusion = (bf16[32,4,2048]{2,1,0:T(4,128)(2,1)S(1)}, bf16[32,4,2048]{2,1,0:T(4,128)(2,1)}) fusion(bf16[64,4,2048]{2,1,0:T(4,128)(2,1)} %all-to-all-done.1), kind=kLoop, calls=%fused_computation.10 | loop fusion | bytes 2097152 | tf_op jit(solution)/shard_map/slice | solution.py:171
  76.1 0.5 collective-permute-start.14
  76.6 1.6 collective-permute-start.18
  78.2 1.7 collective-permute-start.15
  79.9 0.8 copy-done.3
  80.7 7.0 %collective-permute-done.24.w3 = bf16[256,2048]{1,0:T(8,128)(2,1)S(1)} collective-permute-done((bf16[256,2048]{1,0:T(8,128)(2,1)}, bf16[256,2048]{1,0:T(8,128)(2,1)S(1)}, u32[]{:S(2)}, u32[]{:S(2)}) %collective-permute-start.24) | collective-permute-done | bytes 1048608 | tf_op jit(solution)/shard_map/ppermute | solution.py:61
  87.7 1.7 collective-permute-done.23.w1
  89.4 0.3 collective-permute-start.21
  89.7 9.3 %collective-permute-done.14.rows_a = bf16[32,4,2048]{2,1,0:T(4,128)(2,1)} collective-permute-done((bf16[32,4,2048]{2,1,0:T(4,128)(2,1)}, bf16[32,4,2048]{2,1,0:T(4,128)(2,1)}, u32[]{:S(2)}, u32[]{:S(2)}) %collective-permute-start.14) | collective-permute-done | bytes 524320 | tf_op jit(solution)/shard_map/ppermute | solution.py:61
  99.0 1.7 collective-permute-start.17
  100.7 0.3 collective-permute-start.19
  101.1 0.8 slice.18
  101.9 1.9 %slice.19 = bf16[128,2048]{1,0:T(8,128)(2,1)} slice(bf16[256,2048]{1,0:T(8,128)(2,1)} %collective-permute-done.23.w1), slice={[128:256], [0:2048]} | slice | bytes 1048576 | tf_op jit(solution)/shard_map/slice | solution.py:165
  103.8 2.9 %collective-permute-start.25 = (bf16[128,2048]{1,0:T(8,128)(2,1)}, bf16[128,2048]{1,0:T(8,128)(2,1)}, u32[]{:S(2)}, u32[]{:S(2)}) collective-permute-start(bf16[128,2048]{1,0:T(8,128)(2,1)} %slice.18), channel_id=1, source_target_pairs={{0,1},{1,2},{2,3},{3,0},{4,5},{5,6},{6,7},{7,4},{8,9},{9,10},{10,1... | collective-permute-start | bytes 1572872 | tf_op jit(solution)/shard_map/ppermute | solution.py:61
  106.7 3.5 %collective-permute-done.15.rows_b = bf16[32,4,2048]{2,1,0:T(4,128)(2,1)S(1)} collective-permute-done((bf16[32,4,2048]{2,1,0:T(4,128)(2,1)S(1)}, bf16[32,4,2048]{2,1,0:T(4,128)(2,1)S(1)}, u32[]{:S(2)}, u32[]{:S(2)}) %collective-permute-start.15) | collective-permute-done | bytes 524320 | tf_op jit(solution)/shard_map/ppermute | solution.py:61
  110.2 0.8 copy-done.6
  111.0 0.8 collective-permute-start.26
  111.8 6.6 %shard_map.161 = bf16[16,32,128]{2,1,0:T(8,128)(2,1)S(1)} custom-call(s32[5]{0:T(128)S(1)} %stack.23.where, bf16[256,128]{1,0:T(8,128)(2,1)S(1)} %get-tuple-element.8.b0.q0, bf16[256,128]{1,0:T(8,128)(2,1)S(1)} %copy-done.12, bf16[256,128]{1,0:T(8,128)(2,1)S(1)} %copy-done.14, bf16[256,128]{1,0:T(8,128)(2,1)S(1)} %copy-done.16, ...), custom_call_target="tpu_custom_call" | custom-call | tf_op jit(solution)/shard_map/pallas_call | solution.py:45
  118.4 0.6 copy-done.8
  119.1 5.9 %all-to-all-start = ((bf16[16,32,128]{2,1,0:T(8,128)(2,1)}), bf16[16,32,128]{2,1,0:T(8,128)(2,1)S(1)}, u32[]{:S(2)}, u32[]{:S(2)}) async-start(bf16[16,32,128]{2,1,0:T(8,128)(2,1)} %copy-done.8), calls=%async_computation | async-start | bytes 262144 | tf_op jit(solution)/shard_map/all_to_all | solution.py:352
  125.0 1.0 copy-done.7
  126.1 1.8 shard_map.165
  127.9 0.9 collective-permute-start.16
  128.9 1.9 %shard_map.167 = bf16[256,256]{1,0:T(8,128)(2,1)S(1)} custom-call(bf16[32,4,2048]{2,1,0:T(4,128)(2,1)} %collective-permute-done.21.rows_a, bf16[32,4,2048]{2,1,0:T(4,128)(2,1)} %collective-permute-done.18.rows_b, bf16[2048,256]{1,0:T(8,128)(2,1)S(1)} %bitcast.14, bf16[2048,256]{1,0:T(8,128)(2,1)S(1)} %bitcast.18), custom_call_target="tpu_custom_call" | custom-call | tf_op jit(solution)/shard_map/pallas_call | solution.py:45
  130.8 2.5 %collective-permute-start.22 = (bf16[256,256]{1,0:T(8,128)(2,1)S(1)}, bf16[256,256]{1,0:T(8,128)(2,1)S(1)}, u32[]{:S(2)}, u32[]{:S(2)}) collective-permute-start(bf16[256,256]{1,0:T(8,128)(2,1)S(1)} %shard_map.167), channel_id=1, source_target_pairs={{0,1},{1,2},{2,3},{3,0},{4,5},{5,6},{6,7},{7,4},{8,9},{9,10},{10,1... | collective-permute-start | bytes 393224 | tf_op jit(solution)/shard_map/ppermute | solution.py:61
  133.3 1.9 %shard_map.166 = bf16[256,256]{1,0:T(8,128)(2,1)S(1)} custom-call(bf16[32,4,2048]{2,1,0:T(4,128)(2,1)} %collective-permute-done.17.rows_a, bf16[32,4,2048]{2,1,0:T(4,128)(2,1)} %collective-permute-done.19.rows_b, bf16[2048,256]{1,0:T(8,128)(2,1)S(1)} %bitcast.15, bf16[2048,256]{1,0:T(8,128)(2,1)S(1)} %bitcast.19), custom_call_target="tpu_custom_call" | custom-call | tf_op jit(solution)/shard_map/pallas_call | solution.py:45
  135.2 0.3 collective-permute-start.20
  135.6 1.8 shard_map.164.h0
  137.4 4.4 %collective-permute-done.20.h2 = bf16[256,256]{1,0:T(8,128)(2,1)S(1)} collective-permute-done((bf16[256,256]{1,0:T(8,128)(2,1)S(1)}, bf16[256,256]{1,0:T(8,128)(2,1)S(1)}, u32[]{:S(2)}, u32[]{:S(2)}) %collective-permute-start.20) | collective-permute-done | bytes 131104 | tf_op jit(solution)/shard_map/ppermute | solution.py:61
  141.8 4.1 %shard_map.168 = bf16[64,4,2048]{2,1,0:T(4,128)(2,1)} custom-call(bf16[256,256]{1,0:T(8,128)(2,1)S(1)} %shard_map.164.h0, bf16[256,256]{1,0:T(8,128)(2,1)S(1)} %collective-permute-done.16.h1, bf16[256,256]{1,0:T(8,128)(2,1)S(1)} %collective-permute-done.20.h2, bf16[256,256]{1,0:T(8,128)(2,1)S(1)} %collective-permute-done.22.h3, ...), custom_call_target="tpu_custom_call" | custom-call | tf_op jit(solution)/shard_map/pallas_call | solution.py:45
  145.9 7.8 %all-to-all-start.2 = ((bf16[64,4,2048]{2,1,0:T(4,128)(2,1)}), bf16[64,4,2048]{2,1,0:T(4,128)(2,1)S(1)}, u32[]{:S(2)}, u32[]{:S(2)}) async-start(bf16[64,4,2048]{2,1,0:T(4,128)(2,1)} %shard_map.168), calls=%async_computation.2 | async-start | bytes 2097152 | tf_op jit(solution)/shard_map/all_to_all | solution.py:185
  153.7 2.2 %copy-done.2 = bf16[1024,2048]{1,0:T(8,128)(2,1)S(1)} copy-done((bf16[1024,2048]{1,0:T(8,128)(2,1)S(1)}, bf16[1024,2048]{1,0:T(8,128)(2,1)}, u32[]{:S(2)}) %copy-start.2) | copy-done | bytes 4194328
  155.9 1.5 shard_map.162
  157.4 25.1 %all-to-all-done.2.returned = bf16[64,4,2048]{2,1,0:T(4,128)(2,1)S(1)} async-done(((bf16[64,4,2048]{2,1,0:T(4,128)(2,1)}), bf16[64,4,2048]{2,1,0:T(4,128)(2,1)S(1)}, u32[]{:S(2)}, u32[]{:S(2)}) %all-to-all-start.2) | async-done | bytes 1048608 | tf_op jit(solution)/shard_map/all_to_all | solution.py:185
  182.6 1.0 shard_map.169
  (57 shorter events, 0.3 us)
Async XLA Ops:
  3.3 0.6 copy-start.17
  3.9 69.6 %all-to-all-start.1 = ((bf16[64,4,2048]{2,1,0:T(4,128)(2,1)}), bf16[64,4,2048]{2,1,0:T(4,128)(2,1)}, u32[]{:S(2)}, u32[]{:S(2)}) async-start(bf16[64,4,2048]{2,1,0:T(4,128)(2,1)} %get-tuple-element.12), calls=%async_computation.1 | async-start | bytes 2097152 | tf_op jit(solution)/shard_map/all_to_all | solution.py:168
  17.4 4.1 %collective-permute-start = (bf16[32,544]{1,0:T(8,128)(2,1)S(1)}, bf16[32,544]{1,0:T(8,128)(2,1)S(1)}, u32[]{:S(2)}, u32[]{:S(2)}) collective-permute-start(bf16[32,544]{1,0:T(8,128)(2,1)S(1)} %shard_map.158.l0), channel_id=1, source_target_pairs={{0,1},{1,2},{2,3},{3,0},{4,5},{5,6},{6,7},{7,4},{8,9},{9,10},{10,1... | collective-permute-start | bytes 104456 | tf_op jit(solution)/shard_map/ppermute | solution.py:61
  18.0 5.5 %collective-permute-start.1 = (bf16[32,544]{1,0:T(8,128)(2,1)S(1)}, bf16[32,544]{1,0:T(8,128)(2,1)S(1)}, u32[]{:S(2)}, u32[]{:S(2)}) collective-permute-start(bf16[32,544]{1,0:T(8,128)(2,1)S(1)} %shard_map.158.l0), channel_id=1, source_target_pairs={{0,2},{1,3},{2,0},{3,1},{4,6},{5,7},{6,4},{7,5},{8,10},{9,11},{10,... | collective-permute-start | bytes 104456 | tf_op jit(solution)/shard_map/ppermute | solution.py:61
  20.4 5.2 %collective-permute-start.2 = (bf16[32,544]{1,0:T(8,128)(2,1)S(1)}, bf16[32,544]{1,0:T(8,128)(2,1)S(1)}, u32[]{:S(2)}, u32[]{:S(2)}) collective-permute-start(bf16[32,544]{1,0:T(8,128)(2,1)S(1)} %shard_map.158.l0), channel_id=1, source_target_pairs={{0,3},{1,0},{2,1},{3,2},{4,7},{5,4},{6,5},{7,6},{8,11},{9,8},{10,9... | collective-permute-start | bytes 104456 | tf_op jit(solution)/shard_map/ppermute | solution.py:61
  27.0 19.3 %collective-permute-start.3 = (bf16[256,128]{1,0:T(8,128)(2,1)S(1)}, bf16[256,128]{1,0:T(8,128)(2,1)S(1)}, u32[]{:S(2)}, u32[]{:S(2)}) collective-permute-start(bf16[256,128]{1,0:T(8,128)(2,1)S(1)} %get-tuple-element.9), channel_id=1, source_target_pairs={{0,64},{64,128},{128,192},{192,0},{1,65},{65,129},{129,193},{193,1... | collective-permute-start | bytes 196616 | tf_op jit(solution)/shard_map/ppermute | solution.py:61
  29.5 21.0 %collective-permute-start.4 = (bf16[256,128]{1,0:T(8,128)(2,1)S(1)}, bf16[256,128]{1,0:T(8,128)(2,1)S(1)}, u32[]{:S(2)}, u32[]{:S(2)}) collective-permute-start(bf16[256,128]{1,0:T(8,128)(2,1)S(1)} %get-tuple-element.10), channel_id=1, source_target_pairs={{0,128},{64,192},{128,0},{192,64},{1,129},{65,193},{129,1},{193,65... | collective-permute-start | bytes 196616 | tf_op jit(solution)/shard_map/ppermute | solution.py:61
  33.3 17.2 %collective-permute-start.5 = (bf16[256,128]{1,0:T(8,128)(2,1)S(1)}, bf16[256,128]{1,0:T(8,128)(2,1)S(1)}, u32[]{:S(2)}, u32[]{:S(2)}) collective-permute-start(bf16[256,128]{1,0:T(8,128)(2,1)S(1)} %get-tuple-element.11), channel_id=1, source_target_pairs={{0,192},{64,0},{128,64},{192,128},{1,193},{65,1},{129,65},{193,129... | collective-permute-start | bytes 196616 | tf_op jit(solution)/shard_map/ppermute | solution.py:61
  46.4 25.8 %copy-start.11 = (bf16[256,128]{1,0:T(8,128)(2,1)}, bf16[256,128]{1,0:T(8,128)(2,1)S(1)}, u32[]{:S(2)}) copy-start(bf16[256,128]{1,0:T(8,128)(2,1)S(1)} %collective-permute-done.3.b1.q1) | copy-start | bytes 196612
  50.5 21.7 %copy-start.13 = (bf16[256,128]{1,0:T(8,128)(2,1)}, bf16[256,128]{1,0:T(8,128)(2,1)S(1)}, u32[]{:S(2)}) copy-start(bf16[256,128]{1,0:T(8,128)(2,1)S(1)} %collective-permute-done.4.b2.q2) | copy-start | bytes 196612
  50.5 21.7 %copy-start.15 = (bf16[256,128]{1,0:T(8,128)(2,1)}, bf16[256,128]{1,0:T(8,128)(2,1)S(1)}, u32[]{:S(2)}) copy-start(bf16[256,128]{1,0:T(8,128)(2,1)S(1)} %collective-permute-done.5.b3.q3) | copy-start | bytes 196612
  50.5 74.5 %copy-start = (bf16[1,2048,256]{2,1,0:T(8,128)(2,1)S(1)}, bf16[1,2048,256]{2,1,0:T(8,128)(2,1)}, u32[]{:S(2)}) copy-start(bf16[1,2048,256]{2,1,0:T(8,128)(2,1)} %param.27) | copy-start | bytes 3145732
  50.5 74.5 %copy-start.1 = (bf16[1,2048,256]{2,1,0:T(8,128)(2,1)S(1)}, bf16[1,2048,256]{2,1,0:T(8,128)(2,1)}, u32[]{:S(2)}) copy-start(bf16[1,2048,256]{2,1,0:T(8,128)(2,1)} %param.28) | copy-start | bytes 3145732
  50.5 5.4 %collective-permute-start.6 = (bf16[4,160,128]{2,1,0:T(8,128)(2,1)S(1)}, bf16[4,160,128]{2,1,0:T(8,128)(2,1)S(1)}, u32[]{:S(2)}, u32[]{:S(2)}) collective-permute-start(bf16[4,160,128]{2,1,0:T(8,128)(2,1)S(1)} %shard_map.160), channel_id=1, source_target_pairs={{0,32},{32,0},{1,33},{33,1},{2,34},{34,2},{3,35},{35,3},{4,36},{36... | collective-permute-start | bytes 491528 | tf_op jit(solution)/shard_map/ppermute | solution.py:61
  56.0 11.5 %collective-permute-start.7 = (bf16[4,160,256]{2,1,0:T(8,128)(2,1)S(1)}, bf16[4,160,256]{2,1,0:T(8,128)(2,1)}, u32[]{:S(2)}, u32[]{:S(2)}) collective-permute-start(bf16[4,160,256]{2,1,0:T(8,128)(2,1)S(1)} %pad_maximum_fusion.refs_0_), channel_id=1, source_target_pairs={{0,8},{8,16},{16,24},{24,0},{1,9},{9,17},{17,25},{25,1},{2,10},{10... | collective-permute-start | bytes 983048 | tf_op jit(solution)/shard_map/ppermute | solution.py:61
  57.5 14.7 %collective-permute-start.8 = (bf16[4,160,256]{2,1,0:T(8,128)(2,1)S(1)}, bf16[4,160,256]{2,1,0:T(8,128)(2,1)}, u32[]{:S(2)}, u32[]{:S(2)}) collective-permute-start(bf16[4,160,256]{2,1,0:T(8,128)(2,1)S(1)} %pad_maximum_fusion.refs_0_), channel_id=1, source_target_pairs={{0,16},{8,24},{16,0},{24,8},{1,17},{9,25},{17,1},{25,9},{2,18},{10... | collective-permute-start | bytes 983048 | tf_op jit(solution)/shard_map/ppermute | solution.py:61
  60.2 12.0 %collective-permute-start.9 = (bf16[4,160,256]{2,1,0:T(8,128)(2,1)S(1)}, bf16[4,160,256]{2,1,0:T(8,128)(2,1)S(1)}, u32[]{:S(2)}, u32[]{:S(2)}) collective-permute-start(bf16[4,160,256]{2,1,0:T(8,128)(2,1)S(1)} %pad_maximum_fusion.refs_0_), channel_id=1, source_target_pairs={{0,24},{8,0},{16,8},{24,16},{1,25},{9,1},{17,9},{25,17},{2,26},{10... | collective-permute-start | bytes 983048 | tf_op jit(solution)/shard_map/ppermute | solution.py:61
  61.7 26.0 %collective-permute-start.24 = (bf16[256,2048]{1,0:T(8,128)(2,1)}, bf16[256,2048]{1,0:T(8,128)(2,1)S(1)}, u32[]{:S(2)}, u32[]{:S(2)}) collective-permute-start(bf16[256,2048]{1,0:T(8,128)(2,1)} %bitcast.21), channel_id=1, source_target_pairs={{0,1},{1,2},{2,3},{3,0},{4,5},{5,6},{6,7},{7,4},{8,9},{9,10},{10,1... | collective-permute-start | bytes 3145736 | tf_op jit(solution)/shard_map/ppermute | solution.py:61
  62.2 27.2 %collective-permute-start.23 = (bf16[256,2048]{1,0:T(8,128)(2,1)}, bf16[256,2048]{1,0:T(8,128)(2,1)}, u32[]{:S(2)}, u32[]{:S(2)}) collective-permute-start(bf16[256,2048]{1,0:T(8,128)(2,1)} %bitcast.22), channel_id=1, source_target_pairs={{0,3},{1,0},{2,1},{3,2},{4,7},{5,4},{6,5},{7,6},{8,11},{9,8},{10,9... | collective-permute-start | bytes 3145736 | tf_op jit(solution)/shard_map/ppermute | solution.py:61
  67.5 8.7 %collective-permute-start.10 = (bf16[4,160,256]{2,1,0:T(8,128)(2,1)S(1)}, bf16[4,160,256]{2,1,0:T(8,128)(2,1)}, u32[]{:S(2)}, u32[]{:S(2)}) collective-permute-start(bf16[4,160,256]{2,1,0:T(8,128)(2,1)S(1)} %pad_maximum_fusion.refs_0_), channel_id=1, source_target_pairs={{0,4},{4,0},{1,5},{5,1},{2,6},{6,2},{3,7},{7,3},{8,12},{12,8},{9,1... | collective-permute-start | bytes 983048 | tf_op jit(solution)/shard_map/ppermute | solution.py:61
  72.2 4.4 %collective-permute-start.11 = (bf16[4,160,256]{2,1,0:T(8,128)(2,1)}, bf16[4,160,256]{2,1,0:T(8,128)(2,1)}, u32[]{:S(2)}, u32[]{:S(2)}) collective-permute-start(bf16[4,160,256]{2,1,0:T(8,128)(2,1)} %collective-permute-done.7.refs_1_), channel_id=1, source_target_pairs={{0,4},{4,0},{1,5},{5,1},{2,6},{6,2},{3,7},{7,3},{8,12},{12,8},{9,1... | collective-permute-start | bytes 983048 | tf_op jit(solution)/shard_map/ppermute | solution.py:61
  72.2 0.7 copy-start.9
  73.0 5.2 %collective-permute-start.12 = (bf16[4,160,256]{2,1,0:T(8,128)(2,1)}, bf16[4,160,256]{2,1,0:T(8,128)(2,1)}, u32[]{:S(2)}, u32[]{:S(2)}) collective-permute-start(bf16[4,160,256]{2,1,0:T(8,128)(2,1)} %collective-permute-done.8.refs_2_), channel_id=1, source_target_pairs={{0,4},{4,0},{1,5},{5,1},{2,6},{6,2},{3,7},{7,3},{8,12},{12,8},{9,1... | collective-permute-start | bytes 983048 | tf_op jit(solution)/shard_map/ppermute | solution.py:61
  73.5 38.3 %copy-start.10 = (bf16[4,160,256]{2,1,0:T(8,128)(2,1)S(1)}, bf16[4,160,256]{2,1,0:T(8,128)(2,1)}, u32[]{:S(2)}) copy-start(bf16[4,160,256]{2,1,0:T(8,128)(2,1)} %copy-done.9) | copy-start | bytes 983044
  73.5 38.3 %copy-start.12 = (bf16[256,128]{1,0:T(8,128)(2,1)S(1)}, bf16[256,128]{1,0:T(8,128)(2,1)}, u32[]{:S(2)}) copy-start(bf16[256,128]{1,0:T(8,128)(2,1)} %copy-done.11) | copy-start | bytes 196612
  73.5 38.3 %copy-start.14 = (bf16[256,128]{1,0:T(8,128)(2,1)S(1)}, bf16[256,128]{1,0:T(8,128)(2,1)}, u32[]{:S(2)}) copy-start(bf16[256,128]{1,0:T(8,128)(2,1)} %copy-done.13) | copy-start | bytes 196612
  73.5 38.3 %copy-start.16 = (bf16[256,128]{1,0:T(8,128)(2,1)S(1)}, bf16[256,128]{1,0:T(8,128)(2,1)}, u32[]{:S(2)}) copy-start(bf16[256,128]{1,0:T(8,128)(2,1)} %copy-done.15) | copy-start | bytes 196612
  76.1 22.9 %collective-permute-start.14 = (bf16[32,4,2048]{2,1,0:T(4,128)(2,1)}, bf16[32,4,2048]{2,1,0:T(4,128)(2,1)}, u32[]{:S(2)}, u32[]{:S(2)}) collective-permute-start(bf16[32,4,2048]{2,1,0:T(4,128)(2,1)} %get-tuple-element.15.rows_a), channel_id=1, source_target_pairs={{0,1},{1,2},{2,3},{3,0},{4,5},{5,6},{6,7},{7,4},{8,9},{9,10},{10,1... | collective-permute-start | bytes 1572872 | tf_op jit(solution)/shard_map/ppermute | solution.py:61
  76.6 24.1 %collective-permute-start.18 = (bf16[32,4,2048]{2,1,0:T(4,128)(2,1)S(1)}, bf16[32,4,2048]{2,1,0:T(4,128)(2,1)}, u32[]{:S(2)}, u32[]{:S(2)}) collective-permute-start(bf16[32,4,2048]{2,1,0:T(4,128)(2,1)S(1)} %get-tuple-element.14.rows_b), channel_id=1, source_target_pairs={{0,3},{1,0},{2,1},{3,2},{4,7},{5,4},{6,5},{7,6},{8,11},{9,8},{10,9... | collective-permute-start | bytes 1572872 | tf_op jit(solution)/shard_map/ppermute | solution.py:61
  78.2 32.0 %collective-permute-start.15 = (bf16[32,4,2048]{2,1,0:T(4,128)(2,1)S(1)}, bf16[32,4,2048]{2,1,0:T(4,128)(2,1)S(1)}, u32[]{:S(2)}, u32[]{:S(2)}) collective-permute-start(bf16[32,4,2048]{2,1,0:T(4,128)(2,1)S(1)} %get-tuple-element.14.rows_b), channel_id=1, source_target_pairs={{0,1},{1,2},{2,3},{3,0},{4,5},{5,6},{6,7},{7,4},{8,9},{9,10},{10,1... | collective-permute-start | bytes 1572872 | tf_op jit(solution)/shard_map/ppermute | solution.py:61
  79.9 0.8 copy-start.3
  87.7 16.1 %collective-permute-start.13 = (bf16[4,160,256]{2,1,0:T(8,128)(2,1)}, bf16[4,160,256]{2,1,0:T(8,128)(2,1)S(1)}, u32[]{:S(2)}, u32[]{:S(2)}) collective-permute-start(bf16[4,160,256]{2,1,0:T(8,128)(2,1)} %copy-done.9), channel_id=1, source_target_pairs={{0,4},{4,0},{1,5},{5,1},{2,6},{6,2},{3,7},{7,3},{8,12},{12,8},{9,1... | collective-permute-start | bytes 983048 | tf_op jit(solution)/shard_map/ppermute | solution.py:61
  89.4 38.5 %collective-permute-start.21 = (bf16[32,4,2048]{2,1,0:T(4,128)(2,1)}, bf16[32,4,2048]{2,1,0:T(4,128)(2,1)}, u32[]{:S(2)}, u32[]{:S(2)}) collective-permute-start(bf16[32,4,2048]{2,1,0:T(4,128)(2,1)} %get-tuple-element.15.rows_a), channel_id=1, source_target_pairs={{0,3},{1,0},{2,1},{3,2},{4,7},{5,4},{6,5},{7,6},{8,11},{9,8},{10,9... | collective-permute-start | bytes 1572872 | tf_op jit(solution)/shard_map/ppermute | solution.py:61
  99.0 31.8 %collective-permute-start.17 = (bf16[32,4,2048]{2,1,0:T(4,128)(2,1)}, bf16[32,4,2048]{2,1,0:T(4,128)(2,1)}, u32[]{:S(2)}, u32[]{:S(2)}) collective-permute-start(bf16[32,4,2048]{2,1,0:T(4,128)(2,1)} %collective-permute-done.14.rows_a), channel_id=1, source_target_pairs={{0,1},{1,2},{2,3},{3,0},{4,5},{5,6},{6,7},{7,4},{8,9},{9,10},{10,1... | collective-permute-start | bytes 1572872 | tf_op jit(solution)/shard_map/ppermute | solution.py:61
  100.7 32.6 %collective-permute-start.19 = (bf16[32,4,2048]{2,1,0:T(4,128)(2,1)}, bf16[32,4,2048]{2,1,0:T(4,128)(2,1)}, u32[]{:S(2)}, u32[]{:S(2)}) collective-permute-start(bf16[32,4,2048]{2,1,0:T(4,128)(2,1)} %collective-permute-done.18.rows_b), channel_id=1, source_target_pairs={{0,3},{1,0},{2,1},{3,2},{4,7},{5,4},{6,5},{7,6},{8,11},{9,8},{10,9... | collective-permute-start | bytes 1572872 | tf_op jit(solution)/shard_map/ppermute | solution.py:61
  103.8 33.6 %collective-permute-start.25 = (bf16[128,2048]{1,0:T(8,128)(2,1)}, bf16[128,2048]{1,0:T(8,128)(2,1)}, u32[]{:S(2)}, u32[]{:S(2)}) collective-permute-start(bf16[128,2048]{1,0:T(8,128)(2,1)} %slice.18), channel_id=1, source_target_pairs={{0,1},{1,2},{2,3},{3,0},{4,5},{5,6},{6,7},{7,4},{8,9},{9,10},{10,1... | collective-permute-start | bytes 1572872 | tf_op jit(solution)/shard_map/ppermute | solution.py:61
  110.2 0.8 copy-start.6
  111.0 26.4 %collective-permute-start.26 = (bf16[128,2048]{1,0:T(8,128)(2,1)}, bf16[128,2048]{1,0:T(8,128)(2,1)}, u32[]{:S(2)}, u32[]{:S(2)}) collective-permute-start(bf16[128,2048]{1,0:T(8,128)(2,1)} %slice.19), channel_id=1, source_target_pairs={{0,3},{1,0},{2,1},{3,2},{4,7},{5,4},{6,5},{7,6},{8,11},{9,8},{10,9... | collective-permute-start | bytes 1572872 | tf_op jit(solution)/shard_map/ppermute | solution.py:61
  118.4 0.7 copy-start.8
  119.1 26.8 %all-to-all-start = ((bf16[16,32,128]{2,1,0:T(8,128)(2,1)}), bf16[16,32,128]{2,1,0:T(8,128)(2,1)S(1)}, u32[]{:S(2)}, u32[]{:S(2)}) async-start(bf16[16,32,128]{2,1,0:T(8,128)(2,1)} %copy-done.8), calls=%async_computation | async-start | bytes 262144 | tf_op jit(solution)/shard_map/all_to_all | solution.py:352
  125.0 1.0 copy-start.7
  126.1 9.5 %copy-start.4 = (bf16[32,4,2048]{2,1,0:T(4,128)(2,1)S(1)}, bf16[32,4,2048]{2,1,0:T(4,128)(2,1)}, u32[]{:S(2)}) copy-start(bf16[32,4,2048]{2,1,0:T(4,128)(2,1)} %copy-done.3) | copy-start | bytes 1572868
  127.9 13.9 %copy-start.5 = (bf16[1,256,2048]{2,1,0:T(8,128)(2,1)S(1)}, bf16[1,256,2048]{2,1,0:T(8,128)(2,1)}, u32[]{:S(2)}) copy-start(bf16[1,256,2048]{2,1,0:T(8,128)(2,1)} %param.29) | copy-start | bytes 3145732
  127.9 9.4 %collective-permute-start.16 = (bf16[256,256]{1,0:T(8,128)(2,1)S(1)}, bf16[256,256]{1,0:T(8,128)(2,1)S(1)}, u32[]{:S(2)}, u32[]{:S(2)}) collective-permute-start(bf16[256,256]{1,0:T(8,128)(2,1)S(1)} %shard_map.165), channel_id=1, source_target_pairs={{0,3},{1,0},{2,1},{3,2},{4,7},{5,4},{6,5},{7,6},{8,11},{9,8},{10,9... | collective-permute-start | bytes 393224 | tf_op jit(solution)/shard_map/ppermute | solution.py:61
  130.8 6.5 %collective-permute-start.22 = (bf16[256,256]{1,0:T(8,128)(2,1)S(1)}, bf16[256,256]{1,0:T(8,128)(2,1)S(1)}, u32[]{:S(2)}, u32[]{:S(2)}) collective-permute-start(bf16[256,256]{1,0:T(8,128)(2,1)S(1)} %shard_map.167), channel_id=1, source_target_pairs={{0,1},{1,2},{2,3},{3,0},{4,5},{5,6},{6,7},{7,4},{8,9},{9,10},{10,1... | collective-permute-start | bytes 393224 | tf_op jit(solution)/shard_map/ppermute | solution.py:61
  135.2 6.6 %collective-permute-start.20 = (bf16[256,256]{1,0:T(8,128)(2,1)S(1)}, bf16[256,256]{1,0:T(8,128)(2,1)S(1)}, u32[]{:S(2)}, u32[]{:S(2)}) collective-permute-start(bf16[256,256]{1,0:T(8,128)(2,1)S(1)} %shard_map.166), channel_id=1, source_target_pairs={{0,2},{1,3},{2,0},{3,1},{4,6},{5,7},{6,4},{7,5},{8,10},{9,11},{10,... | collective-permute-start | bytes 393224 | tf_op jit(solution)/shard_map/ppermute | solution.py:61
  145.9 36.7 %copy-start.18 = (bf16[256,128]{1,0:T(8,128)(2,1)S(1)}, bf16[256,128]{1,0:T(8,128)(2,1)}, u32[]{:S(2)}) copy-start(bf16[256,128]{1,0:T(8,128)(2,1)} %copy-done.17) | copy-start | bytes 196612
  145.9 36.7 %all-to-all-start.2 = ((bf16[64,4,2048]{2,1,0:T(4,128)(2,1)}), bf16[64,4,2048]{2,1,0:T(4,128)(2,1)S(1)}, u32[]{:S(2)}, u32[]{:S(2)}) async-start(bf16[64,4,2048]{2,1,0:T(4,128)(2,1)} %shard_map.168), calls=%async_computation.2 | async-start | bytes 2097152 | tf_op jit(solution)/shard_map/all_to_all | solution.py:185
  153.7 2.2 %copy-start.2 = (bf16[1024,2048]{1,0:T(8,128)(2,1)S(1)}, bf16[1024,2048]{1,0:T(8,128)(2,1)}, u32[]{:S(2)}) copy-start(bf16[1024,2048]{1,0:T(8,128)(2,1)} %out_proj.1) | copy-start | bytes 12582916

commit v5 on v4

--- a/solution.py
+++ b/solution.py
@@ -183,7 +183,7 @@
     down = [w_down, down_right] + down_far + [down_left]
     result = call(down_kernel, shape, hidden + down)
     returned = lax.all_to_all(result, EP, split_axis=0, concat_axis=0, tiled=True)
-    mixed = project(parts, out_proj)
+    mixed = project(where, parts, out_proj, latent.shape[0])
     shape = jax.ShapeDtypeStruct((rows, width), BF)
     return mixed, call(combine_kernel, shape, [returned, shares], place=False)
 
@@ -236,7 +236,7 @@
 
 
 def attend_kernel(where, q0, q1, q2, q3, *refs):
-    blocks, (out, q_s, top_s, acc_s) = refs[:8], refs[8:]
+    blocks, outs, (q_s, top_s, acc_s) = refs[:8], refs[8:12], refs[12:]
     zh, zl, y, c, x = (where[i] for i in range(5))
     strip = q0.shape[1]
     span = blocks[0].shape[2]
@@ -280,21 +280,43 @@
             key_y = lax.rem(y - k + 4, 4)
             key_at = (col_zl * 8 + key_y * 2 + jnp.bitwise_xor(c, m)) * strip + col_x
             masks.append(key_at <= query_at)
-        for g in range(4):
+
+        def one_group(g, _, group=group, masks=masks):
             from_zh = lax.rem(zh - g + 4, 4)
-            parts = [block[from_zh] for block in group]
-            advance(slice(g * strip, (g + 1) * strip), parts, masks)
-            if g < 3:
-                advance(slice((g + 1) * strip, 4 * strip), parts, None)
+            parts = [block.at[from_zh] for block in group]
+
+            def later(s, _):
+                advance(pl.ds(pl.multiple_of(s * strip, strip), strip), parts, None)
+                return 0
+
+            advance(pl.ds(pl.multiple_of(g * strip, strip), strip), parts, masks)
+            return lax.fori_loop(g + 1, 4, later, 0)
+
+        lax.fori_loop(0, 4, one_group, 0)
     total = acc_s[...]
-    divided = total / jnp.concatenate([total[:, V_DIM:], total[:, V_DIM:]], axis=1)
-    out[...] = divided.reshape(out.shape).astype(BF)
-
-
-def project_kernel(parts, out_proj, out):
-    order = [zh * 4 + x for x in range(4) for zh in range(4)]
-    beside = jnp.concatenate([parts[i, :, :V_DIM] for i in order], axis=1)
-    out[...] = mm(beside, out_proj[...]).astype(BF)
+    acc_s[:, :V_DIM] = total[:, :V_DIM] / total[:, V_DIM:]
+    for j, out in enumerate(outs):
+        at = pl.multiple_of(lax.rem(zh - j + 4, 4) * strip, strip)
+        out[...] = acc_s[pl.ds(at, strip), :V_DIM].astype(BF)
+
+
+def spread_kernel(where, a0, a1, a2, a3, o0, o1, o2, o3, heads, parts):
+    for j, a in enumerate((a0, a1, a2, a3)):
+        heads[lax.rem(where[0] + j, 4)] = a[...]
+    beside = jnp.concatenate([heads[h] for h in range(4)], axis=1)
+    parts[...] = beside.reshape(parts.shape)
+    for k, out in enumerate((o0, o1, o2, o3)):
+        out[...] = parts[lax.rem(where[4] + k, 4)]
+
+
+def project_kernel(where, a0, a1, a2, a3, out_proj, out, parts):
+    width = a0.shape[1]
+    for k, a in enumerate((a0, a1, a2, a3)):
+        parts[lax.rem(where[4] - k + 4, 4)] = a[...]
+    total = mm(parts[0], out_proj[:width, :])
+    for h in range(1, 4):
+        total = total + mm(parts[h], out_proj[h * width : (h + 1) * width, :])
+    out[...] = total.astype(BF)
 
 
 def query_and_pair(where, query, latent, rope_key, latent_gain, key_up, value_up):
@@ -340,7 +362,7 @@
     column = column + [shifted(part, "c", 1) for part in column]
     parts = call(
         attend_kernel,
-        jax.ShapeDtypeStruct((16, strip // 4, 2 * V_DIM), BF),
+        [jax.ShapeDtypeStruct((strip, V_DIM), BF)] * 4,
         blocks + column,
         where,
         [
@@ -349,12 +371,27 @@
             pltpu.VMEM((4 * strip, 128), F32),
         ],
     )
-    return lax.all_to_all(parts, ("zh", "x"), split_axis=0, concat_axis=0, tiled=True)
-
-
-def project(parts, out_proj):
-    shape = jax.ShapeDtypeStruct((parts.shape[1], out_proj.shape[1]), BF)
-    return call(project_kernel, shape, [parts, out_proj], place=False)
+    return [parts[0]] + [shifted(parts[j], "zh", -j) for j in range(1, 4)]
+
+
+def project(where, parts, out_proj, own):
+    strip = parts[0].shape[0]
+    parts = call(
+        spread_kernel,
+        [jax.ShapeDtypeStruct((own, 4 * V_DIM), BF)] * 4,
+        parts,
+        where,
+        [pltpu.VMEM((4, strip, V_DIM), BF), pltpu.VMEM((4, own, 4 * V_DIM), BF)],
+    )
+    parts = [parts[0]] + [shifted(parts[k], "x", k) for k in range(1, 4)]
+    return call(
+        project_kernel,
+        jax.ShapeDtypeStruct((own, out_proj.shape[1]), BF),
+        parts + [out_proj],
+        where,
+        [pltpu.VMEM((4, own, 4 * V_DIM), BF)],
+        place=False,
+    )
 
 
 def body(

time: 184 us -> 204 us (1.11)
  the two profiles are of different devices: /device:TPU:6 before, /device:TPU:32 now
where the time goes in v5:
time: 204 us
  waiting for transfers between devices  102 us (50%)
  starting transfers between devices  68.7 us (34%)
  Pallas kernels  28.5 us (14%)
  local copies, waits for them, and re-layouts  2.91 us (1%)
    ppermute x33, waiting for transfers between devices, shifted(): return lax.ppermute(value, axis, [(i, (i + amount) % n) for i in range(n)])  78 us
    ppermute x33, starting transfers between devices, shifted(): return lax.ppermute(value, axis, [(i, (i + amount) % n) for i in range(n)])  50.8 us
    pallas_call x13, Pallas kernels, call(): pl.pallas_call(kernel, in_specs=specs, out_specs=VMEM_SPEC if single else...  28.5 us
    all_to_all x1, waiting for transfers between devices, both_halves(): lax.all_to_all(outgoing, EP, split_axis=0, concat_axis=0, tiled=True)  24.5 us
    all_to_all x1, starting transfers between devices, both_halves(): lax.all_to_all(outgoing, EP, split_axis=0, concat_axis=0, tiled=True)  12 us
    all_to_all x1, starting transfers between devices, both_halves(): lax.all_to_all(result, EP, split_axis=0, concat_axis=0, tiled=True)  5.98 us
  transfers between devices with their start and end apart: 35, of which 23 were waited for; matrix products, arithmetic and copies ran while one was open for 2% of the time, Pallas kernels for 10%

profile of v5, /device:TPU:32, one launch (start us, length us, event | category | flops | bytes accessed | tf_op | source)
XLA Modules:
  0.0 203.9 jit_solution(6815235791328910951)
XLA Ops:
  0.7 2.8 %shard_map.164 = (bf16[64,4,2048]{2,1,0:T(4,128)(2,1)}, bf16[256,128]{1,0:T(8,128)(2,1)S(1)}) custom-call(bf16[64,2048]{1,0:T(8,128)(2,1)} %tokens.1, f32[1,2048]{1,0:T(1,128)} %bitcast.24, s32[2,64]{1,0:T(2,128)} %bitcast.26, f32[1,64]{1,0:T(1,128)} %bitcast.28, f32[2,64]{1,0:T(2,128)} %bitcast.27), custom_call_target="tpu_custom_call" | custom-call | tf_op jit(solution)/shard_map/pallas_call | solution.py:45
  3.4 12.0 %all-to-all-start = ((bf16[64,4,2048]{2,1,0:T(4,128)(2,1)}), bf16[64,4,2048]{2,1,0:T(4,128)(2,1)}, u32[]{:S(2)}, u32[]{:S(2)}) async-start(bf16[64,4,2048]{2,1,0:T(4,128)(2,1)} %get-tuple-element.28), calls=%async_computation | async-start | bytes 2097152 | tf_op jit(solution)/shard_map/all_to_all | solution.py:168
  15.4 1.6 collective-permute-start.30
  16.9 1.8 collective-permute-start.29
  18.7 24.5 %all-to-all-done = bf16[64,4,2048]{2,1,0:T(4,128)(2,1)} async-done(((bf16[64,4,2048]{2,1,0:T(4,128)(2,1)}), bf16[64,4,2048]{2,1,0:T(4,128)(2,1)}, u32[]{:S(2)}, u32[]{:S(2)}) %all-to-all-start) | async-done | bytes 1048608 | tf_op jit(solution)/shard_map/all_to_all | solution.py:168
  43.2 1.7 fusion
  44.9 1.6 collective-permute-start.20
  46.4 1.8 collective-permute-start.24
  48.5 3.0 %collective-permute-start.27 = (bf16[32,4,2048]{2,1,0:T(4,128)(2,1)S(1)}, bf16[32,4,2048]{2,1,0:T(4,128)(2,1)S(1)}, u32[]{:S(2)}, u32[]{:S(2)}) collective-permute-start(bf16[32,4,2048]{2,1,0:T(4,128)(2,1)S(1)} %get-tuple-element.31.rows_a), channel_id=1, source_target_pairs={{0,3},{1,0},{2,1},{3,2},{4,7},{5,4},{6,5},{7,6},{8,11},{9,8},{10,9... | collective-permute-start | bytes 1572872 | tf_op jit(solution)/shard_map/ppermute | solution.py:61
  51.4 9.5 %collective-permute-done.20.rows_a = bf16[32,4,2048]{2,1,0:T(4,128)(2,1)S(1)} collective-permute-done((bf16[32,4,2048]{2,1,0:T(4,128)(2,1)S(1)}, bf16[32,4,2048]{2,1,0:T(4,128)(2,1)S(1)}, u32[]{:S(2)}, u32[]{:S(2)}) %collective-permute-start.20) | collective-permute-done | bytes 524320 | tf_op jit(solution)/shard_map/ppermute | solution.py:61
  61.2 3.0 %collective-permute-start.25 = (bf16[32,4,2048]{2,1,0:T(4,128)(2,1)S(1)}, bf16[32,4,2048]{2,1,0:T(4,128)(2,1)S(1)}, u32[]{:S(2)}, u32[]{:S(2)}) collective-permute-start(bf16[32,4,2048]{2,1,0:T(4,128)(2,1)S(1)} %collective-permute-done.24.rows_b), channel_id=1, source_target_pairs={{0,3},{1,0},{2,1},{3,2},{4,7},{5,4},{6,5},{7,6},{8,11},{9,8},{10,9... | collective-permute-start | bytes 1572872 | tf_op jit(solution)/shard_map/ppermute | solution.py:61
  64.4 1.1 slice.19
  65.4 6.8 %collective-permute-done.21.rows_b = bf16[32,4,2048]{2,1,0:T(4,128)(2,1)S(1)} collective-permute-done((bf16[32,4,2048]{2,1,0:T(4,128)(2,1)S(1)}, bf16[32,4,2048]{2,1,0:T(4,128)(2,1)S(1)}, u32[]{:S(2)}, u32[]{:S(2)}) %collective-permute-start.21) | collective-permute-done | bytes 524320 | tf_op jit(solution)/shard_map/ppermute | solution.py:61
  72.2 1.5 collective-permute-start.32
  73.8 0.7 shard_map.166
  74.5 0.9 collective-permute-start.22
  75.4 0.7 shard_map.168
  76.2 7.3 %collective-permute-done.23.rows_a = bf16[32,4,2048]{2,1,0:T(4,128)(2,1)S(1)} collective-permute-done((bf16[32,4,2048]{2,1,0:T(4,128)(2,1)S(1)}, bf16[32,4,2048]{2,1,0:T(4,128)(2,1)S(1)}, u32[]{:S(2)}, u32[]{:S(2)}) %collective-permute-start.23) | collective-permute-done | bytes 524320 | tf_op jit(solution)/shard_map/ppermute | solution.py:61
  83.4 0.3 collective-permute-start.28
  83.7 0.7 shard_map.167
  84.5 2.8 %collective-permute-start.26 = (bf16[256,256]{1,0:T(8,128)(2,1)S(1)}, bf16[256,256]{1,0:T(8,128)(2,1)S(1)}, u32[]{:S(2)}, u32[]{:S(2)}) collective-permute-start(bf16[256,256]{1,0:T(8,128)(2,1)S(1)} %shard_map.167), channel_id=1, source_target_pairs={{0,2},{1,3},{2,0},{3,1},{4,6},{5,7},{6,4},{7,5},{8,10},{9,11},{10,... | collective-permute-start | bytes 393224 | tf_op jit(solution)/shard_map/ppermute | solution.py:61
  87.3 0.7 shard_map.165.h0
  88.0 6.7 %collective-permute-done.31.w2a = bf16[128,2048]{1,0:T(8,128)(2,1)S(1)} collective-permute-done((bf16[128,2048]{1,0:T(8,128)(2,1)S(1)}, bf16[128,2048]{1,0:T(8,128)(2,1)S(1)}, u32[]{:S(2)}, u32[]{:S(2)}) %collective-permute-start.31) | collective-permute-done | bytes 524320 | tf_op jit(solution)/shard_map/ppermute | solution.py:61
  94.9 3.9 %collective-permute-done.22.h1 = bf16[256,256]{1,0:T(8,128)(2,1)S(1)} collective-permute-done((bf16[256,256]{1,0:T(8,128)(2,1)S(1)}, bf16[256,256]{1,0:T(8,128)(2,1)S(1)}, u32[]{:S(2)}, u32[]{:S(2)}) %collective-permute-start.22) | collective-permute-done | bytes 131104 | tf_op jit(solution)/shard_map/ppermute | solution.py:61
  98.9 1.7 collective-permute-done.26.h2
  100.6 3.8 %shard_map.169 = bf16[64,4,2048]{2,1,0:T(4,128)(2,1)} custom-call(bf16[256,256]{1,0:T(8,128)(2,1)S(1)} %shard_map.165.h0, bf16[256,256]{1,0:T(8,128)(2,1)S(1)} %collective-permute-done.22.h1, bf16[256,256]{1,0:T(8,128)(2,1)S(1)} %collective-permute-done.26.h2, bf16[256,256]{1,0:T(8,128)(2,1)S(1)} %collective-permute-done.28.h3, ...), custom_call_target="tpu_custom_call" | custom-call | tf_op jit(solution)/shard_map/pallas_call | solution.py:45
  104.4 6.0 %all-to-all-start.1 = ((bf16[64,4,2048]{2,1,0:T(4,128)(2,1)}), bf16[64,4,2048]{2,1,0:T(4,128)(2,1)S(1)}, u32[]{:S(2)}, u32[]{:S(2)}) async-start(bf16[64,4,2048]{2,1,0:T(4,128)(2,1)} %shard_map.169), calls=%async_computation.1 | async-start | bytes 2097152 | tf_op jit(solution)/shard_map/all_to_all | solution.py:185
  110.6 0.9 shard_map.158.l0
  111.5 1.2 collective-permute-start
  112.7 2.3 %collective-permute-start.1 = (bf16[32,544]{1,0:T(8,128)(2,1)S(1)}, bf16[32,544]{1,0:T(8,128)(2,1)S(1)}, u32[]{:S(2)}, u32[]{:S(2)}) collective-permute-start(bf16[32,544]{1,0:T(8,128)(2,1)S(1)} %shard_map.158.l0), channel_id=1, source_target_pairs={{0,2},{1,3},{2,0},{3,1},{4,6},{5,7},{6,4},{7,5},{8,10},{9,11},{10,... | collective-permute-start | bytes 104456 | tf_op jit(solution)/shard_map/ppermute | solution.py:61
  115.0 0.5 collective-permute-start.2
  115.7 1.2 collective-permute-done.l1
  116.9 1.3 collective-permute-done.1.l2
  118.2 0.8 collective-permute-done.2.l3
  119.0 1.4 shard_map.159
  120.5 2.5 %collective-permute-start.3 = (bf16[256,128]{1,0:T(8,128)(2,1)S(1)}, bf16[256,128]{1,0:T(8,128)(2,1)S(1)}, u32[]{:S(2)}, u32[]{:S(2)}) collective-permute-start(bf16[256,128]{1,0:T(8,128)(2,1)S(1)} %get-tuple-element.17), channel_id=1, source_target_pairs={{0,64},{64,128},{128,192},{192,0},{1,65},{65,129},{129,193},{193,1... | collective-permute-start | bytes 196616 | tf_op jit(solution)/shard_map/ppermute | solution.py:61
  122.9 2.9 %collective-permute-start.4 = (bf16[256,128]{1,0:T(8,128)(2,1)S(1)}, bf16[256,128]{1,0:T(8,128)(2,1)S(1)}, u32[]{:S(2)}, u32[]{:S(2)}) collective-permute-start(bf16[256,128]{1,0:T(8,128)(2,1)S(1)} %get-tuple-element.18), channel_id=1, source_target_pairs={{0,128},{64,192},{128,0},{192,64},{1,129},{65,193},{129,1},{193,65... | collective-permute-start | bytes 196616 | tf_op jit(solution)/shard_map/ppermute | solution.py:61
  125.8 3.5 %collective-permute-start.5 = (bf16[256,128]{1,0:T(8,128)(2,1)S(1)}, bf16[256,128]{1,0:T(8,128)(2,1)S(1)}, u32[]{:S(2)}, u32[]{:S(2)}) collective-permute-start(bf16[256,128]{1,0:T(8,128)(2,1)S(1)} %get-tuple-element.19), channel_id=1, source_target_pairs={{0,192},{64,0},{128,64},{192,128},{1,193},{65,1},{129,65},{193,129... | collective-permute-start | bytes 196616 | tf_op jit(solution)/shard_map/ppermute | solution.py:61
  129.3 9.7 %collective-permute-done.3.b1.q1 = bf16[256,128]{1,0:T(8,128)(2,1)S(1)} collective-permute-done((bf16[256,128]{1,0:T(8,128)(2,1)S(1)}, bf16[256,128]{1,0:T(8,128)(2,1)S(1)}, u32[]{:S(2)}, u32[]{:S(2)}) %collective-permute-start.3) | collective-permute-done | bytes 65568 | tf_op jit(solution)/shard_map/ppermute | solution.py:61
  139.0 3.8 %collective-permute-done.4.b2.q2 = bf16[256,128]{1,0:T(8,128)(2,1)S(1)} collective-permute-done((bf16[256,128]{1,0:T(8,128)(2,1)S(1)}, bf16[256,128]{1,0:T(8,128)(2,1)S(1)}, u32[]{:S(2)}, u32[]{:S(2)}) %collective-permute-start.4) | collective-permute-done | bytes 65568 | tf_op jit(solution)/shard_map/ppermute | solution.py:61
  142.9 2.5 %collective-permute-start.6 = (bf16[4,160,128]{2,1,0:T(8,128)(2,1)S(1)}, bf16[4,160,128]{2,1,0:T(8,128)(2,1)S(1)}, u32[]{:S(2)}, u32[]{:S(2)}) collective-permute-start(bf16[4,160,128]{2,1,0:T(8,128)(2,1)S(1)} %shard_map.160), channel_id=1, source_target_pairs={{0,32},{32,0},{1,33},{33,1},{2,34},{34,2},{3,35},{35,3},{4,36},{36... | collective-permute-start | bytes 491528 | tf_op jit(solution)/shard_map/ppermute | solution.py:61
  145.4 3.3 %collective-permute-done.6 = bf16[4,160,128]{2,1,0:T(8,128)(2,1)S(1)} collective-permute-done((bf16[4,160,128]{2,1,0:T(8,128)(2,1)S(1)}, bf16[4,160,128]{2,1,0:T(8,128)(2,1)S(1)}, u32[]{:S(2)}, u32[]{:S(2)}) %collective-permute-start.6) | collective-permute-done | bytes 163872 | tf_op jit(solution)/shard_map/ppermute | solution.py:61
  148.7 1.6 collective-permute-start.7
  150.3 2.7 %collective-permute-start.8 = (bf16[4,160,256]{2,1,0:T(8,128)(2,1)S(1)}, bf16[4,160,256]{2,1,0:T(8,128)(2,1)S(1)}, u32[]{:S(2)}, u32[]{:S(2)}) collective-permute-start(bf16[4,160,256]{2,1,0:T(8,128)(2,1)S(1)} %pad_maximum_fusion.refs_0_), channel_id=1, source_target_pairs={{0,16},{8,24},{16,0},{24,8},{1,17},{9,25},{17,1},{25,9},{2,18},{10... | collective-permute-start | bytes 983048 | tf_op jit(solution)/shard_map/ppermute | solution.py:61
  153.0 1.4 collective-permute-start.9
  154.4 5.5 %collective-permute-done.7.refs_1_ = bf16[4,160,256]{2,1,0:T(8,128)(2,1)S(1)} collective-permute-done((bf16[4,160,256]{2,1,0:T(8,128)(2,1)S(1)}, bf16[4,160,256]{2,1,0:T(8,128)(2,1)S(1)}, u32[]{:S(2)}, u32[]{:S(2)}) %collective-permute-start.7) | collective-permute-done | bytes 327712 | tf_op jit(solution)/shard_map/ppermute | solution.py:61
  159.9 5.4 %collective-permute-done.8.refs_2_ = bf16[4,160,256]{2,1,0:T(8,128)(2,1)S(1)} collective-permute-done((bf16[4,160,256]{2,1,0:T(8,128)(2,1)S(1)}, bf16[4,160,256]{2,1,0:T(8,128)(2,1)S(1)}, u32[]{:S(2)}, u32[]{:S(2)}) %collective-permute-start.8) | collective-permute-done | bytes 327712 | tf_op jit(solution)/shard_map/ppermute | solution.py:61
  165.3 0.5 collective-permute-start.13
  165.8 1.1 collective-permute-done.12.refs_6_
  166.9 0.5 collective-permute-done.13.refs_7_
  167.4 13.0 %shard_map.161 = (bf16[128,64]{1,0:T(8,128)(2,1)S(1)}, bf16[128,64]{1,0:T(8,128)(2,1)S(1)}, bf16[128,64]{1,0:T(8,128)(2,1)S(1)}, bf16[128,64]{1,0:T(8,128)(2,1)S(1)}) custom-call(s32[5]{0:T(128)S(1)} %stack.23.where, bf16[256,128]{1,0:T(8,128)(2,1)S(1)} %get-tuple-element.16.b0.q0, bf16[256,128]{1,0:T(8,128)(2,1)S(1)} %collective-permute-done.3.b1.q1, ...), custom_call_target="tpu_custom_call" | custom-call | tf_op jit(solution)/shard_map/pallas_call | solution.py:45
  180.4 3.1 %collective-permute-start.14 = (bf16[128,64]{1,0:T(8,128)(2,1)S(1)}, bf16[128,64]{1,0:T(8,128)(2,1)S(1)}, u32[]{:S(2)}, u32[]{:S(2)}) collective-permute-start(bf16[128,64]{1,0:T(8,128)(2,1)S(1)} %get-tuple-element.21), channel_id=1, source_target_pairs={{0,192},{64,0},{128,64},{192,128},{1,193},{65,1},{129,65},{193,129... | collective-permute-start | bytes 49160 | tf_op jit(solution)/shard_map/ppermute | solution.py:61
  183.4 3.4 %collective-permute-start.15 = (bf16[128,64]{1,0:T(8,128)(2,1)S(1)}, bf16[128,64]{1,0:T(8,128)(2,1)S(1)}, u32[]{:S(2)}, u32[]{:S(2)}) collective-permute-start(bf16[128,64]{1,0:T(8,128)(2,1)S(1)} %get-tuple-element.22), channel_id=1, source_target_pairs={{0,128},{64,192},{128,0},{192,64},{1,129},{65,193},{129,1},{193,65... | collective-permute-start | bytes 49160 | tf_op jit(solution)/shard_map/ppermute | solution.py:61
  186.8 4.4 %collective-permute-done.15.a2 = bf16[128,64]{1,0:T(8,128)(2,1)S(1)} collective-permute-done((bf16[128,64]{1,0:T(8,128)(2,1)S(1)}, bf16[128,64]{1,0:T(8,128)(2,1)S(1)}, u32[]{:S(2)}, u32[]{:S(2)}) %collective-permute-start.15) | collective-permute-done | bytes 16416 | tf_op jit(solution)/shard_map/ppermute | solution.py:61
  191.2 1.6 collective-permute-done.16.a3
  192.9 0.7 shard_map.162
  193.5 1.2 collective-permute-start.17
  194.7 2.3 %collective-permute-start.18 = (bf16[32,256]{1,0:T(8,128)(2,1)S(1)}, bf16[32,256]{1,0:T(8,128)(2,1)S(1)}, u32[]{:S(2)}, u32[]{:S(2)}) collective-permute-start(bf16[32,256]{1,0:T(8,128)(2,1)S(1)} %get-tuple-element.26), channel_id=1, source_target_pairs={{0,2},{1,3},{2,0},{3,1},{4,6},{5,7},{6,4},{7,5},{8,10},{9,11},{10,... | collective-permute-start | bytes 49160 | tf_op jit(solution)/shard_map/ppermute | solution.py:61
  197.0 0.5 collective-permute-start.19
  197.5 1.0 collective-permute-done.17.a1
  198.5 1.4 collective-permute-done.18.a2
  200.0 0.8 collective-permute-done.19.a3
  200.8 2.0 shard_map.163
  202.8 1.0 shard_map.170
  (38 shorter events, 1.5 us)
Async XLA Ops:
  0.6 73.1 %copy-start = (bf16[1,2048,256]{2,1,0:T(8,128)(2,1)S(1)}, bf16[1,2048,256]{2,1,0:T(8,128)(2,1)}, u32[]{:S(2)}) copy-start(bf16[1,2048,256]{2,1,0:T(8,128)(2,1)} %param.27) | copy-start | bytes 3145732
  0.6 73.1 %copy-start.1 = (bf16[1,2048,256]{2,1,0:T(8,128)(2,1)S(1)}, bf16[1,2048,256]{2,1,0:T(8,128)(2,1)}, u32[]{:S(2)}) copy-start(bf16[1,2048,256]{2,1,0:T(8,128)(2,1)} %param.28) | copy-start | bytes 3145732
  3.4 39.8 %all-to-all-start = ((bf16[64,4,2048]{2,1,0:T(4,128)(2,1)}), bf16[64,4,2048]{2,1,0:T(4,128)(2,1)}, u32[]{:S(2)}, u32[]{:S(2)}) async-start(bf16[64,4,2048]{2,1,0:T(4,128)(2,1)} %get-tuple-element.28), calls=%async_computation | async-start | bytes 2097152 | tf_op jit(solution)/shard_map/all_to_all | solution.py:168
  15.4 33.1 %collective-permute-start.30 = (bf16[256,2048]{1,0:T(8,128)(2,1)}, bf16[256,2048]{1,0:T(8,128)(2,1)S(1)}, u32[]{:S(2)}, u32[]{:S(2)}) collective-permute-start(bf16[256,2048]{1,0:T(8,128)(2,1)} %bitcast.21), channel_id=1, source_target_pairs={{0,1},{1,2},{2,3},{3,0},{4,5},{5,6},{6,7},{7,4},{8,9},{9,10},{10,1... | collective-permute-start | bytes 3145736 | tf_op jit(solution)/shard_map/ppermute | solution.py:61
  16.9 47.3 %collective-permute-start.29 = (bf16[256,2048]{1,0:T(8,128)(2,1)}, bf16[256,2048]{1,0:T(8,128)(2,1)}, u32[]{:S(2)}, u32[]{:S(2)}) collective-permute-start(bf16[256,2048]{1,0:T(8,128)(2,1)} %bitcast.22), channel_id=1, source_target_pairs={{0,3},{1,0},{2,1},{3,2},{4,7},{5,4},{6,5},{7,6},{8,11},{9,8},{10,9... | collective-permute-start | bytes 3145736 | tf_op jit(solution)/shard_map/ppermute | solution.py:61
  44.9 16.1 %collective-permute-start.20 = (bf16[32,4,2048]{2,1,0:T(4,128)(2,1)S(1)}, bf16[32,4,2048]{2,1,0:T(4,128)(2,1)S(1)}, u32[]{:S(2)}, u32[]{:S(2)}) collective-permute-start(bf16[32,4,2048]{2,1,0:T(4,128)(2,1)S(1)} %get-tuple-element.31.rows_a), channel_id=1, source_target_pairs={{0,1},{1,2},{2,3},{3,0},{4,5},{5,6},{6,7},{7,4},{8,9},{9,10},{10,1... | collective-permute-start | bytes 1572872 | tf_op jit(solution)/shard_map/ppermute | solution.py:61
  46.4 14.8 %collective-permute-start.24 = (bf16[32,4,2048]{2,1,0:T(4,128)(2,1)S(1)}, bf16[32,4,2048]{2,1,0:T(4,128)(2,1)S(1)}, u32[]{:S(2)}, u32[]{:S(2)}) collective-permute-start(bf16[32,4,2048]{2,1,0:T(4,128)(2,1)S(1)} %get-tuple-element.30.rows_b), channel_id=1, source_target_pairs={{0,3},{1,0},{2,1},{3,2},{4,7},{5,4},{6,5},{7,6},{8,11},{9,8},{10,9... | collective-permute-start | bytes 1572872 | tf_op jit(solution)/shard_map/ppermute | solution.py:61
  48.2 24.0 %collective-permute-start.21 = (bf16[32,4,2048]{2,1,0:T(4,128)(2,1)S(1)}, bf16[32,4,2048]{2,1,0:T(4,128)(2,1)S(1)}, u32[]{:S(2)}, u32[]{:S(2)}) collective-permute-start(bf16[32,4,2048]{2,1,0:T(4,128)(2,1)S(1)} %get-tuple-element.30.rows_b), channel_id=1, source_target_pairs={{0,1},{1,2},{2,3},{3,0},{4,5},{5,6},{6,7},{7,4},{8,9},{9,10},{10,1... | collective-permute-start | bytes 1572872 | tf_op jit(solution)/shard_map/ppermute | solution.py:61
  48.5 26.0 %collective-permute-start.27 = (bf16[32,4,2048]{2,1,0:T(4,128)(2,1)S(1)}, bf16[32,4,2048]{2,1,0:T(4,128)(2,1)S(1)}, u32[]{:S(2)}, u32[]{:S(2)}) collective-permute-start(bf16[32,4,2048]{2,1,0:T(4,128)(2,1)S(1)} %get-tuple-element.31.rows_a), channel_id=1, source_target_pairs={{0,3},{1,0},{2,1},{3,2},{4,7},{5,4},{6,5},{7,6},{8,11},{9,8},{10,9... | collective-permute-start | bytes 1572872 | tf_op jit(solution)/shard_map/ppermute | solution.py:61
  61.0 22.5 %collective-permute-start.23 = (bf16[32,4,2048]{2,1,0:T(4,128)(2,1)S(1)}, bf16[32,4,2048]{2,1,0:T(4,128)(2,1)S(1)}, u32[]{:S(2)}, u32[]{:S(2)}) collective-permute-start(bf16[32,4,2048]{2,1,0:T(4,128)(2,1)S(1)} %collective-permute-done.20.rows_a), channel_id=1, source_target_pairs={{0,1},{1,2},{2,3},{3,0},{4,5},{5,6},{6,7},{7,4},{8,9},{9,10},{10,1... | collective-permute-start | bytes 1572872 | tf_op jit(solution)/shard_map/ppermute | solution.py:61
  61.2 22.5 %collective-permute-start.25 = (bf16[32,4,2048]{2,1,0:T(4,128)(2,1)S(1)}, bf16[32,4,2048]{2,1,0:T(4,128)(2,1)S(1)}, u32[]{:S(2)}, u32[]{:S(2)}) collective-permute-start(bf16[32,4,2048]{2,1,0:T(4,128)(2,1)S(1)} %collective-permute-done.24.rows_b), channel_id=1, source_target_pairs={{0,3},{1,0},{2,1},{3,2},{4,7},{5,4},{6,5},{7,6},{8,11},{9,8},{10,9... | collective-permute-start | bytes 1572872 | tf_op jit(solution)/shard_map/ppermute | solution.py:61
  64.3 30.4 %collective-permute-start.31 = (bf16[128,2048]{1,0:T(8,128)(2,1)S(1)}, bf16[128,2048]{1,0:T(8,128)(2,1)S(1)}, u32[]{:S(2)}, u32[]{:S(2)}) collective-permute-start(bf16[128,2048]{1,0:T(8,128)(2,1)S(1)} %slice.18), channel_id=1, source_target_pairs={{0,1},{1,2},{2,3},{3,0},{4,5},{5,6},{6,7},{7,4},{8,9},{9,10},{10,1... | collective-permute-start | bytes 1572872 | tf_op jit(solution)/shard_map/ppermute | solution.py:61
  72.2 22.7 %collective-permute-start.32 = (bf16[128,2048]{1,0:T(8,128)(2,1)S(1)}, bf16[128,2048]{1,0:T(8,128)(2,1)S(1)}, u32[]{:S(2)}, u32[]{:S(2)}) collective-permute-start(bf16[128,2048]{1,0:T(8,128)(2,1)S(1)} %slice.19), channel_id=1, source_target_pairs={{0,3},{1,0},{2,1},{3,2},{4,7},{5,4},{6,5},{7,6},{8,11},{9,8},{10,9... | collective-permute-start | bytes 1572872 | tf_op jit(solution)/shard_map/ppermute | solution.py:61
  74.5 26.1 %copy-start.3 = (bf16[1,256,2048]{2,1,0:T(8,128)(2,1)S(1)}, bf16[1,256,2048]{2,1,0:T(8,128)(2,1)}, u32[]{:S(2)}) copy-start(bf16[1,256,2048]{2,1,0:T(8,128)(2,1)} %param.29) | copy-start | bytes 3145732
  74.5 24.4 %collective-permute-start.22 = (bf16[256,256]{1,0:T(8,128)(2,1)S(1)}, bf16[256,256]{1,0:T(8,128)(2,1)S(1)}, u32[]{:S(2)}, u32[]{:S(2)}) collective-permute-start(bf16[256,256]{1,0:T(8,128)(2,1)S(1)} %shard_map.166), channel_id=1, source_target_pairs={{0,3},{1,0},{2,1},{3,2},{4,7},{5,4},{6,5},{7,6},{8,11},{9,8},{10,9... | collective-permute-start | bytes 393224 | tf_op jit(solution)/shard_map/ppermute | solution.py:61
  83.4 15.4 %collective-permute-start.28 = (bf16[256,256]{1,0:T(8,128)(2,1)S(1)}, bf16[256,256]{1,0:T(8,128)(2,1)S(1)}, u32[]{:S(2)}, u32[]{:S(2)}) collective-permute-start(bf16[256,256]{1,0:T(8,128)(2,1)S(1)} %shard_map.168), channel_id=1, source_target_pairs={{0,1},{1,2},{2,3},{3,0},{4,5},{5,6},{6,7},{7,4},{8,9},{9,10},{10,1... | collective-permute-start | bytes 393224 | tf_op jit(solution)/shard_map/ppermute | solution.py:61
  84.5 16.1 %collective-permute-start.26 = (bf16[256,256]{1,0:T(8,128)(2,1)S(1)}, bf16[256,256]{1,0:T(8,128)(2,1)S(1)}, u32[]{:S(2)}, u32[]{:S(2)}) collective-permute-start(bf16[256,256]{1,0:T(8,128)(2,1)S(1)} %shard_map.167), channel_id=1, source_target_pairs={{0,2},{1,3},{2,0},{3,1},{4,6},{5,7},{6,4},{7,5},{8,10},{9,11},{10,... | collective-permute-start | bytes 393224 | tf_op jit(solution)/shard_map/ppermute | solution.py:61
  104.4 98.5 %all-to-all-start.1 = ((bf16[64,4,2048]{2,1,0:T(4,128)(2,1)}), bf16[64,4,2048]{2,1,0:T(4,128)(2,1)S(1)}, u32[]{:S(2)}, u32[]{:S(2)}) async-start(bf16[64,4,2048]{2,1,0:T(4,128)(2,1)} %shard_map.169), calls=%async_computation.1 | async-start | bytes 2097152 | tf_op jit(solution)/shard_map/all_to_all | solution.py:185
  111.5 5.4 %collective-permute-start = (bf16[32,544]{1,0:T(8,128)(2,1)S(1)}, bf16[32,544]{1,0:T(8,128)(2,1)S(1)}, u32[]{:S(2)}, u32[]{:S(2)}) collective-permute-start(bf16[32,544]{1,0:T(8,128)(2,1)S(1)} %shard_map.158.l0), channel_id=1, source_target_pairs={{0,1},{1,2},{2,3},{3,0},{4,5},{5,6},{6,7},{7,4},{8,9},{9,10},{10,1... | collective-permute-start | bytes 104456 | tf_op jit(solution)/shard_map/ppermute | solution.py:61
  112.7 5.5 %collective-permute-start.1 = (bf16[32,544]{1,0:T(8,128)(2,1)S(1)}, bf16[32,544]{1,0:T(8,128)(2,1)S(1)}, u32[]{:S(2)}, u32[]{:S(2)}) collective-permute-start(bf16[32,544]{1,0:T(8,128)(2,1)S(1)} %shard_map.158.l0), channel_id=1, source_target_pairs={{0,2},{1,3},{2,0},{3,1},{4,6},{5,7},{6,4},{7,5},{8,10},{9,11},{10,... | collective-permute-start | bytes 104456 | tf_op jit(solution)/shard_map/ppermute | solution.py:61
  115.0 4.0 %collective-permute-start.2 = (bf16[32,544]{1,0:T(8,128)(2,1)S(1)}, bf16[32,544]{1,0:T(8,128)(2,1)S(1)}, u32[]{:S(2)}, u32[]{:S(2)}) collective-permute-start(bf16[32,544]{1,0:T(8,128)(2,1)S(1)} %shard_map.158.l0), channel_id=1, source_target_pairs={{0,3},{1,0},{2,1},{3,2},{4,7},{5,4},{6,5},{7,6},{8,11},{9,8},{10,9... | collective-permute-start | bytes 104456 | tf_op jit(solution)/shard_map/ppermute | solution.py:61
  115.7 85.1 %copy-start.2 = (bf16[1024,2048]{1,0:T(8,128)(2,1)S(1)}, bf16[1024,2048]{1,0:T(8,128)(2,1)}, u32[]{:S(2)}) copy-start(bf16[1024,2048]{1,0:T(8,128)(2,1)} %out_proj.1) | copy-start | bytes 12582916
  120.5 18.5 %collective-permute-start.3 = (bf16[256,128]{1,0:T(8,128)(2,1)S(1)}, bf16[256,128]{1,0:T(8,128)(2,1)S(1)}, u32[]{:S(2)}, u32[]{:S(2)}) collective-permute-start(bf16[256,128]{1,0:T(8,128)(2,1)S(1)} %get-tuple-element.17), channel_id=1, source_target_pairs={{0,64},{64,128},{128,192},{192,0},{1,65},{65,129},{129,193},{193,1... | collective-permute-start | bytes 196616 | tf_op jit(solution)/shard_map/ppermute | solution.py:61
  122.9 19.9 %collective-permute-start.4 = (bf16[256,128]{1,0:T(8,128)(2,1)S(1)}, bf16[256,128]{1,0:T(8,128)(2,1)S(1)}, u32[]{:S(2)}, u32[]{:S(2)}) collective-permute-start(bf16[256,128]{1,0:T(8,128)(2,1)S(1)} %get-tuple-element.18), channel_id=1, source_target_pairs={{0,128},{64,192},{128,0},{192,64},{1,129},{65,193},{129,1},{193,65... | collective-permute-start | bytes 196616 | tf_op jit(solution)/shard_map/ppermute | solution.py:61
  125.8 17.0 %collective-permute-start.5 = (bf16[256,128]{1,0:T(8,128)(2,1)S(1)}, bf16[256,128]{1,0:T(8,128)(2,1)S(1)}, u32[]{:S(2)}, u32[]{:S(2)}) collective-permute-start(bf16[256,128]{1,0:T(8,128)(2,1)S(1)} %get-tuple-element.19), channel_id=1, source_target_pairs={{0,192},{64,0},{128,64},{192,128},{1,193},{65,1},{129,65},{193,129... | collective-permute-start | bytes 196616 | tf_op jit(solution)/shard_map/ppermute | solution.py:61
  142.9 5.8 %collective-permute-start.6 = (bf16[4,160,128]{2,1,0:T(8,128)(2,1)S(1)}, bf16[4,160,128]{2,1,0:T(8,128)(2,1)S(1)}, u32[]{:S(2)}, u32[]{:S(2)}) collective-permute-start(bf16[4,160,128]{2,1,0:T(8,128)(2,1)S(1)} %shard_map.160), channel_id=1, source_target_pairs={{0,32},{32,0},{1,33},{33,1},{2,34},{34,2},{3,35},{35,3},{4,36},{36... | collective-permute-start | bytes 491528 | tf_op jit(solution)/shard_map/ppermute | solution.py:61
  148.7 11.2 %collective-permute-start.7 = (bf16[4,160,256]{2,1,0:T(8,128)(2,1)S(1)}, bf16[4,160,256]{2,1,0:T(8,128)(2,1)S(1)}, u32[]{:S(2)}, u32[]{:S(2)}) collective-permute-start(bf16[4,160,256]{2,1,0:T(8,128)(2,1)S(1)} %pad_maximum_fusion.refs_0_), channel_id=1, source_target_pairs={{0,8},{8,16},{16,24},{24,0},{1,9},{9,17},{17,25},{25,1},{2,10},{10... | collective-permute-start | bytes 983048 | tf_op jit(solution)/shard_map/ppermute | solution.py:61
  150.3 15.0 %collective-permute-start.8 = (bf16[4,160,256]{2,1,0:T(8,128)(2,1)S(1)}, bf16[4,160,256]{2,1,0:T(8,128)(2,1)S(1)}, u32[]{:S(2)}, u32[]{:S(2)}) collective-permute-start(bf16[4,160,256]{2,1,0:T(8,128)(2,1)S(1)} %pad_maximum_fusion.refs_0_), channel_id=1, source_target_pairs={{0,16},{8,24},{16,0},{24,8},{1,17},{9,25},{17,1},{25,9},{2,18},{10... | collective-permute-start | bytes 983048 | tf_op jit(solution)/shard_map/ppermute | solution.py:61
  153.0 12.3 %collective-permute-start.9 = (bf16[4,160,256]{2,1,0:T(8,128)(2,1)S(1)}, bf16[4,160,256]{2,1,0:T(8,128)(2,1)S(1)}, u32[]{:S(2)}, u32[]{:S(2)}) collective-permute-start(bf16[4,160,256]{2,1,0:T(8,128)(2,1)S(1)} %pad_maximum_fusion.refs_0_), channel_id=1, source_target_pairs={{0,24},{8,0},{16,8},{24,16},{1,25},{9,1},{17,9},{25,17},{2,26},{10... | collective-permute-start | bytes 983048 | tf_op jit(solution)/shard_map/ppermute | solution.py:61
  154.4 11.4 %collective-permute-start.10 = (bf16[4,160,256]{2,1,0:T(8,128)(2,1)S(1)}, bf16[4,160,256]{2,1,0:T(8,128)(2,1)S(1)}, u32[]{:S(2)}, u32[]{:S(2)}) collective-permute-start(bf16[4,160,256]{2,1,0:T(8,128)(2,1)S(1)} %pad_maximum_fusion.refs_0_), channel_id=1, source_target_pairs={{0,4},{4,0},{1,5},{5,1},{2,6},{6,2},{3,7},{7,3},{8,12},{12,8},{9,1... | collective-permute-start | bytes 983048 | tf_op jit(solution)/shard_map/ppermute | solution.py:61
  159.9 5.9 %collective-permute-start.11 = (bf16[4,160,256]{2,1,0:T(8,128)(2,1)S(1)}, bf16[4,160,256]{2,1,0:T(8,128)(2,1)S(1)}, u32[]{:S(2)}, u32[]{:S(2)}) collective-permute-start(bf16[4,160,256]{2,1,0:T(8,128)(2,1)S(1)} %collective-permute-done.7.refs_1_), channel_id=1, source_target_pairs={{0,4},{4,0},{1,5},{5,1},{2,6},{6,2},{3,7},{7,3},{8,12},{12,8},{9,1... | collective-permute-start | bytes 983048 | tf_op jit(solution)/shard_map/ppermute | solution.py:61
  165.3 1.6 collective-permute-start.12
  165.3 2.1 %collective-permute-start.13 = (bf16[4,160,256]{2,1,0:T(8,128)(2,1)S(1)}, bf16[4,160,256]{2,1,0:T(8,128)(2,1)S(1)}, u32[]{:S(2)}, u32[]{:S(2)}) collective-permute-start(bf16[4,160,256]{2,1,0:T(8,128)(2,1)S(1)} %collective-permute-done.9.refs_3_), channel_id=1, source_target_pairs={{0,4},{4,0},{1,5},{5,1},{2,6},{6,2},{3,7},{7,3},{8,12},{12,8},{9,1... | collective-permute-start | bytes 983048 | tf_op jit(solution)/shard_map/ppermute | solution.py:61
  180.4 6.5 %collective-permute-start.14 = (bf16[128,64]{1,0:T(8,128)(2,1)S(1)}, bf16[128,64]{1,0:T(8,128)(2,1)S(1)}, u32[]{:S(2)}, u32[]{:S(2)}) collective-permute-start(bf16[128,64]{1,0:T(8,128)(2,1)S(1)} %get-tuple-element.21), channel_id=1, source_target_pairs={{0,192},{64,0},{128,64},{192,128},{1,193},{65,1},{129,65},{193,129... | collective-permute-start | bytes 49160 | tf_op jit(solution)/shard_map/ppermute | solution.py:61
  183.4 7.8 %collective-permute-start.15 = (bf16[128,64]{1,0:T(8,128)(2,1)S(1)}, bf16[128,64]{1,0:T(8,128)(2,1)S(1)}, u32[]{:S(2)}, u32[]{:S(2)}) collective-permute-start(bf16[128,64]{1,0:T(8,128)(2,1)S(1)} %get-tuple-element.22), channel_id=1, source_target_pairs={{0,128},{64,192},{128,0},{192,64},{1,129},{65,193},{129,1},{193,65... | collective-permute-start | bytes 49160 | tf_op jit(solution)/shard_map/ppermute | solution.py:61
  186.8 6.0 %collective-permute-start.16 = (bf16[128,64]{1,0:T(8,128)(2,1)S(1)}, bf16[128,64]{1,0:T(8,128)(2,1)S(1)}, u32[]{:S(2)}, u32[]{:S(2)}) collective-permute-start(bf16[128,64]{1,0:T(8,128)(2,1)S(1)} %get-tuple-element.23), channel_id=1, source_target_pairs={{0,64},{64,128},{128,192},{192,0},{1,65},{65,129},{129,193},{193,1... | collective-permute-start | bytes 49160 | tf_op jit(solution)/shard_map/ppermute | solution.py:61
  193.5 5.0 %collective-permute-start.17 = (bf16[32,256]{1,0:T(8,128)(2,1)S(1)}, bf16[32,256]{1,0:T(8,128)(2,1)S(1)}, u32[]{:S(2)}, u32[]{:S(2)}) collective-permute-start(bf16[32,256]{1,0:T(8,128)(2,1)S(1)} %get-tuple-element.25), channel_id=1, source_target_pairs={{0,1},{1,2},{2,3},{3,0},{4,5},{5,6},{6,7},{7,4},{8,9},{9,10},{10,1... | collective-permute-start | bytes 49160 | tf_op jit(solution)/shard_map/ppermute | solution.py:61
  194.7 5.2 %collective-permute-start.18 = (bf16[32,256]{1,0:T(8,128)(2,1)S(1)}, bf16[32,256]{1,0:T(8,128)(2,1)S(1)}, u32[]{:S(2)}, u32[]{:S(2)}) collective-permute-start(bf16[32,256]{1,0:T(8,128)(2,1)S(1)} %get-tuple-element.26), channel_id=1, source_target_pairs={{0,2},{1,3},{2,0},{3,1},{4,6},{5,7},{6,4},{7,5},{8,10},{9,11},{10,... | collective-permute-start | bytes 49160 | tf_op jit(solution)/shard_map/ppermute | solution.py:61
  197.0 3.7 %collective-permute-start.19 = (bf16[32,256]{1,0:T(8,128)(2,1)S(1)}, bf16[32,256]{1,0:T(8,128)(2,1)S(1)}, u32[]{:S(2)}, u32[]{:S(2)}) collective-permute-start(bf16[32,256]{1,0:T(8,128)(2,1)S(1)} %get-tuple-element.27), channel_id=1, source_target_pairs={{0,3},{1,0},{2,1},{3,2},{4,7},{5,4},{6,5},{7,6},{8,11},{9,8},{10,9... | collective-permute-start | bytes 49160 | tf_op jit(solution)/shard_map/ppermute | solution.py:61

commit v6 on v5

--- a/solution.py
+++ b/solution.py
@@ -28,7 +28,7 @@
 VMEM_SPEC = pl.BlockSpec(memory_space=pltpu.VMEM)
 
 
-def call(kernel, out_shape, arrays, where=None, scratch=(), limit=16 << 20, unplaced=(), place=True):
+def call(kernel, out_shape, arrays, where=None, scratch=(), limit=8 << 20, unplaced=(), place=True):
     arrays = [
         pltpu.with_memory_space_constraint(a, pltpu.HBM if i in unplaced else pltpu.VMEM)
         for i, a in enumerate(arrays)
@@ -111,18 +111,28 @@
     )
 
 
-def hidden_kernel(rows_a, rows_b, w_gate, w_up, out):
-    half = out.shape[0] // 2
-    for at, rows in ((0, rows_a), (half, rows_b)):
-        got = rows[...].reshape(half, w_gate.shape[0])
-        gate = mm(got, w_gate[...])
-        up = mm(got, w_up[...])
-        out[at : at + half, :] = (gate / (1.0 + jnp.exp(-gate)) * up).astype(BF)
+def hidden_kernel(rows_a, rows_b, w_gate, w_up, out, gate_s, up_s):
+    half, span = out.shape[0] // 2, 512
+    gate_s[...] = jnp.zeros(gate_s.shape, F32)
+    up_s[...] = jnp.zeros(up_s.shape, F32)
+
+    def add(step, _):
+        cols = pl.ds(pl.multiple_of(step * span, span), span)
+        for at, rows in ((0, rows_a), (half, rows_b)):
+            got = rows[:, :, cols].reshape(half, span)
+            gate_s[at : at + half, :] += mm(got, w_gate[cols, :])
+            up_s[at : at + half, :] += mm(got, w_up[cols, :])
+        return 0
+
+    lax.fori_loop(0, w_gate.shape[0] // span, add, 0)
+    gate = gate_s[...]
+    out[...] = (gate / (1.0 + jnp.exp(-gate)) * up_s[...]).astype(BF)
 
 
 def hidden_of(rows_a, rows_b, w_gate, w_up):
     shape = jax.ShapeDtypeStruct((2 * rows_a.shape[0] * CAP, w_gate.shape[1]), BF)
-    return call(hidden_kernel, shape, [rows_a, rows_b, w_gate, w_up])
+    scratch = [pltpu.VMEM(shape.shape, F32)] * 2
+    return call(hidden_kernel, shape, [rows_a, rows_b, w_gate, w_up], scratch=scratch)
 
 
 def down_kernel(h0, h1, h2, h3, w0, w1, w2a, w2b, w3, out):
@@ -281,18 +291,12 @@
             key_at = (col_zl * 8 + key_y * 2 + jnp.bitwise_xor(c, m)) * strip + col_x
             masks.append(key_at <= query_at)
 
-        def one_group(g, _, group=group, masks=masks):
+        for g in range(4):
             from_zh = lax.rem(zh - g + 4, 4)
-            parts = [block.at[from_zh] for block in group]
-
-            def later(s, _):
-                advance(pl.ds(pl.multiple_of(s * strip, strip), strip), parts, None)
-                return 0
-
-            advance(pl.ds(pl.multiple_of(g * strip, strip), strip), parts, masks)
-            return lax.fori_loop(g + 1, 4, later, 0)
-
-        lax.fori_loop(0, 4, one_group, 0)
+            parts = [block[from_zh] for block in group]
+            advance(slice(g * strip, (g + 1) * strip), parts, masks)
+            if g < 3:
+                advance(slice((g + 1) * strip, 4 * strip), parts, None)
     total = acc_s[...]
     acc_s[:, :V_DIM] = total[:, :V_DIM] / total[:, V_DIM:]
     for j, out in enumerate(outs):

time: 204 us -> 197 us (0.966)
  Pallas kernels: 28.5 us -> 23.9 us
    pallas_call x13, Pallas kernels: 28.5 us -> 23.9 us  [call(): pl.pallas_call(kernel, in_specs=specs, out_specs=VMEM_SPEC if single else...]
    ppermute x33, waiting for transfers between devices: 78 us -> 75.5 us  [shifted(): return lax.ppermute(value, axis, [(i, (i + amount) % n) for i in range(n)])]
  transfers between devices with their start and end apart: 35 -> 35, of which waited for: 23 -> 23; matrix products, arithmetic and copies ran while one was open for 2% -> 2% of each run, Pallas kernels for 10% -> 8%
where the time goes in v6:
time: 197 us
  waiting for transfers between devices  100 us (51%)
  starting transfers between devices  68.7 us (35%)
  Pallas kernels  23.9 us (12%)
  local copies, waits for them, and re-layouts  2.9 us (1%)
    ppermute x33, waiting for transfers between devices, shifted(): return lax.ppermute(value, axis, [(i, (i + amount) % n) for i in range(n)])  75.5 us
    ppermute x33, starting transfers between devices, shifted(): return lax.ppermute(value, axis, [(i, (i + amount) % n) for i in range(n)])  50.8 us
    all_to_all x1, waiting for transfers between devices, both_halves(): lax.all_to_all(outgoing, EP, split_axis=0, concat_axis=0, tiled=True)  24.5 us
    pallas_call x13, Pallas kernels, call(): pl.pallas_call(kernel, in_specs=specs, out_specs=VMEM_SPEC if single else...  23.9 us
    all_to_all x1, starting transfers between devices, both_halves(): lax.all_to_all(outgoing, EP, split_axis=0, concat_axis=0, tiled=True)  12 us
    all_to_all x1, starting transfers between devices, both_halves(): lax.all_to_all(result, EP, split_axis=0, concat_axis=0, tiled=True)  5.98 us
  transfers between devices with their start and end apart: 35, of which 23 were waited for; matrix products, arithmetic and copies ran while one was open for 2% of the time, Pallas kernels for 8%

profile of v6, /device:TPU:32, one launch (start us, length us, event | category | flops | bytes accessed | tf_op | source)
XLA Modules:
  0.0 196.7 jit_solution(1433122070806856290)
XLA Ops:
  0.7 2.8 %shard_map.164 = (bf16[64,4,2048]{2,1,0:T(4,128)(2,1)}, bf16[256,128]{1,0:T(8,128)(2,1)S(1)}) custom-call(bf16[64,2048]{1,0:T(8,128)(2,1)} %tokens.1, f32[1,2048]{1,0:T(1,128)} %bitcast.24, s32[2,64]{1,0:T(2,128)} %bitcast.26, f32[1,64]{1,0:T(1,128)} %bitcast.28, f32[2,64]{1,0:T(2,128)} %bitcast.27), custom_call_target="tpu_custom_call" | custom-call | tf_op jit(solution)/shard_map/pallas_call | solution.py:45
  3.4 12.0 %all-to-all-start = ((bf16[64,4,2048]{2,1,0:T(4,128)(2,1)}), bf16[64,4,2048]{2,1,0:T(4,128)(2,1)}, u32[]{:S(2)}, u32[]{:S(2)}) async-start(bf16[64,4,2048]{2,1,0:T(4,128)(2,1)} %get-tuple-element.28), calls=%async_computation | async-start | bytes 2097152 | tf_op jit(solution)/shard_map/all_to_all | solution.py:178
  15.4 1.6 collective-permute-start.30
  16.9 1.8 collective-permute-start.29
  18.7 24.5 %all-to-all-done = bf16[64,4,2048]{2,1,0:T(4,128)(2,1)} async-done(((bf16[64,4,2048]{2,1,0:T(4,128)(2,1)}), bf16[64,4,2048]{2,1,0:T(4,128)(2,1)}, u32[]{:S(2)}, u32[]{:S(2)}) %all-to-all-start) | async-done | bytes 1048608 | tf_op jit(solution)/shard_map/all_to_all | solution.py:178
  43.2 1.7 fusion
  44.9 1.6 collective-permute-start.20
  46.4 1.8 collective-permute-start.24
  48.5 3.0 %collective-permute-start.27 = (bf16[32,4,2048]{2,1,0:T(4,128)(2,1)S(1)}, bf16[32,4,2048]{2,1,0:T(4,128)(2,1)S(1)}, u32[]{:S(2)}, u32[]{:S(2)}) collective-permute-start(bf16[32,4,2048]{2,1,0:T(4,128)(2,1)S(1)} %get-tuple-element.31.rows_a), channel_id=1, source_target_pairs={{0,3},{1,0},{2,1},{3,2},{4,7},{5,4},{6,5},{7,6},{8,11},{9,8},{10,9... | collective-permute-start | bytes 1572872 | tf_op jit(solution)/shard_map/ppermute | solution.py:61
  51.4 9.5 %collective-permute-done.20.rows_a = bf16[32,4,2048]{2,1,0:T(4,128)(2,1)S(1)} collective-permute-done((bf16[32,4,2048]{2,1,0:T(4,128)(2,1)S(1)}, bf16[32,4,2048]{2,1,0:T(4,128)(2,1)S(1)}, u32[]{:S(2)}, u32[]{:S(2)}) %collective-permute-start.20) | collective-permute-done | bytes 524320 | tf_op jit(solution)/shard_map/ppermute | solution.py:61
  61.2 3.0 %collective-permute-start.25 = (bf16[32,4,2048]{2,1,0:T(4,128)(2,1)S(1)}, bf16[32,4,2048]{2,1,0:T(4,128)(2,1)S(1)}, u32[]{:S(2)}, u32[]{:S(2)}) collective-permute-start(bf16[32,4,2048]{2,1,0:T(4,128)(2,1)S(1)} %collective-permute-done.24.rows_b), channel_id=1, source_target_pairs={{0,3},{1,0},{2,1},{3,2},{4,7},{5,4},{6,5},{7,6},{8,11},{9,8},{10,9... | collective-permute-start | bytes 1572872 | tf_op jit(solution)/shard_map/ppermute | solution.py:61
  64.4 1.1 slice.19
  65.4 6.8 %collective-permute-done.21.rows_b = bf16[32,4,2048]{2,1,0:T(4,128)(2,1)S(1)} collective-permute-done((bf16[32,4,2048]{2,1,0:T(4,128)(2,1)S(1)}, bf16[32,4,2048]{2,1,0:T(4,128)(2,1)S(1)}, u32[]{:S(2)}, u32[]{:S(2)}) %collective-permute-start.21) | collective-permute-done | bytes 524320 | tf_op jit(solution)/shard_map/ppermute | solution.py:61
  72.2 1.5 collective-permute-start.32
  73.7 1.4 shard_map.166
  75.1 0.9 collective-permute-start.22
  76.0 1.4 shard_map.168
  77.4 6.0 %collective-permute-done.23.rows_a = bf16[32,4,2048]{2,1,0:T(4,128)(2,1)S(1)} collective-permute-done((bf16[32,4,2048]{2,1,0:T(4,128)(2,1)S(1)}, bf16[32,4,2048]{2,1,0:T(4,128)(2,1)S(1)}, u32[]{:S(2)}, u32[]{:S(2)}) %collective-permute-start.23) | collective-permute-done | bytes 524320 | tf_op jit(solution)/shard_map/ppermute | solution.py:61
  83.4 0.3 collective-permute-start.28
  83.7 1.4 shard_map.167
  85.1 2.8 %collective-permute-start.26 = (bf16[256,256]{1,0:T(8,128)(2,1)S(1)}, bf16[256,256]{1,0:T(8,128)(2,1)S(1)}, u32[]{:S(2)}, u32[]{:S(2)}) collective-permute-start(bf16[256,256]{1,0:T(8,128)(2,1)S(1)} %shard_map.167), channel_id=1, source_target_pairs={{0,2},{1,3},{2,0},{3,1},{4,6},{5,7},{6,4},{7,5},{8,10},{9,11},{10,... | collective-permute-start | bytes 393224 | tf_op jit(solution)/shard_map/ppermute | solution.py:61
  87.9 1.4 shard_map.165.h0
  89.3 5.4 %collective-permute-done.31.w2a = bf16[128,2048]{1,0:T(8,128)(2,1)S(1)} collective-permute-done((bf16[128,2048]{1,0:T(8,128)(2,1)S(1)}, bf16[128,2048]{1,0:T(8,128)(2,1)S(1)}, u32[]{:S(2)}, u32[]{:S(2)}) %collective-permute-start.31) | collective-permute-done | bytes 524320 | tf_op jit(solution)/shard_map/ppermute | solution.py:61
  94.9 3.9 %collective-permute-done.22.h1 = bf16[256,256]{1,0:T(8,128)(2,1)S(1)} collective-permute-done((bf16[256,256]{1,0:T(8,128)(2,1)S(1)}, bf16[256,256]{1,0:T(8,128)(2,1)S(1)}, u32[]{:S(2)}, u32[]{:S(2)}) %collective-permute-start.22) | collective-permute-done | bytes 131104 | tf_op jit(solution)/shard_map/ppermute | solution.py:61
  98.9 1.7 collective-permute-done.26.h2
  100.5 3.8 %shard_map.169 = bf16[64,4,2048]{2,1,0:T(4,128)(2,1)} custom-call(bf16[256,256]{1,0:T(8,128)(2,1)S(1)} %shard_map.165.h0, bf16[256,256]{1,0:T(8,128)(2,1)S(1)} %collective-permute-done.22.h1, bf16[256,256]{1,0:T(8,128)(2,1)S(1)} %collective-permute-done.26.h2, bf16[256,256]{1,0:T(8,128)(2,1)S(1)} %collective-permute-done.28.h3, ...), custom_call_target="tpu_custom_call" | custom-call | tf_op jit(solution)/shard_map/pallas_call | solution.py:45
  104.4 6.0 %all-to-all-start.1 = ((bf16[64,4,2048]{2,1,0:T(4,128)(2,1)}), bf16[64,4,2048]{2,1,0:T(4,128)(2,1)S(1)}, u32[]{:S(2)}, u32[]{:S(2)}) async-start(bf16[64,4,2048]{2,1,0:T(4,128)(2,1)} %shard_map.169), calls=%async_computation.1 | async-start | bytes 2097152 | tf_op jit(solution)/shard_map/all_to_all | solution.py:195
  110.6 0.9 shard_map.158.l0
  111.5 1.2 collective-permute-start
  112.7 2.3 %collective-permute-start.1 = (bf16[32,544]{1,0:T(8,128)(2,1)S(1)}, bf16[32,544]{1,0:T(8,128)(2,1)S(1)}, u32[]{:S(2)}, u32[]{:S(2)}) collective-permute-start(bf16[32,544]{1,0:T(8,128)(2,1)S(1)} %shard_map.158.l0), channel_id=1, source_target_pairs={{0,2},{1,3},{2,0},{3,1},{4,6},{5,7},{6,4},{7,5},{8,10},{9,11},{10,... | collective-permute-start | bytes 104456 | tf_op jit(solution)/shard_map/ppermute | solution.py:61
  115.0 0.5 collective-permute-start.2
  115.7 1.2 collective-permute-done.l1
  116.9 1.3 collective-permute-done.1.l2
  118.2 0.8 collective-permute-done.2.l3
  119.0 1.4 shard_map.159
  120.5 2.5 %collective-permute-start.3 = (bf16[256,128]{1,0:T(8,128)(2,1)S(1)}, bf16[256,128]{1,0:T(8,128)(2,1)S(1)}, u32[]{:S(2)}, u32[]{:S(2)}) collective-permute-start(bf16[256,128]{1,0:T(8,128)(2,1)S(1)} %get-tuple-element.17), channel_id=1, source_target_pairs={{0,64},{64,128},{128,192},{192,0},{1,65},{65,129},{129,193},{193,1... | collective-permute-start | bytes 196616 | tf_op jit(solution)/shard_map/ppermute | solution.py:61
  122.9 2.9 %collective-permute-start.4 = (bf16[256,128]{1,0:T(8,128)(2,1)S(1)}, bf16[256,128]{1,0:T(8,128)(2,1)S(1)}, u32[]{:S(2)}, u32[]{:S(2)}) collective-permute-start(bf16[256,128]{1,0:T(8,128)(2,1)S(1)} %get-tuple-element.18), channel_id=1, source_target_pairs={{0,128},{64,192},{128,0},{192,64},{1,129},{65,193},{129,1},{193,65... | collective-permute-start | bytes 196616 | tf_op jit(solution)/shard_map/ppermute | solution.py:61
  125.8 3.5 %collective-permute-start.5 = (bf16[256,128]{1,0:T(8,128)(2,1)S(1)}, bf16[256,128]{1,0:T(8,128)(2,1)S(1)}, u32[]{:S(2)}, u32[]{:S(2)}) collective-permute-start(bf16[256,128]{1,0:T(8,128)(2,1)S(1)} %get-tuple-element.19), channel_id=1, source_target_pairs={{0,192},{64,0},{128,64},{192,128},{1,193},{65,1},{129,65},{193,129... | collective-permute-start | bytes 196616 | tf_op jit(solution)/shard_map/ppermute | solution.py:61
  129.3 9.7 %collective-permute-done.3.b1.q1 = bf16[256,128]{1,0:T(8,128)(2,1)S(1)} collective-permute-done((bf16[256,128]{1,0:T(8,128)(2,1)S(1)}, bf16[256,128]{1,0:T(8,128)(2,1)S(1)}, u32[]{:S(2)}, u32[]{:S(2)}) %collective-permute-start.3) | collective-permute-done | bytes 65568 | tf_op jit(solution)/shard_map/ppermute | solution.py:61
  139.0 3.8 %collective-permute-done.4.b2.q2 = bf16[256,128]{1,0:T(8,128)(2,1)S(1)} collective-permute-done((bf16[256,128]{1,0:T(8,128)(2,1)S(1)}, bf16[256,128]{1,0:T(8,128)(2,1)S(1)}, u32[]{:S(2)}, u32[]{:S(2)}) %collective-permute-start.4) | collective-permute-done | bytes 65568 | tf_op jit(solution)/shard_map/ppermute | solution.py:61
  142.8 2.5 %collective-permute-start.6 = (bf16[4,160,128]{2,1,0:T(8,128)(2,1)S(1)}, bf16[4,160,128]{2,1,0:T(8,128)(2,1)S(1)}, u32[]{:S(2)}, u32[]{:S(2)}) collective-permute-start(bf16[4,160,128]{2,1,0:T(8,128)(2,1)S(1)} %shard_map.160), channel_id=1, source_target_pairs={{0,32},{32,0},{1,33},{33,1},{2,34},{34,2},{3,35},{35,3},{4,36},{36... | collective-permute-start | bytes 491528 | tf_op jit(solution)/shard_map/ppermute | solution.py:61
  145.4 3.3 %collective-permute-done.6 = bf16[4,160,128]{2,1,0:T(8,128)(2,1)S(1)} collective-permute-done((bf16[4,160,128]{2,1,0:T(8,128)(2,1)S(1)}, bf16[4,160,128]{2,1,0:T(8,128)(2,1)S(1)}, u32[]{:S(2)}, u32[]{:S(2)}) %collective-permute-start.6) | collective-permute-done | bytes 163872 | tf_op jit(solution)/shard_map/ppermute | solution.py:61
  148.7 1.6 collective-permute-start.7
  150.3 2.7 %collective-permute-start.8 = (bf16[4,160,256]{2,1,0:T(8,128)(2,1)S(1)}, bf16[4,160,256]{2,1,0:T(8,128)(2,1)S(1)}, u32[]{:S(2)}, u32[]{:S(2)}) collective-permute-start(bf16[4,160,256]{2,1,0:T(8,128)(2,1)S(1)} %pad_maximum_fusion.refs_0_), channel_id=1, source_target_pairs={{0,16},{8,24},{16,0},{24,8},{1,17},{9,25},{17,1},{25,9},{2,18},{10... | collective-permute-start | bytes 983048 | tf_op jit(solution)/shard_map/ppermute | solution.py:61
  153.0 1.4 collective-permute-start.9
  154.4 5.5 %collective-permute-done.7.refs_1_ = bf16[4,160,256]{2,1,0:T(8,128)(2,1)S(1)} collective-permute-done((bf16[4,160,256]{2,1,0:T(8,128)(2,1)S(1)}, bf16[4,160,256]{2,1,0:T(8,128)(2,1)S(1)}, u32[]{:S(2)}, u32[]{:S(2)}) %collective-permute-start.7) | collective-permute-done | bytes 327712 | tf_op jit(solution)/shard_map/ppermute | solution.py:61
  159.9 5.4 %collective-permute-done.8.refs_2_ = bf16[4,160,256]{2,1,0:T(8,128)(2,1)S(1)} collective-permute-done((bf16[4,160,256]{2,1,0:T(8,128)(2,1)S(1)}, bf16[4,160,256]{2,1,0:T(8,128)(2,1)S(1)}, u32[]{:S(2)}, u32[]{:S(2)}) %collective-permute-start.8) | collective-permute-done | bytes 327712 | tf_op jit(solution)/shard_map/ppermute | solution.py:61
  165.3 0.5 collective-permute-start.13
  165.8 1.1 collective-permute-done.12.refs_6_
  166.9 0.5 collective-permute-done.13.refs_7_
  167.4 5.8 %shard_map.161 = (bf16[128,64]{1,0:T(8,128)(2,1)S(1)}, bf16[128,64]{1,0:T(8,128)(2,1)S(1)}, bf16[128,64]{1,0:T(8,128)(2,1)S(1)}, bf16[128,64]{1,0:T(8,128)(2,1)S(1)}) custom-call(s32[5]{0:T(128)S(1)} %stack.23.where, bf16[256,128]{1,0:T(8,128)(2,1)S(1)} %get-tuple-element.16.b0.q0, bf16[256,128]{1,0:T(8,128)(2,1)S(1)} %collective-permute-done.3.b1.q1, ...), custom_call_target="tpu_custom_call" | custom-call | tf_op jit(solution)/shard_map/pallas_call | solution.py:45
  173.2 3.1 %collective-permute-start.14 = (bf16[128,64]{1,0:T(8,128)(2,1)S(1)}, bf16[128,64]{1,0:T(8,128)(2,1)S(1)}, u32[]{:S(2)}, u32[]{:S(2)}) collective-permute-start(bf16[128,64]{1,0:T(8,128)(2,1)S(1)} %get-tuple-element.21), channel_id=1, source_target_pairs={{0,192},{64,0},{128,64},{192,128},{1,193},{65,1},{129,65},{193,129... | collective-permute-start | bytes 49160 | tf_op jit(solution)/shard_map/ppermute | solution.py:61
  176.3 3.4 %collective-permute-start.15 = (bf16[128,64]{1,0:T(8,128)(2,1)S(1)}, bf16[128,64]{1,0:T(8,128)(2,1)S(1)}, u32[]{:S(2)}, u32[]{:S(2)}) collective-permute-start(bf16[128,64]{1,0:T(8,128)(2,1)S(1)} %get-tuple-element.22), channel_id=1, source_target_pairs={{0,128},{64,192},{128,0},{192,64},{1,129},{65,193},{129,1},{193,65... | collective-permute-start | bytes 49160 | tf_op jit(solution)/shard_map/ppermute | solution.py:61
  179.7 4.4 %collective-permute-done.15.a2 = bf16[128,64]{1,0:T(8,128)(2,1)S(1)} collective-permute-done((bf16[128,64]{1,0:T(8,128)(2,1)S(1)}, bf16[128,64]{1,0:T(8,128)(2,1)S(1)}, u32[]{:S(2)}, u32[]{:S(2)}) %collective-permute-start.15) | collective-permute-done | bytes 16416 | tf_op jit(solution)/shard_map/ppermute | solution.py:61
  184.1 1.6 collective-permute-done.16.a3
  185.7 0.7 shard_map.162
  186.3 1.2 collective-permute-start.17
  187.6 2.3 %collective-permute-start.18 = (bf16[32,256]{1,0:T(8,128)(2,1)S(1)}, bf16[32,256]{1,0:T(8,128)(2,1)S(1)}, u32[]{:S(2)}, u32[]{:S(2)}) collective-permute-start(bf16[32,256]{1,0:T(8,128)(2,1)S(1)} %get-tuple-element.26), channel_id=1, source_target_pairs={{0,2},{1,3},{2,0},{3,1},{4,6},{5,7},{6,4},{7,5},{8,10},{9,11},{10,... | collective-permute-start | bytes 49160 | tf_op jit(solution)/shard_map/ppermute | solution.py:61
  189.9 0.5 collective-permute-start.19
  190.3 1.0 collective-permute-done.17.a1
  191.4 1.4 collective-permute-done.18.a2
  192.8 0.8 collective-permute-done.19.a3
  193.6 2.0 %shard_map.163 = bf16[32,2048]{1,0:T(8,128)(2,1)} custom-call(s32[5]{0:T(128)S(1)} %stack.23.where, bf16[32,256]{1,0:T(8,128)(2,1)S(1)} %get-tuple-element.24.a0, bf16[32,256]{1,0:T(8,128)(2,1)S(1)} %collective-permute-done.17.a1, bf16[32,256]{1,0:T(8,128)(2,1)S(1)} %collective-permute-done.18.a2, bf16[32,256]{1,0:T(8,128)(2,1)S(1)} %collective-permute-done.19.a3, ...), custom_call_target="tpu_custom_call" | custom-call | tf_op jit(solution)/shard_map/pallas_call | solution.py:45
  195.7 1.0 shard_map.170
  (38 shorter events, 1.5 us)
Async XLA Ops:
  0.6 73.1 %copy-start = (bf16[1,2048,256]{2,1,0:T(8,128)(2,1)S(1)}, bf16[1,2048,256]{2,1,0:T(8,128)(2,1)}, u32[]{:S(2)}) copy-start(bf16[1,2048,256]{2,1,0:T(8,128)(2,1)} %param.27) | copy-start | bytes 3145732
  0.6 73.1 %copy-start.1 = (bf16[1,2048,256]{2,1,0:T(8,128)(2,1)S(1)}, bf16[1,2048,256]{2,1,0:T(8,128)(2,1)}, u32[]{:S(2)}) copy-start(bf16[1,2048,256]{2,1,0:T(8,128)(2,1)} %param.28) | copy-start | bytes 3145732
  3.4 39.8 %all-to-all-start = ((bf16[64,4,2048]{2,1,0:T(4,128)(2,1)}), bf16[64,4,2048]{2,1,0:T(4,128)(2,1)}, u32[]{:S(2)}, u32[]{:S(2)}) async-start(bf16[64,4,2048]{2,1,0:T(4,128)(2,1)} %get-tuple-element.28), calls=%async_computation | async-start | bytes 2097152 | tf_op jit(solution)/shard_map/all_to_all | solution.py:178
  15.4 33.1 %collective-permute-start.30 = (bf16[256,2048]{1,0:T(8,128)(2,1)}, bf16[256,2048]{1,0:T(8,128)(2,1)S(1)}, u32[]{:S(2)}, u32[]{:S(2)}) collective-permute-start(bf16[256,2048]{1,0:T(8,128)(2,1)} %bitcast.21), channel_id=1, source_target_pairs={{0,1},{1,2},{2,3},{3,0},{4,5},{5,6},{6,7},{7,4},{8,9},{9,10},{10,1... | collective-permute-start | bytes 3145736 | tf_op jit(solution)/shard_map/ppermute | solution.py:61
  16.9 47.3 %collective-permute-start.29 = (bf16[256,2048]{1,0:T(8,128)(2,1)}, bf16[256,2048]{1,0:T(8,128)(2,1)}, u32[]{:S(2)}, u32[]{:S(2)}) collective-permute-start(bf16[256,2048]{1,0:T(8,128)(2,1)} %bitcast.22), channel_id=1, source_target_pairs={{0,3},{1,0},{2,1},{3,2},{4,7},{5,4},{6,5},{7,6},{8,11},{9,8},{10,9... | collective-permute-start | bytes 3145736 | tf_op jit(solution)/shard_map/ppermute | solution.py:61
  44.9 16.1 %collective-permute-start.20 = (bf16[32,4,2048]{2,1,0:T(4,128)(2,1)S(1)}, bf16[32,4,2048]{2,1,0:T(4,128)(2,1)S(1)}, u32[]{:S(2)}, u32[]{:S(2)}) collective-permute-start(bf16[32,4,2048]{2,1,0:T(4,128)(2,1)S(1)} %get-tuple-element.31.rows_a), channel_id=1, source_target_pairs={{0,1},{1,2},{2,3},{3,0},{4,5},{5,6},{6,7},{7,4},{8,9},{9,10},{10,1... | collective-permute-start | bytes 1572872 | tf_op jit(solution)/shard_map/ppermute | solution.py:61
  46.4 14.8 %collective-permute-start.24 = (bf16[32,4,2048]{2,1,0:T(4,128)(2,1)S(1)}, bf16[32,4,2048]{2,1,0:T(4,128)(2,1)S(1)}, u32[]{:S(2)}, u32[]{:S(2)}) collective-permute-start(bf16[32,4,2048]{2,1,0:T(4,128)(2,1)S(1)} %get-tuple-element.30.rows_b), channel_id=1, source_target_pairs={{0,3},{1,0},{2,1},{3,2},{4,7},{5,4},{6,5},{7,6},{8,11},{9,8},{10,9... | collective-permute-start | bytes 1572872 | tf_op jit(solution)/shard_map/ppermute | solution.py:61
  48.2 24.0 %collective-permute-start.21 = (bf16[32,4,2048]{2,1,0:T(4,128)(2,1)S(1)}, bf16[32,4,2048]{2,1,0:T(4,128)(2,1)S(1)}, u32[]{:S(2)}, u32[]{:S(2)}) collective-permute-start(bf16[32,4,2048]{2,1,0:T(4,128)(2,1)S(1)} %get-tuple-element.30.rows_b), channel_id=1, source_target_pairs={{0,1},{1,2},{2,3},{3,0},{4,5},{5,6},{6,7},{7,4},{8,9},{9,10},{10,1... | collective-permute-start | bytes 1572872 | tf_op jit(solution)/shard_map/ppermute | solution.py:61
  48.5 26.7 %collective-permute-start.27 = (bf16[32,4,2048]{2,1,0:T(4,128)(2,1)S(1)}, bf16[32,4,2048]{2,1,0:T(4,128)(2,1)S(1)}, u32[]{:S(2)}, u32[]{:S(2)}) collective-permute-start(bf16[32,4,2048]{2,1,0:T(4,128)(2,1)S(1)} %get-tuple-element.31.rows_a), channel_id=1, source_target_pairs={{0,3},{1,0},{2,1},{3,2},{4,7},{5,4},{6,5},{7,6},{8,11},{9,8},{10,9... | collective-permute-start | bytes 1572872 | tf_op jit(solution)/shard_map/ppermute | solution.py:61
  61.0 22.5 %collective-permute-start.23 = (bf16[32,4,2048]{2,1,0:T(4,128)(2,1)S(1)}, bf16[32,4,2048]{2,1,0:T(4,128)(2,1)S(1)}, u32[]{:S(2)}, u32[]{:S(2)}) collective-permute-start(bf16[32,4,2048]{2,1,0:T(4,128)(2,1)S(1)} %collective-permute-done.20.rows_a), channel_id=1, source_target_pairs={{0,1},{1,2},{2,3},{3,0},{4,5},{5,6},{6,7},{7,4},{8,9},{9,10},{10,1... | collective-permute-start | bytes 1572872 | tf_op jit(solution)/shard_map/ppermute | solution.py:61
  61.2 22.5 %collective-permute-start.25 = (bf16[32,4,2048]{2,1,0:T(4,128)(2,1)S(1)}, bf16[32,4,2048]{2,1,0:T(4,128)(2,1)S(1)}, u32[]{:S(2)}, u32[]{:S(2)}) collective-permute-start(bf16[32,4,2048]{2,1,0:T(4,128)(2,1)S(1)} %collective-permute-done.24.rows_b), channel_id=1, source_target_pairs={{0,3},{1,0},{2,1},{3,2},{4,7},{5,4},{6,5},{7,6},{8,11},{9,8},{10,9... | collective-permute-start | bytes 1572872 | tf_op jit(solution)/shard_map/ppermute | solution.py:61
  64.3 30.4 %collective-permute-start.31 = (bf16[128,2048]{1,0:T(8,128)(2,1)S(1)}, bf16[128,2048]{1,0:T(8,128)(2,1)S(1)}, u32[]{:S(2)}, u32[]{:S(2)}) collective-permute-start(bf16[128,2048]{1,0:T(8,128)(2,1)S(1)} %slice.18), channel_id=1, source_target_pairs={{0,1},{1,2},{2,3},{3,0},{4,5},{5,6},{6,7},{7,4},{8,9},{9,10},{10,1... | collective-permute-start | bytes 1572872 | tf_op jit(solution)/shard_map/ppermute | solution.py:61
  72.2 22.7 %collective-permute-start.32 = (bf16[128,2048]{1,0:T(8,128)(2,1)S(1)}, bf16[128,2048]{1,0:T(8,128)(2,1)S(1)}, u32[]{:S(2)}, u32[]{:S(2)}) collective-permute-start(bf16[128,2048]{1,0:T(8,128)(2,1)S(1)} %slice.19), channel_id=1, source_target_pairs={{0,3},{1,0},{2,1},{3,2},{4,7},{5,4},{6,5},{7,6},{8,11},{9,8},{10,9... | collective-permute-start | bytes 1572872 | tf_op jit(solution)/shard_map/ppermute | solution.py:61
  75.1 25.4 %copy-start.3 = (bf16[1,256,2048]{2,1,0:T(8,128)(2,1)S(1)}, bf16[1,256,2048]{2,1,0:T(8,128)(2,1)}, u32[]{:S(2)}) copy-start(bf16[1,256,2048]{2,1,0:T(8,128)(2,1)} %param.29) | copy-start | bytes 3145732
  75.1 23.7 %collective-permute-start.22 = (bf16[256,256]{1,0:T(8,128)(2,1)S(1)}, bf16[256,256]{1,0:T(8,128)(2,1)S(1)}, u32[]{:S(2)}, u32[]{:S(2)}) collective-permute-start(bf16[256,256]{1,0:T(8,128)(2,1)S(1)} %shard_map.166), channel_id=1, source_target_pairs={{0,3},{1,0},{2,1},{3,2},{4,7},{5,4},{6,5},{7,6},{8,11},{9,8},{10,9... | collective-permute-start | bytes 393224 | tf_op jit(solution)/shard_map/ppermute | solution.py:61
  83.4 15.4 %collective-permute-start.28 = (bf16[256,256]{1,0:T(8,128)(2,1)S(1)}, bf16[256,256]{1,0:T(8,128)(2,1)S(1)}, u32[]{:S(2)}, u32[]{:S(2)}) collective-permute-start(bf16[256,256]{1,0:T(8,128)(2,1)S(1)} %shard_map.168), channel_id=1, source_target_pairs={{0,1},{1,2},{2,3},{3,0},{4,5},{5,6},{6,7},{7,4},{8,9},{9,10},{10,1... | collective-permute-start | bytes 393224 | tf_op jit(solution)/shard_map/ppermute | solution.py:61
  85.1 15.5 %collective-permute-start.26 = (bf16[256,256]{1,0:T(8,128)(2,1)S(1)}, bf16[256,256]{1,0:T(8,128)(2,1)S(1)}, u32[]{:S(2)}, u32[]{:S(2)}) collective-permute-start(bf16[256,256]{1,0:T(8,128)(2,1)S(1)} %shard_map.167), channel_id=1, source_target_pairs={{0,2},{1,3},{2,0},{3,1},{4,6},{5,7},{6,4},{7,5},{8,10},{9,11},{10,... | collective-permute-start | bytes 393224 | tf_op jit(solution)/shard_map/ppermute | solution.py:61
  104.4 91.3 %all-to-all-start.1 = ((bf16[64,4,2048]{2,1,0:T(4,128)(2,1)}), bf16[64,4,2048]{2,1,0:T(4,128)(2,1)S(1)}, u32[]{:S(2)}, u32[]{:S(2)}) async-start(bf16[64,4,2048]{2,1,0:T(4,128)(2,1)} %shard_map.169), calls=%async_computation.1 | async-start | bytes 2097152 | tf_op jit(solution)/shard_map/all_to_all | solution.py:195
  111.5 5.4 %collective-permute-start = (bf16[32,544]{1,0:T(8,128)(2,1)S(1)}, bf16[32,544]{1,0:T(8,128)(2,1)S(1)}, u32[]{:S(2)}, u32[]{:S(2)}) collective-permute-start(bf16[32,544]{1,0:T(8,128)(2,1)S(1)} %shard_map.158.l0), channel_id=1, source_target_pairs={{0,1},{1,2},{2,3},{3,0},{4,5},{5,6},{6,7},{7,4},{8,9},{9,10},{10,1... | collective-permute-start | bytes 104456 | tf_op jit(solution)/shard_map/ppermute | solution.py:61
  112.7 5.5 %collective-permute-start.1 = (bf16[32,544]{1,0:T(8,128)(2,1)S(1)}, bf16[32,544]{1,0:T(8,128)(2,1)S(1)}, u32[]{:S(2)}, u32[]{:S(2)}) collective-permute-start(bf16[32,544]{1,0:T(8,128)(2,1)S(1)} %shard_map.158.l0), channel_id=1, source_target_pairs={{0,2},{1,3},{2,0},{3,1},{4,6},{5,7},{6,4},{7,5},{8,10},{9,11},{10,... | collective-permute-start | bytes 104456 | tf_op jit(solution)/shard_map/ppermute | solution.py:61
  115.0 4.0 %collective-permute-start.2 = (bf16[32,544]{1,0:T(8,128)(2,1)S(1)}, bf16[32,544]{1,0:T(8,128)(2,1)S(1)}, u32[]{:S(2)}, u32[]{:S(2)}) collective-permute-start(bf16[32,544]{1,0:T(8,128)(2,1)S(1)} %shard_map.158.l0), channel_id=1, source_target_pairs={{0,3},{1,0},{2,1},{3,2},{4,7},{5,4},{6,5},{7,6},{8,11},{9,8},{10,9... | collective-permute-start | bytes 104456 | tf_op jit(solution)/shard_map/ppermute | solution.py:61
  115.7 77.9 %copy-start.2 = (bf16[1024,2048]{1,0:T(8,128)(2,1)S(1)}, bf16[1024,2048]{1,0:T(8,128)(2,1)}, u32[]{:S(2)}) copy-start(bf16[1024,2048]{1,0:T(8,128)(2,1)} %out_proj.1) | copy-start | bytes 12582916
  120.5 18.5 %collective-permute-start.3 = (bf16[256,128]{1,0:T(8,128)(2,1)S(1)}, bf16[256,128]{1,0:T(8,128)(2,1)S(1)}, u32[]{:S(2)}, u32[]{:S(2)}) collective-permute-start(bf16[256,128]{1,0:T(8,128)(2,1)S(1)} %get-tuple-element.17), channel_id=1, source_target_pairs={{0,64},{64,128},{128,192},{192,0},{1,65},{65,129},{129,193},{193,1... | collective-permute-start | bytes 196616 | tf_op jit(solution)/shard_map/ppermute | solution.py:61
  122.9 19.9 %collective-permute-start.4 = (bf16[256,128]{1,0:T(8,128)(2,1)S(1)}, bf16[256,128]{1,0:T(8,128)(2,1)S(1)}, u32[]{:S(2)}, u32[]{:S(2)}) collective-permute-start(bf16[256,128]{1,0:T(8,128)(2,1)S(1)} %get-tuple-element.18), channel_id=1, source_target_pairs={{0,128},{64,192},{128,0},{192,64},{1,129},{65,193},{129,1},{193,65... | collective-permute-start | bytes 196616 | tf_op jit(solution)/shard_map/ppermute | solution.py:61
  125.8 17.0 %collective-permute-start.5 = (bf16[256,128]{1,0:T(8,128)(2,1)S(1)}, bf16[256,128]{1,0:T(8,128)(2,1)S(1)}, u32[]{:S(2)}, u32[]{:S(2)}) collective-permute-start(bf16[256,128]{1,0:T(8,128)(2,1)S(1)} %get-tuple-element.19), channel_id=1, source_target_pairs={{0,192},{64,0},{128,64},{192,128},{1,193},{65,1},{129,65},{193,129... | collective-permute-start | bytes 196616 | tf_op jit(solution)/shard_map/ppermute | solution.py:61
  142.8 5.8 %collective-permute-start.6 = (bf16[4,160,128]{2,1,0:T(8,128)(2,1)S(1)}, bf16[4,160,128]{2,1,0:T(8,128)(2,1)S(1)}, u32[]{:S(2)}, u32[]{:S(2)}) collective-permute-start(bf16[4,160,128]{2,1,0:T(8,128)(2,1)S(1)} %shard_map.160), channel_id=1, source_target_pairs={{0,32},{32,0},{1,33},{33,1},{2,34},{34,2},{3,35},{35,3},{4,36},{36... | collective-permute-start | bytes 491528 | tf_op jit(solution)/shard_map/ppermute | solution.py:61
  148.7 11.2 %collective-permute-start.7 = (bf16[4,160,256]{2,1,0:T(8,128)(2,1)S(1)}, bf16[4,160,256]{2,1,0:T(8,128)(2,1)S(1)}, u32[]{:S(2)}, u32[]{:S(2)}) collective-permute-start(bf16[4,160,256]{2,1,0:T(8,128)(2,1)S(1)} %pad_maximum_fusion.refs_0_), channel_id=1, source_target_pairs={{0,8},{8,16},{16,24},{24,0},{1,9},{9,17},{17,25},{25,1},{2,10},{10... | collective-permute-start | bytes 983048 | tf_op jit(solution)/shard_map/ppermute | solution.py:61
  150.3 15.0 %collective-permute-start.8 = (bf16[4,160,256]{2,1,0:T(8,128)(2,1)S(1)}, bf16[4,160,256]{2,1,0:T(8,128)(2,1)S(1)}, u32[]{:S(2)}, u32[]{:S(2)}) collective-permute-start(bf16[4,160,256]{2,1,0:T(8,128)(2,1)S(1)} %pad_maximum_fusion.refs_0_), channel_id=1, source_target_pairs={{0,16},{8,24},{16,0},{24,8},{1,17},{9,25},{17,1},{25,9},{2,18},{10... | collective-permute-start | bytes 983048 | tf_op jit(solution)/shard_map/ppermute | solution.py:61
  153.0 12.3 %collective-permute-start.9 = (bf16[4,160,256]{2,1,0:T(8,128)(2,1)S(1)}, bf16[4,160,256]{2,1,0:T(8,128)(2,1)S(1)}, u32[]{:S(2)}, u32[]{:S(2)}) collective-permute-start(bf16[4,160,256]{2,1,0:T(8,128)(2,1)S(1)} %pad_maximum_fusion.refs_0_), channel_id=1, source_target_pairs={{0,24},{8,0},{16,8},{24,16},{1,25},{9,1},{17,9},{25,17},{2,26},{10... | collective-permute-start | bytes 983048 | tf_op jit(solution)/shard_map/ppermute | solution.py:61
  154.4 11.4 %collective-permute-start.10 = (bf16[4,160,256]{2,1,0:T(8,128)(2,1)S(1)}, bf16[4,160,256]{2,1,0:T(8,128)(2,1)S(1)}, u32[]{:S(2)}, u32[]{:S(2)}) collective-permute-start(bf16[4,160,256]{2,1,0:T(8,128)(2,1)S(1)} %pad_maximum_fusion.refs_0_), channel_id=1, source_target_pairs={{0,4},{4,0},{1,5},{5,1},{2,6},{6,2},{3,7},{7,3},{8,12},{12,8},{9,1... | collective-permute-start | bytes 983048 | tf_op jit(solution)/shard_map/ppermute | solution.py:61
  159.9 5.9 %collective-permute-start.11 = (bf16[4,160,256]{2,1,0:T(8,128)(2,1)S(1)}, bf16[4,160,256]{2,1,0:T(8,128)(2,1)S(1)}, u32[]{:S(2)}, u32[]{:S(2)}) collective-permute-start(bf16[4,160,256]{2,1,0:T(8,128)(2,1)S(1)} %collective-permute-done.7.refs_1_), channel_id=1, source_target_pairs={{0,4},{4,0},{1,5},{5,1},{2,6},{6,2},{3,7},{7,3},{8,12},{12,8},{9,1... | collective-permute-start | bytes 983048 | tf_op jit(solution)/shard_map/ppermute | solution.py:61
  165.3 1.6 collective-permute-start.12
  165.3 2.1 %collective-permute-start.13 = (bf16[4,160,256]{2,1,0:T(8,128)(2,1)S(1)}, bf16[4,160,256]{2,1,0:T(8,128)(2,1)S(1)}, u32[]{:S(2)}, u32[]{:S(2)}) collective-permute-start(bf16[4,160,256]{2,1,0:T(8,128)(2,1)S(1)} %collective-permute-done.9.refs_3_), channel_id=1, source_target_pairs={{0,4},{4,0},{1,5},{5,1},{2,6},{6,2},{3,7},{7,3},{8,12},{12,8},{9,1... | collective-permute-start | bytes 983048 | tf_op jit(solution)/shard_map/ppermute | solution.py:61
  173.2 6.5 %collective-permute-start.14 = (bf16[128,64]{1,0:T(8,128)(2,1)S(1)}, bf16[128,64]{1,0:T(8,128)(2,1)S(1)}, u32[]{:S(2)}, u32[]{:S(2)}) collective-permute-start(bf16[128,64]{1,0:T(8,128)(2,1)S(1)} %get-tuple-element.21), channel_id=1, source_target_pairs={{0,192},{64,0},{128,64},{192,128},{1,193},{65,1},{129,65},{193,129... | collective-permute-start | bytes 49160 | tf_op jit(solution)/shard_map/ppermute | solution.py:61
  176.3 7.8 %collective-permute-start.15 = (bf16[128,64]{1,0:T(8,128)(2,1)S(1)}, bf16[128,64]{1,0:T(8,128)(2,1)S(1)}, u32[]{:S(2)}, u32[]{:S(2)}) collective-permute-start(bf16[128,64]{1,0:T(8,128)(2,1)S(1)} %get-tuple-element.22), channel_id=1, source_target_pairs={{0,128},{64,192},{128,0},{192,64},{1,129},{65,193},{129,1},{193,65... | collective-permute-start | bytes 49160 | tf_op jit(solution)/shard_map/ppermute | solution.py:61
  179.7 6.0 %collective-permute-start.16 = (bf16[128,64]{1,0:T(8,128)(2,1)S(1)}, bf16[128,64]{1,0:T(8,128)(2,1)S(1)}, u32[]{:S(2)}, u32[]{:S(2)}) collective-permute-start(bf16[128,64]{1,0:T(8,128)(2,1)S(1)} %get-tuple-element.23), channel_id=1, source_target_pairs={{0,64},{64,128},{128,192},{192,0},{1,65},{65,129},{129,193},{193,1... | collective-permute-start | bytes 49160 | tf_op jit(solution)/shard_map/ppermute | solution.py:61
  186.3 5.0 %collective-permute-start.17 = (bf16[32,256]{1,0:T(8,128)(2,1)S(1)}, bf16[32,256]{1,0:T(8,128)(2,1)S(1)}, u32[]{:S(2)}, u32[]{:S(2)}) collective-permute-start(bf16[32,256]{1,0:T(8,128)(2,1)S(1)} %get-tuple-element.25), channel_id=1, source_target_pairs={{0,1},{1,2},{2,3},{3,0},{4,5},{5,6},{6,7},{7,4},{8,9},{9,10},{10,1... | collective-permute-start | bytes 49160 | tf_op jit(solution)/shard_map/ppermute | solution.py:61
  187.6 5.2 %collective-permute-start.18 = (bf16[32,256]{1,0:T(8,128)(2,1)S(1)}, bf16[32,256]{1,0:T(8,128)(2,1)S(1)}, u32[]{:S(2)}, u32[]{:S(2)}) collective-permute-start(bf16[32,256]{1,0:T(8,128)(2,1)S(1)} %get-tuple-element.26), channel_id=1, source_target_pairs={{0,2},{1,3},{2,0},{3,1},{4,6},{5,7},{6,4},{7,5},{8,10},{9,11},{10,... | collective-permute-start | bytes 49160 | tf_op jit(solution)/shard_map/ppermute | solution.py:61
  189.9 3.7 %collective-permute-start.19 = (bf16[32,256]{1,0:T(8,128)(2,1)S(1)}, bf16[32,256]{1,0:T(8,128)(2,1)S(1)}, u32[]{:S(2)}, u32[]{:S(2)}) collective-permute-start(bf16[32,256]{1,0:T(8,128)(2,1)S(1)} %get-tuple-element.27), channel_id=1, source_target_pairs={{0,3},{1,0},{2,1},{3,2},{4,7},{5,4},{6,5},{7,6},{8,11},{9,8},{10,9... | collective-permute-start | bytes 49160 | tf_op jit(solution)/shard_map/ppermute | solution.py:61

commit v7 on v6

--- a/solution.py
+++ b/solution.py
@@ -28,8 +28,8 @@
 VMEM_SPEC = pl.BlockSpec(memory_space=pltpu.VMEM)
 
 
-def call(kernel, out_shape, arrays, where=None, scratch=(), limit=8 << 20, unplaced=(), place=True):
-    arrays = [
+def call(kernel, out_shape, arrays, where=None, scratch=(), limit=8 << 20, unplaced=(), place=True, free=False, **more):
+    arrays = arrays if free else [
         pltpu.with_memory_space_constraint(a, pltpu.HBM if i in unplaced else pltpu.VMEM)
         for i, a in enumerate(arrays)
     ]
@@ -42,13 +42,15 @@
             out_shape = pltpu.VMEM(out_shape.shape, out_shape.dtype)
         else:
             out_shape = [pltpu.VMEM(s.shape, s.dtype) for s in out_shape]
+    outs = VMEM_SPEC if single else [VMEM_SPEC] * len(out_shape)
     return pl.pallas_call(
         kernel,
         in_specs=specs,
-        out_specs=VMEM_SPEC if single else [VMEM_SPEC] * len(out_shape),
+        out_specs=more.pop("out_specs", outs),
         out_shape=out_shape,
         scratch_shapes=list(scratch),
         compiler_params=pltpu.CompilerParams(vmem_limit_bytes=limit),
+        **more,
     )(*arrays)
 
 
@@ -73,33 +75,44 @@
     return widened * lax.rsqrt(jnp.mean(widened * widened, axis=-1, keepdims=True) + epsilon) * gain
 
 
-def dispatch_kernel(tokens, gain, routes, group_prob, expert_prob, outgoing, shares_out):
+def dispatch_kernel(
+    tokens, gain, routes, group_prob, expert_prob, outgoing, shares_out, normed_s, mine_s
+):
+    step = pl.program_id(0)
     rows = tokens.shape[0]
     experts, cap, width = outgoing.shape
-    slots = experts * cap
-    normed = rms_scale(tokens[...], gain[...]).astype(BF)
-    slot = lax.broadcasted_iota(jnp.int32, (slots, rows), 0)
-    expert = slot // cap
-    first = routes[0:1, :] == expert
-    second = routes[1:2, :] == expert
-    named = (first | second).astype(BF)
-    before = lax.broadcasted_iota(jnp.int32, (rows, rows), 0) < lax.broadcasted_iota(
-        jnp.int32, (rows, rows), 1
-    )
-    prior = mm(named, before.astype(BF))
-    mine = (first | second) & (prior == (slot % cap).astype(F32))
-    outgoing[...] = mm(mine.astype(BF), normed).reshape(experts, cap, width).astype(BF)
-    probs = expert_prob[...]
-    shares = group_prob[...] * probs / jnp.sum(probs, axis=0, keepdims=True)
-    weights = jnp.where(first, shares[0:1, :], shares[1:2, :])
-    weights = jnp.where(mine, weights, 0.0)
-    high = weights.astype(BF)
-    shares_out[:, 0:rows] = high
-    shares_out[:, rows : 2 * rows] = (weights - high.astype(F32)).astype(BF)
+    slots = shares_out.shape[0]
+
+    @pl.when(step == 0)
+    def _():
+        normed_s[...] = rms_scale(tokens[...], gain[...]).astype(BF)
+        slot = lax.broadcasted_iota(jnp.int32, (slots, rows), 0)
+        expert = slot // cap
+        first = routes[0:1, :] == expert
+        second = routes[1:2, :] == expert
+        named = (first | second).astype(BF)
+        before = lax.broadcasted_iota(jnp.int32, (rows, rows), 0) < lax.broadcasted_iota(
+            jnp.int32, (rows, rows), 1
+        )
+        prior = mm(named, before.astype(BF))
+        mine = (first | second) & (prior == (slot % cap).astype(F32))
+        mine_s[...] = mine.astype(BF)
+        probs = expert_prob[...]
+        shares = group_prob[...] * probs / jnp.sum(probs, axis=0, keepdims=True)
+        weights = jnp.where(first, shares[0:1, :], shares[1:2, :])
+        weights = jnp.where(mine, weights, 0.0)
+        high = weights.astype(BF)
+        shares_out[:, 0:rows] = high
+        shares_out[:, rows : 2 * rows] = (weights - high.astype(F32)).astype(BF)
+
+    at = pl.multiple_of(step * experts * cap, experts * cap)
+    chosen = mine_s[pl.ds(at, experts * cap), :]
+    outgoing[...] = mm(chosen, normed_s[...]).reshape(experts, cap, width).astype(BF)
 
 
 def dispatch(tokens, gain, routes, group_prob, expert_prob, experts):
     rows, width = tokens.shape
+    block = pl.BlockSpec((experts // 4, CAP, width), lambda i: (i, 0, 0))
     return call(
         dispatch_kernel,
         (
@@ -108,6 +121,10 @@
         ),
         [tokens, gain[None, :], routes.T, group_prob[None, :], expert_prob.T],
         unplaced=range(5),
+        place=False,
+        scratch=[pltpu.VMEM((rows, width), BF), pltpu.VMEM((experts * CAP, rows), BF)],
+        grid=(4,),
+        out_specs=[block, VMEM_SPEC],
     )
 
 
@@ -135,11 +152,18 @@
     return call(hidden_kernel, shape, [rows_a, rows_b, w_gate, w_up], scratch=scratch)
 
 
-def down_kernel(h0, h1, h2, h3, w0, w1, w2a, w2b, w3, out):
-    half = w2a.shape[0]
-    total = mm(h0[...], w0[...]) + mm(h1[...], w1[...]) + mm(h3[...], w3[...])
-    total = total + mm(h2[:, :half], w2a[...]) + mm(h2[:, half:], w2b[...])
-    out[...] = total.reshape(out.shape).astype(BF)
+def stage_kernel(w0, w1, w2a, w2b, w3, out):
+    at = 0
+    for piece in (w0, w1, w2a, w2b, w3):
+        out[at : at + piece.shape[0], :] = piece[...]
+        at += piece.shape[0]
+
+
+def down_kernel(h0, h1, h2, h3, weights, out):
+    experts, cap, _ = out.shape
+    rows = pl.ds(pl.multiple_of(pl.program_id(0) * experts * cap, experts * cap), experts * cap)
+    hidden = jnp.concatenate([h[rows, :] for h in (h0, h1, h2, h3)], axis=1)
+    out[...] = mm(hidden, weights[...]).reshape(out.shape).astype(BF)
 
 
 def combine_kernel(returned, shares, out):
@@ -173,7 +197,14 @@
     down_left, down_right = shifted(w_down, "x", 1), shifted(w_down, "x", -1)
     units = w_down.shape[0] // 2
     cut_a, cut_b = down_left[:units], down_right[units:]
-    down_far = [shifted(cut_a, "x", 1), shifted(cut_b, "x", -1)]
+    down = [w_down, down_right]
+    down += [shifted(cut_a, "x", 1), shifted(cut_b, "x", -1)]
+    down = call(
+        stage_kernel,
+        jax.ShapeDtypeStruct((4 * w_down.shape[0], width), BF),
+        down + [down_left],
+        free=True,
+    )
     outgoing, shares = dispatch(tokens, moe_gain, routes, group_prob, expert_prob, experts)
     arrived = lax.all_to_all(outgoing, EP, split_axis=0, concat_axis=0, tiled=True)
     queries, pair = query_and_pair(where, query, latent, rope_key, latent_gain, key_up, value_up)
@@ -190,8 +221,8 @@
         shifted(hidden_of(right_a, right_b, w_gate, w_up), "x", 1),
     ]
     shape = jax.ShapeDtypeStruct((experts, CAP, width), BF)
-    down = [w_down, down_right] + down_far + [down_left]
-    result = call(down_kernel, shape, hidden + down)
+    block = pl.BlockSpec((experts // 4, CAP, width), lambda i: (i, 0, 0))
+    result = call(down_kernel, shape, hidden + [down], place=False, grid=(4,), out_specs=block)
     returned = lax.all_to_all(result, EP, split_axis=0, concat_axis=0, tiled=True)
     mixed = project(where, parts, out_proj, latent.shape[0])
     shape = jax.ShapeDtypeStruct((rows, width), BF)

time: 197 us -> 200 us (1.015)
  the two profiles are of different devices: /device:TPU:32 before, /device:TPU:34 now
where the time goes in v7:
time: 200 us
  waiting for transfers between devices  103 us (52%)
  starting transfers between devices  66 us (33%)
  Pallas kernels  26.6 us (13%)
  local copies, waits for them, and re-layouts  2.89 us (1%)
    ppermute x33, waiting for transfers between devices, shifted(): return lax.ppermute(value, axis, [(i, (i + amount) % n) for i in range(n)])  77.4 us
    ppermute x33, starting transfers between devices, shifted(): return lax.ppermute(value, axis, [(i, (i + amount) % n) for i in range(n)])  48.1 us
    pallas_call x14, Pallas kernels, call(): pl.pallas_call(kernel, in_specs=specs, out_specs=more.pop('out_specs', ou...  26.6 us
    all_to_all x1, waiting for transfers between devices, both_halves(): lax.all_to_all(outgoing, EP, split_axis=0, concat_axis=0, tiled=True)  25.7 us
    all_to_all x1, starting transfers between devices, both_halves(): lax.all_to_all(outgoing, EP, split_axis=0, concat_axis=0, tiled=True)  12 us
    all_to_all x1, starting transfers between devices, both_halves(): lax.all_to_all(result, EP, split_axis=0, concat_axis=0, tiled=True)  5.98 us
  transfers between devices with their start and end apart: 35, of which 20 were waited for; matrix products, arithmetic and copies ran while one was open for 2% of the time, Pallas kernels for 9%

profile of v7, /device:TPU:34, one launch (start us, length us, event | category | flops | bytes accessed | tf_op | source)
XLA Modules:
  0.0 199.9 jit_solution(527316200870077041)
XLA Ops:
  0.7 3.6 %shard_map.164 = (bf16[64,4,2048]{2,1,0:T(4,128)(2,1)}, bf16[256,128]{1,0:T(8,128)(2,1)S(1)}) custom-call(bf16[64,2048]{1,0:T(8,128)(2,1)} %tokens.1, f32[1,2048]{1,0:T(1,128)} %bitcast.24, s32[2,64]{1,0:T(2,128)} %bitcast.26, f32[1,64]{1,0:T(1,128)} %bitcast.28, f32[2,64]{1,0:T(2,128)} %bitcast.27), custom_call_target="tpu_custom_call" | custom-call | tf_op jit(solution)/shard_map/pallas_call | solution.py:46
  4.2 12.0 %all-to-all-start = ((bf16[64,4,2048]{2,1,0:T(4,128)(2,1)}), bf16[64,4,2048]{2,1,0:T(4,128)(2,1)}, u32[]{:S(2)}, u32[]{:S(2)}) async-start(bf16[64,4,2048]{2,1,0:T(4,128)(2,1)} %get-tuple-element.28), calls=%async_computation | async-start | bytes 2097152 | tf_op jit(solution)/shard_map/all_to_all | solution.py:209
  16.2 1.6 collective-permute-start.30
  17.8 0.5 collective-permute-start.29
  18.3 25.7 %all-to-all-done = bf16[64,4,2048]{2,1,0:T(4,128)(2,1)} async-done(((bf16[64,4,2048]{2,1,0:T(4,128)(2,1)}), bf16[64,4,2048]{2,1,0:T(4,128)(2,1)}, u32[]{:S(2)}, u32[]{:S(2)}) %all-to-all-start) | async-done | bytes 1048608 | tf_op jit(solution)/shard_map/all_to_all | solution.py:209
  44.0 1.7 fusion
  45.7 0.6 collective-permute-start.24
  46.3 1.5 collective-permute-start.20
  47.8 1.3 collective-permute-start.27
  49.1 0.8 collective-permute-start.21
  49.8 10.7 %collective-permute-done.24.rows_b = bf16[32,4,2048]{2,1,0:T(4,128)(2,1)S(1)} collective-permute-done((bf16[32,4,2048]{2,1,0:T(4,128)(2,1)S(1)}, bf16[32,4,2048]{2,1,0:T(4,128)(2,1)S(1)}, u32[]{:S(2)}, u32[]{:S(2)}) %collective-permute-start.24) | collective-permute-done | bytes 524320 | tf_op jit(solution)/shard_map/ppermute | solution.py:63
  60.6 0.8 collective-permute-start.25
  61.4 0.5 collective-permute-done.20.rows_a
  61.8 0.8 collective-permute-start.23
  62.7 2.0 collective-permute-start.31
  64.6 1.1 slice.19
  65.7 6.1 %collective-permute-done.27.rows_a = bf16[32,4,2048]{2,1,0:T(4,128)(2,1)S(1)} collective-permute-done((bf16[32,4,2048]{2,1,0:T(4,128)(2,1)S(1)}, bf16[32,4,2048]{2,1,0:T(4,128)(2,1)S(1)}, u32[]{:S(2)}, u32[]{:S(2)}) %collective-permute-start.27) | collective-permute-done | bytes 524320 | tf_op jit(solution)/shard_map/ppermute | solution.py:63
  71.8 0.8 collective-permute-start.32
  72.6 1.4 shard_map.168
  74.0 1.3 collective-permute-start.28
  75.3 1.4 shard_map.166
  76.7 6.4 %collective-permute-done.25.rows_b = bf16[32,4,2048]{2,1,0:T(4,128)(2,1)S(1)} collective-permute-done((bf16[32,4,2048]{2,1,0:T(4,128)(2,1)S(1)}, bf16[32,4,2048]{2,1,0:T(4,128)(2,1)S(1)}, u32[]{:S(2)}, u32[]{:S(2)}) %collective-permute-start.25) | collective-permute-done | bytes 524320 | tf_op jit(solution)/shard_map/ppermute | solution.py:63
  83.0 0.8 collective-permute-start.22
  83.8 0.5 collective-permute-done.23.rows_a
  84.3 1.4 shard_map.167
  85.7 2.2 %collective-permute-start.26 = (bf16[256,256]{1,0:T(8,128)(2,1)S(1)}, bf16[256,256]{1,0:T(8,128)(2,1)S(1)}, u32[]{:S(2)}, u32[]{:S(2)}) collective-permute-start(bf16[256,256]{1,0:T(8,128)(2,1)S(1)} %shard_map.167), channel_id=1, source_target_pairs={{0,2},{1,3},{2,0},{3,1},{4,6},{5,7},{6,4},{7,5},{8,10},{9,11},{10,... | collective-permute-start | bytes 393224 | tf_op jit(solution)/shard_map/ppermute | solution.py:63
  87.8 7.7 %collective-permute-done.31.w2a = bf16[128,2048]{1,0:T(8,128)(2,1)S(1)} collective-permute-done((bf16[128,2048]{1,0:T(8,128)(2,1)S(1)}, bf16[128,2048]{1,0:T(8,128)(2,1)S(1)}, u32[]{:S(2)}, u32[]{:S(2)}) %collective-permute-start.31) | collective-permute-done | bytes 524320 | tf_op jit(solution)/shard_map/ppermute | solution.py:63
  95.5 1.5 shard_map.169.weights
  97.0 1.4 shard_map.165.h0
  98.4 1.7 collective-permute-done.26.h2
  100.1 4.2 %shard_map.170 = bf16[64,4,2048]{2,1,0:T(4,128)(2,1)} custom-call(bf16[256,256]{1,0:T(8,128)(2,1)S(1)} %shard_map.165.h0, bf16[256,256]{1,0:T(8,128)(2,1)S(1)} %collective-permute-done.22.h1, bf16[256,256]{1,0:T(8,128)(2,1)S(1)} %collective-permute-done.26.h2, bf16[256,256]{1,0:T(8,128)(2,1)S(1)} %collective-permute-done.28.h3, ...), custom_call_target="tpu_custom_call" | custom-call | tf_op jit(solution)/shard_map/pallas_call | solution.py:46
  104.3 6.0 %all-to-all-start.1 = ((bf16[64,4,2048]{2,1,0:T(4,128)(2,1)}), bf16[64,4,2048]{2,1,0:T(4,128)(2,1)S(1)}, u32[]{:S(2)}, u32[]{:S(2)}) async-start(bf16[64,4,2048]{2,1,0:T(4,128)(2,1)} %shard_map.170), calls=%async_computation.1 | async-start | bytes 2097152 | tf_op jit(solution)/shard_map/all_to_all | solution.py:226
  110.6 0.9 shard_map.158.l0
  111.4 3.4 %collective-permute-start.2 = (bf16[32,544]{1,0:T(8,128)(2,1)S(1)}, bf16[32,544]{1,0:T(8,128)(2,1)S(1)}, u32[]{:S(2)}, u32[]{:S(2)}) collective-permute-start(bf16[32,544]{1,0:T(8,128)(2,1)S(1)} %shard_map.158.l0), channel_id=1, source_target_pairs={{0,3},{1,0},{2,1},{3,2},{4,7},{5,4},{6,5},{7,6},{8,11},{9,8},{10,9... | collective-permute-start | bytes 104456 | tf_op jit(solution)/shard_map/ppermute | solution.py:63
  114.8 1.7 collective-permute-start
  116.8 3.6 %collective-permute-done.1.l2 = bf16[32,544]{1,0:T(8,128)(2,1)S(1)} collective-permute-done((bf16[32,544]{1,0:T(8,128)(2,1)S(1)}, bf16[32,544]{1,0:T(8,128)(2,1)S(1)}, u32[]{:S(2)}, u32[]{:S(2)}) %collective-permute-start.1) | collective-permute-done | bytes 34848 | tf_op jit(solution)/shard_map/ppermute | solution.py:63
  120.4 1.4 shard_map.159
  121.8 2.5 %collective-permute-start.3 = (bf16[256,128]{1,0:T(8,128)(2,1)S(1)}, bf16[256,128]{1,0:T(8,128)(2,1)S(1)}, u32[]{:S(2)}, u32[]{:S(2)}) collective-permute-start(bf16[256,128]{1,0:T(8,128)(2,1)S(1)} %get-tuple-element.17), channel_id=1, source_target_pairs={{0,64},{64,128},{128,192},{192,0},{1,65},{65,129},{129,193},{193,1... | collective-permute-start | bytes 196616 | tf_op jit(solution)/shard_map/ppermute | solution.py:63
  124.3 2.9 %collective-permute-start.4 = (bf16[256,128]{1,0:T(8,128)(2,1)S(1)}, bf16[256,128]{1,0:T(8,128)(2,1)S(1)}, u32[]{:S(2)}, u32[]{:S(2)}) collective-permute-start(bf16[256,128]{1,0:T(8,128)(2,1)S(1)} %get-tuple-element.18), channel_id=1, source_target_pairs={{0,128},{64,192},{128,0},{192,64},{1,129},{65,193},{129,1},{193,65... | collective-permute-start | bytes 196616 | tf_op jit(solution)/shard_map/ppermute | solution.py:63
  127.2 3.5 %collective-permute-start.5 = (bf16[256,128]{1,0:T(8,128)(2,1)S(1)}, bf16[256,128]{1,0:T(8,128)(2,1)S(1)}, u32[]{:S(2)}, u32[]{:S(2)}) collective-permute-start(bf16[256,128]{1,0:T(8,128)(2,1)S(1)} %get-tuple-element.19), channel_id=1, source_target_pairs={{0,192},{64,0},{128,64},{192,128},{1,193},{65,1},{129,65},{193,129... | collective-permute-start | bytes 196616 | tf_op jit(solution)/shard_map/ppermute | solution.py:63
  130.6 8.3 %collective-permute-done.3.b1.q1 = bf16[256,128]{1,0:T(8,128)(2,1)S(1)} collective-permute-done((bf16[256,128]{1,0:T(8,128)(2,1)S(1)}, bf16[256,128]{1,0:T(8,128)(2,1)S(1)}, u32[]{:S(2)}, u32[]{:S(2)}) %collective-permute-start.3) | collective-permute-done | bytes 65568 | tf_op jit(solution)/shard_map/ppermute | solution.py:63
  138.9 3.8 %collective-permute-done.4.b2.q2 = bf16[256,128]{1,0:T(8,128)(2,1)S(1)} collective-permute-done((bf16[256,128]{1,0:T(8,128)(2,1)S(1)}, bf16[256,128]{1,0:T(8,128)(2,1)S(1)}, u32[]{:S(2)}, u32[]{:S(2)}) %collective-permute-start.4) | collective-permute-done | bytes 65568 | tf_op jit(solution)/shard_map/ppermute | solution.py:63
  142.8 2.5 %collective-permute-start.6 = (bf16[4,160,128]{2,1,0:T(8,128)(2,1)S(1)}, bf16[4,160,128]{2,1,0:T(8,128)(2,1)S(1)}, u32[]{:S(2)}, u32[]{:S(2)}) collective-permute-start(bf16[4,160,128]{2,1,0:T(8,128)(2,1)S(1)} %shard_map.160), channel_id=1, source_target_pairs={{0,32},{32,0},{1,33},{33,1},{2,34},{34,2},{3,35},{35,3},{4,36},{36... | collective-permute-start | bytes 491528 | tf_op jit(solution)/shard_map/ppermute | solution.py:63
  145.3 3.3 %collective-permute-done.6 = bf16[4,160,128]{2,1,0:T(8,128)(2,1)S(1)} collective-permute-done((bf16[4,160,128]{2,1,0:T(8,128)(2,1)S(1)}, bf16[4,160,128]{2,1,0:T(8,128)(2,1)S(1)}, u32[]{:S(2)}, u32[]{:S(2)}) %collective-permute-start.6) | collective-permute-done | bytes 163872 | tf_op jit(solution)/shard_map/ppermute | solution.py:63
  148.7 2.8 %collective-permute-start.9 = (bf16[4,160,256]{2,1,0:T(8,128)(2,1)S(1)}, bf16[4,160,256]{2,1,0:T(8,128)(2,1)S(1)}, u32[]{:S(2)}, u32[]{:S(2)}) collective-permute-start(bf16[4,160,256]{2,1,0:T(8,128)(2,1)S(1)} %pad_maximum_fusion.refs_0_), channel_id=1, source_target_pairs={{0,24},{8,0},{16,8},{24,16},{1,25},{9,1},{17,9},{25,17},{2,26},{10... | collective-permute-start | bytes 983048 | tf_op jit(solution)/shard_map/ppermute | solution.py:63
  151.5 0.8 collective-permute-start.8
  152.3 0.9 collective-permute-start.7
  153.2 10.2 %collective-permute-done.9.refs_3_ = bf16[4,160,256]{2,1,0:T(8,128)(2,1)S(1)} collective-permute-done((bf16[4,160,256]{2,1,0:T(8,128)(2,1)S(1)}, bf16[4,160,256]{2,1,0:T(8,128)(2,1)S(1)}, u32[]{:S(2)}, u32[]{:S(2)}) %collective-permute-start.9) | collective-permute-done | bytes 327712 | tf_op jit(solution)/shard_map/ppermute | solution.py:63
  163.3 0.2 collective-permute-done.8.refs_2_
  163.5 0.3 collective-permute-start.12
  163.8 3.2 %collective-permute-done.7.refs_1_ = bf16[4,160,256]{2,1,0:T(8,128)(2,1)S(1)} collective-permute-done((bf16[4,160,256]{2,1,0:T(8,128)(2,1)S(1)}, bf16[4,160,256]{2,1,0:T(8,128)(2,1)S(1)}, u32[]{:S(2)}, u32[]{:S(2)}) %collective-permute-start.7) | collective-permute-done | bytes 327712 | tf_op jit(solution)/shard_map/ppermute | solution.py:63
  167.0 1.6 collective-permute-done.11.refs_5_
  168.6 5.8 %shard_map.161 = (bf16[128,64]{1,0:T(8,128)(2,1)S(1)}, bf16[128,64]{1,0:T(8,128)(2,1)S(1)}, bf16[128,64]{1,0:T(8,128)(2,1)S(1)}, bf16[128,64]{1,0:T(8,128)(2,1)S(1)}) custom-call(s32[5]{0:T(128)S(1)} %stack.23.where, bf16[256,128]{1,0:T(8,128)(2,1)S(1)} %get-tuple-element.16.b0.q0, bf16[256,128]{1,0:T(8,128)(2,1)S(1)} %collective-permute-done.3.b1.q1, ...), custom_call_target="tpu_custom_call" | custom-call | tf_op jit(solution)/shard_map/pallas_call | solution.py:46
  174.5 3.1 %collective-permute-start.14 = (bf16[128,64]{1,0:T(8,128)(2,1)S(1)}, bf16[128,64]{1,0:T(8,128)(2,1)S(1)}, u32[]{:S(2)}, u32[]{:S(2)}) collective-permute-start(bf16[128,64]{1,0:T(8,128)(2,1)S(1)} %get-tuple-element.21), channel_id=1, source_target_pairs={{0,192},{64,0},{128,64},{192,128},{1,193},{65,1},{129,65},{193,129... | collective-permute-start | bytes 49160 | tf_op jit(solution)/shard_map/ppermute | solution.py:63
  177.5 3.4 %collective-permute-start.15 = (bf16[128,64]{1,0:T(8,128)(2,1)S(1)}, bf16[128,64]{1,0:T(8,128)(2,1)S(1)}, u32[]{:S(2)}, u32[]{:S(2)}) collective-permute-start(bf16[128,64]{1,0:T(8,128)(2,1)S(1)} %get-tuple-element.22), channel_id=1, source_target_pairs={{0,128},{64,192},{128,0},{192,64},{1,129},{65,193},{129,1},{193,65... | collective-permute-start | bytes 49160 | tf_op jit(solution)/shard_map/ppermute | solution.py:63
  180.9 4.4 %collective-permute-done.15.a2 = bf16[128,64]{1,0:T(8,128)(2,1)S(1)} collective-permute-done((bf16[128,64]{1,0:T(8,128)(2,1)S(1)}, bf16[128,64]{1,0:T(8,128)(2,1)S(1)}, u32[]{:S(2)}, u32[]{:S(2)}) %collective-permute-start.15) | collective-permute-done | bytes 16416 | tf_op jit(solution)/shard_map/ppermute | solution.py:63
  185.3 1.6 collective-permute-done.16.a3
  186.9 0.7 shard_map.162
  187.6 1.9 collective-permute-start.17
  189.5 3.6 %collective-permute-start.18 = (bf16[32,256]{1,0:T(8,128)(2,1)S(1)}, bf16[32,256]{1,0:T(8,128)(2,1)S(1)}, u32[]{:S(2)}, u32[]{:S(2)}) collective-permute-start(bf16[32,256]{1,0:T(8,128)(2,1)S(1)} %get-tuple-element.26), channel_id=1, source_target_pairs={{0,2},{1,3},{2,0},{3,1},{4,6},{5,7},{6,4},{7,5},{8,10},{9,11},{10,... | collective-permute-start | bytes 49160 | tf_op jit(solution)/shard_map/ppermute | solution.py:63
  193.1 1.7 collective-permute-done.18.a2
  194.8 2.0 %collective-permute-done.19.a3 = bf16[32,256]{1,0:T(8,128)(2,1)S(1)} collective-permute-done((bf16[32,256]{1,0:T(8,128)(2,1)S(1)}, bf16[32,256]{1,0:T(8,128)(2,1)S(1)}, u32[]{:S(2)}, u32[]{:S(2)}) %collective-permute-start.19) | collective-permute-done | bytes 16416 | tf_op jit(solution)/shard_map/ppermute | solution.py:63
  196.8 2.0 %shard_map.163 = bf16[32,2048]{1,0:T(8,128)(2,1)} custom-call(s32[5]{0:T(128)S(1)} %stack.23.where, bf16[32,256]{1,0:T(8,128)(2,1)S(1)} %get-tuple-element.24.a0, bf16[32,256]{1,0:T(8,128)(2,1)S(1)} %collective-permute-done.17.a1, bf16[32,256]{1,0:T(8,128)(2,1)S(1)} %collective-permute-done.18.a2, bf16[32,256]{1,0:T(8,128)(2,1)S(1)} %collective-permute-done.19.a3, ...), custom_call_target="tpu_custom_call" | custom-call | tf_op jit(solution)/shard_map/pallas_call | solution.py:46
  198.9 1.0 shard_map.171
  (39 shorter events, 0.6 us)
Async XLA Ops:
  0.6 72.0 %copy-start.1 = (bf16[1,2048,256]{2,1,0:T(8,128)(2,1)S(1)}, bf16[1,2048,256]{2,1,0:T(8,128)(2,1)}, u32[]{:S(2)}) copy-start(bf16[1,2048,256]{2,1,0:T(8,128)(2,1)} %param.28) | copy-start | bytes 3145732
  0.6 72.0 %copy-start = (bf16[1,2048,256]{2,1,0:T(8,128)(2,1)S(1)}, bf16[1,2048,256]{2,1,0:T(8,128)(2,1)}, u32[]{:S(2)}) copy-start(bf16[1,2048,256]{2,1,0:T(8,128)(2,1)} %param.27) | copy-start | bytes 3145732
  4.2 39.8 %all-to-all-start = ((bf16[64,4,2048]{2,1,0:T(4,128)(2,1)}), bf16[64,4,2048]{2,1,0:T(4,128)(2,1)}, u32[]{:S(2)}, u32[]{:S(2)}) async-start(bf16[64,4,2048]{2,1,0:T(4,128)(2,1)} %get-tuple-element.28), calls=%async_computation | async-start | bytes 2097152 | tf_op jit(solution)/shard_map/all_to_all | solution.py:209
  16.2 32.9 %collective-permute-start.30 = (bf16[256,2048]{1,0:T(8,128)(2,1)}, bf16[256,2048]{1,0:T(8,128)(2,1)S(1)}, u32[]{:S(2)}, u32[]{:S(2)}) collective-permute-start(bf16[256,2048]{1,0:T(8,128)(2,1)} %bitcast.21), channel_id=1, source_target_pairs={{0,1},{1,2},{2,3},{3,0},{4,5},{5,6},{6,7},{7,4},{8,9},{9,10},{10,1... | collective-permute-start | bytes 3145736 | tf_op jit(solution)/shard_map/ppermute | solution.py:63
  17.8 44.9 %collective-permute-start.29 = (bf16[256,2048]{1,0:T(8,128)(2,1)}, bf16[256,2048]{1,0:T(8,128)(2,1)}, u32[]{:S(2)}, u32[]{:S(2)}) collective-permute-start(bf16[256,2048]{1,0:T(8,128)(2,1)} %bitcast.22), channel_id=1, source_target_pairs={{0,3},{1,0},{2,1},{3,2},{4,7},{5,4},{6,5},{7,6},{8,11},{9,8},{10,9... | collective-permute-start | bytes 3145736 | tf_op jit(solution)/shard_map/ppermute | solution.py:63
  45.7 14.9 %collective-permute-start.24 = (bf16[32,4,2048]{2,1,0:T(4,128)(2,1)S(1)}, bf16[32,4,2048]{2,1,0:T(4,128)(2,1)S(1)}, u32[]{:S(2)}, u32[]{:S(2)}) collective-permute-start(bf16[32,4,2048]{2,1,0:T(4,128)(2,1)S(1)} %get-tuple-element.30.rows_b), channel_id=1, source_target_pairs={{0,3},{1,0},{2,1},{3,2},{4,7},{5,4},{6,5},{7,6},{8,11},{9,8},{10,9... | collective-permute-start | bytes 1572872 | tf_op jit(solution)/shard_map/ppermute | solution.py:63
  46.3 15.5 %collective-permute-start.20 = (bf16[32,4,2048]{2,1,0:T(4,128)(2,1)S(1)}, bf16[32,4,2048]{2,1,0:T(4,128)(2,1)S(1)}, u32[]{:S(2)}, u32[]{:S(2)}) collective-permute-start(bf16[32,4,2048]{2,1,0:T(4,128)(2,1)S(1)} %get-tuple-element.31.rows_a), channel_id=1, source_target_pairs={{0,1},{1,2},{2,3},{3,0},{4,5},{5,6},{6,7},{7,4},{8,9},{9,10},{10,1... | collective-permute-start | bytes 1572872 | tf_op jit(solution)/shard_map/ppermute | solution.py:63
  47.8 24.0 %collective-permute-start.27 = (bf16[32,4,2048]{2,1,0:T(4,128)(2,1)S(1)}, bf16[32,4,2048]{2,1,0:T(4,128)(2,1)S(1)}, u32[]{:S(2)}, u32[]{:S(2)}) collective-permute-start(bf16[32,4,2048]{2,1,0:T(4,128)(2,1)S(1)} %get-tuple-element.31.rows_a), channel_id=1, source_target_pairs={{0,3},{1,0},{2,1},{3,2},{4,7},{5,4},{6,5},{7,6},{8,11},{9,8},{10,9... | collective-permute-start | bytes 1572872 | tf_op jit(solution)/shard_map/ppermute | solution.py:63
  49.1 24.9 %collective-permute-start.21 = (bf16[32,4,2048]{2,1,0:T(4,128)(2,1)S(1)}, bf16[32,4,2048]{2,1,0:T(4,128)(2,1)S(1)}, u32[]{:S(2)}, u32[]{:S(2)}) collective-permute-start(bf16[32,4,2048]{2,1,0:T(4,128)(2,1)S(1)} %get-tuple-element.30.rows_b), channel_id=1, source_target_pairs={{0,1},{1,2},{2,3},{3,0},{4,5},{5,6},{6,7},{7,4},{8,9},{9,10},{10,1... | collective-permute-start | bytes 1572872 | tf_op jit(solution)/shard_map/ppermute | solution.py:63
  60.6 22.5 %collective-permute-start.25 = (bf16[32,4,2048]{2,1,0:T(4,128)(2,1)S(1)}, bf16[32,4,2048]{2,1,0:T(4,128)(2,1)S(1)}, u32[]{:S(2)}, u32[]{:S(2)}) collective-permute-start(bf16[32,4,2048]{2,1,0:T(4,128)(2,1)S(1)} %collective-permute-done.24.rows_b), channel_id=1, source_target_pairs={{0,3},{1,0},{2,1},{3,2},{4,7},{5,4},{6,5},{7,6},{8,11},{9,8},{10,9... | collective-permute-start | bytes 1572872 | tf_op jit(solution)/shard_map/ppermute | solution.py:63
  61.8 22.5 %collective-permute-start.23 = (bf16[32,4,2048]{2,1,0:T(4,128)(2,1)S(1)}, bf16[32,4,2048]{2,1,0:T(4,128)(2,1)S(1)}, u32[]{:S(2)}, u32[]{:S(2)}) collective-permute-start(bf16[32,4,2048]{2,1,0:T(4,128)(2,1)S(1)} %collective-permute-done.20.rows_a), channel_id=1, source_target_pairs={{0,1},{1,2},{2,3},{3,0},{4,5},{5,6},{6,7},{7,4},{8,9},{9,10},{10,1... | collective-permute-start | bytes 1572872 | tf_op jit(solution)/shard_map/ppermute | solution.py:63
  62.7 32.9 %collective-permute-start.31 = (bf16[128,2048]{1,0:T(8,128)(2,1)S(1)}, bf16[128,2048]{1,0:T(8,128)(2,1)S(1)}, u32[]{:S(2)}, u32[]{:S(2)}) collective-permute-start(bf16[128,2048]{1,0:T(8,128)(2,1)S(1)} %slice.18), channel_id=1, source_target_pairs={{0,1},{1,2},{2,3},{3,0},{4,5},{5,6},{6,7},{7,4},{8,9},{9,10},{10,1... | collective-permute-start | bytes 1572872 | tf_op jit(solution)/shard_map/ppermute | solution.py:63
  71.8 23.7 %collective-permute-start.32 = (bf16[128,2048]{1,0:T(8,128)(2,1)S(1)}, bf16[128,2048]{1,0:T(8,128)(2,1)S(1)}, u32[]{:S(2)}, u32[]{:S(2)}) collective-permute-start(bf16[128,2048]{1,0:T(8,128)(2,1)S(1)} %slice.19), channel_id=1, source_target_pairs={{0,3},{1,0},{2,1},{3,2},{4,7},{5,4},{6,5},{7,6},{8,11},{9,8},{10,9... | collective-permute-start | bytes 1572872 | tf_op jit(solution)/shard_map/ppermute | solution.py:63
  72.6 22.9 %copy-start.3 = (bf16[1,256,2048]{2,1,0:T(8,128)(2,1)S(1)}, bf16[1,256,2048]{2,1,0:T(8,128)(2,1)}, u32[]{:S(2)}) copy-start(bf16[1,256,2048]{2,1,0:T(8,128)(2,1)} %param.29) | copy-start | bytes 3145732
  74.0 24.4 %collective-permute-start.28 = (bf16[256,256]{1,0:T(8,128)(2,1)S(1)}, bf16[256,256]{1,0:T(8,128)(2,1)S(1)}, u32[]{:S(2)}, u32[]{:S(2)}) collective-permute-start(bf16[256,256]{1,0:T(8,128)(2,1)S(1)} %shard_map.168), channel_id=1, source_target_pairs={{0,1},{1,2},{2,3},{3,0},{4,5},{5,6},{6,7},{7,4},{8,9},{9,10},{10,1... | collective-permute-start | bytes 393224 | tf_op jit(solution)/shard_map/ppermute | solution.py:63
  83.0 15.4 %collective-permute-start.22 = (bf16[256,256]{1,0:T(8,128)(2,1)S(1)}, bf16[256,256]{1,0:T(8,128)(2,1)S(1)}, u32[]{:S(2)}, u32[]{:S(2)}) collective-permute-start(bf16[256,256]{1,0:T(8,128)(2,1)S(1)} %shard_map.166), channel_id=1, source_target_pairs={{0,3},{1,0},{2,1},{3,2},{4,7},{5,4},{6,5},{7,6},{8,11},{9,8},{10,9... | collective-permute-start | bytes 393224 | tf_op jit(solution)/shard_map/ppermute | solution.py:63
  85.7 14.4 %collective-permute-start.26 = (bf16[256,256]{1,0:T(8,128)(2,1)S(1)}, bf16[256,256]{1,0:T(8,128)(2,1)S(1)}, u32[]{:S(2)}, u32[]{:S(2)}) collective-permute-start(bf16[256,256]{1,0:T(8,128)(2,1)S(1)} %shard_map.167), channel_id=1, source_target_pairs={{0,2},{1,3},{2,0},{3,1},{4,6},{5,7},{6,4},{7,5},{8,10},{9,11},{10,... | collective-permute-start | bytes 393224 | tf_op jit(solution)/shard_map/ppermute | solution.py:63
  104.3 94.6 %all-to-all-start.1 = ((bf16[64,4,2048]{2,1,0:T(4,128)(2,1)}), bf16[64,4,2048]{2,1,0:T(4,128)(2,1)S(1)}, u32[]{:S(2)}, u32[]{:S(2)}) async-start(bf16[64,4,2048]{2,1,0:T(4,128)(2,1)} %shard_map.170), calls=%async_computation.1 | async-start | bytes 2097152 | tf_op jit(solution)/shard_map/all_to_all | solution.py:226
  111.4 5.3 %collective-permute-start.2 = (bf16[32,544]{1,0:T(8,128)(2,1)S(1)}, bf16[32,544]{1,0:T(8,128)(2,1)S(1)}, u32[]{:S(2)}, u32[]{:S(2)}) collective-permute-start(bf16[32,544]{1,0:T(8,128)(2,1)S(1)} %shard_map.158.l0), channel_id=1, source_target_pairs={{0,3},{1,0},{2,1},{3,2},{4,7},{5,4},{6,5},{7,6},{8,11},{9,8},{10,9... | collective-permute-start | bytes 104456 | tf_op jit(solution)/shard_map/ppermute | solution.py:63
  114.8 5.5 %collective-permute-start.1 = (bf16[32,544]{1,0:T(8,128)(2,1)S(1)}, bf16[32,544]{1,0:T(8,128)(2,1)S(1)}, u32[]{:S(2)}, u32[]{:S(2)}) collective-permute-start(bf16[32,544]{1,0:T(8,128)(2,1)S(1)} %shard_map.158.l0), channel_id=1, source_target_pairs={{0,2},{1,3},{2,0},{3,1},{4,6},{5,7},{6,4},{7,5},{8,10},{9,11},{10,... | collective-permute-start | bytes 104456 | tf_op jit(solution)/shard_map/ppermute | solution.py:63
  114.8 5.5 %collective-permute-start = (bf16[32,544]{1,0:T(8,128)(2,1)S(1)}, bf16[32,544]{1,0:T(8,128)(2,1)S(1)}, u32[]{:S(2)}, u32[]{:S(2)}) collective-permute-start(bf16[32,544]{1,0:T(8,128)(2,1)S(1)} %shard_map.158.l0), channel_id=1, source_target_pairs={{0,1},{1,2},{2,3},{3,0},{4,5},{5,6},{6,7},{7,4},{8,9},{9,10},{10,1... | collective-permute-start | bytes 104456 | tf_op jit(solution)/shard_map/ppermute | solution.py:63
  116.8 80.0 %copy-start.2 = (bf16[1024,2048]{1,0:T(8,128)(2,1)S(1)}, bf16[1024,2048]{1,0:T(8,128)(2,1)}, u32[]{:S(2)}) copy-start(bf16[1024,2048]{1,0:T(8,128)(2,1)} %out_proj.1) | copy-start | bytes 12582916
  121.8 17.2 %collective-permute-start.3 = (bf16[256,128]{1,0:T(8,128)(2,1)S(1)}, bf16[256,128]{1,0:T(8,128)(2,1)S(1)}, u32[]{:S(2)}, u32[]{:S(2)}) collective-permute-start(bf16[256,128]{1,0:T(8,128)(2,1)S(1)} %get-tuple-element.17), channel_id=1, source_target_pairs={{0,64},{64,128},{128,192},{192,0},{1,65},{65,129},{129,193},{193,1... | collective-permute-start | bytes 196616 | tf_op jit(solution)/shard_map/ppermute | solution.py:63
  124.3 18.5 %collective-permute-start.4 = (bf16[256,128]{1,0:T(8,128)(2,1)S(1)}, bf16[256,128]{1,0:T(8,128)(2,1)S(1)}, u32[]{:S(2)}, u32[]{:S(2)}) collective-permute-start(bf16[256,128]{1,0:T(8,128)(2,1)S(1)} %get-tuple-element.18), channel_id=1, source_target_pairs={{0,128},{64,192},{128,0},{192,64},{1,129},{65,193},{129,1},{193,65... | collective-permute-start | bytes 196616 | tf_op jit(solution)/shard_map/ppermute | solution.py:63
  127.2 15.6 %collective-permute-start.5 = (bf16[256,128]{1,0:T(8,128)(2,1)S(1)}, bf16[256,128]{1,0:T(8,128)(2,1)S(1)}, u32[]{:S(2)}, u32[]{:S(2)}) collective-permute-start(bf16[256,128]{1,0:T(8,128)(2,1)S(1)} %get-tuple-element.19), channel_id=1, source_target_pairs={{0,192},{64,0},{128,64},{192,128},{1,193},{65,1},{129,65},{193,129... | collective-permute-start | bytes 196616 | tf_op jit(solution)/shard_map/ppermute | solution.py:63
  142.8 5.8 %collective-permute-start.6 = (bf16[4,160,128]{2,1,0:T(8,128)(2,1)S(1)}, bf16[4,160,128]{2,1,0:T(8,128)(2,1)S(1)}, u32[]{:S(2)}, u32[]{:S(2)}) collective-permute-start(bf16[4,160,128]{2,1,0:T(8,128)(2,1)S(1)} %shard_map.160), channel_id=1, source_target_pairs={{0,32},{32,0},{1,33},{33,1},{2,34},{34,2},{3,35},{35,3},{4,36},{36... | collective-permute-start | bytes 491528 | tf_op jit(solution)/shard_map/ppermute | solution.py:63
  148.7 14.7 %collective-permute-start.9 = (bf16[4,160,256]{2,1,0:T(8,128)(2,1)S(1)}, bf16[4,160,256]{2,1,0:T(8,128)(2,1)S(1)}, u32[]{:S(2)}, u32[]{:S(2)}) collective-permute-start(bf16[4,160,256]{2,1,0:T(8,128)(2,1)S(1)} %pad_maximum_fusion.refs_0_), channel_id=1, source_target_pairs={{0,24},{8,0},{16,8},{24,16},{1,25},{9,1},{17,9},{25,17},{2,26},{10... | collective-permute-start | bytes 983048 | tf_op jit(solution)/shard_map/ppermute | solution.py:63
  151.5 12.1 %collective-permute-start.8 = (bf16[4,160,256]{2,1,0:T(8,128)(2,1)S(1)}, bf16[4,160,256]{2,1,0:T(8,128)(2,1)S(1)}, u32[]{:S(2)}, u32[]{:S(2)}) collective-permute-start(bf16[4,160,256]{2,1,0:T(8,128)(2,1)S(1)} %pad_maximum_fusion.refs_0_), channel_id=1, source_target_pairs={{0,16},{8,24},{16,0},{24,8},{1,17},{9,25},{17,1},{25,9},{2,18},{10... | collective-permute-start | bytes 983048 | tf_op jit(solution)/shard_map/ppermute | solution.py:63
  152.3 14.7 %collective-permute-start.7 = (bf16[4,160,256]{2,1,0:T(8,128)(2,1)S(1)}, bf16[4,160,256]{2,1,0:T(8,128)(2,1)S(1)}, u32[]{:S(2)}, u32[]{:S(2)}) collective-permute-start(bf16[4,160,256]{2,1,0:T(8,128)(2,1)S(1)} %pad_maximum_fusion.refs_0_), channel_id=1, source_target_pairs={{0,8},{8,16},{16,24},{24,0},{1,9},{9,17},{17,25},{25,1},{2,10},{10... | collective-permute-start | bytes 983048 | tf_op jit(solution)/shard_map/ppermute | solution.py:63
  153.2 13.8 %collective-permute-start.10 = (bf16[4,160,256]{2,1,0:T(8,128)(2,1)S(1)}, bf16[4,160,256]{2,1,0:T(8,128)(2,1)S(1)}, u32[]{:S(2)}, u32[]{:S(2)}) collective-permute-start(bf16[4,160,256]{2,1,0:T(8,128)(2,1)S(1)} %pad_maximum_fusion.refs_0_), channel_id=1, source_target_pairs={{0,4},{4,0},{1,5},{5,1},{2,6},{6,2},{3,7},{7,3},{8,12},{12,8},{9,1... | collective-permute-start | bytes 983048 | tf_op jit(solution)/shard_map/ppermute | solution.py:63
  163.3 3.7 %collective-permute-start.13 = (bf16[4,160,256]{2,1,0:T(8,128)(2,1)S(1)}, bf16[4,160,256]{2,1,0:T(8,128)(2,1)S(1)}, u32[]{:S(2)}, u32[]{:S(2)}) collective-permute-start(bf16[4,160,256]{2,1,0:T(8,128)(2,1)S(1)} %collective-permute-done.9.refs_3_), channel_id=1, source_target_pairs={{0,4},{4,0},{1,5},{5,1},{2,6},{6,2},{3,7},{7,3},{8,12},{12,8},{9,1... | collective-permute-start | bytes 983048 | tf_op jit(solution)/shard_map/ppermute | solution.py:63
  163.5 3.5 %collective-permute-start.12 = (bf16[4,160,256]{2,1,0:T(8,128)(2,1)S(1)}, bf16[4,160,256]{2,1,0:T(8,128)(2,1)S(1)}, u32[]{:S(2)}, u32[]{:S(2)}) collective-permute-start(bf16[4,160,256]{2,1,0:T(8,128)(2,1)S(1)} %collective-permute-done.8.refs_2_), channel_id=1, source_target_pairs={{0,4},{4,0},{1,5},{5,1},{2,6},{6,2},{3,7},{7,3},{8,12},{12,8},{9,1... | collective-permute-start | bytes 983048 | tf_op jit(solution)/shard_map/ppermute | solution.py:63
  167.0 1.6 collective-permute-start.11
  174.5 6.5 %collective-permute-start.14 = (bf16[128,64]{1,0:T(8,128)(2,1)S(1)}, bf16[128,64]{1,0:T(8,128)(2,1)S(1)}, u32[]{:S(2)}, u32[]{:S(2)}) collective-permute-start(bf16[128,64]{1,0:T(8,128)(2,1)S(1)} %get-tuple-element.21), channel_id=1, source_target_pairs={{0,192},{64,0},{128,64},{192,128},{1,193},{65,1},{129,65},{193,129... | collective-permute-start | bytes 49160 | tf_op jit(solution)/shard_map/ppermute | solution.py:63
  177.5 7.8 %collective-permute-start.15 = (bf16[128,64]{1,0:T(8,128)(2,1)S(1)}, bf16[128,64]{1,0:T(8,128)(2,1)S(1)}, u32[]{:S(2)}, u32[]{:S(2)}) collective-permute-start(bf16[128,64]{1,0:T(8,128)(2,1)S(1)} %get-tuple-element.22), channel_id=1, source_target_pairs={{0,128},{64,192},{128,0},{192,64},{1,129},{65,193},{129,1},{193,65... | collective-permute-start | bytes 49160 | tf_op jit(solution)/shard_map/ppermute | solution.py:63
  180.9 6.0 %collective-permute-start.16 = (bf16[128,64]{1,0:T(8,128)(2,1)S(1)}, bf16[128,64]{1,0:T(8,128)(2,1)S(1)}, u32[]{:S(2)}, u32[]{:S(2)}) collective-permute-start(bf16[128,64]{1,0:T(8,128)(2,1)S(1)} %get-tuple-element.23), channel_id=1, source_target_pairs={{0,64},{64,128},{128,192},{192,0},{1,65},{65,129},{129,193},{193,1... | collective-permute-start | bytes 49160 | tf_op jit(solution)/shard_map/ppermute | solution.py:63
  187.6 5.5 %collective-permute-start.17 = (bf16[32,256]{1,0:T(8,128)(2,1)S(1)}, bf16[32,256]{1,0:T(8,128)(2,1)S(1)}, u32[]{:S(2)}, u32[]{:S(2)}) collective-permute-start(bf16[32,256]{1,0:T(8,128)(2,1)S(1)} %get-tuple-element.25), channel_id=1, source_target_pairs={{0,1},{1,2},{2,3},{3,0},{4,5},{5,6},{6,7},{7,4},{8,9},{9,10},{10,1... | collective-permute-start | bytes 49160 | tf_op jit(solution)/shard_map/ppermute | solution.py:63
  189.5 5.3 %collective-permute-start.18 = (bf16[32,256]{1,0:T(8,128)(2,1)S(1)}, bf16[32,256]{1,0:T(8,128)(2,1)S(1)}, u32[]{:S(2)}, u32[]{:S(2)}) collective-permute-start(bf16[32,256]{1,0:T(8,128)(2,1)S(1)} %get-tuple-element.26), channel_id=1, source_target_pairs={{0,2},{1,3},{2,0},{3,1},{4,6},{5,7},{6,4},{7,5},{8,10},{9,11},{10,... | collective-permute-start | bytes 49160 | tf_op jit(solution)/shard_map/ppermute | solution.py:63
  193.1 3.7 %collective-permute-start.19 = (bf16[32,256]{1,0:T(8,128)(2,1)S(1)}, bf16[32,256]{1,0:T(8,128)(2,1)S(1)}, u32[]{:S(2)}, u32[]{:S(2)}) collective-permute-start(bf16[32,256]{1,0:T(8,128)(2,1)S(1)} %get-tuple-element.27), channel_id=1, source_target_pairs={{0,3},{1,0},{2,1},{3,2},{4,7},{5,4},{6,5},{7,6},{8,11},{9,8},{10,9... | collective-permute-start | bytes 49160 | tf_op jit(solution)/shard_map/ppermute | solution.py:63

commit v8 on v6

--- a/solution.py
+++ b/solution.py
@@ -1,3 +1,5 @@
+import functools
+
 import jax
 import jax.numpy as jnp
 from jax import lax
@@ -73,11 +75,21 @@
     return widened * lax.rsqrt(jnp.mean(widened * widened, axis=-1, keepdims=True) + epsilon) * gain
 
 
-def dispatch_kernel(tokens, gain, routes, group_prob, expert_prob, outgoing, shares_out):
+def over_columns(width, span, work):
+    def step(i, _):
+        work(pl.ds(pl.multiple_of(i * span, span), span))
+        return 0
+
+    lax.fori_loop(0, width // span, step, 0)
+
+
+def dispatch_kernel(
+    tokens, gain, routes, group_prob, expert_prob, outgoing, shares_out, normed_s
+):
     rows = tokens.shape[0]
     experts, cap, width = outgoing.shape
     slots = experts * cap
-    normed = rms_scale(tokens[...], gain[...]).astype(BF)
+    normed_s[...] = rms_scale(tokens[...], gain[...]).astype(BF)
     slot = lax.broadcasted_iota(jnp.int32, (slots, rows), 0)
     expert = slot // cap
     first = routes[0:1, :] == expert
@@ -88,7 +100,13 @@
     )
     prior = mm(named, before.astype(BF))
     mine = (first | second) & (prior == (slot % cap).astype(F32))
-    outgoing[...] = mm(mine.astype(BF), normed).reshape(experts, cap, width).astype(BF)
+    chosen = mine.astype(BF)
+
+    def send(cols):
+        part = mm(chosen, normed_s[:, cols]).astype(BF)
+        outgoing[:, :, cols] = part.reshape(experts, cap, part.shape[1])
+
+    over_columns(width, 512, send)
     probs = expert_prob[...]
     shares = group_prob[...] * probs / jnp.sum(probs, axis=0, keepdims=True)
     weights = jnp.where(first, shares[0:1, :], shares[1:2, :])
@@ -108,6 +126,8 @@
         ),
         [tokens, gain[None, :], routes.T, group_prob[None, :], expert_prob.T],
         unplaced=range(5),
+        place=False,
+        scratch=[pltpu.VMEM((rows, width), BF)],
     )
 
 
@@ -137,9 +157,15 @@
 
 def down_kernel(h0, h1, h2, h3, w0, w1, w2a, w2b, w3, out):
     half = w2a.shape[0]
-    total = mm(h0[...], w0[...]) + mm(h1[...], w1[...]) + mm(h3[...], w3[...])
-    total = total + mm(h2[:, :half], w2a[...]) + mm(h2[:, half:], w2b[...])
-    out[...] = total.reshape(out.shape).astype(BF)
+    experts, cap, width = out.shape
+    own, right, far, left = h0[...], h1[...], h2[...], h3[...]
+
+    def lower(cols):
+        total = mm(own, w0[:, cols]) + mm(right, w1[:, cols]) + mm(left, w3[:, cols])
+        total = total + mm(far[:, :half], w2a[:, cols]) + mm(far[:, half:], w2b[:, cols])
+        out[:, :, cols] = total.astype(BF).reshape(experts, cap, total.shape[1])
+
+    over_columns(width, 512, lower)
 
 
 def combine_kernel(returned, shares, out):
@@ -191,7 +217,7 @@
     ]
     shape = jax.ShapeDtypeStruct((experts, CAP, width), BF)
     down = [w_down, down_right] + down_far + [down_left]
-    result = call(down_kernel, shape, hidden + down)
+    result = call(down_kernel, shape, hidden + down, place=False)
     returned = lax.all_to_all(result, EP, split_axis=0, concat_axis=0, tiled=True)
     mixed = project(where, parts, out_proj, latent.shape[0])
     shape = jax.ShapeDtypeStruct((rows, width), BF)
@@ -245,17 +271,25 @@
         out[j] = block[QK_DIM:, :]
 
 
-def attend_kernel(where, q0, q1, q2, q3, *refs):
-    blocks, outs, (q_s, top_s, acc_s) = refs[:8], refs[8:12], refs[12:]
+def attend_kernel(where, *refs, columns, first):
     zh, zl, y, c, x = (where[i] for i in range(5))
-    strip = q0.shape[1]
+    count = 2 * len(columns)
+    if first:
+        queries, blocks, (q_s, top_s, acc_s) = refs[:4], refs[4 : 4 + count], refs[4 + count :]
+        strip = queries[0].shape[1]
+        for j, q in enumerate(queries):
+            at = pl.multiple_of(lax.rem(zh - j + 4, 4) * strip, strip)
+            q_s[pl.ds(at, strip), :] = q[:QK_DIM, :].astype(F32).T.astype(BF)
+        top_s[...] = jnp.full(top_s.shape, masked_value, F32)
+        acc_s[...] = jnp.zeros(acc_s.shape, F32)
+    else:
+        q_s, top_in, acc_in = refs[:3]
+        blocks, outs, (top_s, acc_s) = refs[3 : 3 + count], refs[3 + count : -2], refs[-2:]
+        strip = outs[0].shape[0]
+        top_s[...] = top_in[...]
+        acc_s[...] = acc_in[...]
     span = blocks[0].shape[2]
     factor = QK_DIM ** (-0.5) * log2_e
-    for j, q in enumerate((q0, q1, q2, q3)):
-        at = pl.multiple_of(lax.rem(zh - j + 4, 4) * strip, strip)
-        q_s[pl.ds(at, strip), :] = q[:QK_DIM, :].astype(F32).T.astype(BF)
-    top_s[...] = jnp.full(top_s.shape, masked_value, F32)
-    acc_s[...] = jnp.zeros(acc_s.shape, F32)
 
     col = lax.broadcasted_iota(jnp.int32, (1, span), 1)
     col_zl = jnp.bitwise_xor(zl, col // strip)
@@ -284,9 +318,9 @@
         acc_s[rows, :] = total
 
     for m in range(2):
-        group = blocks[4 * m : 4 * m + 4]
+        group = blocks[m * len(columns) : (m + 1) * len(columns)]
         masks = []
-        for k in range(4):
+        for k in columns:
             key_y = lax.rem(y - k + 4, 4)
             key_at = (col_zl * 8 + key_y * 2 + jnp.bitwise_xor(c, m)) * strip + col_x
             masks.append(key_at <= query_at)
@@ -297,6 +331,8 @@
             advance(slice(g * strip, (g + 1) * strip), parts, masks)
             if g < 3:
                 advance(slice((g + 1) * strip, 4 * strip), parts, None)
+    if first:
+        return
     total = acc_s[...]
     acc_s[:, :V_DIM] = total[:, :V_DIM] / total[:, V_DIM:]
     for j, out in enumerate(outs):
@@ -363,17 +399,24 @@
 def attend(where, blocks, pair):
     strip = blocks[0].shape[1]
     column = [pair] + [shifted(pair, "y", k) for k in range(1, 4)]
-    column = column + [shifted(part, "c", 1) for part in column]
+    other = [shifted(part, "c", 1) for part in column]
+    early, late = (0, 1, 3), (2,)
+    state = call(
+        functools.partial(attend_kernel, columns=early, first=True),
+        [
+            jax.ShapeDtypeStruct((4 * strip, QK_DIM), BF),
+            jax.ShapeDtypeStruct((4 * strip, 128), F32),
+            jax.ShapeDtypeStruct((4 * strip, 128), F32),
+        ],
+        blocks + [column[k] for k in early] + [other[k] for k in early],
+        where,
+    )
     parts = call(
-        attend_kernel,
+        functools.partial(attend_kernel, columns=late, first=False),
         [jax.ShapeDtypeStruct((strip, V_DIM), BF)] * 4,
-        blocks + column,
+        list(state) + [column[k] for k in late] + [other[k] for k in late],
         where,
-        [
-            pltpu.VMEM((4 * strip, QK_DIM), BF),
-            pltpu.VMEM((4 * strip, 128), F32),
-            pltpu.VMEM((4 * strip, 128), F32),
-        ],
+        [pltpu.VMEM((4 * strip, 128), F32), pltpu.VMEM((4 * strip, 128), F32)],
     )
     return [parts[0]] + [shifted(parts[j], "zh", -j) for j in range(1, 4)]
 

time: 197 us -> 200 us (1.015)
  the two profiles are of different devices: /device:TPU:32 before, /device:TPU:56 now
where the time goes in v8:
time: 200 us; the launch traced here: 199 us
  waiting for transfers between devices  100 us (50%)
  starting transfers between devices  67.2 us (34%)
  Pallas kernels  27.8 us (14%)
  local copies, waits for them, and re-layouts  2.9 us (1%)
    ppermute x33, waiting for transfers between devices, shifted(): return lax.ppermute(value, axis, [(i, (i + amount) % n) for i in range(n)])  75.6 us
    ppermute x33, starting transfers between devices, shifted(): return lax.ppermute(value, axis, [(i, (i + amount) % n) for i in range(n)])  49 us
    pallas_call x14, Pallas kernels, call(): pl.pallas_call(kernel, in_specs=specs, out_specs=VMEM_SPEC if single else...  27.8 us
    all_to_all x1, waiting for transfers between devices, both_halves(): lax.all_to_all(outgoing, EP, split_axis=0, concat_axis=0, tiled=True)  24.5 us
    all_to_all x1, starting transfers between devices, both_halves(): lax.all_to_all(outgoing, EP, split_axis=0, concat_axis=0, tiled=True)  11.6 us
    all_to_all x1, starting transfers between devices, both_halves(): lax.all_to_all(result, EP, split_axis=0, concat_axis=0, tiled=True)  6.54 us
  transfers between devices with their start and end apart: 35, of which 22 were waited for; matrix products, arithmetic and copies ran while one was open for 2% of the time, Pallas kernels for 10%

profile of v8, /device:TPU:56, one launch (start us, length us, event | category | flops | bytes accessed | tf_op | source)
XLA Modules:
  0.0 199.3 jit_solution(8524424394541712989)
XLA Ops:
  0.7 3.2 %shard_map.165 = (bf16[64,4,2048]{2,1,0:T(4,128)(2,1)}, bf16[256,128]{1,0:T(8,128)(2,1)S(1)}) custom-call(bf16[64,2048]{1,0:T(8,128)(2,1)} %tokens.1, f32[1,2048]{1,0:T(1,128)} %bitcast.24, s32[2,64]{1,0:T(2,128)} %bitcast.26, f32[1,64]{1,0:T(1,128)} %bitcast.28, f32[2,64]{1,0:T(2,128)} %bitcast.27), custom_call_target="tpu_custom_call" | custom-call | tf_op jit(solution)/shard_map/pallas_call | solution.py:47
  3.8 11.6 %all-to-all-start = ((bf16[64,4,2048]{2,1,0:T(4,128)(2,1)}), bf16[64,4,2048]{2,1,0:T(4,128)(2,1)}, u32[]{:S(2)}, u32[]{:S(2)}) async-start(bf16[64,4,2048]{2,1,0:T(4,128)(2,1)} %get-tuple-element.34), calls=%async_computation | async-start | bytes 2097152 | tf_op jit(solution)/shard_map/all_to_all | solution.py:204
  15.4 1.6 collective-permute-start.30
  17.0 1.7 collective-permute-start.29
  18.7 24.5 %all-to-all-done = bf16[64,4,2048]{2,1,0:T(4,128)(2,1)} async-done(((bf16[64,4,2048]{2,1,0:T(4,128)(2,1)}), bf16[64,4,2048]{2,1,0:T(4,128)(2,1)}, u32[]{:S(2)}, u32[]{:S(2)}) %all-to-all-start) | async-done | bytes 1048608 | tf_op jit(solution)/shard_map/all_to_all | solution.py:204
  43.3 1.7 fusion
  45.0 1.6 collective-permute-start.20
  46.5 1.7 collective-permute-start.24
  48.3 0.3 collective-permute-start.21
  48.6 3.0 %collective-permute-start.27 = (bf16[32,4,2048]{2,1,0:T(4,128)(2,1)S(1)}, bf16[32,4,2048]{2,1,0:T(4,128)(2,1)S(1)}, u32[]{:S(2)}, u32[]{:S(2)}) collective-permute-start(bf16[32,4,2048]{2,1,0:T(4,128)(2,1)S(1)} %get-tuple-element.37.rows_a), channel_id=1, source_target_pairs={{0,3},{1,0},{2,1},{3,2},{4,7},{5,4},{6,5},{7,6},{8,11},{9,8},{10,9... | collective-permute-start | bytes 1572872 | tf_op jit(solution)/shard_map/ppermute | solution.py:63
  51.5 9.5 %collective-permute-done.20.rows_a = bf16[32,4,2048]{2,1,0:T(4,128)(2,1)S(1)} collective-permute-done((bf16[32,4,2048]{2,1,0:T(4,128)(2,1)S(1)}, bf16[32,4,2048]{2,1,0:T(4,128)(2,1)S(1)}, u32[]{:S(2)}, u32[]{:S(2)}) %collective-permute-start.20) | collective-permute-done | bytes 524320 | tf_op jit(solution)/shard_map/ppermute | solution.py:63
  61.3 3.0 %collective-permute-start.25 = (bf16[32,4,2048]{2,1,0:T(4,128)(2,1)S(1)}, bf16[32,4,2048]{2,1,0:T(4,128)(2,1)S(1)}, u32[]{:S(2)}, u32[]{:S(2)}) collective-permute-start(bf16[32,4,2048]{2,1,0:T(4,128)(2,1)S(1)} %collective-permute-done.24.rows_b), channel_id=1, source_target_pairs={{0,3},{1,0},{2,1},{3,2},{4,7},{5,4},{6,5},{7,6},{8,11},{9,8},{10,9... | collective-permute-start | bytes 1572872 | tf_op jit(solution)/shard_map/ppermute | solution.py:63
  64.4 1.1 slice.19
  65.5 6.8 %collective-permute-done.21.rows_b = bf16[32,4,2048]{2,1,0:T(4,128)(2,1)S(1)} collective-permute-done((bf16[32,4,2048]{2,1,0:T(4,128)(2,1)S(1)}, bf16[32,4,2048]{2,1,0:T(4,128)(2,1)S(1)}, u32[]{:S(2)}, u32[]{:S(2)}) %collective-permute-start.21) | collective-permute-done | bytes 524320 | tf_op jit(solution)/shard_map/ppermute | solution.py:63
  72.3 1.5 collective-permute-start.32
  73.8 1.4 shard_map.167
  75.2 0.9 collective-permute-start.22
  76.1 1.4 shard_map.169
  77.5 6.0 %collective-permute-done.23.rows_a = bf16[32,4,2048]{2,1,0:T(4,128)(2,1)S(1)} collective-permute-done((bf16[32,4,2048]{2,1,0:T(4,128)(2,1)S(1)}, bf16[32,4,2048]{2,1,0:T(4,128)(2,1)S(1)}, u32[]{:S(2)}, u32[]{:S(2)}) %collective-permute-start.23) | collective-permute-done | bytes 524320 | tf_op jit(solution)/shard_map/ppermute | solution.py:63
  83.8 1.4 shard_map.168
  85.2 3.0 %collective-permute-start.26 = (bf16[256,256]{1,0:T(8,128)(2,1)S(1)}, bf16[256,256]{1,0:T(8,128)(2,1)S(1)}, u32[]{:S(2)}, u32[]{:S(2)}) collective-permute-start(bf16[256,256]{1,0:T(8,128)(2,1)S(1)} %shard_map.168), channel_id=1, source_target_pairs={{0,2},{1,3},{2,0},{3,1},{4,6},{5,7},{6,4},{7,5},{8,10},{9,11},{10,... | collective-permute-start | bytes 393224 | tf_op jit(solution)/shard_map/ppermute | solution.py:63
  88.2 1.4 shard_map.166.h0
  89.5 5.2 %collective-permute-done.31.w2a = bf16[128,2048]{1,0:T(8,128)(2,1)S(1)} collective-permute-done((bf16[128,2048]{1,0:T(8,128)(2,1)S(1)}, bf16[128,2048]{1,0:T(8,128)(2,1)S(1)}, u32[]{:S(2)}, u32[]{:S(2)}) %collective-permute-start.31) | collective-permute-done | bytes 524320 | tf_op jit(solution)/shard_map/ppermute | solution.py:63
  95.0 2.6 %collective-permute-done.22.h1 = bf16[256,256]{1,0:T(8,128)(2,1)S(1)} collective-permute-done((bf16[256,256]{1,0:T(8,128)(2,1)S(1)}, bf16[256,256]{1,0:T(8,128)(2,1)S(1)}, u32[]{:S(2)}, u32[]{:S(2)}) %collective-permute-start.22) | collective-permute-done | bytes 131104 | tf_op jit(solution)/shard_map/ppermute | solution.py:63
  97.7 2.4 %collective-permute-done.26.h2 = bf16[256,256]{1,0:T(8,128)(2,1)S(1)} collective-permute-done((bf16[256,256]{1,0:T(8,128)(2,1)S(1)}, bf16[256,256]{1,0:T(8,128)(2,1)S(1)}, u32[]{:S(2)}, u32[]{:S(2)}) %collective-permute-start.26) | collective-permute-done | bytes 131104 | tf_op jit(solution)/shard_map/ppermute | solution.py:63
  100.1 4.3 %shard_map.170 = bf16[64,4,2048]{2,1,0:T(4,128)(2,1)} custom-call(bf16[256,256]{1,0:T(8,128)(2,1)S(1)} %shard_map.166.h0, bf16[256,256]{1,0:T(8,128)(2,1)S(1)} %collective-permute-done.22.h1, bf16[256,256]{1,0:T(8,128)(2,1)S(1)} %collective-permute-done.26.h2, bf16[256,256]{1,0:T(8,128)(2,1)S(1)} %collective-permute-done.28.h3, ...), custom_call_target="tpu_custom_call" | custom-call | tf_op jit(solution)/shard_map/pallas_call | solution.py:47
  104.4 6.5 %all-to-all-start.1 = ((bf16[64,4,2048]{2,1,0:T(4,128)(2,1)}), bf16[64,4,2048]{2,1,0:T(4,128)(2,1)S(1)}, u32[]{:S(2)}, u32[]{:S(2)}) async-start(bf16[64,4,2048]{2,1,0:T(4,128)(2,1)} %shard_map.170), calls=%async_computation.1 | async-start | bytes 2097152 | tf_op jit(solution)/shard_map/all_to_all | solution.py:221
  111.2 0.9 shard_map.158.l0
  112.1 1.2 collective-permute-start
  113.3 2.3 %collective-permute-start.1 = (bf16[32,544]{1,0:T(8,128)(2,1)S(1)}, bf16[32,544]{1,0:T(8,128)(2,1)S(1)}, u32[]{:S(2)}, u32[]{:S(2)}) collective-permute-start(bf16[32,544]{1,0:T(8,128)(2,1)S(1)} %shard_map.158.l0), channel_id=1, source_target_pairs={{0,2},{1,3},{2,0},{3,1},{4,6},{5,7},{6,4},{7,5},{8,10},{9,11},{10,... | collective-permute-start | bytes 104456 | tf_op jit(solution)/shard_map/ppermute | solution.py:63
  115.6 0.5 collective-permute-start.2
  116.3 1.2 collective-permute-done.l1
  117.5 1.3 collective-permute-done.1.l2
  118.8 0.8 collective-permute-done.2.l3
  119.6 1.4 shard_map.159
  121.0 2.5 %collective-permute-start.3 = (bf16[256,128]{1,0:T(8,128)(2,1)S(1)}, bf16[256,128]{1,0:T(8,128)(2,1)S(1)}, u32[]{:S(2)}, u32[]{:S(2)}) collective-permute-start(bf16[256,128]{1,0:T(8,128)(2,1)S(1)} %get-tuple-element.20), channel_id=1, source_target_pairs={{0,64},{64,128},{128,192},{192,0},{1,65},{65,129},{129,193},{193,1... | collective-permute-start | bytes 196616 | tf_op jit(solution)/shard_map/ppermute | solution.py:63
  123.6 2.9 %collective-permute-start.4 = (bf16[256,128]{1,0:T(8,128)(2,1)S(1)}, bf16[256,128]{1,0:T(8,128)(2,1)S(1)}, u32[]{:S(2)}, u32[]{:S(2)}) collective-permute-start(bf16[256,128]{1,0:T(8,128)(2,1)S(1)} %get-tuple-element.21), channel_id=1, source_target_pairs={{0,128},{64,192},{128,0},{192,64},{1,129},{65,193},{129,1},{193,65... | collective-permute-start | bytes 196616 | tf_op jit(solution)/shard_map/ppermute | solution.py:63
  126.5 3.5 %collective-permute-start.5 = (bf16[256,128]{1,0:T(8,128)(2,1)S(1)}, bf16[256,128]{1,0:T(8,128)(2,1)S(1)}, u32[]{:S(2)}, u32[]{:S(2)}) collective-permute-start(bf16[256,128]{1,0:T(8,128)(2,1)S(1)} %get-tuple-element.22), channel_id=1, source_target_pairs={{0,192},{64,0},{128,64},{192,128},{1,193},{65,1},{129,65},{193,129... | collective-permute-start | bytes 196616 | tf_op jit(solution)/shard_map/ppermute | solution.py:63
  129.9 8.8 %collective-permute-done.3.b1.refs_1_ = bf16[256,128]{1,0:T(8,128)(2,1)S(1)} collective-permute-done((bf16[256,128]{1,0:T(8,128)(2,1)S(1)}, bf16[256,128]{1,0:T(8,128)(2,1)S(1)}, u32[]{:S(2)}, u32[]{:S(2)}) %collective-permute-start.3) | collective-permute-done | bytes 65568 | tf_op jit(solution)/shard_map/ppermute | solution.py:63
  138.7 4.5 %collective-permute-done.4.b2.refs_2_ = bf16[256,128]{1,0:T(8,128)(2,1)S(1)} collective-permute-done((bf16[256,128]{1,0:T(8,128)(2,1)S(1)}, bf16[256,128]{1,0:T(8,128)(2,1)S(1)}, u32[]{:S(2)}, u32[]{:S(2)}) %collective-permute-start.4) | collective-permute-done | bytes 65568 | tf_op jit(solution)/shard_map/ppermute | solution.py:63
  143.3 2.8 %collective-permute-start.6 = (bf16[4,160,128]{2,1,0:T(8,128)(2,1)S(1)}, bf16[4,160,128]{2,1,0:T(8,128)(2,1)S(1)}, u32[]{:S(2)}, u32[]{:S(2)}) collective-permute-start(bf16[4,160,128]{2,1,0:T(8,128)(2,1)S(1)} %shard_map.160), channel_id=1, source_target_pairs={{0,32},{32,0},{1,33},{33,1},{2,34},{34,2},{3,35},{35,3},{4,36},{36... | collective-permute-start | bytes 491528 | tf_op jit(solution)/shard_map/ppermute | solution.py:63
  146.0 3.3 %collective-permute-done.6 = bf16[4,160,128]{2,1,0:T(8,128)(2,1)S(1)} collective-permute-done((bf16[4,160,128]{2,1,0:T(8,128)(2,1)S(1)}, bf16[4,160,128]{2,1,0:T(8,128)(2,1)S(1)}, u32[]{:S(2)}, u32[]{:S(2)}) %collective-permute-start.6) | collective-permute-done | bytes 163872 | tf_op jit(solution)/shard_map/ppermute | solution.py:63
  149.4 0.6 collective-permute-start.7
  150.0 1.5 collective-permute-start.8
  151.5 1.4 collective-permute-start.12
  152.9 7.1 %collective-permute-done.7.refs_5_ = bf16[4,160,256]{2,1,0:T(8,128)(2,1)S(1)} collective-permute-done((bf16[4,160,256]{2,1,0:T(8,128)(2,1)S(1)}, bf16[4,160,256]{2,1,0:T(8,128)(2,1)S(1)}, u32[]{:S(2)}, u32[]{:S(2)}) %collective-permute-start.7) | collective-permute-done | bytes 327712 | tf_op jit(solution)/shard_map/ppermute | solution.py:63
  160.0 5.3 %collective-permute-done.8.refs_6_ = bf16[4,160,256]{2,1,0:T(8,128)(2,1)S(1)} collective-permute-done((bf16[4,160,256]{2,1,0:T(8,128)(2,1)S(1)}, bf16[4,160,256]{2,1,0:T(8,128)(2,1)S(1)}, u32[]{:S(2)}, u32[]{:S(2)}) %collective-permute-start.8) | collective-permute-done | bytes 327712 | tf_op jit(solution)/shard_map/ppermute | solution.py:63
  165.3 0.5 collective-permute-start.13
  165.9 1.1 collective-permute-done.11.refs_9_
  167.0 5.3 %shard_map.161 = (bf16[512,96]{1,0:T(8,128)(2,1)S(1)}, f32[512,128]{1,0:T(8,128)S(1)}, f32[512,128]{1,0:T(8,128)S(1)}) custom-call(s32[5]{0:T(128)S(1)} %stack.23.where, bf16[256,128]{1,0:T(8,128)(2,1)S(1)} %get-tuple-element.19.b0.refs_0_, bf16[256,128]{1,0:T(8,128)(2,1)S(1)} %collective-permute-done.3.b1.refs_1_, ...), custom_call_target="tpu_custom_call" | custom-call | tf_op jit(solution)/shard_map/pallas_call | solution.py:47
  172.3 3.5 %shard_map.162 = (bf16[128,64]{1,0:T(8,128)(2,1)S(1)}, bf16[128,64]{1,0:T(8,128)(2,1)S(1)}, bf16[128,64]{1,0:T(8,128)(2,1)S(1)}, bf16[128,64]{1,0:T(8,128)(2,1)S(1)}) custom-call(s32[5]{0:T(128)S(1)} %stack.23.where, bf16[512,96]{1,0:T(8,128)(2,1)S(1)} %get-tuple-element.23.refs_0_, f32[512,128]{1,0:T(8,128)S(1)} %get-tuple-element.24.refs_1_, ...), custom_call_target="tpu_custom_call" | custom-call | tf_op jit(solution)/shard_map/pallas_call | solution.py:47
  175.8 2.8 %collective-permute-start.14 = (bf16[128,64]{1,0:T(8,128)(2,1)S(1)}, bf16[128,64]{1,0:T(8,128)(2,1)S(1)}, u32[]{:S(2)}, u32[]{:S(2)}) collective-permute-start(bf16[128,64]{1,0:T(8,128)(2,1)S(1)} %get-tuple-element.27), channel_id=1, source_target_pairs={{0,192},{64,0},{128,64},{192,128},{1,193},{65,1},{129,65},{193,129... | collective-permute-start | bytes 49160 | tf_op jit(solution)/shard_map/ppermute | solution.py:63
  178.6 3.6 %collective-permute-start.15 = (bf16[128,64]{1,0:T(8,128)(2,1)S(1)}, bf16[128,64]{1,0:T(8,128)(2,1)S(1)}, u32[]{:S(2)}, u32[]{:S(2)}) collective-permute-start(bf16[128,64]{1,0:T(8,128)(2,1)S(1)} %get-tuple-element.28), channel_id=1, source_target_pairs={{0,128},{64,192},{128,0},{192,64},{1,129},{65,193},{129,1},{193,65... | collective-permute-start | bytes 49160 | tf_op jit(solution)/shard_map/ppermute | solution.py:63
  182.3 4.2 %collective-permute-done.15.a2 = bf16[128,64]{1,0:T(8,128)(2,1)S(1)} collective-permute-done((bf16[128,64]{1,0:T(8,128)(2,1)S(1)}, bf16[128,64]{1,0:T(8,128)(2,1)S(1)}, u32[]{:S(2)}, u32[]{:S(2)}) %collective-permute-start.15) | collective-permute-done | bytes 16416 | tf_op jit(solution)/shard_map/ppermute | solution.py:63
  186.5 1.8 collective-permute-done.16.a3
  188.3 0.7 shard_map.163
  188.9 1.2 collective-permute-start.17
  190.1 2.3 %collective-permute-start.18 = (bf16[32,256]{1,0:T(8,128)(2,1)S(1)}, bf16[32,256]{1,0:T(8,128)(2,1)S(1)}, u32[]{:S(2)}, u32[]{:S(2)}) collective-permute-start(bf16[32,256]{1,0:T(8,128)(2,1)S(1)} %get-tuple-element.32), channel_id=1, source_target_pairs={{0,2},{1,3},{2,0},{3,1},{4,6},{5,7},{6,4},{7,5},{8,10},{9,11},{10,... | collective-permute-start | bytes 49160 | tf_op jit(solution)/shard_map/ppermute | solution.py:63
  192.5 0.5 collective-permute-start.19
  192.9 1.0 collective-permute-done.17.a1
  194.0 1.4 collective-permute-done.18.a2
  195.4 0.8 collective-permute-done.19.a3
  196.2 2.0 %shard_map.164 = bf16[32,2048]{1,0:T(8,128)(2,1)} custom-call(s32[5]{0:T(128)S(1)} %stack.23.where, bf16[32,256]{1,0:T(8,128)(2,1)S(1)} %get-tuple-element.30.a0, bf16[32,256]{1,0:T(8,128)(2,1)S(1)} %collective-permute-done.17.a1, bf16[32,256]{1,0:T(8,128)(2,1)S(1)} %collective-permute-done.18.a2, bf16[32,256]{1,0:T(8,128)(2,1)S(1)} %collective-permute-done.19.a3, ...), custom_call_target="tpu_custom_call" | custom-call | tf_op jit(solution)/shard_map/pallas_call | solution.py:47
  198.2 1.0 shard_map.171
  (39 shorter events, 1.5 us)
Async XLA Ops:
  0.6 73.2 %copy-start = (bf16[1,2048,256]{2,1,0:T(8,128)(2,1)S(1)}, bf16[1,2048,256]{2,1,0:T(8,128)(2,1)}, u32[]{:S(2)}) copy-start(bf16[1,2048,256]{2,1,0:T(8,128)(2,1)} %param.27) | copy-start | bytes 3145732
  0.6 73.2 %copy-start.1 = (bf16[1,2048,256]{2,1,0:T(8,128)(2,1)S(1)}, bf16[1,2048,256]{2,1,0:T(8,128)(2,1)}, u32[]{:S(2)}) copy-start(bf16[1,2048,256]{2,1,0:T(8,128)(2,1)} %param.28) | copy-start | bytes 3145732
  3.8 39.5 %all-to-all-start = ((bf16[64,4,2048]{2,1,0:T(4,128)(2,1)}), bf16[64,4,2048]{2,1,0:T(4,128)(2,1)}, u32[]{:S(2)}, u32[]{:S(2)}) async-start(bf16[64,4,2048]{2,1,0:T(4,128)(2,1)} %get-tuple-element.34), calls=%async_computation | async-start | bytes 2097152 | tf_op jit(solution)/shard_map/all_to_all | solution.py:204
  15.4 33.1 %collective-permute-start.30 = (bf16[256,2048]{1,0:T(8,128)(2,1)}, bf16[256,2048]{1,0:T(8,128)(2,1)S(1)}, u32[]{:S(2)}, u32[]{:S(2)}) collective-permute-start(bf16[256,2048]{1,0:T(8,128)(2,1)} %bitcast.21), channel_id=1, source_target_pairs={{0,1},{1,2},{2,3},{3,0},{4,5},{5,6},{6,7},{7,4},{8,9},{9,10},{10,1... | collective-permute-start | bytes 3145736 | tf_op jit(solution)/shard_map/ppermute | solution.py:63
  17.0 47.3 %collective-permute-start.29 = (bf16[256,2048]{1,0:T(8,128)(2,1)}, bf16[256,2048]{1,0:T(8,128)(2,1)}, u32[]{:S(2)}, u32[]{:S(2)}) collective-permute-start(bf16[256,2048]{1,0:T(8,128)(2,1)} %bitcast.22), channel_id=1, source_target_pairs={{0,3},{1,0},{2,1},{3,2},{4,7},{5,4},{6,5},{7,6},{8,11},{9,8},{10,9... | collective-permute-start | bytes 3145736 | tf_op jit(solution)/shard_map/ppermute | solution.py:63
  45.0 16.1 %collective-permute-start.20 = (bf16[32,4,2048]{2,1,0:T(4,128)(2,1)S(1)}, bf16[32,4,2048]{2,1,0:T(4,128)(2,1)S(1)}, u32[]{:S(2)}, u32[]{:S(2)}) collective-permute-start(bf16[32,4,2048]{2,1,0:T(4,128)(2,1)S(1)} %get-tuple-element.37.rows_a), channel_id=1, source_target_pairs={{0,1},{1,2},{2,3},{3,0},{4,5},{5,6},{6,7},{7,4},{8,9},{9,10},{10,1... | collective-permute-start | bytes 1572872 | tf_op jit(solution)/shard_map/ppermute | solution.py:63
  46.5 14.8 %collective-permute-start.24 = (bf16[32,4,2048]{2,1,0:T(4,128)(2,1)S(1)}, bf16[32,4,2048]{2,1,0:T(4,128)(2,1)S(1)}, u32[]{:S(2)}, u32[]{:S(2)}) collective-permute-start(bf16[32,4,2048]{2,1,0:T(4,128)(2,1)S(1)} %get-tuple-element.36.rows_b), channel_id=1, source_target_pairs={{0,3},{1,0},{2,1},{3,2},{4,7},{5,4},{6,5},{7,6},{8,11},{9,8},{10,9... | collective-permute-start | bytes 1572872 | tf_op jit(solution)/shard_map/ppermute | solution.py:63
  48.3 24.0 %collective-permute-start.21 = (bf16[32,4,2048]{2,1,0:T(4,128)(2,1)S(1)}, bf16[32,4,2048]{2,1,0:T(4,128)(2,1)S(1)}, u32[]{:S(2)}, u32[]{:S(2)}) collective-permute-start(bf16[32,4,2048]{2,1,0:T(4,128)(2,1)S(1)} %get-tuple-element.36.rows_b), channel_id=1, source_target_pairs={{0,1},{1,2},{2,3},{3,0},{4,5},{5,6},{6,7},{7,4},{8,9},{9,10},{10,1... | collective-permute-start | bytes 1572872 | tf_op jit(solution)/shard_map/ppermute | solution.py:63
  48.6 26.7 %collective-permute-start.27 = (bf16[32,4,2048]{2,1,0:T(4,128)(2,1)S(1)}, bf16[32,4,2048]{2,1,0:T(4,128)(2,1)S(1)}, u32[]{:S(2)}, u32[]{:S(2)}) collective-permute-start(bf16[32,4,2048]{2,1,0:T(4,128)(2,1)S(1)} %get-tuple-element.37.rows_a), channel_id=1, source_target_pairs={{0,3},{1,0},{2,1},{3,2},{4,7},{5,4},{6,5},{7,6},{8,11},{9,8},{10,9... | collective-permute-start | bytes 1572872 | tf_op jit(solution)/shard_map/ppermute | solution.py:63
  61.1 22.5 %collective-permute-start.23 = (bf16[32,4,2048]{2,1,0:T(4,128)(2,1)S(1)}, bf16[32,4,2048]{2,1,0:T(4,128)(2,1)S(1)}, u32[]{:S(2)}, u32[]{:S(2)}) collective-permute-start(bf16[32,4,2048]{2,1,0:T(4,128)(2,1)S(1)} %collective-permute-done.20.rows_a), channel_id=1, source_target_pairs={{0,1},{1,2},{2,3},{3,0},{4,5},{5,6},{6,7},{7,4},{8,9},{9,10},{10,1... | collective-permute-start | bytes 1572872 | tf_op jit(solution)/shard_map/ppermute | solution.py:63
  61.3 22.5 %collective-permute-start.25 = (bf16[32,4,2048]{2,1,0:T(4,128)(2,1)S(1)}, bf16[32,4,2048]{2,1,0:T(4,128)(2,1)S(1)}, u32[]{:S(2)}, u32[]{:S(2)}) collective-permute-start(bf16[32,4,2048]{2,1,0:T(4,128)(2,1)S(1)} %collective-permute-done.24.rows_b), channel_id=1, source_target_pairs={{0,3},{1,0},{2,1},{3,2},{4,7},{5,4},{6,5},{7,6},{8,11},{9,8},{10,9... | collective-permute-start | bytes 1572872 | tf_op jit(solution)/shard_map/ppermute | solution.py:63
  64.4 30.4 %collective-permute-start.31 = (bf16[128,2048]{1,0:T(8,128)(2,1)S(1)}, bf16[128,2048]{1,0:T(8,128)(2,1)S(1)}, u32[]{:S(2)}, u32[]{:S(2)}) collective-permute-start(bf16[128,2048]{1,0:T(8,128)(2,1)S(1)} %slice.18), channel_id=1, source_target_pairs={{0,1},{1,2},{2,3},{3,0},{4,5},{5,6},{6,7},{7,4},{8,9},{9,10},{10,1... | collective-permute-start | bytes 1572872 | tf_op jit(solution)/shard_map/ppermute | solution.py:63
  72.3 22.8 %collective-permute-start.32 = (bf16[128,2048]{1,0:T(8,128)(2,1)S(1)}, bf16[128,2048]{1,0:T(8,128)(2,1)S(1)}, u32[]{:S(2)}, u32[]{:S(2)}) collective-permute-start(bf16[128,2048]{1,0:T(8,128)(2,1)S(1)} %slice.19), channel_id=1, source_target_pairs={{0,3},{1,0},{2,1},{3,2},{4,7},{5,4},{6,5},{7,6},{8,11},{9,8},{10,9... | collective-permute-start | bytes 1572872 | tf_op jit(solution)/shard_map/ppermute | solution.py:63
  75.2 24.9 %copy-start.3 = (bf16[1,256,2048]{2,1,0:T(8,128)(2,1)S(1)}, bf16[1,256,2048]{2,1,0:T(8,128)(2,1)}, u32[]{:S(2)}) copy-start(bf16[1,256,2048]{2,1,0:T(8,128)(2,1)} %param.29) | copy-start | bytes 3145732
  75.2 22.4 %collective-permute-start.22 = (bf16[256,256]{1,0:T(8,128)(2,1)S(1)}, bf16[256,256]{1,0:T(8,128)(2,1)S(1)}, u32[]{:S(2)}, u32[]{:S(2)}) collective-permute-start(bf16[256,256]{1,0:T(8,128)(2,1)S(1)} %shard_map.167), channel_id=1, source_target_pairs={{0,3},{1,0},{2,1},{3,2},{4,7},{5,4},{6,5},{7,6},{8,11},{9,8},{10,9... | collective-permute-start | bytes 393224 | tf_op jit(solution)/shard_map/ppermute | solution.py:63
  83.5 14.2 %collective-permute-start.28 = (bf16[256,256]{1,0:T(8,128)(2,1)S(1)}, bf16[256,256]{1,0:T(8,128)(2,1)S(1)}, u32[]{:S(2)}, u32[]{:S(2)}) collective-permute-start(bf16[256,256]{1,0:T(8,128)(2,1)S(1)} %shard_map.169), channel_id=1, source_target_pairs={{0,1},{1,2},{2,3},{3,0},{4,5},{5,6},{6,7},{7,4},{8,9},{9,10},{10,1... | collective-permute-start | bytes 393224 | tf_op jit(solution)/shard_map/ppermute | solution.py:63
  85.2 14.9 %collective-permute-start.26 = (bf16[256,256]{1,0:T(8,128)(2,1)S(1)}, bf16[256,256]{1,0:T(8,128)(2,1)S(1)}, u32[]{:S(2)}, u32[]{:S(2)}) collective-permute-start(bf16[256,256]{1,0:T(8,128)(2,1)S(1)} %shard_map.168), channel_id=1, source_target_pairs={{0,2},{1,3},{2,0},{3,1},{4,6},{5,7},{6,4},{7,5},{8,10},{9,11},{10,... | collective-permute-start | bytes 393224 | tf_op jit(solution)/shard_map/ppermute | solution.py:63
  104.4 93.9 %all-to-all-start.1 = ((bf16[64,4,2048]{2,1,0:T(4,128)(2,1)}), bf16[64,4,2048]{2,1,0:T(4,128)(2,1)S(1)}, u32[]{:S(2)}, u32[]{:S(2)}) async-start(bf16[64,4,2048]{2,1,0:T(4,128)(2,1)} %shard_map.170), calls=%async_computation.1 | async-start | bytes 2097152 | tf_op jit(solution)/shard_map/all_to_all | solution.py:221
  112.1 5.4 %collective-permute-start = (bf16[32,544]{1,0:T(8,128)(2,1)S(1)}, bf16[32,544]{1,0:T(8,128)(2,1)S(1)}, u32[]{:S(2)}, u32[]{:S(2)}) collective-permute-start(bf16[32,544]{1,0:T(8,128)(2,1)S(1)} %shard_map.158.l0), channel_id=1, source_target_pairs={{0,1},{1,2},{2,3},{3,0},{4,5},{5,6},{6,7},{7,4},{8,9},{9,10},{10,1... | collective-permute-start | bytes 104456 | tf_op jit(solution)/shard_map/ppermute | solution.py:63
  113.3 5.5 %collective-permute-start.1 = (bf16[32,544]{1,0:T(8,128)(2,1)S(1)}, bf16[32,544]{1,0:T(8,128)(2,1)S(1)}, u32[]{:S(2)}, u32[]{:S(2)}) collective-permute-start(bf16[32,544]{1,0:T(8,128)(2,1)S(1)} %shard_map.158.l0), channel_id=1, source_target_pairs={{0,2},{1,3},{2,0},{3,1},{4,6},{5,7},{6,4},{7,5},{8,10},{9,11},{10,... | collective-permute-start | bytes 104456 | tf_op jit(solution)/shard_map/ppermute | solution.py:63
  115.6 4.0 %collective-permute-start.2 = (bf16[32,544]{1,0:T(8,128)(2,1)S(1)}, bf16[32,544]{1,0:T(8,128)(2,1)S(1)}, u32[]{:S(2)}, u32[]{:S(2)}) collective-permute-start(bf16[32,544]{1,0:T(8,128)(2,1)S(1)} %shard_map.158.l0), channel_id=1, source_target_pairs={{0,3},{1,0},{2,1},{3,2},{4,7},{5,4},{6,5},{7,6},{8,11},{9,8},{10,9... | collective-permute-start | bytes 104456 | tf_op jit(solution)/shard_map/ppermute | solution.py:63
  116.3 79.9 %copy-start.2 = (bf16[1024,2048]{1,0:T(8,128)(2,1)S(1)}, bf16[1024,2048]{1,0:T(8,128)(2,1)}, u32[]{:S(2)}) copy-start(bf16[1024,2048]{1,0:T(8,128)(2,1)} %out_proj.1) | copy-start | bytes 12582916
  121.0 17.7 %collective-permute-start.3 = (bf16[256,128]{1,0:T(8,128)(2,1)S(1)}, bf16[256,128]{1,0:T(8,128)(2,1)S(1)}, u32[]{:S(2)}, u32[]{:S(2)}) collective-permute-start(bf16[256,128]{1,0:T(8,128)(2,1)S(1)} %get-tuple-element.20), channel_id=1, source_target_pairs={{0,64},{64,128},{128,192},{192,0},{1,65},{65,129},{129,193},{193,1... | collective-permute-start | bytes 196616 | tf_op jit(solution)/shard_map/ppermute | solution.py:63
  123.6 19.7 %collective-permute-start.4 = (bf16[256,128]{1,0:T(8,128)(2,1)S(1)}, bf16[256,128]{1,0:T(8,128)(2,1)S(1)}, u32[]{:S(2)}, u32[]{:S(2)}) collective-permute-start(bf16[256,128]{1,0:T(8,128)(2,1)S(1)} %get-tuple-element.21), channel_id=1, source_target_pairs={{0,128},{64,192},{128,0},{192,64},{1,129},{65,193},{129,1},{193,65... | collective-permute-start | bytes 196616 | tf_op jit(solution)/shard_map/ppermute | solution.py:63
  126.5 16.8 %collective-permute-start.5 = (bf16[256,128]{1,0:T(8,128)(2,1)S(1)}, bf16[256,128]{1,0:T(8,128)(2,1)S(1)}, u32[]{:S(2)}, u32[]{:S(2)}) collective-permute-start(bf16[256,128]{1,0:T(8,128)(2,1)S(1)} %get-tuple-element.22), channel_id=1, source_target_pairs={{0,192},{64,0},{128,64},{192,128},{1,193},{65,1},{129,65},{193,129... | collective-permute-start | bytes 196616 | tf_op jit(solution)/shard_map/ppermute | solution.py:63
  143.3 6.1 %collective-permute-start.6 = (bf16[4,160,128]{2,1,0:T(8,128)(2,1)S(1)}, bf16[4,160,128]{2,1,0:T(8,128)(2,1)S(1)}, u32[]{:S(2)}, u32[]{:S(2)}) collective-permute-start(bf16[4,160,128]{2,1,0:T(8,128)(2,1)S(1)} %shard_map.160), channel_id=1, source_target_pairs={{0,32},{32,0},{1,33},{33,1},{2,34},{34,2},{3,35},{35,3},{4,36},{36... | collective-permute-start | bytes 491528 | tf_op jit(solution)/shard_map/ppermute | solution.py:63
  149.4 10.7 %collective-permute-start.7 = (bf16[4,160,256]{2,1,0:T(8,128)(2,1)S(1)}, bf16[4,160,256]{2,1,0:T(8,128)(2,1)S(1)}, u32[]{:S(2)}, u32[]{:S(2)}) collective-permute-start(bf16[4,160,256]{2,1,0:T(8,128)(2,1)S(1)} %pad_maximum_fusion.refs_4_), channel_id=1, source_target_pairs={{0,8},{8,16},{16,24},{24,0},{1,9},{9,17},{17,25},{25,1},{2,10},{10... | collective-permute-start | bytes 983048 | tf_op jit(solution)/shard_map/ppermute | solution.py:63
  150.0 15.4 %collective-permute-start.8 = (bf16[4,160,256]{2,1,0:T(8,128)(2,1)S(1)}, bf16[4,160,256]{2,1,0:T(8,128)(2,1)S(1)}, u32[]{:S(2)}, u32[]{:S(2)}) collective-permute-start(bf16[4,160,256]{2,1,0:T(8,128)(2,1)S(1)} %pad_maximum_fusion.refs_4_), channel_id=1, source_target_pairs={{0,24},{8,0},{16,8},{24,16},{1,25},{9,1},{17,9},{25,17},{2,26},{10... | collective-permute-start | bytes 983048 | tf_op jit(solution)/shard_map/ppermute | solution.py:63
  151.5 13.9 %collective-permute-start.12 = (bf16[4,160,256]{2,1,0:T(8,128)(2,1)S(1)}, bf16[4,160,256]{2,1,0:T(8,128)(2,1)S(1)}, u32[]{:S(2)}, u32[]{:S(2)}) collective-permute-start(bf16[4,160,256]{2,1,0:T(8,128)(2,1)S(1)} %pad_maximum_fusion.refs_4_), channel_id=1, source_target_pairs={{0,16},{8,24},{16,0},{24,8},{1,17},{9,25},{17,1},{25,9},{2,18},{10... | collective-permute-start | bytes 983048 | tf_op jit(solution)/shard_map/ppermute | solution.py:63
  152.9 13.0 %collective-permute-start.9 = (bf16[4,160,256]{2,1,0:T(8,128)(2,1)S(1)}, bf16[4,160,256]{2,1,0:T(8,128)(2,1)S(1)}, u32[]{:S(2)}, u32[]{:S(2)}) collective-permute-start(bf16[4,160,256]{2,1,0:T(8,128)(2,1)S(1)} %pad_maximum_fusion.refs_4_), channel_id=1, source_target_pairs={{0,4},{4,0},{1,5},{5,1},{2,6},{6,2},{3,7},{7,3},{8,12},{12,8},{9,1... | collective-permute-start | bytes 983048 | tf_op jit(solution)/shard_map/ppermute | solution.py:63
  160.0 5.8 %collective-permute-start.10 = (bf16[4,160,256]{2,1,0:T(8,128)(2,1)S(1)}, bf16[4,160,256]{2,1,0:T(8,128)(2,1)S(1)}, u32[]{:S(2)}, u32[]{:S(2)}) collective-permute-start(bf16[4,160,256]{2,1,0:T(8,128)(2,1)S(1)} %collective-permute-done.7.refs_5_), channel_id=1, source_target_pairs={{0,4},{4,0},{1,5},{5,1},{2,6},{6,2},{3,7},{7,3},{8,12},{12,8},{9,1... | collective-permute-start | bytes 983048 | tf_op jit(solution)/shard_map/ppermute | solution.py:63
  165.3 1.6 collective-permute-start.11
  165.3 6.9 %collective-permute-start.13 = (bf16[4,160,256]{2,1,0:T(8,128)(2,1)S(1)}, bf16[4,160,256]{2,1,0:T(8,128)(2,1)S(1)}, u32[]{:S(2)}, u32[]{:S(2)}) collective-permute-start(bf16[4,160,256]{2,1,0:T(8,128)(2,1)S(1)} %collective-permute-done.12.refs_3_), channel_id=1, source_target_pairs={{0,4},{4,0},{1,5},{5,1},{2,6},{6,2},{3,7},{7,3},{8,12},{12,8},{9,1... | collective-permute-start | bytes 983048 | tf_op jit(solution)/shard_map/ppermute | solution.py:63
  175.8 6.4 %collective-permute-start.14 = (bf16[128,64]{1,0:T(8,128)(2,1)S(1)}, bf16[128,64]{1,0:T(8,128)(2,1)S(1)}, u32[]{:S(2)}, u32[]{:S(2)}) collective-permute-start(bf16[128,64]{1,0:T(8,128)(2,1)S(1)} %get-tuple-element.27), channel_id=1, source_target_pairs={{0,192},{64,0},{128,64},{192,128},{1,193},{65,1},{129,65},{193,129... | collective-permute-start | bytes 49160 | tf_op jit(solution)/shard_map/ppermute | solution.py:63
  178.6 7.8 %collective-permute-start.15 = (bf16[128,64]{1,0:T(8,128)(2,1)S(1)}, bf16[128,64]{1,0:T(8,128)(2,1)S(1)}, u32[]{:S(2)}, u32[]{:S(2)}) collective-permute-start(bf16[128,64]{1,0:T(8,128)(2,1)S(1)} %get-tuple-element.28), channel_id=1, source_target_pairs={{0,128},{64,192},{128,0},{192,64},{1,129},{65,193},{129,1},{193,65... | collective-permute-start | bytes 49160 | tf_op jit(solution)/shard_map/ppermute | solution.py:63
  182.3 6.0 %collective-permute-start.16 = (bf16[128,64]{1,0:T(8,128)(2,1)S(1)}, bf16[128,64]{1,0:T(8,128)(2,1)S(1)}, u32[]{:S(2)}, u32[]{:S(2)}) collective-permute-start(bf16[128,64]{1,0:T(8,128)(2,1)S(1)} %get-tuple-element.29), channel_id=1, source_target_pairs={{0,64},{64,128},{128,192},{192,0},{1,65},{65,129},{129,193},{193,1... | collective-permute-start | bytes 49160 | tf_op jit(solution)/shard_map/ppermute | solution.py:63
  188.9 5.0 %collective-permute-start.17 = (bf16[32,256]{1,0:T(8,128)(2,1)S(1)}, bf16[32,256]{1,0:T(8,128)(2,1)S(1)}, u32[]{:S(2)}, u32[]{:S(2)}) collective-permute-start(bf16[32,256]{1,0:T(8,128)(2,1)S(1)} %get-tuple-element.31), channel_id=1, source_target_pairs={{0,1},{1,2},{2,3},{3,0},{4,5},{5,6},{6,7},{7,4},{8,9},{9,10},{10,1... | collective-permute-start | bytes 49160 | tf_op jit(solution)/shard_map/ppermute | solution.py:63
  190.1 5.2 %collective-permute-start.18 = (bf16[32,256]{1,0:T(8,128)(2,1)S(1)}, bf16[32,256]{1,0:T(8,128)(2,1)S(1)}, u32[]{:S(2)}, u32[]{:S(2)}) collective-permute-start(bf16[32,256]{1,0:T(8,128)(2,1)S(1)} %get-tuple-element.32), channel_id=1, source_target_pairs={{0,2},{1,3},{2,0},{3,1},{4,6},{5,7},{6,4},{7,5},{8,10},{9,11},{10,... | collective-permute-start | bytes 49160 | tf_op jit(solution)/shard_map/ppermute | solution.py:63
  192.5 3.7 %collective-permute-start.19 = (bf16[32,256]{1,0:T(8,128)(2,1)S(1)}, bf16[32,256]{1,0:T(8,128)(2,1)S(1)}, u32[]{:S(2)}, u32[]{:S(2)}) collective-permute-start(bf16[32,256]{1,0:T(8,128)(2,1)S(1)} %get-tuple-element.33), channel_id=1, source_target_pairs={{0,3},{1,0},{2,1},{3,2},{4,7},{5,4},{6,5},{7,6},{8,11},{9,8},{10,9... | collective-permute-start | bytes 49160 | tf_op jit(solution)/shard_map/ppermute | solution.py:63

commit v9 on v6

--- a/solution.py
+++ b/solution.py
@@ -299,28 +299,27 @@
                 advance(slice((g + 1) * strip, 4 * strip), parts, None)
     total = acc_s[...]
     acc_s[:, :V_DIM] = total[:, :V_DIM] / total[:, V_DIM:]
-    for j, out in enumerate(outs):
-        at = pl.multiple_of(lax.rem(zh - j + 4, 4) * strip, strip)
-        out[...] = acc_s[pl.ds(at, strip), :V_DIM].astype(BF)
+    own = strip // 4
+    for k, out in enumerate(outs):
+        for g in range(4):
+            at = pl.multiple_of(g * strip + lax.rem(x + k, 4) * own, own)
+            out[g * own : (g + 1) * own, :] = acc_s[pl.ds(at, own), :V_DIM].astype(BF)
 
 
 def spread_kernel(where, a0, a1, a2, a3, o0, o1, o2, o3, heads, parts):
-    for j, a in enumerate((a0, a1, a2, a3)):
-        heads[lax.rem(where[0] + j, 4)] = a[...]
+    for k, a in enumerate((a0, a1, a2, a3)):
+        heads[lax.rem(where[4] - k + 4, 4)] = a[...]
     beside = jnp.concatenate([heads[h] for h in range(4)], axis=1)
     parts[...] = beside.reshape(parts.shape)
-    for k, out in enumerate((o0, o1, o2, o3)):
-        out[...] = parts[lax.rem(where[4] + k, 4)]
+    for j, out in enumerate((o0, o1, o2, o3)):
+        out[...] = parts[lax.rem(where[0] + j, 4)]
 
 
 def project_kernel(where, a0, a1, a2, a3, out_proj, out, parts):
-    width = a0.shape[1]
-    for k, a in enumerate((a0, a1, a2, a3)):
-        parts[lax.rem(where[4] - k + 4, 4)] = a[...]
-    total = mm(parts[0], out_proj[:width, :])
-    for h in range(1, 4):
-        total = total + mm(parts[h], out_proj[h * width : (h + 1) * width, :])
-    out[...] = total.astype(BF)
+    for j, a in enumerate((a0, a1, a2, a3)):
+        parts[lax.rem(where[0] - j + 4, 4)] = a[...]
+    pieces = [parts[h % 4, :, h // 4 * V_DIM : (h // 4 + 1) * V_DIM] for h in range(16)]
+    out[...] = mm(jnp.concatenate(pieces, axis=1), out_proj[...]).astype(BF)
 
 
 def query_and_pair(where, query, latent, rope_key, latent_gain, key_up, value_up):
@@ -375,7 +374,7 @@
             pltpu.VMEM((4 * strip, 128), F32),
         ],
     )
-    return [parts[0]] + [shifted(parts[j], "zh", -j) for j in range(1, 4)]
+    return [parts[0]] + [shifted(parts[k], "x", k) for k in range(1, 4)]
 
 
 def project(where, parts, out_proj, own):
@@ -387,7 +386,7 @@
         where,
         [pltpu.VMEM((4, strip, V_DIM), BF), pltpu.VMEM((4, own, 4 * V_DIM), BF)],
     )
-    parts = [parts[0]] + [shifted(parts[k], "x", k) for k in range(1, 4)]
+    parts = [parts[0]] + [shifted(parts[j], "zh", j) for j in range(1, 4)]
     return call(
         project_kernel,
         jax.ShapeDtypeStruct((own, out_proj.shape[1]), BF),

time: 197 us -> 196 us (level)
  the two profiles are of different devices: /device:TPU:32 before, /device:TPU:8 now
where the time goes in v9:
time: 196 us; the launch traced here: 195 us
  waiting for transfers between devices  101 us (52%)
  starting transfers between devices  65.7 us (34%)
  Pallas kernels  23.9 us (12%)
  local copies, waits for them, and re-layouts  2.9 us (1%)
    ppermute x33, waiting for transfers between devices, shifted(): return lax.ppermute(value, axis, [(i, (i + amount) % n) for i in range(n)])  76.1 us
    ppermute x33, starting transfers between devices, shifted(): return lax.ppermute(value, axis, [(i, (i + amount) % n) for i in range(n)])  46.9 us
    all_to_all x1, waiting for transfers between devices, both_halves(): lax.all_to_all(outgoing, EP, split_axis=0, concat_axis=0, tiled=True)  25.4 us
    pallas_call x13, Pallas kernels, call(): pl.pallas_call(kernel, in_specs=specs, out_specs=VMEM_SPEC if single else...  23.9 us
    all_to_all x1, starting transfers between devices, both_halves(): lax.all_to_all(outgoing, EP, split_axis=0, concat_axis=0, tiled=True)  12.3 us
    all_to_all x1, starting transfers between devices, both_halves(): lax.all_to_all(result, EP, split_axis=0, concat_axis=0, tiled=True)  6.5 us
  transfers between devices with their start and end apart: 35, of which 24 were waited for; matrix products, arithmetic and copies ran while one was open for 2% of the time, Pallas kernels for 8%

profile of v9, /device:TPU:8, one launch (start us, length us, event | category | flops | bytes accessed | tf_op | source)
XLA Modules:
  0.0 195.2 jit_solution(9285660295023474249)
XLA Ops:
  0.7 2.8 %shard_map.164 = (bf16[64,4,2048]{2,1,0:T(4,128)(2,1)}, bf16[256,128]{1,0:T(8,128)(2,1)S(1)}) custom-call(bf16[64,2048]{1,0:T(8,128)(2,1)} %tokens.1, f32[1,2048]{1,0:T(1,128)} %bitcast.24, s32[2,64]{1,0:T(2,128)} %bitcast.26, f32[1,64]{1,0:T(1,128)} %bitcast.28, f32[2,64]{1,0:T(2,128)} %bitcast.27), custom_call_target="tpu_custom_call" | custom-call | tf_op jit(solution)/shard_map/pallas_call | solution.py:45
  3.4 12.3 %all-to-all-start = ((bf16[64,4,2048]{2,1,0:T(4,128)(2,1)}), bf16[64,4,2048]{2,1,0:T(4,128)(2,1)}, u32[]{:S(2)}, u32[]{:S(2)}) async-start(bf16[64,4,2048]{2,1,0:T(4,128)(2,1)} %get-tuple-element.28), calls=%async_computation | async-start | bytes 2097152 | tf_op jit(solution)/shard_map/all_to_all | solution.py:178
  15.7 1.6 collective-permute-start.30
  17.3 1.8 collective-permute-start.29
  19.0 25.4 %all-to-all-done = bf16[64,4,2048]{2,1,0:T(4,128)(2,1)} async-done(((bf16[64,4,2048]{2,1,0:T(4,128)(2,1)}), bf16[64,4,2048]{2,1,0:T(4,128)(2,1)}, u32[]{:S(2)}, u32[]{:S(2)}) %all-to-all-start) | async-done | bytes 1048608 | tf_op jit(solution)/shard_map/all_to_all | solution.py:178
  44.4 1.7 fusion
  46.1 1.6 collective-permute-start.20
  47.6 1.8 collective-permute-start.24
  49.7 3.0 %collective-permute-start.27 = (bf16[32,4,2048]{2,1,0:T(4,128)(2,1)S(1)}, bf16[32,4,2048]{2,1,0:T(4,128)(2,1)S(1)}, u32[]{:S(2)}, u32[]{:S(2)}) collective-permute-start(bf16[32,4,2048]{2,1,0:T(4,128)(2,1)S(1)} %get-tuple-element.31.rows_a), channel_id=1, source_target_pairs={{0,3},{1,0},{2,1},{3,2},{4,7},{5,4},{6,5},{7,6},{8,11},{9,8},{10,9... | collective-permute-start | bytes 1572872 | tf_op jit(solution)/shard_map/ppermute | solution.py:61
  52.6 9.5 %collective-permute-done.20.rows_a = bf16[32,4,2048]{2,1,0:T(4,128)(2,1)S(1)} collective-permute-done((bf16[32,4,2048]{2,1,0:T(4,128)(2,1)S(1)}, bf16[32,4,2048]{2,1,0:T(4,128)(2,1)S(1)}, u32[]{:S(2)}, u32[]{:S(2)}) %collective-permute-start.20) | collective-permute-done | bytes 524320 | tf_op jit(solution)/shard_map/ppermute | solution.py:61
  62.4 3.0 %collective-permute-start.25 = (bf16[32,4,2048]{2,1,0:T(4,128)(2,1)S(1)}, bf16[32,4,2048]{2,1,0:T(4,128)(2,1)S(1)}, u32[]{:S(2)}, u32[]{:S(2)}) collective-permute-start(bf16[32,4,2048]{2,1,0:T(4,128)(2,1)S(1)} %collective-permute-done.24.rows_b), channel_id=1, source_target_pairs={{0,3},{1,0},{2,1},{3,2},{4,7},{5,4},{6,5},{7,6},{8,11},{9,8},{10,9... | collective-permute-start | bytes 1572872 | tf_op jit(solution)/shard_map/ppermute | solution.py:61
  65.6 1.1 slice.19
  66.6 6.8 %collective-permute-done.21.rows_b = bf16[32,4,2048]{2,1,0:T(4,128)(2,1)S(1)} collective-permute-done((bf16[32,4,2048]{2,1,0:T(4,128)(2,1)S(1)}, bf16[32,4,2048]{2,1,0:T(4,128)(2,1)S(1)}, u32[]{:S(2)}, u32[]{:S(2)}) %collective-permute-start.21) | collective-permute-done | bytes 524320 | tf_op jit(solution)/shard_map/ppermute | solution.py:61
  73.4 1.5 collective-permute-start.32
  74.9 1.4 shard_map.166
  76.3 0.9 collective-permute-start.22
  77.2 1.4 shard_map.168
  78.6 6.0 %collective-permute-done.23.rows_a = bf16[32,4,2048]{2,1,0:T(4,128)(2,1)S(1)} collective-permute-done((bf16[32,4,2048]{2,1,0:T(4,128)(2,1)S(1)}, bf16[32,4,2048]{2,1,0:T(4,128)(2,1)S(1)}, u32[]{:S(2)}, u32[]{:S(2)}) %collective-permute-start.23) | collective-permute-done | bytes 524320 | tf_op jit(solution)/shard_map/ppermute | solution.py:61
  84.6 0.3 collective-permute-start.28
  84.9 1.4 shard_map.167
  86.3 2.8 %collective-permute-start.26 = (bf16[256,256]{1,0:T(8,128)(2,1)S(1)}, bf16[256,256]{1,0:T(8,128)(2,1)S(1)}, u32[]{:S(2)}, u32[]{:S(2)}) collective-permute-start(bf16[256,256]{1,0:T(8,128)(2,1)S(1)} %shard_map.167), channel_id=1, source_target_pairs={{0,2},{1,3},{2,0},{3,1},{4,6},{5,7},{6,4},{7,5},{8,10},{9,11},{10,... | collective-permute-start | bytes 393224 | tf_op jit(solution)/shard_map/ppermute | solution.py:61
  89.1 1.4 shard_map.165.h0
  90.5 4.7 %collective-permute-done.31.w2a = bf16[128,2048]{1,0:T(8,128)(2,1)S(1)} collective-permute-done((bf16[128,2048]{1,0:T(8,128)(2,1)S(1)}, bf16[128,2048]{1,0:T(8,128)(2,1)S(1)}, u32[]{:S(2)}, u32[]{:S(2)}) %collective-permute-start.31) | collective-permute-done | bytes 524320 | tf_op jit(solution)/shard_map/ppermute | solution.py:61
  95.2 1.0 collective-permute-done.32.w2b
  96.1 2.5 %collective-permute-done.22.h1 = bf16[256,256]{1,0:T(8,128)(2,1)S(1)} collective-permute-done((bf16[256,256]{1,0:T(8,128)(2,1)S(1)}, bf16[256,256]{1,0:T(8,128)(2,1)S(1)}, u32[]{:S(2)}, u32[]{:S(2)}) %collective-permute-start.22) | collective-permute-done | bytes 131104 | tf_op jit(solution)/shard_map/ppermute | solution.py:61
  98.7 1.7 collective-permute-done.26.h2
  100.4 3.8 %shard_map.169 = bf16[64,4,2048]{2,1,0:T(4,128)(2,1)} custom-call(bf16[256,256]{1,0:T(8,128)(2,1)S(1)} %shard_map.165.h0, bf16[256,256]{1,0:T(8,128)(2,1)S(1)} %collective-permute-done.22.h1, bf16[256,256]{1,0:T(8,128)(2,1)S(1)} %collective-permute-done.26.h2, bf16[256,256]{1,0:T(8,128)(2,1)S(1)} %collective-permute-done.28.h3, ...), custom_call_target="tpu_custom_call" | custom-call | tf_op jit(solution)/shard_map/pallas_call | solution.py:45
  104.2 6.5 %all-to-all-start.1 = ((bf16[64,4,2048]{2,1,0:T(4,128)(2,1)}), bf16[64,4,2048]{2,1,0:T(4,128)(2,1)S(1)}, u32[]{:S(2)}, u32[]{:S(2)}) async-start(bf16[64,4,2048]{2,1,0:T(4,128)(2,1)} %shard_map.169), calls=%async_computation.1 | async-start | bytes 2097152 | tf_op jit(solution)/shard_map/all_to_all | solution.py:195
  111.0 0.9 shard_map.158.l0
  111.8 1.2 collective-permute-start
  113.1 2.3 %collective-permute-start.1 = (bf16[32,544]{1,0:T(8,128)(2,1)S(1)}, bf16[32,544]{1,0:T(8,128)(2,1)S(1)}, u32[]{:S(2)}, u32[]{:S(2)}) collective-permute-start(bf16[32,544]{1,0:T(8,128)(2,1)S(1)} %shard_map.158.l0), channel_id=1, source_target_pairs={{0,2},{1,3},{2,0},{3,1},{4,6},{5,7},{6,4},{7,5},{8,10},{9,11},{10,... | collective-permute-start | bytes 104456 | tf_op jit(solution)/shard_map/ppermute | solution.py:61
  115.4 0.5 collective-permute-start.2
  116.0 1.2 collective-permute-done.l1
  117.3 1.3 collective-permute-done.1.l2
  118.6 0.8 collective-permute-done.2.l3
  119.4 1.4 shard_map.159
  120.8 2.4 %collective-permute-start.3 = (bf16[256,128]{1,0:T(8,128)(2,1)S(1)}, bf16[256,128]{1,0:T(8,128)(2,1)S(1)}, u32[]{:S(2)}, u32[]{:S(2)}) collective-permute-start(bf16[256,128]{1,0:T(8,128)(2,1)S(1)} %get-tuple-element.17), channel_id=1, source_target_pairs={{0,64},{64,128},{128,192},{192,0},{1,65},{65,129},{129,193},{193,1... | collective-permute-start | bytes 196616 | tf_op jit(solution)/shard_map/ppermute | solution.py:61
  123.2 3.8 %collective-permute-start.4 = (bf16[256,128]{1,0:T(8,128)(2,1)S(1)}, bf16[256,128]{1,0:T(8,128)(2,1)S(1)}, u32[]{:S(2)}, u32[]{:S(2)}) collective-permute-start(bf16[256,128]{1,0:T(8,128)(2,1)S(1)} %get-tuple-element.18), channel_id=1, source_target_pairs={{0,128},{64,192},{128,0},{192,64},{1,129},{65,193},{129,1},{193,65... | collective-permute-start | bytes 196616 | tf_op jit(solution)/shard_map/ppermute | solution.py:61
  127.0 3.5 %collective-permute-start.5 = (bf16[256,128]{1,0:T(8,128)(2,1)S(1)}, bf16[256,128]{1,0:T(8,128)(2,1)S(1)}, u32[]{:S(2)}, u32[]{:S(2)}) collective-permute-start(bf16[256,128]{1,0:T(8,128)(2,1)S(1)} %get-tuple-element.19), channel_id=1, source_target_pairs={{0,192},{64,0},{128,64},{192,128},{1,193},{65,1},{129,65},{193,129... | collective-permute-start | bytes 196616 | tf_op jit(solution)/shard_map/ppermute | solution.py:61
  130.5 10.8 %collective-permute-done.3.b1.q1 = bf16[256,128]{1,0:T(8,128)(2,1)S(1)} collective-permute-done((bf16[256,128]{1,0:T(8,128)(2,1)S(1)}, bf16[256,128]{1,0:T(8,128)(2,1)S(1)}, u32[]{:S(2)}, u32[]{:S(2)}) %collective-permute-start.3) | collective-permute-done | bytes 65568 | tf_op jit(solution)/shard_map/ppermute | solution.py:61
  141.3 3.8 %collective-permute-done.4.b2.q2 = bf16[256,128]{1,0:T(8,128)(2,1)S(1)} collective-permute-done((bf16[256,128]{1,0:T(8,128)(2,1)S(1)}, bf16[256,128]{1,0:T(8,128)(2,1)S(1)}, u32[]{:S(2)}, u32[]{:S(2)}) %collective-permute-start.4) | collective-permute-done | bytes 65568 | tf_op jit(solution)/shard_map/ppermute | solution.py:61
  145.2 5.3 %collective-permute-done.6 = bf16[4,160,128]{2,1,0:T(8,128)(2,1)S(1)} collective-permute-done((bf16[4,160,128]{2,1,0:T(8,128)(2,1)S(1)}, bf16[4,160,128]{2,1,0:T(8,128)(2,1)S(1)}, u32[]{:S(2)}, u32[]{:S(2)}) %collective-permute-start.6) | collective-permute-done | bytes 163872 | tf_op jit(solution)/shard_map/ppermute | solution.py:61
  150.5 1.6 collective-permute-start.7
  152.1 1.1 collective-permute-start.8
  153.2 2.1 %collective-permute-start.9 = (bf16[4,160,256]{2,1,0:T(8,128)(2,1)S(1)}, bf16[4,160,256]{2,1,0:T(8,128)(2,1)S(1)}, u32[]{:S(2)}, u32[]{:S(2)}) collective-permute-start(bf16[4,160,256]{2,1,0:T(8,128)(2,1)S(1)} %pad_maximum_fusion.refs_0_), channel_id=1, source_target_pairs={{0,24},{8,0},{16,8},{24,16},{1,25},{9,1},{17,9},{25,17},{2,26},{10... | collective-permute-start | bytes 983048 | tf_op jit(solution)/shard_map/ppermute | solution.py:61
  155.3 8.2 %collective-permute-done.7.refs_1_ = bf16[4,160,256]{2,1,0:T(8,128)(2,1)S(1)} collective-permute-done((bf16[4,160,256]{2,1,0:T(8,128)(2,1)S(1)}, bf16[4,160,256]{2,1,0:T(8,128)(2,1)S(1)}, u32[]{:S(2)}, u32[]{:S(2)}) %collective-permute-start.7) | collective-permute-done | bytes 327712 | tf_op jit(solution)/shard_map/ppermute | solution.py:61
  163.7 0.3 collective-permute-start.12
  164.0 2.4 %collective-permute-done.9.refs_3_ = bf16[4,160,256]{2,1,0:T(8,128)(2,1)S(1)} collective-permute-done((bf16[4,160,256]{2,1,0:T(8,128)(2,1)S(1)}, bf16[4,160,256]{2,1,0:T(8,128)(2,1)S(1)}, u32[]{:S(2)}, u32[]{:S(2)}) %collective-permute-start.9) | collective-permute-done | bytes 327712 | tf_op jit(solution)/shard_map/ppermute | solution.py:61
  166.4 1.6 collective-permute-done.13.refs_7_
  168.0 5.8 %shard_map.161 = (bf16[128,64]{1,0:T(8,128)(2,1)S(1)}, bf16[128,64]{1,0:T(8,128)(2,1)S(1)}, bf16[128,64]{1,0:T(8,128)(2,1)S(1)}, bf16[128,64]{1,0:T(8,128)(2,1)S(1)}) custom-call(s32[5]{0:T(128)S(1)} %stack.23.where, bf16[256,128]{1,0:T(8,128)(2,1)S(1)} %get-tuple-element.16.b0.q0, bf16[256,128]{1,0:T(8,128)(2,1)S(1)} %collective-permute-done.3.b1.q1, ...), custom_call_target="tpu_custom_call" | custom-call | tf_op jit(solution)/shard_map/pallas_call | solution.py:45
  173.9 1.2 collective-permute-start.14
  175.1 2.3 %collective-permute-start.15 = (bf16[128,64]{1,0:T(8,128)(2,1)S(1)}, bf16[128,64]{1,0:T(8,128)(2,1)S(1)}, u32[]{:S(2)}, u32[]{:S(2)}) collective-permute-start(bf16[128,64]{1,0:T(8,128)(2,1)S(1)} %get-tuple-element.22), channel_id=1, source_target_pairs={{0,2},{1,3},{2,0},{3,1},{4,6},{5,7},{6,4},{7,5},{8,10},{9,11},{10,... | collective-permute-start | bytes 49160 | tf_op jit(solution)/shard_map/ppermute | solution.py:61
  177.4 0.5 collective-permute-start.16
  177.8 1.2 collective-permute-done.14.a1
  179.1 1.4 collective-permute-done.15.a2
  180.5 0.8 collective-permute-done.16.a3
  181.3 0.7 shard_map.162
  182.0 1.1 collective-permute-start.17
  183.1 4.2 %collective-permute-start.18 = (bf16[32,256]{1,0:T(8,128)(2,1)S(1)}, bf16[32,256]{1,0:T(8,128)(2,1)S(1)}, u32[]{:S(2)}, u32[]{:S(2)}) collective-permute-start(bf16[32,256]{1,0:T(8,128)(2,1)S(1)} %get-tuple-element.26), channel_id=1, source_target_pairs={{0,128},{64,192},{128,0},{192,64},{1,129},{65,193},{129,1},{193,65... | collective-permute-start | bytes 49160 | tf_op jit(solution)/shard_map/ppermute | solution.py:61
  187.3 0.6 collective-permute-done.17.a1
  187.9 2.8 %collective-permute-done.18.a2 = bf16[32,256]{1,0:T(8,128)(2,1)S(1)} collective-permute-done((bf16[32,256]{1,0:T(8,128)(2,1)S(1)}, bf16[32,256]{1,0:T(8,128)(2,1)S(1)}, u32[]{:S(2)}, u32[]{:S(2)}) %collective-permute-start.18) | collective-permute-done | bytes 16416 | tf_op jit(solution)/shard_map/ppermute | solution.py:61
  190.7 1.4 collective-permute-done.19.a3
  192.1 2.1 %shard_map.163 = bf16[32,2048]{1,0:T(8,128)(2,1)} custom-call(s32[5]{0:T(128)S(1)} %stack.23.where, bf16[32,256]{1,0:T(8,128)(2,1)S(1)} %get-tuple-element.24.a0, bf16[32,256]{1,0:T(8,128)(2,1)S(1)} %collective-permute-done.17.a1, bf16[32,256]{1,0:T(8,128)(2,1)S(1)} %collective-permute-done.18.a2, bf16[32,256]{1,0:T(8,128)(2,1)S(1)} %collective-permute-done.19.a3, ...), custom_call_target="tpu_custom_call" | custom-call | tf_op jit(solution)/shard_map/pallas_call | solution.py:45
  194.2 1.0 shard_map.170
  (38 shorter events, 1.5 us)
Async XLA Ops:
  0.6 74.3 %copy-start = (bf16[1,2048,256]{2,1,0:T(8,128)(2,1)S(1)}, bf16[1,2048,256]{2,1,0:T(8,128)(2,1)}, u32[]{:S(2)}) copy-start(bf16[1,2048,256]{2,1,0:T(8,128)(2,1)} %param.27) | copy-start | bytes 3145732
  0.6 74.3 %copy-start.1 = (bf16[1,2048,256]{2,1,0:T(8,128)(2,1)S(1)}, bf16[1,2048,256]{2,1,0:T(8,128)(2,1)}, u32[]{:S(2)}) copy-start(bf16[1,2048,256]{2,1,0:T(8,128)(2,1)} %param.28) | copy-start | bytes 3145732
  3.4 41.0 %all-to-all-start = ((bf16[64,4,2048]{2,1,0:T(4,128)(2,1)}), bf16[64,4,2048]{2,1,0:T(4,128)(2,1)}, u32[]{:S(2)}, u32[]{:S(2)}) async-start(bf16[64,4,2048]{2,1,0:T(4,128)(2,1)} %get-tuple-element.28), calls=%async_computation | async-start | bytes 2097152 | tf_op jit(solution)/shard_map/all_to_all | solution.py:178
  15.7 34.0 %collective-permute-start.30 = (bf16[256,2048]{1,0:T(8,128)(2,1)}, bf16[256,2048]{1,0:T(8,128)(2,1)S(1)}, u32[]{:S(2)}, u32[]{:S(2)}) collective-permute-start(bf16[256,2048]{1,0:T(8,128)(2,1)} %bitcast.21), channel_id=1, source_target_pairs={{0,1},{1,2},{2,3},{3,0},{4,5},{5,6},{6,7},{7,4},{8,9},{9,10},{10,1... | collective-permute-start | bytes 3145736 | tf_op jit(solution)/shard_map/ppermute | solution.py:61
  17.3 48.2 %collective-permute-start.29 = (bf16[256,2048]{1,0:T(8,128)(2,1)}, bf16[256,2048]{1,0:T(8,128)(2,1)}, u32[]{:S(2)}, u32[]{:S(2)}) collective-permute-start(bf16[256,2048]{1,0:T(8,128)(2,1)} %bitcast.22), channel_id=1, source_target_pairs={{0,3},{1,0},{2,1},{3,2},{4,7},{5,4},{6,5},{7,6},{8,11},{9,8},{10,9... | collective-permute-start | bytes 3145736 | tf_op jit(solution)/shard_map/ppermute | solution.py:61
  46.1 16.1 %collective-permute-start.20 = (bf16[32,4,2048]{2,1,0:T(4,128)(2,1)S(1)}, bf16[32,4,2048]{2,1,0:T(4,128)(2,1)S(1)}, u32[]{:S(2)}, u32[]{:S(2)}) collective-permute-start(bf16[32,4,2048]{2,1,0:T(4,128)(2,1)S(1)} %get-tuple-element.31.rows_a), channel_id=1, source_target_pairs={{0,1},{1,2},{2,3},{3,0},{4,5},{5,6},{6,7},{7,4},{8,9},{9,10},{10,1... | collective-permute-start | bytes 1572872 | tf_op jit(solution)/shard_map/ppermute | solution.py:61
  47.6 14.8 %collective-permute-start.24 = (bf16[32,4,2048]{2,1,0:T(4,128)(2,1)S(1)}, bf16[32,4,2048]{2,1,0:T(4,128)(2,1)S(1)}, u32[]{:S(2)}, u32[]{:S(2)}) collective-permute-start(bf16[32,4,2048]{2,1,0:T(4,128)(2,1)S(1)} %get-tuple-element.30.rows_b), channel_id=1, source_target_pairs={{0,3},{1,0},{2,1},{3,2},{4,7},{5,4},{6,5},{7,6},{8,11},{9,8},{10,9... | collective-permute-start | bytes 1572872 | tf_op jit(solution)/shard_map/ppermute | solution.py:61
  49.4 24.0 %collective-permute-start.21 = (bf16[32,4,2048]{2,1,0:T(4,128)(2,1)S(1)}, bf16[32,4,2048]{2,1,0:T(4,128)(2,1)S(1)}, u32[]{:S(2)}, u32[]{:S(2)}) collective-permute-start(bf16[32,4,2048]{2,1,0:T(4,128)(2,1)S(1)} %get-tuple-element.30.rows_b), channel_id=1, source_target_pairs={{0,1},{1,2},{2,3},{3,0},{4,5},{5,6},{6,7},{7,4},{8,9},{9,10},{10,1... | collective-permute-start | bytes 1572872 | tf_op jit(solution)/shard_map/ppermute | solution.py:61
  49.7 26.7 %collective-permute-start.27 = (bf16[32,4,2048]{2,1,0:T(4,128)(2,1)S(1)}, bf16[32,4,2048]{2,1,0:T(4,128)(2,1)S(1)}, u32[]{:S(2)}, u32[]{:S(2)}) collective-permute-start(bf16[32,4,2048]{2,1,0:T(4,128)(2,1)S(1)} %get-tuple-element.31.rows_a), channel_id=1, source_target_pairs={{0,3},{1,0},{2,1},{3,2},{4,7},{5,4},{6,5},{7,6},{8,11},{9,8},{10,9... | collective-permute-start | bytes 1572872 | tf_op jit(solution)/shard_map/ppermute | solution.py:61
  62.2 22.5 %collective-permute-start.23 = (bf16[32,4,2048]{2,1,0:T(4,128)(2,1)S(1)}, bf16[32,4,2048]{2,1,0:T(4,128)(2,1)S(1)}, u32[]{:S(2)}, u32[]{:S(2)}) collective-permute-start(bf16[32,4,2048]{2,1,0:T(4,128)(2,1)S(1)} %collective-permute-done.20.rows_a), channel_id=1, source_target_pairs={{0,1},{1,2},{2,3},{3,0},{4,5},{5,6},{6,7},{7,4},{8,9},{9,10},{10,1... | collective-permute-start | bytes 1572872 | tf_op jit(solution)/shard_map/ppermute | solution.py:61
  62.4 22.5 %collective-permute-start.25 = (bf16[32,4,2048]{2,1,0:T(4,128)(2,1)S(1)}, bf16[32,4,2048]{2,1,0:T(4,128)(2,1)S(1)}, u32[]{:S(2)}, u32[]{:S(2)}) collective-permute-start(bf16[32,4,2048]{2,1,0:T(4,128)(2,1)S(1)} %collective-permute-done.24.rows_b), channel_id=1, source_target_pairs={{0,3},{1,0},{2,1},{3,2},{4,7},{5,4},{6,5},{7,6},{8,11},{9,8},{10,9... | collective-permute-start | bytes 1572872 | tf_op jit(solution)/shard_map/ppermute | solution.py:61
  65.5 29.7 %collective-permute-start.31 = (bf16[128,2048]{1,0:T(8,128)(2,1)S(1)}, bf16[128,2048]{1,0:T(8,128)(2,1)S(1)}, u32[]{:S(2)}, u32[]{:S(2)}) collective-permute-start(bf16[128,2048]{1,0:T(8,128)(2,1)S(1)} %slice.18), channel_id=1, source_target_pairs={{0,1},{1,2},{2,3},{3,0},{4,5},{5,6},{6,7},{7,4},{8,9},{9,10},{10,1... | collective-permute-start | bytes 1572872 | tf_op jit(solution)/shard_map/ppermute | solution.py:61
  73.4 22.7 %collective-permute-start.32 = (bf16[128,2048]{1,0:T(8,128)(2,1)S(1)}, bf16[128,2048]{1,0:T(8,128)(2,1)S(1)}, u32[]{:S(2)}, u32[]{:S(2)}) collective-permute-start(bf16[128,2048]{1,0:T(8,128)(2,1)S(1)} %slice.19), channel_id=1, source_target_pairs={{0,3},{1,0},{2,1},{3,2},{4,7},{5,4},{6,5},{7,6},{8,11},{9,8},{10,9... | collective-permute-start | bytes 1572872 | tf_op jit(solution)/shard_map/ppermute | solution.py:61
  76.3 24.1 %copy-start.3 = (bf16[1,256,2048]{2,1,0:T(8,128)(2,1)S(1)}, bf16[1,256,2048]{2,1,0:T(8,128)(2,1)}, u32[]{:S(2)}) copy-start(bf16[1,256,2048]{2,1,0:T(8,128)(2,1)} %param.29) | copy-start | bytes 3145732
  76.3 22.3 %collective-permute-start.22 = (bf16[256,256]{1,0:T(8,128)(2,1)S(1)}, bf16[256,256]{1,0:T(8,128)(2,1)S(1)}, u32[]{:S(2)}, u32[]{:S(2)}) collective-permute-start(bf16[256,256]{1,0:T(8,128)(2,1)S(1)} %shard_map.166), channel_id=1, source_target_pairs={{0,3},{1,0},{2,1},{3,2},{4,7},{5,4},{6,5},{7,6},{8,11},{9,8},{10,9... | collective-permute-start | bytes 393224 | tf_op jit(solution)/shard_map/ppermute | solution.py:61
  84.6 14.1 %collective-permute-start.28 = (bf16[256,256]{1,0:T(8,128)(2,1)S(1)}, bf16[256,256]{1,0:T(8,128)(2,1)S(1)}, u32[]{:S(2)}, u32[]{:S(2)}) collective-permute-start(bf16[256,256]{1,0:T(8,128)(2,1)S(1)} %shard_map.168), channel_id=1, source_target_pairs={{0,1},{1,2},{2,3},{3,0},{4,5},{5,6},{6,7},{7,4},{8,9},{9,10},{10,1... | collective-permute-start | bytes 393224 | tf_op jit(solution)/shard_map/ppermute | solution.py:61
  86.3 14.1 %collective-permute-start.26 = (bf16[256,256]{1,0:T(8,128)(2,1)S(1)}, bf16[256,256]{1,0:T(8,128)(2,1)S(1)}, u32[]{:S(2)}, u32[]{:S(2)}) collective-permute-start(bf16[256,256]{1,0:T(8,128)(2,1)S(1)} %shard_map.167), channel_id=1, source_target_pairs={{0,2},{1,3},{2,0},{3,1},{4,6},{5,7},{6,4},{7,5},{8,10},{9,11},{10,... | collective-permute-start | bytes 393224 | tf_op jit(solution)/shard_map/ppermute | solution.py:61
  104.2 90.0 %all-to-all-start.1 = ((bf16[64,4,2048]{2,1,0:T(4,128)(2,1)}), bf16[64,4,2048]{2,1,0:T(4,128)(2,1)S(1)}, u32[]{:S(2)}, u32[]{:S(2)}) async-start(bf16[64,4,2048]{2,1,0:T(4,128)(2,1)} %shard_map.169), calls=%async_computation.1 | async-start | bytes 2097152 | tf_op jit(solution)/shard_map/all_to_all | solution.py:195
  111.8 5.4 %collective-permute-start = (bf16[32,544]{1,0:T(8,128)(2,1)S(1)}, bf16[32,544]{1,0:T(8,128)(2,1)S(1)}, u32[]{:S(2)}, u32[]{:S(2)}) collective-permute-start(bf16[32,544]{1,0:T(8,128)(2,1)S(1)} %shard_map.158.l0), channel_id=1, source_target_pairs={{0,1},{1,2},{2,3},{3,0},{4,5},{5,6},{6,7},{7,4},{8,9},{9,10},{10,1... | collective-permute-start | bytes 104456 | tf_op jit(solution)/shard_map/ppermute | solution.py:61
  113.1 5.5 %collective-permute-start.1 = (bf16[32,544]{1,0:T(8,128)(2,1)S(1)}, bf16[32,544]{1,0:T(8,128)(2,1)S(1)}, u32[]{:S(2)}, u32[]{:S(2)}) collective-permute-start(bf16[32,544]{1,0:T(8,128)(2,1)S(1)} %shard_map.158.l0), channel_id=1, source_target_pairs={{0,2},{1,3},{2,0},{3,1},{4,6},{5,7},{6,4},{7,5},{8,10},{9,11},{10,... | collective-permute-start | bytes 104456 | tf_op jit(solution)/shard_map/ppermute | solution.py:61
  115.4 4.0 %collective-permute-start.2 = (bf16[32,544]{1,0:T(8,128)(2,1)S(1)}, bf16[32,544]{1,0:T(8,128)(2,1)S(1)}, u32[]{:S(2)}, u32[]{:S(2)}) collective-permute-start(bf16[32,544]{1,0:T(8,128)(2,1)S(1)} %shard_map.158.l0), channel_id=1, source_target_pairs={{0,3},{1,0},{2,1},{3,2},{4,7},{5,4},{6,5},{7,6},{8,11},{9,8},{10,9... | collective-permute-start | bytes 104456 | tf_op jit(solution)/shard_map/ppermute | solution.py:61
  116.0 76.0 %copy-start.2 = (bf16[1024,2048]{1,0:T(8,128)(2,1)S(1)}, bf16[1024,2048]{1,0:T(8,128)(2,1)}, u32[]{:S(2)}) copy-start(bf16[1024,2048]{1,0:T(8,128)(2,1)} %out_proj.1) | copy-start | bytes 12582916
  120.8 20.5 %collective-permute-start.3 = (bf16[256,128]{1,0:T(8,128)(2,1)S(1)}, bf16[256,128]{1,0:T(8,128)(2,1)S(1)}, u32[]{:S(2)}, u32[]{:S(2)}) collective-permute-start(bf16[256,128]{1,0:T(8,128)(2,1)S(1)} %get-tuple-element.17), channel_id=1, source_target_pairs={{0,64},{64,128},{128,192},{192,0},{1,65},{65,129},{129,193},{193,1... | collective-permute-start | bytes 196616 | tf_op jit(solution)/shard_map/ppermute | solution.py:61
  123.2 21.8 %collective-permute-start.4 = (bf16[256,128]{1,0:T(8,128)(2,1)S(1)}, bf16[256,128]{1,0:T(8,128)(2,1)S(1)}, u32[]{:S(2)}, u32[]{:S(2)}) collective-permute-start(bf16[256,128]{1,0:T(8,128)(2,1)S(1)} %get-tuple-element.18), channel_id=1, source_target_pairs={{0,128},{64,192},{128,0},{192,64},{1,129},{65,193},{129,1},{193,65... | collective-permute-start | bytes 196616 | tf_op jit(solution)/shard_map/ppermute | solution.py:61
  127.0 18.0 %collective-permute-start.5 = (bf16[256,128]{1,0:T(8,128)(2,1)S(1)}, bf16[256,128]{1,0:T(8,128)(2,1)S(1)}, u32[]{:S(2)}, u32[]{:S(2)}) collective-permute-start(bf16[256,128]{1,0:T(8,128)(2,1)S(1)} %get-tuple-element.19), channel_id=1, source_target_pairs={{0,192},{64,0},{128,64},{192,128},{1,193},{65,1},{129,65},{193,129... | collective-permute-start | bytes 196616 | tf_op jit(solution)/shard_map/ppermute | solution.py:61
  145.1 5.4 %collective-permute-start.6 = (bf16[4,160,128]{2,1,0:T(8,128)(2,1)S(1)}, bf16[4,160,128]{2,1,0:T(8,128)(2,1)S(1)}, u32[]{:S(2)}, u32[]{:S(2)}) collective-permute-start(bf16[4,160,128]{2,1,0:T(8,128)(2,1)S(1)} %shard_map.160), channel_id=1, source_target_pairs={{0,32},{32,0},{1,33},{33,1},{2,34},{34,2},{3,35},{35,3},{4,36},{36... | collective-permute-start | bytes 491528 | tf_op jit(solution)/shard_map/ppermute | solution.py:61
  150.5 13.0 %collective-permute-start.7 = (bf16[4,160,256]{2,1,0:T(8,128)(2,1)S(1)}, bf16[4,160,256]{2,1,0:T(8,128)(2,1)S(1)}, u32[]{:S(2)}, u32[]{:S(2)}) collective-permute-start(bf16[4,160,256]{2,1,0:T(8,128)(2,1)S(1)} %pad_maximum_fusion.refs_0_), channel_id=1, source_target_pairs={{0,8},{8,16},{16,24},{24,0},{1,9},{9,17},{17,25},{25,1},{2,10},{10... | collective-permute-start | bytes 983048 | tf_op jit(solution)/shard_map/ppermute | solution.py:61
  152.1 11.6 %collective-permute-start.8 = (bf16[4,160,256]{2,1,0:T(8,128)(2,1)S(1)}, bf16[4,160,256]{2,1,0:T(8,128)(2,1)S(1)}, u32[]{:S(2)}, u32[]{:S(2)}) collective-permute-start(bf16[4,160,256]{2,1,0:T(8,128)(2,1)S(1)} %pad_maximum_fusion.refs_0_), channel_id=1, source_target_pairs={{0,16},{8,24},{16,0},{24,8},{1,17},{9,25},{17,1},{25,9},{2,18},{10... | collective-permute-start | bytes 983048 | tf_op jit(solution)/shard_map/ppermute | solution.py:61
  153.2 13.2 %collective-permute-start.9 = (bf16[4,160,256]{2,1,0:T(8,128)(2,1)S(1)}, bf16[4,160,256]{2,1,0:T(8,128)(2,1)S(1)}, u32[]{:S(2)}, u32[]{:S(2)}) collective-permute-start(bf16[4,160,256]{2,1,0:T(8,128)(2,1)S(1)} %pad_maximum_fusion.refs_0_), channel_id=1, source_target_pairs={{0,24},{8,0},{16,8},{24,16},{1,25},{9,1},{17,9},{25,17},{2,26},{10... | collective-permute-start | bytes 983048 | tf_op jit(solution)/shard_map/ppermute | solution.py:61
  155.3 11.1 %collective-permute-start.10 = (bf16[4,160,256]{2,1,0:T(8,128)(2,1)S(1)}, bf16[4,160,256]{2,1,0:T(8,128)(2,1)S(1)}, u32[]{:S(2)}, u32[]{:S(2)}) collective-permute-start(bf16[4,160,256]{2,1,0:T(8,128)(2,1)S(1)} %pad_maximum_fusion.refs_0_), channel_id=1, source_target_pairs={{0,4},{4,0},{1,5},{5,1},{2,6},{6,2},{3,7},{7,3},{8,12},{12,8},{9,1... | collective-permute-start | bytes 983048 | tf_op jit(solution)/shard_map/ppermute | solution.py:61
  163.5 2.9 %collective-permute-start.11 = (bf16[4,160,256]{2,1,0:T(8,128)(2,1)S(1)}, bf16[4,160,256]{2,1,0:T(8,128)(2,1)S(1)}, u32[]{:S(2)}, u32[]{:S(2)}) collective-permute-start(bf16[4,160,256]{2,1,0:T(8,128)(2,1)S(1)} %collective-permute-done.7.refs_1_), channel_id=1, source_target_pairs={{0,4},{4,0},{1,5},{5,1},{2,6},{6,2},{3,7},{7,3},{8,12},{12,8},{9,1... | collective-permute-start | bytes 983048 | tf_op jit(solution)/shard_map/ppermute | solution.py:61
  163.7 2.7 %collective-permute-start.12 = (bf16[4,160,256]{2,1,0:T(8,128)(2,1)S(1)}, bf16[4,160,256]{2,1,0:T(8,128)(2,1)S(1)}, u32[]{:S(2)}, u32[]{:S(2)}) collective-permute-start(bf16[4,160,256]{2,1,0:T(8,128)(2,1)S(1)} %collective-permute-done.8.refs_2_), channel_id=1, source_target_pairs={{0,4},{4,0},{1,5},{5,1},{2,6},{6,2},{3,7},{7,3},{8,12},{12,8},{9,1... | collective-permute-start | bytes 983048 | tf_op jit(solution)/shard_map/ppermute | solution.py:61
  166.4 1.6 collective-permute-start.13
  173.9 5.2 %collective-permute-start.14 = (bf16[128,64]{1,0:T(8,128)(2,1)S(1)}, bf16[128,64]{1,0:T(8,128)(2,1)S(1)}, u32[]{:S(2)}, u32[]{:S(2)}) collective-permute-start(bf16[128,64]{1,0:T(8,128)(2,1)S(1)} %get-tuple-element.21), channel_id=1, source_target_pairs={{0,1},{1,2},{2,3},{3,0},{4,5},{5,6},{6,7},{7,4},{8,9},{9,10},{10,1... | collective-permute-start | bytes 49160 | tf_op jit(solution)/shard_map/ppermute | solution.py:61
  175.1 5.4 %collective-permute-start.15 = (bf16[128,64]{1,0:T(8,128)(2,1)S(1)}, bf16[128,64]{1,0:T(8,128)(2,1)S(1)}, u32[]{:S(2)}, u32[]{:S(2)}) collective-permute-start(bf16[128,64]{1,0:T(8,128)(2,1)S(1)} %get-tuple-element.22), channel_id=1, source_target_pairs={{0,2},{1,3},{2,0},{3,1},{4,6},{5,7},{6,4},{7,5},{8,10},{9,11},{10,... | collective-permute-start | bytes 49160 | tf_op jit(solution)/shard_map/ppermute | solution.py:61
  177.4 3.9 %collective-permute-start.16 = (bf16[128,64]{1,0:T(8,128)(2,1)S(1)}, bf16[128,64]{1,0:T(8,128)(2,1)S(1)}, u32[]{:S(2)}, u32[]{:S(2)}) collective-permute-start(bf16[128,64]{1,0:T(8,128)(2,1)S(1)} %get-tuple-element.23), channel_id=1, source_target_pairs={{0,3},{1,0},{2,1},{3,2},{4,7},{5,4},{6,5},{7,6},{8,11},{9,8},{10,9... | collective-permute-start | bytes 49160 | tf_op jit(solution)/shard_map/ppermute | solution.py:61
  182.0 5.9 %collective-permute-start.17 = (bf16[32,256]{1,0:T(8,128)(2,1)S(1)}, bf16[32,256]{1,0:T(8,128)(2,1)S(1)}, u32[]{:S(2)}, u32[]{:S(2)}) collective-permute-start(bf16[32,256]{1,0:T(8,128)(2,1)S(1)} %get-tuple-element.25), channel_id=1, source_target_pairs={{0,64},{64,128},{128,192},{192,0},{1,65},{65,129},{129,193},{193,1... | collective-permute-start | bytes 49160 | tf_op jit(solution)/shard_map/ppermute | solution.py:61
  183.1 7.6 %collective-permute-start.18 = (bf16[32,256]{1,0:T(8,128)(2,1)S(1)}, bf16[32,256]{1,0:T(8,128)(2,1)S(1)}, u32[]{:S(2)}, u32[]{:S(2)}) collective-permute-start(bf16[32,256]{1,0:T(8,128)(2,1)S(1)} %get-tuple-element.26), channel_id=1, source_target_pairs={{0,128},{64,192},{128,0},{192,64},{1,129},{65,193},{129,1},{193,65... | collective-permute-start | bytes 49160 | tf_op jit(solution)/shard_map/ppermute | solution.py:61
  187.3 4.8 %collective-permute-start.19 = (bf16[32,256]{1,0:T(8,128)(2,1)S(1)}, bf16[32,256]{1,0:T(8,128)(2,1)S(1)}, u32[]{:S(2)}, u32[]{:S(2)}) collective-permute-start(bf16[32,256]{1,0:T(8,128)(2,1)S(1)} %get-tuple-element.27), channel_id=1, source_target_pairs={{0,192},{64,0},{128,64},{192,128},{1,193},{65,1},{129,65},{193,129... | collective-permute-start | bytes 49160 | tf_op jit(solution)/shard_map/ppermute | solution.py:61

commit v10 on v9

--- a/solution.py
+++ b/solution.py
@@ -28,7 +28,7 @@
 VMEM_SPEC = pl.BlockSpec(memory_space=pltpu.VMEM)
 
 
-def call(kernel, out_shape, arrays, where=None, scratch=(), limit=8 << 20, unplaced=(), place=True):
+def call(kernel, out_shape, arrays, where=None, scratch=(), limit=8 << 20, unplaced=(), place=pltpu.VMEM):
     arrays = [
         pltpu.with_memory_space_constraint(a, pltpu.HBM if i in unplaced else pltpu.VMEM)
         for i, a in enumerate(arrays)
@@ -37,11 +37,11 @@
     if where is not None:
         arrays, specs = [where] + arrays, [SMEM_SPEC] + specs
     single = not isinstance(out_shape, (list, tuple))
-    if place:
+    if place is not None:
         if single:
-            out_shape = pltpu.VMEM(out_shape.shape, out_shape.dtype)
+            out_shape = place(out_shape.shape, out_shape.dtype)
         else:
-            out_shape = [pltpu.VMEM(s.shape, s.dtype) for s in out_shape]
+            out_shape = [place(s.shape, s.dtype) for s in out_shape]
     return pl.pallas_call(
         kernel,
         in_specs=specs,
@@ -59,6 +59,19 @@
 def shifted(value, axis, amount):
     n = lax.axis_size(axis)
     return lax.ppermute(value, axis, [(i, (i + amount) % n) for i in range(n)])
+
+
+def paired(value, mate):
+    n = lax.axis_size("x")
+    return lax.ppermute(value, "x", [(i, mate(i)) for i in range(n)])
+
+
+def weight_mate(i):
+    return i ^ 1
+
+
+def row_mate(i):
+    return 3 - i
 
 
 def trig(positions):
@@ -108,38 +121,39 @@
         ),
         [tokens, gain[None, :], routes.T, group_prob[None, :], expert_prob.T],
         unplaced=range(5),
-    )
-
-
-def hidden_kernel(rows_a, rows_b, w_gate, w_up, out, gate_s, up_s):
-    half, span = out.shape[0] // 2, 512
+        place=pltpu.HBM,
+    )
+
+
+def hidden_kernel(rows, gate_a, up_a, gate_b, up_b, out, gate_s, up_s):
+    count, span, units = out.shape[0], 1024, gate_a.shape[1]
     gate_s[...] = jnp.zeros(gate_s.shape, F32)
     up_s[...] = jnp.zeros(up_s.shape, F32)
 
     def add(step, _):
         cols = pl.ds(pl.multiple_of(step * span, span), span)
-        for at, rows in ((0, rows_a), (half, rows_b)):
-            got = rows[:, :, cols].reshape(half, span)
-            gate_s[at : at + half, :] += mm(got, w_gate[cols, :])
-            up_s[at : at + half, :] += mm(got, w_up[cols, :])
+        got = rows[:, :, cols].reshape(count, span)
+        for at, gate, up in ((0, gate_a, up_a), (units, gate_b, up_b)):
+            gate_s[:, at : at + units] += mm(got, gate[cols, :])
+            up_s[:, at : at + units] += mm(got, up[cols, :])
         return 0
 
-    lax.fori_loop(0, w_gate.shape[0] // span, add, 0)
+    lax.fori_loop(0, gate_a.shape[0] // span, add, 0)
     gate = gate_s[...]
     out[...] = (gate / (1.0 + jnp.exp(-gate)) * up_s[...]).astype(BF)
 
 
-def hidden_of(rows_a, rows_b, w_gate, w_up):
-    shape = jax.ShapeDtypeStruct((2 * rows_a.shape[0] * CAP, w_gate.shape[1]), BF)
+def hidden_of(rows, weights):
+    shape = jax.ShapeDtypeStruct((rows.shape[0] * CAP, 2 * weights[0].shape[1]), BF)
     scratch = [pltpu.VMEM(shape.shape, F32)] * 2
-    return call(hidden_kernel, shape, [rows_a, rows_b, w_gate, w_up], scratch=scratch)
-
-
-def down_kernel(h0, h1, h2, h3, w0, w1, w2a, w2b, w3, out):
-    half = w2a.shape[0]
-    total = mm(h0[...], w0[...]) + mm(h1[...], w1[...]) + mm(h3[...], w3[...])
-    total = total + mm(h2[:, :half], w2a[...]) + mm(h2[:, half:], w2b[...])
-    out[...] = total.reshape(out.shape).astype(BF)
+    return call(hidden_kernel, shape, [rows] + weights, scratch=scratch)
+
+
+def down_kernel(own, mate, w0, w1, w2, w3, out):
+    units = w0.shape[0]
+    total = mm(own[:, :units], w0[...]) + mm(own[:, units:], w1[...])
+    total = total + mm(mate[:, :units], w2[...]) + mm(mate[:, units:], w3[...])
+    out[...] = total.astype(BF).reshape(out.shape)
 
 
 def combine_kernel(returned, shares, out):
@@ -170,32 +184,24 @@
     experts = lax.axis_size(EP)
     rows, width = tokens.shape
     w_gate, w_up, w_down = w_gate[0], w_up[0], w_down[0]
-    down_left, down_right = shifted(w_down, "x", 1), shifted(w_down, "x", -1)
-    units = w_down.shape[0] // 2
-    cut_a, cut_b = down_left[:units], down_right[units:]
-    down_far = [shifted(cut_a, "x", 1), shifted(cut_b, "x", -1)]
+    down_w, down_r = paired(w_down, weight_mate), paired(w_down, row_mate)
+    down_rw = paired(down_w, row_mate)
+    gate_w, up_w = paired(w_gate, weight_mate), paired(w_up, weight_mate)
+    weights = [w_gate, w_up, gate_w, up_w]
     outgoing, shares = dispatch(tokens, moe_gain, routes, group_prob, expert_prob, experts)
     arrived = lax.all_to_all(outgoing, EP, split_axis=0, concat_axis=0, tiled=True)
     queries, pair = query_and_pair(where, query, latent, rope_key, latent_gain, key_up, value_up)
-    half = experts // 2
-    a, b = arrived[:half], arrived[half:]
-    left_a, right_b = shifted(a, "x", 1), shifted(b, "x", -1)
-    left_b, right_a = shifted(b, "x", 1), shifted(a, "x", -1)
-    far_a, far_b = shifted(left_a, "x", 1), shifted(right_b, "x", -1)
+    mate_rows = paired(arrived, row_mate)
     parts = attend(where, queries, pair)
-    hidden = [
-        hidden_of(a, b, w_gate, w_up),
-        shifted(hidden_of(left_a, left_b, w_gate, w_up), "x", -1),
-        shifted(hidden_of(far_a, far_b, w_gate, w_up), "x", 2),
-        shifted(hidden_of(right_a, right_b, w_gate, w_up), "x", 1),
-    ]
+    mate_hidden = paired(hidden_of(mate_rows, weights), row_mate)
+    own_hidden = hidden_of(arrived, weights)
     shape = jax.ShapeDtypeStruct((experts, CAP, width), BF)
-    down = [w_down, down_right] + down_far + [down_left]
-    result = call(down_kernel, shape, hidden + down)
+    arrays = [own_hidden, mate_hidden, w_down, down_w, down_r, down_rw]
+    result = call(down_kernel, shape, arrays, place=pltpu.HBM)
     returned = lax.all_to_all(result, EP, split_axis=0, concat_axis=0, tiled=True)
     mixed = project(where, parts, out_proj, latent.shape[0])
     shape = jax.ShapeDtypeStruct((rows, width), BF)
-    return mixed, call(combine_kernel, shape, [returned, shares], place=False)
+    return mixed, call(combine_kernel, shape, [returned, shares], place=None)
 
 
 def latent_kernel(latent, gain, rope_key, cosine, sine, out):
@@ -315,11 +321,15 @@
         out[...] = parts[lax.rem(where[0] + j, 4)]
 
 
-def project_kernel(where, a0, a1, a2, a3, out_proj, out, parts):
-    for j, a in enumerate((a0, a1, a2, a3)):
-        parts[lax.rem(where[0] - j + 4, 4)] = a[...]
-    pieces = [parts[h % 4, :, h // 4 * V_DIM : (h // 4 + 1) * V_DIM] for h in range(16)]
-    out[...] = mm(jnp.concatenate(pieces, axis=1), out_proj[...]).astype(BF)
+def project_kernel(where, a0, a1, a2, a3, out_proj, out, parts, rows):
+    @pl.when(pl.program_id(0) == 0)
+    def _():
+        for j, a in enumerate((a0, a1, a2, a3)):
+            parts[lax.rem(where[0] - j + 4, 4)] = a[...]
+        pieces = [parts[h % 4, :, h // 4 * V_DIM : (h // 4 + 1) * V_DIM] for h in range(16)]
+        rows[...] = jnp.concatenate(pieces, axis=1)
+
+    out[...] = mm(rows[...], out_proj[...]).astype(BF)
 
 
 def query_and_pair(where, query, latent, rope_key, latent_gain, key_up, value_up):
@@ -387,14 +397,22 @@
         [pltpu.VMEM((4, strip, V_DIM), BF), pltpu.VMEM((4, own, 4 * V_DIM), BF)],
     )
     parts = [parts[0]] + [shifted(parts[j], "zh", j) for j in range(1, 4)]
-    return call(
+    height, width = out_proj.shape
+    span = width // 4
+    built = pl.pallas_call(
         project_kernel,
-        jax.ShapeDtypeStruct((own, out_proj.shape[1]), BF),
-        parts + [out_proj],
-        where,
-        [pltpu.VMEM((4, own, 4 * V_DIM), BF)],
-        place=False,
-    )
+        grid=(4,),
+        in_specs=[SMEM_SPEC]
+        + [VMEM_SPEC] * 4
+        + [pl.BlockSpec((height, span), lambda i: (0, i))],
+        out_specs=pl.BlockSpec((own, span), lambda i: (0, i)),
+        out_shape=jax.ShapeDtypeStruct((own, width), BF),
+        scratch_shapes=[pltpu.VMEM((4, own, 4 * V_DIM), BF), pltpu.VMEM((own, height), BF)],
+        compiler_params=pltpu.CompilerParams(vmem_limit_bytes=8 << 20),
+        name="project",
+    )
+    parts = [pltpu.with_memory_space_constraint(a, pltpu.VMEM) for a in parts]
+    return built(where, *parts, pltpu.with_memory_space_constraint(out_proj, pltpu.HBM))
 
 
 def body(

time: 196 us -> 218 us (1.11)
  the two profiles are of different devices: /device:TPU:8 before, /device:TPU:224 now
where the time goes in v10:
time: 218 us; the launch traced here: 214 us
  waiting for transfers between devices  127 us (58%)
  starting transfers between devices  59.3 us (27%)
  Pallas kernels  23.7 us (11%)
  local copies, waits for them, and re-layouts  2.55 us (1%)
    ppermute x7, waiting for transfers between devices, paired(): return lax.ppermute(value, 'x', [(i, mate(i)) for i in range(n)])  62.4 us
    ppermute x20, waiting for transfers between devices, shifted(): return lax.ppermute(value, axis, [(i, (i + amount) % n) for i in range(n)])  41.4 us
    ppermute x20, starting transfers between devices, shifted(): return lax.ppermute(value, axis, [(i, (i + amount) % n) for i in range(n)])  30.5 us
    all_to_all x1, waiting for transfers between devices, both_halves(): lax.all_to_all(outgoing, EP, split_axis=0, concat_axis=0, tiled=True)  23.3 us
    pallas_call x10, Pallas kernels, call(): pl.pallas_call(kernel, in_specs=specs, out_specs=VMEM_SPEC if single else...  19.2 us
    ppermute x7, starting transfers between devices, paired(): return lax.ppermute(value, 'x', [(i, mate(i)) for i in range(n)])  12.4 us
    all_to_all x1, starting transfers between devices, both_halves(): lax.all_to_all(outgoing, EP, split_axis=0, concat_axis=0, tiled=True)  9.3 us
    all_to_all x1, starting transfers between devices, both_halves(): lax.all_to_all(result, EP, split_axis=0, concat_axis=0, tiled=True)  7.09 us
  transfers between devices with their start and end apart: 29, of which 20 were waited for; matrix products, arithmetic and copies ran while one was open for 0% of the time, Pallas kernels for 8%

profile of v10, /device:TPU:224, one launch (start us, length us, event | category | flops | bytes accessed | tf_op | source)
XLA Modules:
  0.0 213.8 jit_solution(5057274166309080251)
XLA Ops:
  0.6 2.6 %shard_map.163 = (bf16[64,4,2048]{2,1,0:T(4,128)(2,1)}, bf16[256,128]{1,0:T(8,128)(2,1)}) custom-call(bf16[64,2048]{1,0:T(8,128)(2,1)} %tokens.1, f32[1,2048]{1,0:T(1,128)} %bitcast.22, s32[2,64]{1,0:T(2,128)} %bitcast.24, f32[1,64]{1,0:T(1,128)} %bitcast.26, f32[2,64]{1,0:T(2,128)} %bitcast.25), custom_call_target="tpu_custom_call" | custom-call | tf_op jit(solution)/shard_map/pallas_call | solution.py:45
  3.3 9.3 %all-to-all-start = ((bf16[64,4,2048]{2,1,0:T(4,128)(2,1)}), bf16[64,4,2048]{2,1,0:T(4,128)(2,1)S(1)}, u32[]{:S(2)}, u32[]{:S(2)}) async-start(bf16[64,4,2048]{2,1,0:T(4,128)(2,1)} %get-tuple-element.28), calls=%async_computation | async-start | bytes 2097152 | tf_op jit(solution)/shard_map/all_to_all | solution.py:192
  12.6 1.6 collective-permute-start.24
  14.1 0.5 collective-permute-start.20
  14.7 1.5 collective-permute-start.21
  16.2 23.3 %all-to-all-done.rows = bf16[64,4,2048]{2,1,0:T(4,128)(2,1)S(1)} async-done(((bf16[64,4,2048]{2,1,0:T(4,128)(2,1)}), bf16[64,4,2048]{2,1,0:T(4,128)(2,1)S(1)}, u32[]{:S(2)}, u32[]{:S(2)}) %all-to-all-start) | async-done | bytes 1048608 | tf_op jit(solution)/shard_map/all_to_all | solution.py:192
  39.5 2.8 %collective-permute-start.22 = (bf16[64,4,2048]{2,1,0:T(4,128)(2,1)S(1)}, bf16[64,4,2048]{2,1,0:T(4,128)(2,1)S(1)}, u32[]{:S(2)}, u32[]{:S(2)}) collective-permute-start(bf16[64,4,2048]{2,1,0:T(4,128)(2,1)S(1)} %all-to-all-done.rows), channel_id=1, source_target_pairs={{0,3},{1,2},{2,1},{3,0},{4,7},{5,6},{6,5},{7,4},{8,11},{9,10},{10,... | collective-permute-start | bytes 3145736 | tf_op jit(solution)/shard_map/ppermute | solution.py:66
  42.2 0.5 collective-permute-start.25
  42.7 0.0 collective-permute-done.24.w1
  42.7 2.8 %collective-permute-start.26 = (bf16[256,2048]{1,0:T(8,128)(2,1)}, bf16[256,2048]{1,0:T(8,128)(2,1)S(1)}, u32[]{:S(2)}, u32[]{:S(2)}) collective-permute-start(bf16[256,2048]{1,0:T(8,128)(2,1)} %collective-permute-done.24.w1), channel_id=1, source_target_pairs={{0,3},{1,2},{2,1},{3,0},{4,7},{5,6},{6,5},{7,4},{8,11},{9,10},{10,... | collective-permute-start | bytes 3145736 | tf_op jit(solution)/shard_map/ppermute | solution.py:66
  45.5 15.9 %collective-permute-done.20.gate_b = bf16[2048,256]{1,0:T(8,128)(2,1)S(1)} collective-permute-done((bf16[2048,256]{1,0:T(8,128)(2,1)}, bf16[2048,256]{1,0:T(8,128)(2,1)S(1)}, u32[]{:S(2)}, u32[]{:S(2)}) %collective-permute-start.20) | collective-permute-done | bytes 1048608 | tf_op jit(solution)/shard_map/ppermute | solution.py:66
  61.4 21.6 %collective-permute-done.21.up_b = bf16[2048,256]{1,0:T(8,128)(2,1)S(1)} collective-permute-done((bf16[2048,256]{1,0:T(8,128)(2,1)}, bf16[2048,256]{1,0:T(8,128)(2,1)S(1)}, u32[]{:S(2)}, u32[]{:S(2)}) %collective-permute-start.21) | collective-permute-done | bytes 1048608 | tf_op jit(solution)/shard_map/ppermute | solution.py:66
  83.0 0.0 collective-permute-done.22.rows
  83.0 1.2 copy-done
  84.2 1.2 copy-done.1
  85.4 1.7 shard_map.165
  87.1 2.8 %collective-permute-start.23 = (bf16[256,512]{1,0:T(8,128)(2,1)S(1)}, bf16[256,512]{1,0:T(8,128)(2,1)S(1)}, u32[]{:S(2)}, u32[]{:S(2)}) collective-permute-start(bf16[256,512]{1,0:T(8,128)(2,1)S(1)} %shard_map.165), channel_id=1, source_target_pairs={{0,3},{1,2},{2,1},{3,0},{4,7},{5,6},{6,5},{7,4},{8,11},{9,10},{10,... | collective-permute-start | bytes 786440 | tf_op jit(solution)/shard_map/ppermute | solution.py:66
  90.0 1.7 shard_map.164.own
  91.6 20.0 %collective-permute-done.26.w3 = bf16[256,2048]{1,0:T(8,128)(2,1)S(1)} collective-permute-done((bf16[256,2048]{1,0:T(8,128)(2,1)}, bf16[256,2048]{1,0:T(8,128)(2,1)S(1)}, u32[]{:S(2)}, u32[]{:S(2)}) %collective-permute-start.26) | collective-permute-done | bytes 1048608 | tf_op jit(solution)/shard_map/ppermute | solution.py:66
  111.7 4.9 %collective-permute-done.23.mate = bf16[256,512]{1,0:T(8,128)(2,1)S(1)} collective-permute-done((bf16[256,512]{1,0:T(8,128)(2,1)S(1)}, bf16[256,512]{1,0:T(8,128)(2,1)S(1)}, u32[]{:S(2)}, u32[]{:S(2)}) %collective-permute-start.23) | collective-permute-done | bytes 262176 | tf_op jit(solution)/shard_map/ppermute | solution.py:66
  116.5 3.5 %shard_map.166 = bf16[64,4,2048]{2,1,0:T(4,128)(2,1)} custom-call(bf16[256,512]{1,0:T(8,128)(2,1)S(1)} %shard_map.164.own, bf16[256,512]{1,0:T(8,128)(2,1)S(1)} %collective-permute-done.23.mate, bf16[256,2048]{1,0:T(8,128)(2,1)S(1)} %bitcast.21, bf16[256,2048]{1,0:T(8,128)(2,1)} %collective-permute-done.24.w1, ...), custom_call_target="tpu_custom_call" | custom-call | tf_op jit(solution)/shard_map/pallas_call | solution.py:45
  120.0 7.1 %all-to-all-start.1 = ((bf16[64,4,2048]{2,1,0:T(4,128)(2,1)}), bf16[64,4,2048]{2,1,0:T(4,128)(2,1)S(1)}, u32[]{:S(2)}, u32[]{:S(2)}) async-start(bf16[64,4,2048]{2,1,0:T(4,128)(2,1)} %shard_map.166), calls=%async_computation.1 | async-start | bytes 2097152 | tf_op jit(solution)/shard_map/all_to_all | solution.py:201
  127.2 0.1 multiply_sine_fusion
  127.3 0.1 pad_maximum_fusion.1
  127.4 0.9 shard_map.158.l0
  128.3 0.4 collective-permute-start
  128.6 3.9 %collective-permute-start.1 = (bf16[32,544]{1,0:T(8,128)(2,1)S(1)}, bf16[32,544]{1,0:T(8,128)(2,1)S(1)}, u32[]{:S(2)}, u32[]{:S(2)}) collective-permute-start(bf16[32,544]{1,0:T(8,128)(2,1)S(1)} %shard_map.158.l0), channel_id=1, source_target_pairs={{0,2},{1,3},{2,0},{3,1},{4,6},{5,7},{6,4},{7,5},{8,10},{9,11},{10,... | collective-permute-start | bytes 104456 | tf_op jit(solution)/shard_map/ppermute | solution.py:61
  132.6 0.2 collective-permute-start.2
  132.8 0.1 multiply_sine_fusion.1
  132.9 0.1 stack.23.where
  133.0 0.6 collective-permute-done.l1
  133.6 1.5 collective-permute-done.1.l2
  135.0 1.6 collective-permute-done.2.l3
  136.6 1.4 shard_map.159
  138.0 1.4 collective-permute-start.3
  139.5 4.6 %collective-permute-start.4 = (bf16[256,128]{1,0:T(8,128)(2,1)S(1)}, bf16[256,128]{1,0:T(8,128)(2,1)S(1)}, u32[]{:S(2)}, u32[]{:S(2)}) collective-permute-start(bf16[256,128]{1,0:T(8,128)(2,1)S(1)} %get-tuple-element.18), channel_id=1, source_target_pairs={{0,128},{64,192},{128,0},{192,64},{1,129},{65,193},{129,1},{193,65... | collective-permute-start | bytes 196616 | tf_op jit(solution)/shard_map/ppermute | solution.py:61
  144.1 0.1 collective-permute-start.5
  144.2 11.8 %collective-permute-done.3.b1.q1 = bf16[256,128]{1,0:T(8,128)(2,1)S(1)} collective-permute-done((bf16[256,128]{1,0:T(8,128)(2,1)S(1)}, bf16[256,128]{1,0:T(8,128)(2,1)S(1)}, u32[]{:S(2)}, u32[]{:S(2)}) %collective-permute-start.3) | collective-permute-done | bytes 65568 | tf_op jit(solution)/shard_map/ppermute | solution.py:61
  156.0 1.2 collective-permute-done.5.b3.q3
  157.2 2.5 %collective-permute-start.6 = (bf16[4,160,128]{2,1,0:T(8,128)(2,1)S(1)}, bf16[4,160,128]{2,1,0:T(8,128)(2,1)S(1)}, u32[]{:S(2)}, u32[]{:S(2)}) collective-permute-start(bf16[4,160,128]{2,1,0:T(8,128)(2,1)S(1)} %shard_map.160), channel_id=1, source_target_pairs={{0,32},{32,0},{1,33},{33,1},{2,34},{34,2},{3,35},{35,3},{4,36},{36... | collective-permute-start | bytes 491528 | tf_op jit(solution)/shard_map/ppermute | solution.py:61
  159.7 4.1 %collective-permute-done.6 = bf16[4,160,128]{2,1,0:T(8,128)(2,1)S(1)} collective-permute-done((bf16[4,160,128]{2,1,0:T(8,128)(2,1)S(1)}, bf16[4,160,128]{2,1,0:T(8,128)(2,1)S(1)}, u32[]{:S(2)}, u32[]{:S(2)}) %collective-permute-start.6) | collective-permute-done | bytes 163872 | tf_op jit(solution)/shard_map/ppermute | solution.py:61
  163.8 1.6 collective-permute-start.7
  165.4 2.8 %collective-permute-start.8 = (bf16[4,160,256]{2,1,0:T(8,128)(2,1)S(1)}, bf16[4,160,256]{2,1,0:T(8,128)(2,1)S(1)}, u32[]{:S(2)}, u32[]{:S(2)}) collective-permute-start(bf16[4,160,256]{2,1,0:T(8,128)(2,1)S(1)} %pad_maximum_fusion.refs_0_), channel_id=1, source_target_pairs={{0,16},{8,24},{16,0},{24,8},{1,17},{9,25},{17,1},{25,9},{2,18},{10... | collective-permute-start | bytes 983048 | tf_op jit(solution)/shard_map/ppermute | solution.py:61
  168.2 1.4 collective-permute-start.9
  169.6 4.8 %collective-permute-done.7.refs_1_ = bf16[4,160,256]{2,1,0:T(8,128)(2,1)S(1)} collective-permute-done((bf16[4,160,256]{2,1,0:T(8,128)(2,1)S(1)}, bf16[4,160,256]{2,1,0:T(8,128)(2,1)S(1)}, u32[]{:S(2)}, u32[]{:S(2)}) %collective-permute-start.7) | collective-permute-done | bytes 327712 | tf_op jit(solution)/shard_map/ppermute | solution.py:61
  174.4 7.7 %collective-permute-done.8.refs_2_ = bf16[4,160,256]{2,1,0:T(8,128)(2,1)S(1)} collective-permute-done((bf16[4,160,256]{2,1,0:T(8,128)(2,1)S(1)}, bf16[4,160,256]{2,1,0:T(8,128)(2,1)S(1)}, u32[]{:S(2)}, u32[]{:S(2)}) %collective-permute-start.8) | collective-permute-done | bytes 327712 | tf_op jit(solution)/shard_map/ppermute | solution.py:61
  182.1 0.5 collective-permute-start.13
  182.6 1.1 collective-permute-done.12.refs_6_
  183.7 0.5 collective-permute-done.13.refs_7_
  184.2 5.8 %shard_map.161 = (bf16[128,64]{1,0:T(8,128)(2,1)S(1)}, bf16[128,64]{1,0:T(8,128)(2,1)S(1)}, bf16[128,64]{1,0:T(8,128)(2,1)S(1)}, bf16[128,64]{1,0:T(8,128)(2,1)S(1)}) custom-call(s32[5]{0:T(128)S(1)} %stack.23.where, bf16[256,128]{1,0:T(8,128)(2,1)S(1)} %get-tuple-element.16.b0.q0, bf16[256,128]{1,0:T(8,128)(2,1)S(1)} %collective-permute-done.3.b1.q1, ...), custom_call_target="tpu_custom_call" | custom-call | tf_op jit(solution)/shard_map/pallas_call | solution.py:45
  190.0 0.4 collective-permute-start.14
  190.4 3.9 %collective-permute-start.15 = (bf16[128,64]{1,0:T(8,128)(2,1)S(1)}, bf16[128,64]{1,0:T(8,128)(2,1)S(1)}, u32[]{:S(2)}, u32[]{:S(2)}) collective-permute-start(bf16[128,64]{1,0:T(8,128)(2,1)S(1)} %get-tuple-element.22), channel_id=1, source_target_pairs={{0,2},{1,3},{2,0},{3,1},{4,6},{5,7},{6,4},{7,5},{8,10},{9,11},{10,... | collective-permute-start | bytes 49160 | tf_op jit(solution)/shard_map/ppermute | solution.py:61
  194.3 0.2 collective-permute-start.16
  194.5 0.7 collective-permute-done.14.a1
  195.2 1.3 collective-permute-done.15.a2
  196.5 1.7 collective-permute-done.16.a3
  198.2 0.7 shard_map.162
  198.9 1.2 collective-permute-start.17
  200.1 2.4 %collective-permute-start.18 = (bf16[32,256]{1,0:T(8,128)(2,1)S(1)}, bf16[32,256]{1,0:T(8,128)(2,1)S(1)}, u32[]{:S(2)}, u32[]{:S(2)}) collective-permute-start(bf16[32,256]{1,0:T(8,128)(2,1)S(1)} %get-tuple-element.26), channel_id=1, source_target_pairs={{0,128},{64,192},{128,0},{192,64},{1,129},{65,193},{129,1},{193,65... | collective-permute-start | bytes 49160 | tf_op jit(solution)/shard_map/ppermute | solution.py:61
  202.5 2.8 %collective-permute-start.19 = (bf16[32,256]{1,0:T(8,128)(2,1)S(1)}, bf16[32,256]{1,0:T(8,128)(2,1)S(1)}, u32[]{:S(2)}, u32[]{:S(2)}) collective-permute-start(bf16[32,256]{1,0:T(8,128)(2,1)S(1)} %get-tuple-element.27), channel_id=1, source_target_pairs={{0,192},{64,0},{128,64},{192,128},{1,193},{65,1},{129,65},{193,129... | collective-permute-start | bytes 49160 | tf_op jit(solution)/shard_map/ppermute | solution.py:61
  205.3 2.5 %collective-permute-done.18.a2 = bf16[32,256]{1,0:T(8,128)(2,1)S(1)} collective-permute-done((bf16[32,256]{1,0:T(8,128)(2,1)S(1)}, bf16[32,256]{1,0:T(8,128)(2,1)S(1)}, u32[]{:S(2)}, u32[]{:S(2)}) %collective-permute-start.18) | collective-permute-done | bytes 16416 | tf_op jit(solution)/shard_map/ppermute | solution.py:61
  207.8 0.6 collective-permute-done.19.a3
  208.3 4.5 %project.1 = bf16[32,2048]{1,0:T(8,128)(2,1)} custom-call(s32[5]{0:T(128)S(1)} %stack.23.where, bf16[32,256]{1,0:T(8,128)(2,1)S(1)} %get-tuple-element.24.a0, bf16[32,256]{1,0:T(8,128)(2,1)S(1)} %collective-permute-done.17.a1, bf16[32,256]{1,0:T(8,128)(2,1)S(1)} %collective-permute-done.18.a2, bf16[32,256]{1,0:T(8,128)(2,1)S(1)} %collective-permute-done.19.a3, ...), custom_call_target="tpu_custom_call" | custom-call | tf_op jit(solution)/shard_map/project/pallas_call | solution.py:415
  212.8 1.0 shard_map.167
  (21 shorter events, 0.1 us)
Async XLA Ops:
  3.3 36.2 %all-to-all-start = ((bf16[64,4,2048]{2,1,0:T(4,128)(2,1)}), bf16[64,4,2048]{2,1,0:T(4,128)(2,1)S(1)}, u32[]{:S(2)}, u32[]{:S(2)}) async-start(bf16[64,4,2048]{2,1,0:T(4,128)(2,1)} %get-tuple-element.28), calls=%async_computation | async-start | bytes 2097152 | tf_op jit(solution)/shard_map/all_to_all | solution.py:192
  12.6 30.2 %collective-permute-start.24 = (bf16[256,2048]{1,0:T(8,128)(2,1)}, bf16[256,2048]{1,0:T(8,128)(2,1)}, u32[]{:S(2)}, u32[]{:S(2)}) collective-permute-start(bf16[256,2048]{1,0:T(8,128)(2,1)} %bitcast.19), channel_id=1, source_target_pairs={{0,1},{1,0},{2,3},{3,2},{4,5},{5,4},{6,7},{7,6},{8,9},{9,8},{10,11... | collective-permute-start | bytes 3145736 | tf_op jit(solution)/shard_map/ppermute | solution.py:66
  14.1 47.2 %collective-permute-start.20 = (bf16[2048,256]{1,0:T(8,128)(2,1)}, bf16[2048,256]{1,0:T(8,128)(2,1)S(1)}, u32[]{:S(2)}, u32[]{:S(2)}) collective-permute-start(bf16[2048,256]{1,0:T(8,128)(2,1)} %bitcast.13), channel_id=1, source_target_pairs={{0,1},{1,0},{2,3},{3,2},{4,5},{5,4},{6,7},{7,6},{8,9},{9,8},{10,11... | collective-permute-start | bytes 3145736 | tf_op jit(solution)/shard_map/ppermute | solution.py:66
  14.7 68.3 %collective-permute-start.21 = (bf16[2048,256]{1,0:T(8,128)(2,1)}, bf16[2048,256]{1,0:T(8,128)(2,1)S(1)}, u32[]{:S(2)}, u32[]{:S(2)}) collective-permute-start(bf16[2048,256]{1,0:T(8,128)(2,1)} %bitcast.16), channel_id=1, source_target_pairs={{0,1},{1,0},{2,3},{3,2},{4,5},{5,4},{6,7},{7,6},{8,9},{9,8},{10,11... | collective-permute-start | bytes 3145736 | tf_op jit(solution)/shard_map/ppermute | solution.py:66
  39.5 43.5 %collective-permute-start.22 = (bf16[64,4,2048]{2,1,0:T(4,128)(2,1)S(1)}, bf16[64,4,2048]{2,1,0:T(4,128)(2,1)S(1)}, u32[]{:S(2)}, u32[]{:S(2)}) collective-permute-start(bf16[64,4,2048]{2,1,0:T(4,128)(2,1)S(1)} %all-to-all-done.rows), channel_id=1, source_target_pairs={{0,3},{1,2},{2,1},{3,0},{4,7},{5,6},{6,5},{7,4},{8,11},{9,10},{10,... | collective-permute-start | bytes 3145736 | tf_op jit(solution)/shard_map/ppermute | solution.py:66
  42.2 49.4 %collective-permute-start.25 = (bf16[256,2048]{1,0:T(8,128)(2,1)}, bf16[256,2048]{1,0:T(8,128)(2,1)S(1)}, u32[]{:S(2)}, u32[]{:S(2)}) collective-permute-start(bf16[256,2048]{1,0:T(8,128)(2,1)} %bitcast.20), channel_id=1, source_target_pairs={{0,3},{1,2},{2,1},{3,0},{4,7},{5,6},{6,5},{7,4},{8,11},{9,10},{10,... | collective-permute-start | bytes 3145736 | tf_op jit(solution)/shard_map/ppermute | solution.py:66
  42.7 68.9 %collective-permute-start.26 = (bf16[256,2048]{1,0:T(8,128)(2,1)}, bf16[256,2048]{1,0:T(8,128)(2,1)S(1)}, u32[]{:S(2)}, u32[]{:S(2)}) collective-permute-start(bf16[256,2048]{1,0:T(8,128)(2,1)} %collective-permute-done.24.w1), channel_id=1, source_target_pairs={{0,3},{1,2},{2,1},{3,0},{4,7},{5,6},{6,5},{7,4},{8,11},{9,10},{10,... | collective-permute-start | bytes 3145736 | tf_op jit(solution)/shard_map/ppermute | solution.py:66
  83.0 1.2 copy-start
  84.2 1.2 copy-start.1
  85.4 31.1 %copy-start.2 = (bf16[1,256,2048]{2,1,0:T(8,128)(2,1)S(1)}, bf16[1,256,2048]{2,1,0:T(8,128)(2,1)}, u32[]{:S(2)}) copy-start(bf16[1,256,2048]{2,1,0:T(8,128)(2,1)} %param.29) | copy-start | bytes 3145732
  87.1 29.4 %collective-permute-start.23 = (bf16[256,512]{1,0:T(8,128)(2,1)S(1)}, bf16[256,512]{1,0:T(8,128)(2,1)S(1)}, u32[]{:S(2)}, u32[]{:S(2)}) collective-permute-start(bf16[256,512]{1,0:T(8,128)(2,1)S(1)} %shard_map.165), channel_id=1, source_target_pairs={{0,3},{1,2},{2,1},{3,0},{4,7},{5,6},{6,5},{7,4},{8,11},{9,10},{10,... | collective-permute-start | bytes 786440 | tf_op jit(solution)/shard_map/ppermute | solution.py:66
  120.0 92.8 %all-to-all-start.1 = ((bf16[64,4,2048]{2,1,0:T(4,128)(2,1)}), bf16[64,4,2048]{2,1,0:T(4,128)(2,1)S(1)}, u32[]{:S(2)}, u32[]{:S(2)}) async-start(bf16[64,4,2048]{2,1,0:T(4,128)(2,1)} %shard_map.166), calls=%async_computation.1 | async-start | bytes 2097152 | tf_op jit(solution)/shard_map/all_to_all | solution.py:201
  128.3 5.3 %collective-permute-start = (bf16[32,544]{1,0:T(8,128)(2,1)S(1)}, bf16[32,544]{1,0:T(8,128)(2,1)S(1)}, u32[]{:S(2)}, u32[]{:S(2)}) collective-permute-start(bf16[32,544]{1,0:T(8,128)(2,1)S(1)} %shard_map.158.l0), channel_id=1, source_target_pairs={{0,1},{1,2},{2,3},{3,0},{4,5},{5,6},{6,7},{7,4},{8,9},{9,10},{10,1... | collective-permute-start | bytes 104456 | tf_op jit(solution)/shard_map/ppermute | solution.py:61
  128.6 6.4 %collective-permute-start.1 = (bf16[32,544]{1,0:T(8,128)(2,1)S(1)}, bf16[32,544]{1,0:T(8,128)(2,1)S(1)}, u32[]{:S(2)}, u32[]{:S(2)}) collective-permute-start(bf16[32,544]{1,0:T(8,128)(2,1)S(1)} %shard_map.158.l0), channel_id=1, source_target_pairs={{0,2},{1,3},{2,0},{3,1},{4,6},{5,7},{6,4},{7,5},{8,10},{9,11},{10,... | collective-permute-start | bytes 104456 | tf_op jit(solution)/shard_map/ppermute | solution.py:61
  132.6 4.0 %collective-permute-start.2 = (bf16[32,544]{1,0:T(8,128)(2,1)S(1)}, bf16[32,544]{1,0:T(8,128)(2,1)S(1)}, u32[]{:S(2)}, u32[]{:S(2)}) collective-permute-start(bf16[32,544]{1,0:T(8,128)(2,1)S(1)} %shard_map.158.l0), channel_id=1, source_target_pairs={{0,3},{1,0},{2,1},{3,2},{4,7},{5,4},{6,5},{7,6},{8,11},{9,8},{10,9... | collective-permute-start | bytes 104456 | tf_op jit(solution)/shard_map/ppermute | solution.py:61
  138.0 18.0 %collective-permute-start.3 = (bf16[256,128]{1,0:T(8,128)(2,1)S(1)}, bf16[256,128]{1,0:T(8,128)(2,1)S(1)}, u32[]{:S(2)}, u32[]{:S(2)}) collective-permute-start(bf16[256,128]{1,0:T(8,128)(2,1)S(1)} %get-tuple-element.17), channel_id=1, source_target_pairs={{0,64},{64,128},{128,192},{192,0},{1,65},{65,129},{129,193},{193,1... | collective-permute-start | bytes 196616 | tf_op jit(solution)/shard_map/ppermute | solution.py:61
  139.5 16.5 %collective-permute-start.4 = (bf16[256,128]{1,0:T(8,128)(2,1)S(1)}, bf16[256,128]{1,0:T(8,128)(2,1)S(1)}, u32[]{:S(2)}, u32[]{:S(2)}) collective-permute-start(bf16[256,128]{1,0:T(8,128)(2,1)S(1)} %get-tuple-element.18), channel_id=1, source_target_pairs={{0,128},{64,192},{128,0},{192,64},{1,129},{65,193},{129,1},{193,65... | collective-permute-start | bytes 196616 | tf_op jit(solution)/shard_map/ppermute | solution.py:61
  144.1 13.1 %collective-permute-start.5 = (bf16[256,128]{1,0:T(8,128)(2,1)S(1)}, bf16[256,128]{1,0:T(8,128)(2,1)S(1)}, u32[]{:S(2)}, u32[]{:S(2)}) collective-permute-start(bf16[256,128]{1,0:T(8,128)(2,1)S(1)} %get-tuple-element.19), channel_id=1, source_target_pairs={{0,192},{64,0},{128,64},{192,128},{1,193},{65,1},{129,65},{193,129... | collective-permute-start | bytes 196616 | tf_op jit(solution)/shard_map/ppermute | solution.py:61
  157.2 55.6 %copy-start.3 = (bf16[256,128]{1,0:T(8,128)(2,1)S(1)}, bf16[256,128]{1,0:T(8,128)(2,1)}, u32[]{:S(2)}) copy-start(bf16[256,128]{1,0:T(8,128)(2,1)} %get-tuple-element.29.shares) | copy-start | bytes 196612
  157.2 6.5 %collective-permute-start.6 = (bf16[4,160,128]{2,1,0:T(8,128)(2,1)S(1)}, bf16[4,160,128]{2,1,0:T(8,128)(2,1)S(1)}, u32[]{:S(2)}, u32[]{:S(2)}) collective-permute-start(bf16[4,160,128]{2,1,0:T(8,128)(2,1)S(1)} %shard_map.160), channel_id=1, source_target_pairs={{0,32},{32,0},{1,33},{33,1},{2,34},{34,2},{3,35},{35,3},{4,36},{36... | collective-permute-start | bytes 491528 | tf_op jit(solution)/shard_map/ppermute | solution.py:61
  163.8 10.6 %collective-permute-start.7 = (bf16[4,160,256]{2,1,0:T(8,128)(2,1)S(1)}, bf16[4,160,256]{2,1,0:T(8,128)(2,1)S(1)}, u32[]{:S(2)}, u32[]{:S(2)}) collective-permute-start(bf16[4,160,256]{2,1,0:T(8,128)(2,1)S(1)} %pad_maximum_fusion.refs_0_), channel_id=1, source_target_pairs={{0,8},{8,16},{16,24},{24,0},{1,9},{9,17},{17,25},{25,1},{2,10},{10... | collective-permute-start | bytes 983048 | tf_op jit(solution)/shard_map/ppermute | solution.py:61
  165.4 16.7 %collective-permute-start.8 = (bf16[4,160,256]{2,1,0:T(8,128)(2,1)S(1)}, bf16[4,160,256]{2,1,0:T(8,128)(2,1)S(1)}, u32[]{:S(2)}, u32[]{:S(2)}) collective-permute-start(bf16[4,160,256]{2,1,0:T(8,128)(2,1)S(1)} %pad_maximum_fusion.refs_0_), channel_id=1, source_target_pairs={{0,16},{8,24},{16,0},{24,8},{1,17},{9,25},{17,1},{25,9},{2,18},{10... | collective-permute-start | bytes 983048 | tf_op jit(solution)/shard_map/ppermute | solution.py:61
  168.2 13.9 %collective-permute-start.9 = (bf16[4,160,256]{2,1,0:T(8,128)(2,1)S(1)}, bf16[4,160,256]{2,1,0:T(8,128)(2,1)S(1)}, u32[]{:S(2)}, u32[]{:S(2)}) collective-permute-start(bf16[4,160,256]{2,1,0:T(8,128)(2,1)S(1)} %pad_maximum_fusion.refs_0_), channel_id=1, source_target_pairs={{0,24},{8,0},{16,8},{24,16},{1,25},{9,1},{17,9},{25,17},{2,26},{10... | collective-permute-start | bytes 983048 | tf_op jit(solution)/shard_map/ppermute | solution.py:61
  169.6 13.0 %collective-permute-start.10 = (bf16[4,160,256]{2,1,0:T(8,128)(2,1)S(1)}, bf16[4,160,256]{2,1,0:T(8,128)(2,1)S(1)}, u32[]{:S(2)}, u32[]{:S(2)}) collective-permute-start(bf16[4,160,256]{2,1,0:T(8,128)(2,1)S(1)} %pad_maximum_fusion.refs_0_), channel_id=1, source_target_pairs={{0,4},{4,0},{1,5},{5,1},{2,6},{6,2},{3,7},{7,3},{8,12},{12,8},{9,1... | collective-permute-start | bytes 983048 | tf_op jit(solution)/shard_map/ppermute | solution.py:61
  174.4 8.2 %collective-permute-start.11 = (bf16[4,160,256]{2,1,0:T(8,128)(2,1)S(1)}, bf16[4,160,256]{2,1,0:T(8,128)(2,1)S(1)}, u32[]{:S(2)}, u32[]{:S(2)}) collective-permute-start(bf16[4,160,256]{2,1,0:T(8,128)(2,1)S(1)} %collective-permute-done.7.refs_1_), channel_id=1, source_target_pairs={{0,4},{4,0},{1,5},{5,1},{2,6},{6,2},{3,7},{7,3},{8,12},{12,8},{9,1... | collective-permute-start | bytes 983048 | tf_op jit(solution)/shard_map/ppermute | solution.py:61
  182.1 1.6 collective-permute-start.12
  182.1 2.1 collective-permute-start.13
  190.0 5.2 %collective-permute-start.14 = (bf16[128,64]{1,0:T(8,128)(2,1)S(1)}, bf16[128,64]{1,0:T(8,128)(2,1)S(1)}, u32[]{:S(2)}, u32[]{:S(2)}) collective-permute-start(bf16[128,64]{1,0:T(8,128)(2,1)S(1)} %get-tuple-element.21), channel_id=1, source_target_pairs={{0,1},{1,2},{2,3},{3,0},{4,5},{5,6},{6,7},{7,4},{8,9},{9,10},{10,1... | collective-permute-start | bytes 49160 | tf_op jit(solution)/shard_map/ppermute | solution.py:61
  190.4 6.2 %collective-permute-start.15 = (bf16[128,64]{1,0:T(8,128)(2,1)S(1)}, bf16[128,64]{1,0:T(8,128)(2,1)S(1)}, u32[]{:S(2)}, u32[]{:S(2)}) collective-permute-start(bf16[128,64]{1,0:T(8,128)(2,1)S(1)} %get-tuple-element.22), channel_id=1, source_target_pairs={{0,2},{1,3},{2,0},{3,1},{4,6},{5,7},{6,4},{7,5},{8,10},{9,11},{10,... | collective-permute-start | bytes 49160 | tf_op jit(solution)/shard_map/ppermute | solution.py:61
  194.3 3.9 %collective-permute-start.16 = (bf16[128,64]{1,0:T(8,128)(2,1)S(1)}, bf16[128,64]{1,0:T(8,128)(2,1)S(1)}, u32[]{:S(2)}, u32[]{:S(2)}) collective-permute-start(bf16[128,64]{1,0:T(8,128)(2,1)S(1)} %get-tuple-element.23), channel_id=1, source_target_pairs={{0,3},{1,0},{2,1},{3,2},{4,7},{5,4},{6,5},{7,6},{8,11},{9,8},{10,9... | collective-permute-start | bytes 49160 | tf_op jit(solution)/shard_map/ppermute | solution.py:61
  198.9 6.4 %collective-permute-start.17 = (bf16[32,256]{1,0:T(8,128)(2,1)S(1)}, bf16[32,256]{1,0:T(8,128)(2,1)S(1)}, u32[]{:S(2)}, u32[]{:S(2)}) collective-permute-start(bf16[32,256]{1,0:T(8,128)(2,1)S(1)} %get-tuple-element.25), channel_id=1, source_target_pairs={{0,64},{64,128},{128,192},{192,0},{1,65},{65,129},{129,193},{193,1... | collective-permute-start | bytes 49160 | tf_op jit(solution)/shard_map/ppermute | solution.py:61
  200.1 7.6 %collective-permute-start.18 = (bf16[32,256]{1,0:T(8,128)(2,1)S(1)}, bf16[32,256]{1,0:T(8,128)(2,1)S(1)}, u32[]{:S(2)}, u32[]{:S(2)}) collective-permute-start(bf16[32,256]{1,0:T(8,128)(2,1)S(1)} %get-tuple-element.26), channel_id=1, source_target_pairs={{0,128},{64,192},{128,0},{192,64},{1,129},{65,193},{129,1},{193,65... | collective-permute-start | bytes 49160 | tf_op jit(solution)/shard_map/ppermute | solution.py:61
  202.5 5.8 %collective-permute-start.19 = (bf16[32,256]{1,0:T(8,128)(2,1)S(1)}, bf16[32,256]{1,0:T(8,128)(2,1)S(1)}, u32[]{:S(2)}, u32[]{:S(2)}) collective-permute-start(bf16[32,256]{1,0:T(8,128)(2,1)S(1)} %get-tuple-element.27), channel_id=1, source_target_pairs={{0,192},{64,0},{128,64},{192,128},{1,193},{65,1},{129,65},{193,129... | collective-permute-start | bytes 49160 | tf_op jit(solution)/shard_map/ppermute | solution.py:61

commit v11 on v6

--- a/solution.py
+++ b/solution.py
@@ -28,7 +28,7 @@
 VMEM_SPEC = pl.BlockSpec(memory_space=pltpu.VMEM)
 
 
-def call(kernel, out_shape, arrays, where=None, scratch=(), limit=8 << 20, unplaced=(), place=True):
+def call(kernel, out_shape, arrays, where=None, scratch=(), limit=8 << 20, unplaced=(), place=pltpu.VMEM):
     arrays = [
         pltpu.with_memory_space_constraint(a, pltpu.HBM if i in unplaced else pltpu.VMEM)
         for i, a in enumerate(arrays)
@@ -37,11 +37,11 @@
     if where is not None:
         arrays, specs = [where] + arrays, [SMEM_SPEC] + specs
     single = not isinstance(out_shape, (list, tuple))
-    if place:
+    if place is not None:
         if single:
-            out_shape = pltpu.VMEM(out_shape.shape, out_shape.dtype)
+            out_shape = place(out_shape.shape, out_shape.dtype)
         else:
-            out_shape = [pltpu.VMEM(s.shape, s.dtype) for s in out_shape]
+            out_shape = [place(s.shape, s.dtype) for s in out_shape]
     return pl.pallas_call(
         kernel,
         in_specs=specs,
@@ -59,6 +59,19 @@
 def shifted(value, axis, amount):
     n = lax.axis_size(axis)
     return lax.ppermute(value, axis, [(i, (i + amount) % n) for i in range(n)])
+
+
+def paired(value, mate):
+    n = lax.axis_size("x")
+    return lax.ppermute(value, "x", [(i, mate(i)) for i in range(n)])
+
+
+def weight_mate(i):
+    return i ^ 1
+
+
+def row_mate(i):
+    return 3 - i
 
 
 def trig(positions):
@@ -108,20 +121,20 @@
         ),
         [tokens, gain[None, :], routes.T, group_prob[None, :], expert_prob.T],
         unplaced=range(5),
-    )
-
-
-def hidden_kernel(rows_a, rows_b, w_gate, w_up, out, gate_s, up_s):
-    half, span = out.shape[0] // 2, 512
+        place=pltpu.HBM,
+    )
+
+
+def hidden_kernel(rows, w_gate, w_up, out, gate_s, up_s):
+    count, span = out.shape[0], 1024
     gate_s[...] = jnp.zeros(gate_s.shape, F32)
     up_s[...] = jnp.zeros(up_s.shape, F32)
 
     def add(step, _):
         cols = pl.ds(pl.multiple_of(step * span, span), span)
-        for at, rows in ((0, rows_a), (half, rows_b)):
-            got = rows[:, :, cols].reshape(half, span)
-            gate_s[at : at + half, :] += mm(got, w_gate[cols, :])
-            up_s[at : at + half, :] += mm(got, w_up[cols, :])
+        got = rows[:, :, cols].reshape(count, span)
+        gate_s[...] += mm(got, w_gate[cols, :])
+        up_s[...] += mm(got, w_up[cols, :])
         return 0
 
     lax.fori_loop(0, w_gate.shape[0] // span, add, 0)
@@ -129,17 +142,21 @@
     out[...] = (gate / (1.0 + jnp.exp(-gate)) * up_s[...]).astype(BF)
 
 
-def hidden_of(rows_a, rows_b, w_gate, w_up):
-    shape = jax.ShapeDtypeStruct((2 * rows_a.shape[0] * CAP, w_gate.shape[1]), BF)
+def hidden_of(rows, weights):
+    shape = jax.ShapeDtypeStruct((rows.shape[0] * CAP, weights[0].shape[1]), BF)
     scratch = [pltpu.VMEM(shape.shape, F32)] * 2
-    return call(hidden_kernel, shape, [rows_a, rows_b, w_gate, w_up], scratch=scratch)
-
-
-def down_kernel(h0, h1, h2, h3, w0, w1, w2a, w2b, w3, out):
-    half = w2a.shape[0]
-    total = mm(h0[...], w0[...]) + mm(h1[...], w1[...]) + mm(h3[...], w3[...])
-    total = total + mm(h2[:, :half], w2a[...]) + mm(h2[:, half:], w2b[...])
-    out[...] = total.reshape(out.shape).astype(BF)
+    return call(hidden_kernel, shape, [rows] + weights, scratch=scratch)
+
+
+def stage_kernel(w0, w1, w2, w3, out):
+    for k, piece in enumerate((w0, w1, w2, w3)):
+        out[k] = piece[...]
+
+
+def down_kernel(h0, h1, h2, h3, weights, out):
+    total = mm(h0[...], weights[0]) + mm(h1[...], weights[1])
+    total = total + mm(h2[...], weights[2]) + mm(h3[...], weights[3])
+    out[...] = total.astype(BF).reshape(out.shape)
 
 
 def combine_kernel(returned, shares, out):
@@ -170,32 +187,28 @@
     experts = lax.axis_size(EP)
     rows, width = tokens.shape
     w_gate, w_up, w_down = w_gate[0], w_up[0], w_down[0]
-    down_left, down_right = shifted(w_down, "x", 1), shifted(w_down, "x", -1)
-    units = w_down.shape[0] // 2
-    cut_a, cut_b = down_left[:units], down_right[units:]
-    down_far = [shifted(cut_a, "x", 1), shifted(cut_b, "x", -1)]
+    down_w, down_r = paired(w_down, weight_mate), paired(w_down, row_mate)
+    down_rw = paired(down_w, row_mate)
+    gate_w, up_w = paired(w_gate, weight_mate), paired(w_up, weight_mate)
+    set_a, set_b = [w_gate, w_up], [gate_w, up_w]
     outgoing, shares = dispatch(tokens, moe_gain, routes, group_prob, expert_prob, experts)
     arrived = lax.all_to_all(outgoing, EP, split_axis=0, concat_axis=0, tiled=True)
     queries, pair = query_and_pair(where, query, latent, rope_key, latent_gain, key_up, value_up)
-    half = experts // 2
-    a, b = arrived[:half], arrived[half:]
-    left_a, right_b = shifted(a, "x", 1), shifted(b, "x", -1)
-    left_b, right_a = shifted(b, "x", 1), shifted(a, "x", -1)
-    far_a, far_b = shifted(left_a, "x", 1), shifted(right_b, "x", -1)
+    mate_rows = paired(arrived, row_mate)
     parts = attend(where, queries, pair)
-    hidden = [
-        hidden_of(a, b, w_gate, w_up),
-        shifted(hidden_of(left_a, left_b, w_gate, w_up), "x", -1),
-        shifted(hidden_of(far_a, far_b, w_gate, w_up), "x", 2),
-        shifted(hidden_of(right_a, right_b, w_gate, w_up), "x", 1),
-    ]
+    own_a = hidden_of(arrived, set_a)
+    mate_a = paired(hidden_of(mate_rows, set_a), row_mate)
+    mate_b = paired(hidden_of(mate_rows, set_b), row_mate)
+    own_b = hidden_of(arrived, set_b)
+    shape = jax.ShapeDtypeStruct((4, *w_down.shape), BF)
+    down = call(stage_kernel, shape, [w_down, down_w, down_r, down_rw], unplaced=range(4))
     shape = jax.ShapeDtypeStruct((experts, CAP, width), BF)
-    down = [w_down, down_right] + down_far + [down_left]
-    result = call(down_kernel, shape, hidden + down)
+    arrays = [own_a, own_b, mate_a, mate_b, down]
+    result = call(down_kernel, shape, arrays, place=pltpu.HBM)
     returned = lax.all_to_all(result, EP, split_axis=0, concat_axis=0, tiled=True)
     mixed = project(where, parts, out_proj, latent.shape[0])
     shape = jax.ShapeDtypeStruct((rows, width), BF)
-    return mixed, call(combine_kernel, shape, [returned, shares], place=False)
+    return mixed, call(combine_kernel, shape, [returned, shares], place=None)
 
 
 def latent_kernel(latent, gain, rope_key, cosine, sine, out):
@@ -394,7 +407,7 @@
         parts + [out_proj],
         where,
         [pltpu.VMEM((4, own, 4 * V_DIM), BF)],
-        place=False,
+        place=None,
     )
 
 

time: 197 us -> 216 us (1.096)
  waiting for transfers between devices: 100 us -> 124 us
  starting transfers between devices: 68.7 us -> 64.1 us
    ppermute x0 -> x8, waiting for transfers between devices: none -> 55.8 us  [paired(): return lax.ppermute(value, 'x', [(i, mate(i)) for i in range(n)])]
    ppermute x33 -> x20, waiting for transfers between devices: 75.5 us -> 41.6 us  [shifted(): return lax.ppermute(value, axis, [(i, (i + amount) % n) for i in range(n)])]
    ppermute x33 -> x20, starting transfers between devices: 50.8 us -> 33.1 us  [shifted(): return lax.ppermute(value, axis, [(i, (i + amount) % n) for i in range(n)])]
    ppermute x0 -> x8, starting transfers between devices: none -> 13 us  [paired(): return lax.ppermute(value, 'x', [(i, mate(i)) for i in range(n)])]
    unnamed x8 -> x16, local copies, waits for them, and re-layouts: 0.02 us -> 3.44 us
    slice x3 -> x0, local copies, waits for them, and re-layouts: 2.79 us -> none  [the longest x1 1.67 us: both_halves(): a, b = (arrived[:half], arrived[half:])]
    pallas_call x13 -> x14, Pallas kernels: 23.9 us -> 23.1 us  [call(): pl.pallas_call(kernel, in_specs=specs, out_specs=VMEM_SPEC if single else...]
  transfers between devices with their start and end apart: 35 -> 30, of which waited for: 23 -> 20; matrix products, arithmetic and copies ran while one was open for 2% -> 0% of each run, Pallas kernels for 8% -> 8%
where the time goes in v11:
time: 216 us
  waiting for transfers between devices  124 us (57%)
  starting transfers between devices  64.1 us (30%)
  Pallas kernels  23.1 us (11%)
  local copies, waits for them, and re-layouts  3.53 us (2%)
    ppermute x8, waiting for transfers between devices, paired(): return lax.ppermute(value, 'x', [(i, mate(i)) for i in range(n)])  55.8 us
    ppermute x20, waiting for transfers between devices, shifted(): return lax.ppermute(value, axis, [(i, (i + amount) % n) for i in range(n)])  41.6 us
    ppermute x20, starting transfers between devices, shifted(): return lax.ppermute(value, axis, [(i, (i + amount) % n) for i in range(n)])  33.1 us
    all_to_all x1, waiting for transfers between devices, both_halves(): lax.all_to_all(outgoing, EP, split_axis=0, concat_axis=0, tiled=True)  26.3 us
    pallas_call x14, Pallas kernels, call(): pl.pallas_call(kernel, in_specs=specs, out_specs=VMEM_SPEC if single else...  23.1 us
    ppermute x8, starting transfers between devices, paired(): return lax.ppermute(value, 'x', [(i, mate(i)) for i in range(n)])  13 us
    all_to_all x1, starting transfers between devices, both_halves(): lax.all_to_all(outgoing, EP, split_axis=0, concat_axis=0, tiled=True)  11.9 us
    all_to_all x1, starting transfers between devices, both_halves(): lax.all_to_all(result, EP, split_axis=0, concat_axis=0, tiled=True)  6.09 us
  transfers between devices with their start and end apart: 30, of which 20 were waited for; matrix products, arithmetic and copies ran while one was open for 0% of the time, Pallas kernels for 8%

profile of v11, /device:TPU:32, one launch (start us, length us, event | category | flops | bytes accessed | tf_op | source)
XLA Modules:
  0.0 215.6 jit_solution(14398035979805815388)
XLA Ops:
  0.6 2.6 %shard_map.164 = (bf16[64,4,2048]{2,1,0:T(4,128)(2,1)}, bf16[256,128]{1,0:T(8,128)(2,1)}) custom-call(bf16[64,2048]{1,0:T(8,128)(2,1)} %tokens.1, f32[1,2048]{1,0:T(1,128)} %bitcast.22, s32[2,64]{1,0:T(2,128)} %bitcast.24, f32[1,64]{1,0:T(1,128)} %bitcast.26, f32[2,64]{1,0:T(2,128)} %bitcast.25), custom_call_target="tpu_custom_call" | custom-call | tf_op jit(solution)/shard_map/pallas_call | solution.py:45
  3.2 11.9 %all-to-all-start = ((bf16[64,4,2048]{2,1,0:T(4,128)(2,1)}), bf16[64,4,2048]{2,1,0:T(4,128)(2,1)S(1)}, u32[]{:S(2)}, u32[]{:S(2)}) async-start(bf16[64,4,2048]{2,1,0:T(4,128)(2,1)} %get-tuple-element.28), calls=%async_computation | async-start | bytes 2097152 | tf_op jit(solution)/shard_map/all_to_all | solution.py:195
  15.2 1.6 collective-permute-start.25
  16.7 26.3 %all-to-all-done.rows = bf16[64,4,2048]{2,1,0:T(4,128)(2,1)S(1)} async-done(((bf16[64,4,2048]{2,1,0:T(4,128)(2,1)}), bf16[64,4,2048]{2,1,0:T(4,128)(2,1)S(1)}, u32[]{:S(2)}, u32[]{:S(2)}) %all-to-all-start) | async-done | bytes 1048608 | tf_op jit(solution)/shard_map/all_to_all | solution.py:195
  43.1 2.8 %collective-permute-start.22 = (bf16[64,4,2048]{2,1,0:T(4,128)(2,1)S(1)}, bf16[64,4,2048]{2,1,0:T(4,128)(2,1)S(1)}, u32[]{:S(2)}, u32[]{:S(2)}) collective-permute-start(bf16[64,4,2048]{2,1,0:T(4,128)(2,1)S(1)} %all-to-all-done.rows), channel_id=1, source_target_pairs={{0,3},{1,2},{2,1},{3,0},{4,7},{5,6},{6,5},{7,4},{8,11},{9,10},{10,... | collective-permute-start | bytes 3145736 | tf_op jit(solution)/shard_map/ppermute | solution.py:66
  45.8 0.2 collective-permute-start.20
  46.0 1.8 collective-permute-start.21
  47.8 0.5 collective-permute-start.26
  48.3 2.8 %collective-permute-start.27 = (bf16[256,2048]{1,0:T(8,128)(2,1)}, bf16[256,2048]{1,0:T(8,128)(2,1)S(1)}, u32[]{:S(2)}, u32[]{:S(2)}) collective-permute-start(bf16[256,2048]{1,0:T(8,128)(2,1)} %collective-permute-done.25.w1), channel_id=1, source_target_pairs={{0,3},{1,2},{2,1},{3,0},{4,7},{5,6},{6,5},{7,4},{8,11},{9,10},{10,... | collective-permute-start | bytes 3145736 | tf_op jit(solution)/shard_map/ppermute | solution.py:66
  51.1 19.2 %collective-permute-done.22.rows = bf16[64,4,2048]{2,1,0:T(4,128)(2,1)S(1)} collective-permute-done((bf16[64,4,2048]{2,1,0:T(4,128)(2,1)S(1)}, bf16[64,4,2048]{2,1,0:T(4,128)(2,1)S(1)}, u32[]{:S(2)}, u32[]{:S(2)}) %collective-permute-start.22) | collective-permute-done | bytes 1048608 | tf_op jit(solution)/shard_map/ppermute | solution.py:66
  70.3 1.2 copy-done
  71.5 1.2 copy-done.2
  72.8 1.0 shard_map.167
  73.7 2.8 %collective-permute-start.23 = (bf16[256,256]{1,0:T(8,128)(2,1)S(1)}, bf16[256,256]{1,0:T(8,128)(2,1)S(1)}, u32[]{:S(2)}, u32[]{:S(2)}) collective-permute-start(bf16[256,256]{1,0:T(8,128)(2,1)S(1)} %shard_map.167), channel_id=1, source_target_pairs={{0,3},{1,2},{2,1},{3,0},{4,7},{5,6},{6,5},{7,4},{8,11},{9,10},{10,... | collective-permute-start | bytes 393224 | tf_op jit(solution)/shard_map/ppermute | solution.py:66
  76.6 16.9 %collective-permute-done.21.w_up = bf16[2048,256]{1,0:T(8,128)(2,1)S(1)} collective-permute-done((bf16[2048,256]{1,0:T(8,128)(2,1)}, bf16[2048,256]{1,0:T(8,128)(2,1)S(1)}, u32[]{:S(2)}, u32[]{:S(2)}) %collective-permute-start.21) | collective-permute-done | bytes 1048608 | tf_op jit(solution)/shard_map/ppermute | solution.py:66
  93.5 1.0 shard_map.168
  94.5 0.6 collective-permute-start.24
  95.1 1.0 shard_map.165.h0
  96.1 1.0 shard_map.166.h1
  97.1 18.1 %collective-permute-done.27.w3 = bf16[256,2048]{1,0:T(8,128)(2,1)S(1)} collective-permute-done((bf16[256,2048]{1,0:T(8,128)(2,1)}, bf16[256,2048]{1,0:T(8,128)(2,1)S(1)}, u32[]{:S(2)}, u32[]{:S(2)}) %collective-permute-start.27) | collective-permute-done | bytes 1048608 | tf_op jit(solution)/shard_map/ppermute | solution.py:66
  115.2 1.0 copy-done.7
  116.2 2.4 %shard_map.169.weights = bf16[4,256,2048]{2,1,0:T(8,128)(2,1)S(1)} custom-call(bf16[256,2048]{1,0:T(8,128)(2,1)} %bitcast.21, bf16[256,2048]{1,0:T(8,128)(2,1)} %collective-permute-done.25.w1, bf16[256,2048]{1,0:T(8,128)(2,1)} %copy-done.6, bf16[256,2048]{1,0:T(8,128)(2,1)} %copy-done.7), custom_call_target="tpu_custom_call" | custom-call | tf_op jit(solution)/shard_map/pallas_call | solution.py:45
  118.7 1.5 collective-permute-done.24.h3
  120.1 2.3 %shard_map.170 = bf16[64,4,2048]{2,1,0:T(4,128)(2,1)} custom-call(bf16[256,256]{1,0:T(8,128)(2,1)S(1)} %shard_map.165.h0, bf16[256,256]{1,0:T(8,128)(2,1)S(1)} %shard_map.166.h1, bf16[256,256]{1,0:T(8,128)(2,1)S(1)} %collective-permute-done.23.h2, bf16[256,256]{1,0:T(8,128)(2,1)S(1)} %collective-permute-done.24.h3, bf16[4,256,2048]{2,1,0:T(8,128)(2,1)S(1)} %shard_map.169.weights), custom_call_target="tpu_custom_call" | custom-call | tf_op jit(solution)/shard_map/pallas_call | solution.py:45
  122.4 6.1 %all-to-all-start.1 = ((bf16[64,4,2048]{2,1,0:T(4,128)(2,1)}), bf16[64,4,2048]{2,1,0:T(4,128)(2,1)S(1)}, u32[]{:S(2)}, u32[]{:S(2)}) async-start(bf16[64,4,2048]{2,1,0:T(4,128)(2,1)} %shard_map.170), calls=%async_computation.1 | async-start | bytes 2097152 | tf_op jit(solution)/shard_map/all_to_all | solution.py:208
  128.6 0.1 multiply_sine_fusion
  128.8 0.9 shard_map.158.l0
  129.7 0.4 collective-permute-start
  130.0 3.9 %collective-permute-start.1 = (bf16[32,544]{1,0:T(8,128)(2,1)S(1)}, bf16[32,544]{1,0:T(8,128)(2,1)S(1)}, u32[]{:S(2)}, u32[]{:S(2)}) collective-permute-start(bf16[32,544]{1,0:T(8,128)(2,1)S(1)} %shard_map.158.l0), channel_id=1, source_target_pairs={{0,2},{1,3},{2,0},{3,1},{4,6},{5,7},{6,4},{7,5},{8,10},{9,11},{10,... | collective-permute-start | bytes 104456 | tf_op jit(solution)/shard_map/ppermute | solution.py:61
  134.0 0.2 collective-permute-start.2
  134.2 0.1 multiply_sine_fusion.1
  134.4 0.5 collective-permute-done.l1
  134.9 1.4 collective-permute-done.1.l2
  136.4 1.6 collective-permute-done.2.l3
  138.0 1.4 shard_map.159
  139.4 2.5 %collective-permute-start.3 = (bf16[256,128]{1,0:T(8,128)(2,1)S(1)}, bf16[256,128]{1,0:T(8,128)(2,1)S(1)}, u32[]{:S(2)}, u32[]{:S(2)}) collective-permute-start(bf16[256,128]{1,0:T(8,128)(2,1)S(1)} %get-tuple-element.17), channel_id=1, source_target_pairs={{0,64},{64,128},{128,192},{192,0},{1,65},{65,129},{129,193},{193,1... | collective-permute-start | bytes 196616 | tf_op jit(solution)/shard_map/ppermute | solution.py:61
  141.9 2.9 %collective-permute-start.4 = (bf16[256,128]{1,0:T(8,128)(2,1)S(1)}, bf16[256,128]{1,0:T(8,128)(2,1)S(1)}, u32[]{:S(2)}, u32[]{:S(2)}) collective-permute-start(bf16[256,128]{1,0:T(8,128)(2,1)S(1)} %get-tuple-element.18), channel_id=1, source_target_pairs={{0,128},{64,192},{128,0},{192,64},{1,129},{65,193},{129,1},{193,65... | collective-permute-start | bytes 196616 | tf_op jit(solution)/shard_map/ppermute | solution.py:61
  144.8 3.5 %collective-permute-start.5 = (bf16[256,128]{1,0:T(8,128)(2,1)S(1)}, bf16[256,128]{1,0:T(8,128)(2,1)S(1)}, u32[]{:S(2)}, u32[]{:S(2)}) collective-permute-start(bf16[256,128]{1,0:T(8,128)(2,1)S(1)} %get-tuple-element.19), channel_id=1, source_target_pairs={{0,192},{64,0},{128,64},{192,128},{1,193},{65,1},{129,65},{193,129... | collective-permute-start | bytes 196616 | tf_op jit(solution)/shard_map/ppermute | solution.py:61
  148.2 8.9 %collective-permute-done.3.b1.q1 = bf16[256,128]{1,0:T(8,128)(2,1)S(1)} collective-permute-done((bf16[256,128]{1,0:T(8,128)(2,1)S(1)}, bf16[256,128]{1,0:T(8,128)(2,1)S(1)}, u32[]{:S(2)}, u32[]{:S(2)}) %collective-permute-start.3) | collective-permute-done | bytes 65568 | tf_op jit(solution)/shard_map/ppermute | solution.py:61
  157.2 3.8 %collective-permute-done.4.b2.q2 = bf16[256,128]{1,0:T(8,128)(2,1)S(1)} collective-permute-done((bf16[256,128]{1,0:T(8,128)(2,1)S(1)}, bf16[256,128]{1,0:T(8,128)(2,1)S(1)}, u32[]{:S(2)}, u32[]{:S(2)}) %collective-permute-start.4) | collective-permute-done | bytes 65568 | tf_op jit(solution)/shard_map/ppermute | solution.py:61
  161.0 2.5 %collective-permute-start.6 = (bf16[4,160,128]{2,1,0:T(8,128)(2,1)S(1)}, bf16[4,160,128]{2,1,0:T(8,128)(2,1)S(1)}, u32[]{:S(2)}, u32[]{:S(2)}) collective-permute-start(bf16[4,160,128]{2,1,0:T(8,128)(2,1)S(1)} %shard_map.160), channel_id=1, source_target_pairs={{0,32},{32,0},{1,33},{33,1},{2,34},{34,2},{3,35},{35,3},{4,36},{36... | collective-permute-start | bytes 491528 | tf_op jit(solution)/shard_map/ppermute | solution.py:61
  163.5 3.3 %collective-permute-done.6 = bf16[4,160,128]{2,1,0:T(8,128)(2,1)S(1)} collective-permute-done((bf16[4,160,128]{2,1,0:T(8,128)(2,1)S(1)}, bf16[4,160,128]{2,1,0:T(8,128)(2,1)S(1)}, u32[]{:S(2)}, u32[]{:S(2)}) %collective-permute-start.6) | collective-permute-done | bytes 163872 | tf_op jit(solution)/shard_map/ppermute | solution.py:61
  166.9 1.6 collective-permute-start.7
  168.4 2.7 %collective-permute-start.8 = (bf16[4,160,256]{2,1,0:T(8,128)(2,1)S(1)}, bf16[4,160,256]{2,1,0:T(8,128)(2,1)S(1)}, u32[]{:S(2)}, u32[]{:S(2)}) collective-permute-start(bf16[4,160,256]{2,1,0:T(8,128)(2,1)S(1)} %pad_maximum_fusion.refs_0_), channel_id=1, source_target_pairs={{0,16},{8,24},{16,0},{24,8},{1,17},{9,25},{17,1},{25,9},{2,18},{10... | collective-permute-start | bytes 983048 | tf_op jit(solution)/shard_map/ppermute | solution.py:61
  171.1 1.4 collective-permute-start.9
  172.6 5.5 %collective-permute-done.7.refs_1_ = bf16[4,160,256]{2,1,0:T(8,128)(2,1)S(1)} collective-permute-done((bf16[4,160,256]{2,1,0:T(8,128)(2,1)S(1)}, bf16[4,160,256]{2,1,0:T(8,128)(2,1)S(1)}, u32[]{:S(2)}, u32[]{:S(2)}) %collective-permute-start.7) | collective-permute-done | bytes 327712 | tf_op jit(solution)/shard_map/ppermute | solution.py:61
  178.1 5.4 %collective-permute-done.8.refs_2_ = bf16[4,160,256]{2,1,0:T(8,128)(2,1)S(1)} collective-permute-done((bf16[4,160,256]{2,1,0:T(8,128)(2,1)S(1)}, bf16[4,160,256]{2,1,0:T(8,128)(2,1)S(1)}, u32[]{:S(2)}, u32[]{:S(2)}) %collective-permute-start.8) | collective-permute-done | bytes 327712 | tf_op jit(solution)/shard_map/ppermute | solution.py:61
  183.4 0.5 collective-permute-start.13
  184.0 1.1 collective-permute-done.12.refs_6_
  185.1 0.5 collective-permute-done.13.refs_7_
  185.5 5.8 %shard_map.161 = (bf16[128,64]{1,0:T(8,128)(2,1)S(1)}, bf16[128,64]{1,0:T(8,128)(2,1)S(1)}, bf16[128,64]{1,0:T(8,128)(2,1)S(1)}, bf16[128,64]{1,0:T(8,128)(2,1)S(1)}) custom-call(s32[5]{0:T(128)S(1)} %stack.23.where, bf16[256,128]{1,0:T(8,128)(2,1)S(1)} %get-tuple-element.16.b0.q0, bf16[256,128]{1,0:T(8,128)(2,1)S(1)} %collective-permute-done.3.b1.q1, ...), custom_call_target="tpu_custom_call" | custom-call | tf_op jit(solution)/shard_map/pallas_call | solution.py:45
  191.3 3.1 %collective-permute-start.14 = (bf16[128,64]{1,0:T(8,128)(2,1)S(1)}, bf16[128,64]{1,0:T(8,128)(2,1)S(1)}, u32[]{:S(2)}, u32[]{:S(2)}) collective-permute-start(bf16[128,64]{1,0:T(8,128)(2,1)S(1)} %get-tuple-element.21), channel_id=1, source_target_pairs={{0,192},{64,0},{128,64},{192,128},{1,193},{65,1},{129,65},{193,129... | collective-permute-start | bytes 49160 | tf_op jit(solution)/shard_map/ppermute | solution.py:61
  194.4 3.4 %collective-permute-start.15 = (bf16[128,64]{1,0:T(8,128)(2,1)S(1)}, bf16[128,64]{1,0:T(8,128)(2,1)S(1)}, u32[]{:S(2)}, u32[]{:S(2)}) collective-permute-start(bf16[128,64]{1,0:T(8,128)(2,1)S(1)} %get-tuple-element.22), channel_id=1, source_target_pairs={{0,128},{64,192},{128,0},{192,64},{1,129},{65,193},{129,1},{193,65... | collective-permute-start | bytes 49160 | tf_op jit(solution)/shard_map/ppermute | solution.py:61
  197.8 4.4 %collective-permute-done.15.a2 = bf16[128,64]{1,0:T(8,128)(2,1)S(1)} collective-permute-done((bf16[128,64]{1,0:T(8,128)(2,1)S(1)}, bf16[128,64]{1,0:T(8,128)(2,1)S(1)}, u32[]{:S(2)}, u32[]{:S(2)}) %collective-permute-start.15) | collective-permute-done | bytes 16416 | tf_op jit(solution)/shard_map/ppermute | solution.py:61
  202.2 1.6 collective-permute-done.16.a3
  203.8 0.7 shard_map.162
  204.5 0.4 collective-permute-start.17
  204.9 3.9 %collective-permute-start.18 = (bf16[32,256]{1,0:T(8,128)(2,1)S(1)}, bf16[32,256]{1,0:T(8,128)(2,1)S(1)}, u32[]{:S(2)}, u32[]{:S(2)}) collective-permute-start(bf16[32,256]{1,0:T(8,128)(2,1)S(1)} %get-tuple-element.26), channel_id=1, source_target_pairs={{0,2},{1,3},{2,0},{3,1},{4,6},{5,7},{6,4},{7,5},{8,10},{9,11},{10,... | collective-permute-start | bytes 49160 | tf_op jit(solution)/shard_map/ppermute | solution.py:61
  208.8 0.2 collective-permute-start.19
  209.0 0.5 collective-permute-done.17.a1
  209.5 1.2 collective-permute-done.18.a2
  210.7 1.9 collective-permute-done.19.a3
  212.5 2.0 shard_map.163
  214.6 1.0 shard_map.171
  (34 shorter events, 0.3 us)
Async XLA Ops:
  3.2 91.8 %copy-start.1 = (bf16[1,2048,256]{2,1,0:T(8,128)(2,1)S(1)}, bf16[1,2048,256]{2,1,0:T(8,128)(2,1)}, u32[]{:S(2)}) copy-start(bf16[1,2048,256]{2,1,0:T(8,128)(2,1)} %param.27) | copy-start | bytes 3145732
  3.2 91.9 %copy-start.3 = (bf16[1,2048,256]{2,1,0:T(8,128)(2,1)S(1)}, bf16[1,2048,256]{2,1,0:T(8,128)(2,1)}, u32[]{:S(2)}) copy-start(bf16[1,2048,256]{2,1,0:T(8,128)(2,1)} %param.28) | copy-start | bytes 3145732
  3.2 39.8 %all-to-all-start = ((bf16[64,4,2048]{2,1,0:T(4,128)(2,1)}), bf16[64,4,2048]{2,1,0:T(4,128)(2,1)S(1)}, u32[]{:S(2)}, u32[]{:S(2)}) async-start(bf16[64,4,2048]{2,1,0:T(4,128)(2,1)} %get-tuple-element.28), calls=%async_computation | async-start | bytes 2097152 | tf_op jit(solution)/shard_map/all_to_all | solution.py:195
  15.2 33.2 %collective-permute-start.25 = (bf16[256,2048]{1,0:T(8,128)(2,1)}, bf16[256,2048]{1,0:T(8,128)(2,1)}, u32[]{:S(2)}, u32[]{:S(2)}) collective-permute-start(bf16[256,2048]{1,0:T(8,128)(2,1)} %bitcast.19), channel_id=1, source_target_pairs={{0,1},{1,0},{2,3},{3,2},{4,5},{5,4},{6,7},{7,6},{8,9},{9,8},{10,11... | collective-permute-start | bytes 3145736 | tf_op jit(solution)/shard_map/ppermute | solution.py:66
  43.1 27.2 %collective-permute-start.22 = (bf16[64,4,2048]{2,1,0:T(4,128)(2,1)S(1)}, bf16[64,4,2048]{2,1,0:T(4,128)(2,1)S(1)}, u32[]{:S(2)}, u32[]{:S(2)}) collective-permute-start(bf16[64,4,2048]{2,1,0:T(4,128)(2,1)S(1)} %all-to-all-done.rows), channel_id=1, source_target_pairs={{0,3},{1,2},{2,1},{3,0},{4,7},{5,6},{6,5},{7,4},{8,11},{9,10},{10,... | collective-permute-start | bytes 3145736 | tf_op jit(solution)/shard_map/ppermute | solution.py:66
  45.8 30.8 %collective-permute-start.20 = (bf16[2048,256]{1,0:T(8,128)(2,1)}, bf16[2048,256]{1,0:T(8,128)(2,1)S(1)}, u32[]{:S(2)}, u32[]{:S(2)}) collective-permute-start(bf16[2048,256]{1,0:T(8,128)(2,1)} %bitcast.13), channel_id=1, source_target_pairs={{0,1},{1,0},{2,3},{3,2},{4,5},{5,4},{6,7},{7,6},{8,9},{9,8},{10,11... | collective-permute-start | bytes 3145736 | tf_op jit(solution)/shard_map/ppermute | solution.py:66
  46.0 47.5 %collective-permute-start.21 = (bf16[2048,256]{1,0:T(8,128)(2,1)}, bf16[2048,256]{1,0:T(8,128)(2,1)S(1)}, u32[]{:S(2)}, u32[]{:S(2)}) collective-permute-start(bf16[2048,256]{1,0:T(8,128)(2,1)} %bitcast.16), channel_id=1, source_target_pairs={{0,1},{1,0},{2,3},{3,2},{4,5},{5,4},{6,7},{7,6},{8,9},{9,8},{10,11... | collective-permute-start | bytes 3145736 | tf_op jit(solution)/shard_map/ppermute | solution.py:66
  47.8 49.2 %collective-permute-start.26 = (bf16[256,2048]{1,0:T(8,128)(2,1)}, bf16[256,2048]{1,0:T(8,128)(2,1)S(1)}, u32[]{:S(2)}, u32[]{:S(2)}) collective-permute-start(bf16[256,2048]{1,0:T(8,128)(2,1)} %bitcast.20), channel_id=1, source_target_pairs={{0,3},{1,2},{2,1},{3,0},{4,7},{5,6},{6,5},{7,4},{8,11},{9,10},{10,... | collective-permute-start | bytes 3145736 | tf_op jit(solution)/shard_map/ppermute | solution.py:66
  48.3 66.9 %collective-permute-start.27 = (bf16[256,2048]{1,0:T(8,128)(2,1)}, bf16[256,2048]{1,0:T(8,128)(2,1)S(1)}, u32[]{:S(2)}, u32[]{:S(2)}) collective-permute-start(bf16[256,2048]{1,0:T(8,128)(2,1)} %collective-permute-done.25.w1), channel_id=1, source_target_pairs={{0,3},{1,2},{2,1},{3,0},{4,7},{5,6},{6,5},{7,4},{8,11},{9,10},{10,... | collective-permute-start | bytes 3145736 | tf_op jit(solution)/shard_map/ppermute | solution.py:66
  70.3 1.2 copy-start
  71.5 1.2 copy-start.2
  73.7 44.9 %collective-permute-start.23 = (bf16[256,256]{1,0:T(8,128)(2,1)S(1)}, bf16[256,256]{1,0:T(8,128)(2,1)S(1)}, u32[]{:S(2)}, u32[]{:S(2)}) collective-permute-start(bf16[256,256]{1,0:T(8,128)(2,1)S(1)} %shard_map.167), channel_id=1, source_target_pairs={{0,3},{1,2},{2,1},{3,0},{4,7},{5,6},{6,5},{7,4},{8,11},{9,10},{10,... | collective-permute-start | bytes 393224 | tf_op jit(solution)/shard_map/ppermute | solution.py:66
  94.5 25.6 %collective-permute-start.24 = (bf16[256,256]{1,0:T(8,128)(2,1)S(1)}, bf16[256,256]{1,0:T(8,128)(2,1)S(1)}, u32[]{:S(2)}, u32[]{:S(2)}) collective-permute-start(bf16[256,256]{1,0:T(8,128)(2,1)S(1)} %shard_map.168), channel_id=1, source_target_pairs={{0,3},{1,2},{2,1},{3,0},{4,7},{5,6},{6,5},{7,4},{8,11},{9,10},{10,... | collective-permute-start | bytes 393224 | tf_op jit(solution)/shard_map/ppermute | solution.py:66
  97.1 18.1 %copy-start.6 = (bf16[256,2048]{1,0:T(8,128)(2,1)}, bf16[256,2048]{1,0:T(8,128)(2,1)S(1)}, u32[]{:S(2)}) copy-start(bf16[256,2048]{1,0:T(8,128)(2,1)S(1)} %collective-permute-done.26.w2) | copy-start | bytes 3145732
  115.2 1.0 copy-start.7
  122.4 92.2 %all-to-all-start.1 = ((bf16[64,4,2048]{2,1,0:T(4,128)(2,1)}), bf16[64,4,2048]{2,1,0:T(4,128)(2,1)S(1)}, u32[]{:S(2)}, u32[]{:S(2)}) async-start(bf16[64,4,2048]{2,1,0:T(4,128)(2,1)} %shard_map.170), calls=%async_computation.1 | async-start | bytes 2097152 | tf_op jit(solution)/shard_map/all_to_all | solution.py:208
  129.7 5.3 %collective-permute-start = (bf16[32,544]{1,0:T(8,128)(2,1)S(1)}, bf16[32,544]{1,0:T(8,128)(2,1)S(1)}, u32[]{:S(2)}, u32[]{:S(2)}) collective-permute-start(bf16[32,544]{1,0:T(8,128)(2,1)S(1)} %shard_map.158.l0), channel_id=1, source_target_pairs={{0,1},{1,2},{2,3},{3,0},{4,5},{5,6},{6,7},{7,4},{8,9},{9,10},{10,1... | collective-permute-start | bytes 104456 | tf_op jit(solution)/shard_map/ppermute | solution.py:61
  130.0 6.4 %collective-permute-start.1 = (bf16[32,544]{1,0:T(8,128)(2,1)S(1)}, bf16[32,544]{1,0:T(8,128)(2,1)S(1)}, u32[]{:S(2)}, u32[]{:S(2)}) collective-permute-start(bf16[32,544]{1,0:T(8,128)(2,1)S(1)} %shard_map.158.l0), channel_id=1, source_target_pairs={{0,2},{1,3},{2,0},{3,1},{4,6},{5,7},{6,4},{7,5},{8,10},{9,11},{10,... | collective-permute-start | bytes 104456 | tf_op jit(solution)/shard_map/ppermute | solution.py:61
  134.0 4.0 %collective-permute-start.2 = (bf16[32,544]{1,0:T(8,128)(2,1)S(1)}, bf16[32,544]{1,0:T(8,128)(2,1)S(1)}, u32[]{:S(2)}, u32[]{:S(2)}) collective-permute-start(bf16[32,544]{1,0:T(8,128)(2,1)S(1)} %shard_map.158.l0), channel_id=1, source_target_pairs={{0,3},{1,0},{2,1},{3,2},{4,7},{5,4},{6,5},{7,6},{8,11},{9,8},{10,9... | collective-permute-start | bytes 104456 | tf_op jit(solution)/shard_map/ppermute | solution.py:61
  134.4 78.1 %copy-start.4 = (bf16[1024,2048]{1,0:T(8,128)(2,1)S(1)}, bf16[1024,2048]{1,0:T(8,128)(2,1)}, u32[]{:S(2)}) copy-start(bf16[1024,2048]{1,0:T(8,128)(2,1)} %out_proj.1) | copy-start | bytes 12582916
  139.4 17.8 %collective-permute-start.3 = (bf16[256,128]{1,0:T(8,128)(2,1)S(1)}, bf16[256,128]{1,0:T(8,128)(2,1)S(1)}, u32[]{:S(2)}, u32[]{:S(2)}) collective-permute-start(bf16[256,128]{1,0:T(8,128)(2,1)S(1)} %get-tuple-element.17), channel_id=1, source_target_pairs={{0,64},{64,128},{128,192},{192,0},{1,65},{65,129},{129,193},{193,1... | collective-permute-start | bytes 196616 | tf_op jit(solution)/shard_map/ppermute | solution.py:61
  141.9 19.1 %collective-permute-start.4 = (bf16[256,128]{1,0:T(8,128)(2,1)S(1)}, bf16[256,128]{1,0:T(8,128)(2,1)S(1)}, u32[]{:S(2)}, u32[]{:S(2)}) collective-permute-start(bf16[256,128]{1,0:T(8,128)(2,1)S(1)} %get-tuple-element.18), channel_id=1, source_target_pairs={{0,128},{64,192},{128,0},{192,64},{1,129},{65,193},{129,1},{193,65... | collective-permute-start | bytes 196616 | tf_op jit(solution)/shard_map/ppermute | solution.py:61
  144.8 16.2 %collective-permute-start.5 = (bf16[256,128]{1,0:T(8,128)(2,1)S(1)}, bf16[256,128]{1,0:T(8,128)(2,1)S(1)}, u32[]{:S(2)}, u32[]{:S(2)}) collective-permute-start(bf16[256,128]{1,0:T(8,128)(2,1)S(1)} %get-tuple-element.19), channel_id=1, source_target_pairs={{0,192},{64,0},{128,64},{192,128},{1,193},{65,1},{129,65},{193,129... | collective-permute-start | bytes 196616 | tf_op jit(solution)/shard_map/ppermute | solution.py:61
  161.0 53.6 %copy-start.5 = (bf16[256,128]{1,0:T(8,128)(2,1)S(1)}, bf16[256,128]{1,0:T(8,128)(2,1)}, u32[]{:S(2)}) copy-start(bf16[256,128]{1,0:T(8,128)(2,1)} %get-tuple-element.29.shares) | copy-start | bytes 196612
  161.0 5.8 %collective-permute-start.6 = (bf16[4,160,128]{2,1,0:T(8,128)(2,1)S(1)}, bf16[4,160,128]{2,1,0:T(8,128)(2,1)S(1)}, u32[]{:S(2)}, u32[]{:S(2)}) collective-permute-start(bf16[4,160,128]{2,1,0:T(8,128)(2,1)S(1)} %shard_map.160), channel_id=1, source_target_pairs={{0,32},{32,0},{1,33},{33,1},{2,34},{34,2},{3,35},{35,3},{4,36},{36... | collective-permute-start | bytes 491528 | tf_op jit(solution)/shard_map/ppermute | solution.py:61
  166.9 11.2 %collective-permute-start.7 = (bf16[4,160,256]{2,1,0:T(8,128)(2,1)S(1)}, bf16[4,160,256]{2,1,0:T(8,128)(2,1)S(1)}, u32[]{:S(2)}, u32[]{:S(2)}) collective-permute-start(bf16[4,160,256]{2,1,0:T(8,128)(2,1)S(1)} %pad_maximum_fusion.refs_0_), channel_id=1, source_target_pairs={{0,8},{8,16},{16,24},{24,0},{1,9},{9,17},{17,25},{25,1},{2,10},{10... | collective-permute-start | bytes 983048 | tf_op jit(solution)/shard_map/ppermute | solution.py:61
  168.4 15.0 %collective-permute-start.8 = (bf16[4,160,256]{2,1,0:T(8,128)(2,1)S(1)}, bf16[4,160,256]{2,1,0:T(8,128)(2,1)S(1)}, u32[]{:S(2)}, u32[]{:S(2)}) collective-permute-start(bf16[4,160,256]{2,1,0:T(8,128)(2,1)S(1)} %pad_maximum_fusion.refs_0_), channel_id=1, source_target_pairs={{0,16},{8,24},{16,0},{24,8},{1,17},{9,25},{17,1},{25,9},{2,18},{10... | collective-permute-start | bytes 983048 | tf_op jit(solution)/shard_map/ppermute | solution.py:61
  171.1 12.3 %collective-permute-start.9 = (bf16[4,160,256]{2,1,0:T(8,128)(2,1)S(1)}, bf16[4,160,256]{2,1,0:T(8,128)(2,1)S(1)}, u32[]{:S(2)}, u32[]{:S(2)}) collective-permute-start(bf16[4,160,256]{2,1,0:T(8,128)(2,1)S(1)} %pad_maximum_fusion.refs_0_), channel_id=1, source_target_pairs={{0,24},{8,0},{16,8},{24,16},{1,25},{9,1},{17,9},{25,17},{2,26},{10... | collective-permute-start | bytes 983048 | tf_op jit(solution)/shard_map/ppermute | solution.py:61
  172.6 11.4 %collective-permute-start.10 = (bf16[4,160,256]{2,1,0:T(8,128)(2,1)S(1)}, bf16[4,160,256]{2,1,0:T(8,128)(2,1)S(1)}, u32[]{:S(2)}, u32[]{:S(2)}) collective-permute-start(bf16[4,160,256]{2,1,0:T(8,128)(2,1)S(1)} %pad_maximum_fusion.refs_0_), channel_id=1, source_target_pairs={{0,4},{4,0},{1,5},{5,1},{2,6},{6,2},{3,7},{7,3},{8,12},{12,8},{9,1... | collective-permute-start | bytes 983048 | tf_op jit(solution)/shard_map/ppermute | solution.py:61
  178.1 5.9 %collective-permute-start.11 = (bf16[4,160,256]{2,1,0:T(8,128)(2,1)S(1)}, bf16[4,160,256]{2,1,0:T(8,128)(2,1)S(1)}, u32[]{:S(2)}, u32[]{:S(2)}) collective-permute-start(bf16[4,160,256]{2,1,0:T(8,128)(2,1)S(1)} %collective-permute-done.7.refs_1_), channel_id=1, source_target_pairs={{0,4},{4,0},{1,5},{5,1},{2,6},{6,2},{3,7},{7,3},{8,12},{12,8},{9,1... | collective-permute-start | bytes 983048 | tf_op jit(solution)/shard_map/ppermute | solution.py:61
  183.4 1.6 collective-permute-start.12
  183.4 2.1 collective-permute-start.13
  191.3 6.5 %collective-permute-start.14 = (bf16[128,64]{1,0:T(8,128)(2,1)S(1)}, bf16[128,64]{1,0:T(8,128)(2,1)S(1)}, u32[]{:S(2)}, u32[]{:S(2)}) collective-permute-start(bf16[128,64]{1,0:T(8,128)(2,1)S(1)} %get-tuple-element.21), channel_id=1, source_target_pairs={{0,192},{64,0},{128,64},{192,128},{1,193},{65,1},{129,65},{193,129... | collective-permute-start | bytes 49160 | tf_op jit(solution)/shard_map/ppermute | solution.py:61
  194.4 7.8 %collective-permute-start.15 = (bf16[128,64]{1,0:T(8,128)(2,1)S(1)}, bf16[128,64]{1,0:T(8,128)(2,1)S(1)}, u32[]{:S(2)}, u32[]{:S(2)}) collective-permute-start(bf16[128,64]{1,0:T(8,128)(2,1)S(1)} %get-tuple-element.22), channel_id=1, source_target_pairs={{0,128},{64,192},{128,0},{192,64},{1,129},{65,193},{129,1},{193,65... | collective-permute-start | bytes 49160 | tf_op jit(solution)/shard_map/ppermute | solution.py:61
  197.8 6.0 %collective-permute-start.16 = (bf16[128,64]{1,0:T(8,128)(2,1)S(1)}, bf16[128,64]{1,0:T(8,128)(2,1)S(1)}, u32[]{:S(2)}, u32[]{:S(2)}) collective-permute-start(bf16[128,64]{1,0:T(8,128)(2,1)S(1)} %get-tuple-element.23), channel_id=1, source_target_pairs={{0,64},{64,128},{128,192},{192,0},{1,65},{65,129},{129,193},{193,1... | collective-permute-start | bytes 49160 | tf_op jit(solution)/shard_map/ppermute | solution.py:61
  204.5 5.0 %collective-permute-start.17 = (bf16[32,256]{1,0:T(8,128)(2,1)S(1)}, bf16[32,256]{1,0:T(8,128)(2,1)S(1)}, u32[]{:S(2)}, u32[]{:S(2)}) collective-permute-start(bf16[32,256]{1,0:T(8,128)(2,1)S(1)} %get-tuple-element.25), channel_id=1, source_target_pairs={{0,1},{1,2},{2,3},{3,0},{4,5},{5,6},{6,7},{7,4},{8,9},{9,10},{10,1... | collective-permute-start | bytes 49160 | tf_op jit(solution)/shard_map/ppermute | solution.py:61
  204.9 5.8 %collective-permute-start.18 = (bf16[32,256]{1,0:T(8,128)(2,1)S(1)}, bf16[32,256]{1,0:T(8,128)(2,1)S(1)}, u32[]{:S(2)}, u32[]{:S(2)}) collective-permute-start(bf16[32,256]{1,0:T(8,128)(2,1)S(1)} %get-tuple-element.26), channel_id=1, source_target_pairs={{0,2},{1,3},{2,0},{3,1},{4,6},{5,7},{6,4},{7,5},{8,10},{9,11},{10,... | collective-permute-start | bytes 49160 | tf_op jit(solution)/shard_map/ppermute | solution.py:61
  208.8 3.7 %collective-permute-start.19 = (bf16[32,256]{1,0:T(8,128)(2,1)S(1)}, bf16[32,256]{1,0:T(8,128)(2,1)S(1)}, u32[]{:S(2)}, u32[]{:S(2)}) collective-permute-start(bf16[32,256]{1,0:T(8,128)(2,1)S(1)} %get-tuple-element.27), channel_id=1, source_target_pairs={{0,3},{1,0},{2,1},{3,2},{4,7},{5,4},{6,5},{7,6},{8,11},{9,8},{10,9... | collective-permute-start | bytes 49160 | tf_op jit(solution)/shard_map/ppermute | solution.py:61

commit v12 on v11

--- a/solution.py
+++ b/solution.py
@@ -148,6 +148,15 @@
     return call(hidden_kernel, shape, [rows] + weights, scratch=scratch)
 
 
+def copy_kernel(value, out):
+    out[...] = value[...]
+
+
+def in_vmem(value):
+    shape = jax.ShapeDtypeStruct(value.shape, value.dtype)
+    return call(copy_kernel, shape, [value], unplaced=[0])
+
+
 def stage_kernel(w0, w1, w2, w3, out):
     for k, piece in enumerate((w0, w1, w2, w3)):
         out[k] = piece[...]
@@ -157,13 +166,6 @@
     total = mm(h0[...], weights[0]) + mm(h1[...], weights[1])
     total = total + mm(h2[...], weights[2]) + mm(h3[...], weights[3])
     out[...] = total.astype(BF).reshape(out.shape)
-
-
-def combine_kernel(returned, shares, out):
-    rows = out.shape[0]
-    got = returned[...].reshape(shares.shape[0], out.shape[1])
-    both = mm(shares[...], got, ((0,), (0,)))
-    out[...] = (both[:rows] + both[rows:]).astype(BF)
 
 
 def both_halves(
@@ -190,7 +192,7 @@
     down_w, down_r = paired(w_down, weight_mate), paired(w_down, row_mate)
     down_rw = paired(down_w, row_mate)
     gate_w, up_w = paired(w_gate, weight_mate), paired(w_up, weight_mate)
-    set_a, set_b = [w_gate, w_up], [gate_w, up_w]
+    set_a, set_b = [w_gate, w_up], [in_vmem(gate_w), up_w]
     outgoing, shares = dispatch(tokens, moe_gain, routes, group_prob, expert_prob, experts)
     arrived = lax.all_to_all(outgoing, EP, split_axis=0, concat_axis=0, tiled=True)
     queries, pair = query_and_pair(where, query, latent, rope_key, latent_gain, key_up, value_up)
@@ -206,9 +208,28 @@
     arrays = [own_a, own_b, mate_a, mate_b, down]
     result = call(down_kernel, shape, arrays, place=pltpu.HBM)
     returned = lax.all_to_all(result, EP, split_axis=0, concat_axis=0, tiled=True)
-    mixed = project(where, parts, out_proj, latent.shape[0])
-    shape = jax.ShapeDtypeStruct((rows, width), BF)
-    return mixed, call(combine_kernel, shape, [returned, shares], place=None)
+    parts = out_parts(where, parts, latent.shape[0])
+    height, span = out_proj.shape[0], width // 4
+    near = [pltpu.with_memory_space_constraint(a, pltpu.VMEM) for a in [returned, shares] + parts]
+    finish = pl.pallas_call(
+        finish_kernel,
+        in_specs=[SMEM_SPEC] + [VMEM_SPEC] * 6 + [pl.BlockSpec(memory_space=pl.ANY)],
+        out_specs=[VMEM_SPEC] * 2,
+        out_shape=[
+            jax.ShapeDtypeStruct((rows, width), BF),
+            jax.ShapeDtypeStruct((latent.shape[0], width), BF),
+        ],
+        scratch_shapes=[
+            pltpu.VMEM((4, latent.shape[0], 4 * V_DIM), BF),
+            pltpu.VMEM((4, height, span), BF),
+            pltpu.SemaphoreType.DMA((4,)),
+        ],
+        compiler_params=pltpu.CompilerParams(vmem_limit_bytes=8 << 20),
+        name="finish",
+    )
+    far = pltpu.with_memory_space_constraint(out_proj, pltpu.HBM)
+    moe_out, mixed = finish(where, *near, far)
+    return mixed, moe_out
 
 
 def latent_kernel(latent, gain, rope_key, cosine, sine, out):
@@ -312,28 +333,43 @@
                 advance(slice((g + 1) * strip, 4 * strip), parts, None)
     total = acc_s[...]
     acc_s[:, :V_DIM] = total[:, :V_DIM] / total[:, V_DIM:]
-    for j, out in enumerate(outs):
-        at = pl.multiple_of(lax.rem(zh - j + 4, 4) * strip, strip)
-        out[...] = acc_s[pl.ds(at, strip), :V_DIM].astype(BF)
+    own = strip // 4
+    for k, out in enumerate(outs):
+        for g in range(4):
+            at = pl.multiple_of(g * strip + lax.rem(x + k, 4) * own, own)
+            out[g * own : (g + 1) * own, :] = acc_s[pl.ds(at, own), :V_DIM].astype(BF)
 
 
 def spread_kernel(where, a0, a1, a2, a3, o0, o1, o2, o3, heads, parts):
-    for j, a in enumerate((a0, a1, a2, a3)):
-        heads[lax.rem(where[0] + j, 4)] = a[...]
+    for k, a in enumerate((a0, a1, a2, a3)):
+        heads[lax.rem(where[4] - k + 4, 4)] = a[...]
     beside = jnp.concatenate([heads[h] for h in range(4)], axis=1)
     parts[...] = beside.reshape(parts.shape)
-    for k, out in enumerate((o0, o1, o2, o3)):
-        out[...] = parts[lax.rem(where[4] + k, 4)]
-
-
-def project_kernel(where, a0, a1, a2, a3, out_proj, out, parts):
-    width = a0.shape[1]
-    for k, a in enumerate((a0, a1, a2, a3)):
-        parts[lax.rem(where[4] - k + 4, 4)] = a[...]
-    total = mm(parts[0], out_proj[:width, :])
-    for h in range(1, 4):
-        total = total + mm(parts[h], out_proj[h * width : (h + 1) * width, :])
-    out[...] = total.astype(BF)
+    for j, out in enumerate((o0, o1, o2, o3)):
+        out[...] = parts[lax.rem(where[0] + j, 4)]
+
+
+def finish_kernel(
+    where, returned, shares, a0, a1, a2, a3, out_proj, moe_out, mixed, parts, weights, sems
+):
+    count, _, span = weights.shape
+    copies = [
+        pltpu.make_async_copy(out_proj.at[:, pl.ds(c * span, span)], weights.at[c], sems.at[c])
+        for c in range(count)
+    ]
+    for copy in copies:
+        copy.start()
+    rows = moe_out.shape[0]
+    got = returned[...].reshape(shares.shape[0], moe_out.shape[1])
+    both = mm(shares[...], got, ((0,), (0,)))
+    moe_out[...] = (both[:rows] + both[rows:]).astype(BF)
+    for j, a in enumerate((a0, a1, a2, a3)):
+        parts[lax.rem(where[0] - j + 4, 4)] = a[...]
+    pieces = [parts[h % 4, :, h // 4 * V_DIM : (h // 4 + 1) * V_DIM] for h in range(16)]
+    beside = jnp.concatenate(pieces, axis=1)
+    for c, copy in enumerate(copies):
+        copy.wait()
+        mixed[:, c * span : (c + 1) * span] = mm(beside, weights[c]).astype(BF)
 
 
 def query_and_pair(where, query, latent, rope_key, latent_gain, key_up, value_up):
@@ -388,10 +424,10 @@
             pltpu.VMEM((4 * strip, 128), F32),
         ],
     )
-    return [parts[0]] + [shifted(parts[j], "zh", -j) for j in range(1, 4)]
-
-
-def project(where, parts, out_proj, own):
+    return [parts[0]] + [shifted(parts[k], "x", k) for k in range(1, 4)]
+
+
+def out_parts(where, parts, own):
     strip = parts[0].shape[0]
     parts = call(
         spread_kernel,
@@ -400,15 +436,8 @@
         where,
         [pltpu.VMEM((4, strip, V_DIM), BF), pltpu.VMEM((4, own, 4 * V_DIM), BF)],
     )
-    parts = [parts[0]] + [shifted(parts[k], "x", k) for k in range(1, 4)]
-    return call(
-        project_kernel,
-        jax.ShapeDtypeStruct((own, out_proj.shape[1]), BF),
-        parts + [out_proj],
-        where,
-        [pltpu.VMEM((4, own, 4 * V_DIM), BF)],
-        place=None,
-    )
+    parts = [parts[0]] + [shifted(parts[j], "zh", j) for j in range(1, 4)]
+    return parts
 
 
 def body(

time: 216 us -> 216 us (level)
  the two profiles are of different devices: /device:TPU:32 before, /device:TPU:224 now
where the time goes in v12:
time: 216 us; the launch traced here: 211 us
  waiting for transfers between devices  123 us (57%)
  starting transfers between devices  60.8 us (28%)
  Pallas kernels  25.4 us (12%)
    ppermute x8, waiting for transfers between devices, paired(): return lax.ppermute(value, 'x', [(i, mate(i)) for i in range(n)])  56.4 us
    ppermute x20, waiting for transfers between devices, shifted(): return lax.ppermute(value, axis, [(i, (i + amount) % n) for i in range(n)])  41.5 us
    ppermute x20, starting transfers between devices, shifted(): return lax.ppermute(value, axis, [(i, (i + amount) % n) for i in range(n)])  30.3 us
    all_to_all x1, waiting for transfers between devices, both_halves(): lax.all_to_all(outgoing, EP, split_axis=0, concat_axis=0, tiled=True)  24.8 us
    pallas_call x13, Pallas kernels, call(): pl.pallas_call(kernel, in_specs=specs, out_specs=VMEM_SPEC if single else...  21.5 us
    ppermute x8, starting transfers between devices, paired(): return lax.ppermute(value, 'x', [(i, mate(i)) for i in range(n)])  14 us
    all_to_all x1, starting transfers between devices, both_halves(): lax.all_to_all(outgoing, EP, split_axis=0, concat_axis=0, tiled=True)  9.29 us
    all_to_all x1, starting transfers between devices, both_halves(): lax.all_to_all(result, EP, split_axis=0, concat_axis=0, tiled=True)  7.22 us
  transfers between devices with their start and end apart: 30, of which 22 were waited for; matrix products, arithmetic and copies ran while one was open for 0% of the time, Pallas kernels for 8%

profile of v12, /device:TPU:224, one launch (start us, length us, event | category | flops | bytes accessed | tf_op | source)
XLA Modules:
  0.0 211.5 jit_solution(5607499212346159634)
XLA Ops:
  0.7 2.8 %shard_map.158 = (bf16[64,4,2048]{2,1,0:T(4,128)(2,1)}, bf16[256,128]{1,0:T(8,128)(2,1)}) custom-call(bf16[64,2048]{1,0:T(8,128)(2,1)} %tokens.1, f32[1,2048]{1,0:T(1,128)} %bitcast.22, s32[2,64]{1,0:T(2,128)} %bitcast.24, f32[1,64]{1,0:T(1,128)} %bitcast.26, f32[2,64]{1,0:T(2,128)} %bitcast.25), custom_call_target="tpu_custom_call" | custom-call | tf_op jit(solution)/shard_map/pallas_call | solution.py:45
  3.4 9.3 %all-to-all-start = ((bf16[64,4,2048]{2,1,0:T(4,128)(2,1)}), bf16[64,4,2048]{2,1,0:T(4,128)(2,1)S(1)}, u32[]{:S(2)}, u32[]{:S(2)}) async-start(bf16[64,4,2048]{2,1,0:T(4,128)(2,1)} %get-tuple-element.18), calls=%async_computation | async-start | bytes 2097152 | tf_op jit(solution)/shard_map/all_to_all | solution.py:197
  12.7 1.6 collective-permute-start.5
  14.3 0.5 collective-permute-start
  14.8 24.8 %all-to-all-done.rows = bf16[64,4,2048]{2,1,0:T(4,128)(2,1)S(1)} async-done(((bf16[64,4,2048]{2,1,0:T(4,128)(2,1)}), bf16[64,4,2048]{2,1,0:T(4,128)(2,1)S(1)}, u32[]{:S(2)}, u32[]{:S(2)}) %all-to-all-start) | async-done | bytes 1048608 | tf_op jit(solution)/shard_map/all_to_all | solution.py:197
  39.6 2.8 %collective-permute-start.2 = (bf16[64,4,2048]{2,1,0:T(4,128)(2,1)S(1)}, bf16[64,4,2048]{2,1,0:T(4,128)(2,1)S(1)}, u32[]{:S(2)}, u32[]{:S(2)}) collective-permute-start(bf16[64,4,2048]{2,1,0:T(4,128)(2,1)S(1)} %all-to-all-done.rows), channel_id=1, source_target_pairs={{0,3},{1,2},{2,1},{3,0},{4,7},{5,6},{6,5},{7,4},{8,11},{9,10},{10,... | collective-permute-start | bytes 3145736 | tf_op jit(solution)/shard_map/ppermute | solution.py:66
  42.4 0.2 collective-permute-start.1
  42.6 1.1 collective-permute-start.6
  43.8 2.1 collective-permute-start.7
  45.9 15.8 %collective-permute-done.value = bf16[2048,256]{1,0:T(8,128)(2,1)} collective-permute-done((bf16[2048,256]{1,0:T(8,128)(2,1)}, bf16[2048,256]{1,0:T(8,128)(2,1)}, u32[]{:S(2)}, u32[]{:S(2)}) %collective-permute-start) | collective-permute-done | bytes 1048608 | tf_op jit(solution)/shard_map/ppermute | solution.py:66
  61.6 1.3 shard_map.160.w_gate
  62.9 4.0 %collective-permute-done.2.rows = bf16[64,4,2048]{2,1,0:T(4,128)(2,1)S(1)} collective-permute-done((bf16[64,4,2048]{2,1,0:T(4,128)(2,1)S(1)}, bf16[64,4,2048]{2,1,0:T(4,128)(2,1)S(1)}, u32[]{:S(2)}, u32[]{:S(2)}) %collective-permute-start.2) | collective-permute-done | bytes 1048608 | tf_op jit(solution)/shard_map/ppermute | solution.py:66
  66.9 1.0 shard_map.162
  67.9 2.8 %collective-permute-start.3 = (bf16[256,256]{1,0:T(8,128)(2,1)S(1)}, bf16[256,256]{1,0:T(8,128)(2,1)S(1)}, u32[]{:S(2)}, u32[]{:S(2)}) collective-permute-start(bf16[256,256]{1,0:T(8,128)(2,1)S(1)} %shard_map.162), channel_id=1, source_target_pairs={{0,3},{1,2},{2,1},{3,0},{4,7},{5,6},{6,5},{7,4},{8,11},{9,10},{10,... | collective-permute-start | bytes 393224 | tf_op jit(solution)/shard_map/ppermute | solution.py:66
  70.7 12.4 %collective-permute-done.1.w_up = bf16[2048,256]{1,0:T(8,128)(2,1)S(1)} collective-permute-done((bf16[2048,256]{1,0:T(8,128)(2,1)}, bf16[2048,256]{1,0:T(8,128)(2,1)S(1)}, u32[]{:S(2)}, u32[]{:S(2)}) %collective-permute-start.1) | collective-permute-done | bytes 1048608 | tf_op jit(solution)/shard_map/ppermute | solution.py:66
  83.2 1.0 shard_map.163
  84.1 2.8 %collective-permute-start.4 = (bf16[256,256]{1,0:T(8,128)(2,1)S(1)}, bf16[256,256]{1,0:T(8,128)(2,1)S(1)}, u32[]{:S(2)}, u32[]{:S(2)}) collective-permute-start(bf16[256,256]{1,0:T(8,128)(2,1)S(1)} %shard_map.163), channel_id=1, source_target_pairs={{0,3},{1,2},{2,1},{3,0},{4,7},{5,6},{6,5},{7,4},{8,11},{9,10},{10,... | collective-permute-start | bytes 393224 | tf_op jit(solution)/shard_map/ppermute | solution.py:66
  87.0 1.0 shard_map.159.h0
  88.0 1.0 shard_map.161.h1
  89.0 0.4 collective-permute-done.6.w2
  89.4 22.5 %collective-permute-done.7.w3 = bf16[256,2048]{1,0:T(8,128)(2,1)S(1)} collective-permute-done((bf16[256,2048]{1,0:T(8,128)(2,1)}, bf16[256,2048]{1,0:T(8,128)(2,1)S(1)}, u32[]{:S(2)}, u32[]{:S(2)}) %collective-permute-start.7) | collective-permute-done | bytes 1048608 | tf_op jit(solution)/shard_map/ppermute | solution.py:66
  111.8 1.0 copy-done.4
  112.8 2.4 %shard_map.164.weights = bf16[4,256,2048]{2,1,0:T(8,128)(2,1)S(1)} custom-call(bf16[256,2048]{1,0:T(8,128)(2,1)} %bitcast.21, bf16[256,2048]{1,0:T(8,128)(2,1)} %collective-permute-done.5.w1, bf16[256,2048]{1,0:T(8,128)(2,1)} %copy-done.3, bf16[256,2048]{1,0:T(8,128)(2,1)} %copy-done.4), custom_call_target="tpu_custom_call" | custom-call | tf_op jit(solution)/shard_map/pallas_call | solution.py:45
  115.3 1.4 collective-permute-done.4.h3
  116.7 2.2 %shard_map.165 = bf16[64,4,2048]{2,1,0:T(4,128)(2,1)} custom-call(bf16[256,256]{1,0:T(8,128)(2,1)S(1)} %shard_map.159.h0, bf16[256,256]{1,0:T(8,128)(2,1)S(1)} %shard_map.161.h1, bf16[256,256]{1,0:T(8,128)(2,1)S(1)} %collective-permute-done.3.h2, bf16[256,256]{1,0:T(8,128)(2,1)S(1)} %collective-permute-done.4.h3, bf16[4,256,2048]{2,1,0:T(8,128)(2,1)S(1)} %shard_map.164.weights), custom_call_target="tpu_custom_call" | custom-call | tf_op jit(solution)/shard_map/pallas_call | solution.py:45
  119.0 7.2 %all-to-all-start.1 = ((bf16[64,4,2048]{2,1,0:T(4,128)(2,1)}), bf16[64,4,2048]{2,1,0:T(4,128)(2,1)S(1)}, u32[]{:S(2)}, u32[]{:S(2)}) async-start(bf16[64,4,2048]{2,1,0:T(4,128)(2,1)} %shard_map.165), calls=%async_computation.1 | async-start | bytes 2097152 | tf_op jit(solution)/shard_map/all_to_all | solution.py:210
  126.2 0.1 multiply_sine_fusion
  126.5 0.9 shard_map.166.l0
  127.3 0.4 collective-permute-start.8
  127.7 3.9 %collective-permute-start.9 = (bf16[32,544]{1,0:T(8,128)(2,1)S(1)}, bf16[32,544]{1,0:T(8,128)(2,1)S(1)}, u32[]{:S(2)}, u32[]{:S(2)}) collective-permute-start(bf16[32,544]{1,0:T(8,128)(2,1)S(1)} %shard_map.166.l0), channel_id=1, source_target_pairs={{0,2},{1,3},{2,0},{3,1},{4,6},{5,7},{6,4},{7,5},{8,10},{9,11},{10,... | collective-permute-start | bytes 104456 | tf_op jit(solution)/shard_map/ppermute | solution.py:61
  131.6 0.2 collective-permute-start.10
  132.1 0.6 collective-permute-done.8.l1
  132.6 1.5 collective-permute-done.9.l2
  134.1 1.6 collective-permute-done.10.l3
  135.6 1.4 shard_map.167
  137.1 1.3 collective-permute-start.11
  138.3 4.6 %collective-permute-start.12 = (bf16[256,128]{1,0:T(8,128)(2,1)S(1)}, bf16[256,128]{1,0:T(8,128)(2,1)S(1)}, u32[]{:S(2)}, u32[]{:S(2)}) collective-permute-start(bf16[256,128]{1,0:T(8,128)(2,1)S(1)} %get-tuple-element.22), channel_id=1, source_target_pairs={{0,128},{64,192},{128,0},{192,64},{1,129},{65,193},{129,1},{193,65... | collective-permute-start | bytes 196616 | tf_op jit(solution)/shard_map/ppermute | solution.py:61
  143.0 0.1 collective-permute-start.13
  143.1 12.0 %collective-permute-done.11.b1.q1 = bf16[256,128]{1,0:T(8,128)(2,1)S(1)} collective-permute-done((bf16[256,128]{1,0:T(8,128)(2,1)S(1)}, bf16[256,128]{1,0:T(8,128)(2,1)S(1)}, u32[]{:S(2)}, u32[]{:S(2)}) %collective-permute-start.11) | collective-permute-done | bytes 65568 | tf_op jit(solution)/shard_map/ppermute | solution.py:61
  155.1 1.2 collective-permute-done.13.b3.q3
  156.3 2.5 %collective-permute-start.14 = (bf16[4,160,128]{2,1,0:T(8,128)(2,1)S(1)}, bf16[4,160,128]{2,1,0:T(8,128)(2,1)S(1)}, u32[]{:S(2)}, u32[]{:S(2)}) collective-permute-start(bf16[4,160,128]{2,1,0:T(8,128)(2,1)S(1)} %shard_map.168), channel_id=1, source_target_pairs={{0,32},{32,0},{1,33},{33,1},{2,34},{34,2},{3,35},{35,3},{4,36},{36... | collective-permute-start | bytes 491528 | tf_op jit(solution)/shard_map/ppermute | solution.py:61
  158.8 4.1 %collective-permute-done.14 = bf16[4,160,128]{2,1,0:T(8,128)(2,1)S(1)} collective-permute-done((bf16[4,160,128]{2,1,0:T(8,128)(2,1)S(1)}, bf16[4,160,128]{2,1,0:T(8,128)(2,1)S(1)}, u32[]{:S(2)}, u32[]{:S(2)}) %collective-permute-start.14) | collective-permute-done | bytes 163872 | tf_op jit(solution)/shard_map/ppermute | solution.py:61
  162.9 1.6 collective-permute-start.15
  164.5 2.8 %collective-permute-start.16 = (bf16[4,160,256]{2,1,0:T(8,128)(2,1)S(1)}, bf16[4,160,256]{2,1,0:T(8,128)(2,1)S(1)}, u32[]{:S(2)}, u32[]{:S(2)}) collective-permute-start(bf16[4,160,256]{2,1,0:T(8,128)(2,1)S(1)} %pad_maximum_fusion.refs_0_), channel_id=1, source_target_pairs={{0,16},{8,24},{16,0},{24,8},{1,17},{9,25},{17,1},{25,9},{2,18},{10... | collective-permute-start | bytes 983048 | tf_op jit(solution)/shard_map/ppermute | solution.py:61
  167.3 1.4 collective-permute-start.17
  168.7 4.8 %collective-permute-done.15.refs_1_ = bf16[4,160,256]{2,1,0:T(8,128)(2,1)S(1)} collective-permute-done((bf16[4,160,256]{2,1,0:T(8,128)(2,1)S(1)}, bf16[4,160,256]{2,1,0:T(8,128)(2,1)S(1)}, u32[]{:S(2)}, u32[]{:S(2)}) %collective-permute-start.15) | collective-permute-done | bytes 327712 | tf_op jit(solution)/shard_map/ppermute | solution.py:61
  173.5 7.7 %collective-permute-done.16.refs_2_ = bf16[4,160,256]{2,1,0:T(8,128)(2,1)S(1)} collective-permute-done((bf16[4,160,256]{2,1,0:T(8,128)(2,1)S(1)}, bf16[4,160,256]{2,1,0:T(8,128)(2,1)S(1)}, u32[]{:S(2)}, u32[]{:S(2)}) %collective-permute-start.16) | collective-permute-done | bytes 327712 | tf_op jit(solution)/shard_map/ppermute | solution.py:61
  181.2 0.5 collective-permute-start.21
  181.7 1.1 collective-permute-done.20.refs_6_
  182.8 0.5 collective-permute-done.21.refs_7_
  183.3 5.8 %shard_map.169 = (bf16[128,64]{1,0:T(8,128)(2,1)S(1)}, bf16[128,64]{1,0:T(8,128)(2,1)S(1)}, bf16[128,64]{1,0:T(8,128)(2,1)S(1)}, bf16[128,64]{1,0:T(8,128)(2,1)S(1)}) custom-call(s32[5]{0:T(128)S(1)} %stack.23.where, bf16[256,128]{1,0:T(8,128)(2,1)S(1)} %get-tuple-element.20.b0.q0, bf16[256,128]{1,0:T(8,128)(2,1)S(1)} %collective-permute-done.11.b1.q1, ...), custom_call_target="tpu_custom_call" | custom-call | tf_op jit(solution)/shard_map/pallas_call | solution.py:45
  189.1 0.4 collective-permute-start.22
  189.4 3.9 %collective-permute-start.23 = (bf16[128,64]{1,0:T(8,128)(2,1)S(1)}, bf16[128,64]{1,0:T(8,128)(2,1)S(1)}, u32[]{:S(2)}, u32[]{:S(2)}) collective-permute-start(bf16[128,64]{1,0:T(8,128)(2,1)S(1)} %get-tuple-element.26), channel_id=1, source_target_pairs={{0,2},{1,3},{2,0},{3,1},{4,6},{5,7},{6,4},{7,5},{8,10},{9,11},{10,... | collective-permute-start | bytes 49160 | tf_op jit(solution)/shard_map/ppermute | solution.py:61
  193.4 0.2 collective-permute-start.24
  193.6 0.7 collective-permute-done.22.a1
  194.3 1.3 collective-permute-done.23.a2
  195.6 1.7 collective-permute-done.24.a3
  197.3 0.7 shard_map.170
  198.0 1.2 collective-permute-start.25
  199.2 2.4 %collective-permute-start.26 = (bf16[32,256]{1,0:T(8,128)(2,1)S(1)}, bf16[32,256]{1,0:T(8,128)(2,1)S(1)}, u32[]{:S(2)}, u32[]{:S(2)}) collective-permute-start(bf16[32,256]{1,0:T(8,128)(2,1)S(1)} %get-tuple-element.30), channel_id=1, source_target_pairs={{0,128},{64,192},{128,0},{192,64},{1,129},{65,193},{129,1},{193,65... | collective-permute-start | bytes 49160 | tf_op jit(solution)/shard_map/ppermute | solution.py:61
  201.5 2.8 %collective-permute-start.27 = (bf16[32,256]{1,0:T(8,128)(2,1)S(1)}, bf16[32,256]{1,0:T(8,128)(2,1)S(1)}, u32[]{:S(2)}, u32[]{:S(2)}) collective-permute-start(bf16[32,256]{1,0:T(8,128)(2,1)S(1)} %get-tuple-element.31), channel_id=1, source_target_pairs={{0,192},{64,0},{128,64},{192,128},{1,193},{65,1},{129,65},{193,129... | collective-permute-start | bytes 49160 | tf_op jit(solution)/shard_map/ppermute | solution.py:61
  204.4 2.5 %collective-permute-done.26.a2 = bf16[32,256]{1,0:T(8,128)(2,1)S(1)} collective-permute-done((bf16[32,256]{1,0:T(8,128)(2,1)S(1)}, bf16[32,256]{1,0:T(8,128)(2,1)S(1)}, u32[]{:S(2)}, u32[]{:S(2)}) %collective-permute-start.26) | collective-permute-done | bytes 16416 | tf_op jit(solution)/shard_map/ppermute | solution.py:61
  206.8 0.6 collective-permute-done.27.a3
  207.4 3.9 %finish.1 = (bf16[64,2048]{1,0:T(8,128)(2,1)}, bf16[32,2048]{1,0:T(8,128)(2,1)}) custom-call(s32[5]{0:T(128)S(1)} %stack.23.where, bf16[64,4,2048]{2,1,0:T(4,128)(2,1)S(1)} %all-to-all-done.1.returned, bf16[256,128]{1,0:T(8,128)(2,1)S(1)} %copy-done.2, bf16[32,256]{1,0:T(8,128)(2,1)S(1)} %get-tuple-element.28.a0, ...), custom_call_target="tpu_custom_call" | custom-call | tf_op jit(solution)/shard_map/finish/pallas_call | solution.py:231
  (28 shorter events, 0.4 us)
Async XLA Ops:
  0.6 66.3 %copy-start = (bf16[1,2048,256]{2,1,0:T(8,128)(2,1)S(1)}, bf16[1,2048,256]{2,1,0:T(8,128)(2,1)}, u32[]{:S(2)}) copy-start(bf16[1,2048,256]{2,1,0:T(8,128)(2,1)} %param.27) | copy-start | bytes 3145732
  0.6 66.3 %copy-start.1 = (bf16[1,2048,256]{2,1,0:T(8,128)(2,1)S(1)}, bf16[1,2048,256]{2,1,0:T(8,128)(2,1)}, u32[]{:S(2)}) copy-start(bf16[1,2048,256]{2,1,0:T(8,128)(2,1)} %param.28) | copy-start | bytes 3145732
  3.4 36.2 %all-to-all-start = ((bf16[64,4,2048]{2,1,0:T(4,128)(2,1)}), bf16[64,4,2048]{2,1,0:T(4,128)(2,1)S(1)}, u32[]{:S(2)}, u32[]{:S(2)}) async-start(bf16[64,4,2048]{2,1,0:T(4,128)(2,1)} %get-tuple-element.18), calls=%async_computation | async-start | bytes 2097152 | tf_op jit(solution)/shard_map/all_to_all | solution.py:197
  12.7 31.1 %collective-permute-start.5 = (bf16[256,2048]{1,0:T(8,128)(2,1)}, bf16[256,2048]{1,0:T(8,128)(2,1)}, u32[]{:S(2)}, u32[]{:S(2)}) collective-permute-start(bf16[256,2048]{1,0:T(8,128)(2,1)} %bitcast.19), channel_id=1, source_target_pairs={{0,1},{1,0},{2,3},{3,2},{4,5},{5,4},{6,7},{7,6},{8,9},{9,8},{10,11... | collective-permute-start | bytes 3145736 | tf_op jit(solution)/shard_map/ppermute | solution.py:66
  14.3 47.3 %collective-permute-start = (bf16[2048,256]{1,0:T(8,128)(2,1)}, bf16[2048,256]{1,0:T(8,128)(2,1)}, u32[]{:S(2)}, u32[]{:S(2)}) collective-permute-start(bf16[2048,256]{1,0:T(8,128)(2,1)} %bitcast.13), channel_id=1, source_target_pairs={{0,1},{1,0},{2,3},{3,2},{4,5},{5,4},{6,7},{7,6},{8,9},{9,8},{10,11... | collective-permute-start | bytes 3145736 | tf_op jit(solution)/shard_map/ppermute | solution.py:66
  39.6 27.2 %collective-permute-start.2 = (bf16[64,4,2048]{2,1,0:T(4,128)(2,1)S(1)}, bf16[64,4,2048]{2,1,0:T(4,128)(2,1)S(1)}, u32[]{:S(2)}, u32[]{:S(2)}) collective-permute-start(bf16[64,4,2048]{2,1,0:T(4,128)(2,1)S(1)} %all-to-all-done.rows), channel_id=1, source_target_pairs={{0,3},{1,2},{2,1},{3,0},{4,7},{5,6},{6,5},{7,4},{8,11},{9,10},{10,... | collective-permute-start | bytes 3145736 | tf_op jit(solution)/shard_map/ppermute | solution.py:66
  42.4 40.7 %collective-permute-start.1 = (bf16[2048,256]{1,0:T(8,128)(2,1)}, bf16[2048,256]{1,0:T(8,128)(2,1)S(1)}, u32[]{:S(2)}, u32[]{:S(2)}) collective-permute-start(bf16[2048,256]{1,0:T(8,128)(2,1)} %bitcast.16), channel_id=1, source_target_pairs={{0,1},{1,0},{2,3},{3,2},{4,5},{5,4},{6,7},{7,6},{8,9},{9,8},{10,11... | collective-permute-start | bytes 3145736 | tf_op jit(solution)/shard_map/ppermute | solution.py:66
  42.6 46.7 %collective-permute-start.6 = (bf16[256,2048]{1,0:T(8,128)(2,1)}, bf16[256,2048]{1,0:T(8,128)(2,1)S(1)}, u32[]{:S(2)}, u32[]{:S(2)}) collective-permute-start(bf16[256,2048]{1,0:T(8,128)(2,1)} %bitcast.20), channel_id=1, source_target_pairs={{0,3},{1,2},{2,1},{3,0},{4,7},{5,6},{6,5},{7,4},{8,11},{9,10},{10,... | collective-permute-start | bytes 3145736 | tf_op jit(solution)/shard_map/ppermute | solution.py:66
  43.8 68.1 %collective-permute-start.7 = (bf16[256,2048]{1,0:T(8,128)(2,1)}, bf16[256,2048]{1,0:T(8,128)(2,1)S(1)}, u32[]{:S(2)}, u32[]{:S(2)}) collective-permute-start(bf16[256,2048]{1,0:T(8,128)(2,1)} %collective-permute-done.5.w1), channel_id=1, source_target_pairs={{0,3},{1,2},{2,1},{3,0},{4,7},{5,6},{6,5},{7,4},{8,11},{9,10},{10,... | collective-permute-start | bytes 3145736 | tf_op jit(solution)/shard_map/ppermute | solution.py:66
  67.9 47.4 %collective-permute-start.3 = (bf16[256,256]{1,0:T(8,128)(2,1)S(1)}, bf16[256,256]{1,0:T(8,128)(2,1)S(1)}, u32[]{:S(2)}, u32[]{:S(2)}) collective-permute-start(bf16[256,256]{1,0:T(8,128)(2,1)S(1)} %shard_map.162), channel_id=1, source_target_pairs={{0,3},{1,2},{2,1},{3,0},{4,7},{5,6},{6,5},{7,4},{8,11},{9,10},{10,... | collective-permute-start | bytes 393224 | tf_op jit(solution)/shard_map/ppermute | solution.py:66
  84.1 32.6 %collective-permute-start.4 = (bf16[256,256]{1,0:T(8,128)(2,1)S(1)}, bf16[256,256]{1,0:T(8,128)(2,1)S(1)}, u32[]{:S(2)}, u32[]{:S(2)}) collective-permute-start(bf16[256,256]{1,0:T(8,128)(2,1)S(1)} %shard_map.163), channel_id=1, source_target_pairs={{0,3},{1,2},{2,1},{3,0},{4,7},{5,6},{6,5},{7,4},{8,11},{9,10},{10,... | collective-permute-start | bytes 393224 | tf_op jit(solution)/shard_map/ppermute | solution.py:66
  89.4 22.5 %copy-start.3 = (bf16[256,2048]{1,0:T(8,128)(2,1)}, bf16[256,2048]{1,0:T(8,128)(2,1)S(1)}, u32[]{:S(2)}) copy-start(bf16[256,2048]{1,0:T(8,128)(2,1)S(1)} %collective-permute-done.6.w2) | copy-start | bytes 3145732
  111.8 1.0 copy-start.4
  119.0 88.4 %copy-start.2 = (bf16[256,128]{1,0:T(8,128)(2,1)S(1)}, bf16[256,128]{1,0:T(8,128)(2,1)}, u32[]{:S(2)}) copy-start(bf16[256,128]{1,0:T(8,128)(2,1)} %get-tuple-element.19.shares) | copy-start | bytes 196612
  119.0 88.4 %all-to-all-start.1 = ((bf16[64,4,2048]{2,1,0:T(4,128)(2,1)}), bf16[64,4,2048]{2,1,0:T(4,128)(2,1)S(1)}, u32[]{:S(2)}, u32[]{:S(2)}) async-start(bf16[64,4,2048]{2,1,0:T(4,128)(2,1)} %shard_map.165), calls=%async_computation.1 | async-start | bytes 2097152 | tf_op jit(solution)/shard_map/all_to_all | solution.py:210
  127.3 5.3 %collective-permute-start.8 = (bf16[32,544]{1,0:T(8,128)(2,1)S(1)}, bf16[32,544]{1,0:T(8,128)(2,1)S(1)}, u32[]{:S(2)}, u32[]{:S(2)}) collective-permute-start(bf16[32,544]{1,0:T(8,128)(2,1)S(1)} %shard_map.166.l0), channel_id=1, source_target_pairs={{0,1},{1,2},{2,3},{3,0},{4,5},{5,6},{6,7},{7,4},{8,9},{9,10},{10,1... | collective-permute-start | bytes 104456 | tf_op jit(solution)/shard_map/ppermute | solution.py:61
  127.7 6.4 %collective-permute-start.9 = (bf16[32,544]{1,0:T(8,128)(2,1)S(1)}, bf16[32,544]{1,0:T(8,128)(2,1)S(1)}, u32[]{:S(2)}, u32[]{:S(2)}) collective-permute-start(bf16[32,544]{1,0:T(8,128)(2,1)S(1)} %shard_map.166.l0), channel_id=1, source_target_pairs={{0,2},{1,3},{2,0},{3,1},{4,6},{5,7},{6,4},{7,5},{8,10},{9,11},{10,... | collective-permute-start | bytes 104456 | tf_op jit(solution)/shard_map/ppermute | solution.py:61
  131.6 4.0 %collective-permute-start.10 = (bf16[32,544]{1,0:T(8,128)(2,1)S(1)}, bf16[32,544]{1,0:T(8,128)(2,1)S(1)}, u32[]{:S(2)}, u32[]{:S(2)}) collective-permute-start(bf16[32,544]{1,0:T(8,128)(2,1)S(1)} %shard_map.166.l0), channel_id=1, source_target_pairs={{0,3},{1,0},{2,1},{3,2},{4,7},{5,4},{6,5},{7,6},{8,11},{9,8},{10,9... | collective-permute-start | bytes 104456 | tf_op jit(solution)/shard_map/ppermute | solution.py:61
  137.1 18.0 %collective-permute-start.11 = (bf16[256,128]{1,0:T(8,128)(2,1)S(1)}, bf16[256,128]{1,0:T(8,128)(2,1)S(1)}, u32[]{:S(2)}, u32[]{:S(2)}) collective-permute-start(bf16[256,128]{1,0:T(8,128)(2,1)S(1)} %get-tuple-element.21), channel_id=1, source_target_pairs={{0,64},{64,128},{128,192},{192,0},{1,65},{65,129},{129,193},{193,1... | collective-permute-start | bytes 196616 | tf_op jit(solution)/shard_map/ppermute | solution.py:61
  138.3 16.7 %collective-permute-start.12 = (bf16[256,128]{1,0:T(8,128)(2,1)S(1)}, bf16[256,128]{1,0:T(8,128)(2,1)S(1)}, u32[]{:S(2)}, u32[]{:S(2)}) collective-permute-start(bf16[256,128]{1,0:T(8,128)(2,1)S(1)} %get-tuple-element.22), channel_id=1, source_target_pairs={{0,128},{64,192},{128,0},{192,64},{1,129},{65,193},{129,1},{193,65... | collective-permute-start | bytes 196616 | tf_op jit(solution)/shard_map/ppermute | solution.py:61
  143.0 13.3 %collective-permute-start.13 = (bf16[256,128]{1,0:T(8,128)(2,1)S(1)}, bf16[256,128]{1,0:T(8,128)(2,1)S(1)}, u32[]{:S(2)}, u32[]{:S(2)}) collective-permute-start(bf16[256,128]{1,0:T(8,128)(2,1)S(1)} %get-tuple-element.23), channel_id=1, source_target_pairs={{0,192},{64,0},{128,64},{192,128},{1,193},{65,1},{129,65},{193,129... | collective-permute-start | bytes 196616 | tf_op jit(solution)/shard_map/ppermute | solution.py:61
  156.3 6.5 %collective-permute-start.14 = (bf16[4,160,128]{2,1,0:T(8,128)(2,1)S(1)}, bf16[4,160,128]{2,1,0:T(8,128)(2,1)S(1)}, u32[]{:S(2)}, u32[]{:S(2)}) collective-permute-start(bf16[4,160,128]{2,1,0:T(8,128)(2,1)S(1)} %shard_map.168), channel_id=1, source_target_pairs={{0,32},{32,0},{1,33},{33,1},{2,34},{34,2},{3,35},{35,3},{4,36},{36... | collective-permute-start | bytes 491528 | tf_op jit(solution)/shard_map/ppermute | solution.py:61
  162.9 10.6 %collective-permute-start.15 = (bf16[4,160,256]{2,1,0:T(8,128)(2,1)S(1)}, bf16[4,160,256]{2,1,0:T(8,128)(2,1)S(1)}, u32[]{:S(2)}, u32[]{:S(2)}) collective-permute-start(bf16[4,160,256]{2,1,0:T(8,128)(2,1)S(1)} %pad_maximum_fusion.refs_0_), channel_id=1, source_target_pairs={{0,8},{8,16},{16,24},{24,0},{1,9},{9,17},{17,25},{25,1},{2,10},{10... | collective-permute-start | bytes 983048 | tf_op jit(solution)/shard_map/ppermute | solution.py:61
  164.5 16.7 %collective-permute-start.16 = (bf16[4,160,256]{2,1,0:T(8,128)(2,1)S(1)}, bf16[4,160,256]{2,1,0:T(8,128)(2,1)S(1)}, u32[]{:S(2)}, u32[]{:S(2)}) collective-permute-start(bf16[4,160,256]{2,1,0:T(8,128)(2,1)S(1)} %pad_maximum_fusion.refs_0_), channel_id=1, source_target_pairs={{0,16},{8,24},{16,0},{24,8},{1,17},{9,25},{17,1},{25,9},{2,18},{10... | collective-permute-start | bytes 983048 | tf_op jit(solution)/shard_map/ppermute | solution.py:61
  167.3 13.9 %collective-permute-start.17 = (bf16[4,160,256]{2,1,0:T(8,128)(2,1)S(1)}, bf16[4,160,256]{2,1,0:T(8,128)(2,1)S(1)}, u32[]{:S(2)}, u32[]{:S(2)}) collective-permute-start(bf16[4,160,256]{2,1,0:T(8,128)(2,1)S(1)} %pad_maximum_fusion.refs_0_), channel_id=1, source_target_pairs={{0,24},{8,0},{16,8},{24,16},{1,25},{9,1},{17,9},{25,17},{2,26},{10... | collective-permute-start | bytes 983048 | tf_op jit(solution)/shard_map/ppermute | solution.py:61
  168.7 13.0 %collective-permute-start.18 = (bf16[4,160,256]{2,1,0:T(8,128)(2,1)S(1)}, bf16[4,160,256]{2,1,0:T(8,128)(2,1)S(1)}, u32[]{:S(2)}, u32[]{:S(2)}) collective-permute-start(bf16[4,160,256]{2,1,0:T(8,128)(2,1)S(1)} %pad_maximum_fusion.refs_0_), channel_id=1, source_target_pairs={{0,4},{4,0},{1,5},{5,1},{2,6},{6,2},{3,7},{7,3},{8,12},{12,8},{9,1... | collective-permute-start | bytes 983048 | tf_op jit(solution)/shard_map/ppermute | solution.py:61
  173.5 8.2 %collective-permute-start.19 = (bf16[4,160,256]{2,1,0:T(8,128)(2,1)S(1)}, bf16[4,160,256]{2,1,0:T(8,128)(2,1)S(1)}, u32[]{:S(2)}, u32[]{:S(2)}) collective-permute-start(bf16[4,160,256]{2,1,0:T(8,128)(2,1)S(1)} %collective-permute-done.15.refs_1_), channel_id=1, source_target_pairs={{0,4},{4,0},{1,5},{5,1},{2,6},{6,2},{3,7},{7,3},{8,12},{12,8},{9,1... | collective-permute-start | bytes 983048 | tf_op jit(solution)/shard_map/ppermute | solution.py:61
  181.2 1.6 collective-permute-start.20
  181.2 2.1 collective-permute-start.21
  189.1 5.2 %collective-permute-start.22 = (bf16[128,64]{1,0:T(8,128)(2,1)S(1)}, bf16[128,64]{1,0:T(8,128)(2,1)S(1)}, u32[]{:S(2)}, u32[]{:S(2)}) collective-permute-start(bf16[128,64]{1,0:T(8,128)(2,1)S(1)} %get-tuple-element.25), channel_id=1, source_target_pairs={{0,1},{1,2},{2,3},{3,0},{4,5},{5,6},{6,7},{7,4},{8,9},{9,10},{10,1... | collective-permute-start | bytes 49160 | tf_op jit(solution)/shard_map/ppermute | solution.py:61
  189.4 6.2 %collective-permute-start.23 = (bf16[128,64]{1,0:T(8,128)(2,1)S(1)}, bf16[128,64]{1,0:T(8,128)(2,1)S(1)}, u32[]{:S(2)}, u32[]{:S(2)}) collective-permute-start(bf16[128,64]{1,0:T(8,128)(2,1)S(1)} %get-tuple-element.26), channel_id=1, source_target_pairs={{0,2},{1,3},{2,0},{3,1},{4,6},{5,7},{6,4},{7,5},{8,10},{9,11},{10,... | collective-permute-start | bytes 49160 | tf_op jit(solution)/shard_map/ppermute | solution.py:61
  193.4 3.9 %collective-permute-start.24 = (bf16[128,64]{1,0:T(8,128)(2,1)S(1)}, bf16[128,64]{1,0:T(8,128)(2,1)S(1)}, u32[]{:S(2)}, u32[]{:S(2)}) collective-permute-start(bf16[128,64]{1,0:T(8,128)(2,1)S(1)} %get-tuple-element.27), channel_id=1, source_target_pairs={{0,3},{1,0},{2,1},{3,2},{4,7},{5,4},{6,5},{7,6},{8,11},{9,8},{10,9... | collective-permute-start | bytes 49160 | tf_op jit(solution)/shard_map/ppermute | solution.py:61
  198.0 6.4 %collective-permute-start.25 = (bf16[32,256]{1,0:T(8,128)(2,1)S(1)}, bf16[32,256]{1,0:T(8,128)(2,1)S(1)}, u32[]{:S(2)}, u32[]{:S(2)}) collective-permute-start(bf16[32,256]{1,0:T(8,128)(2,1)S(1)} %get-tuple-element.29), channel_id=1, source_target_pairs={{0,64},{64,128},{128,192},{192,0},{1,65},{65,129},{129,193},{193,1... | collective-permute-start | bytes 49160 | tf_op jit(solution)/shard_map/ppermute | solution.py:61
  199.2 7.6 %collective-permute-start.26 = (bf16[32,256]{1,0:T(8,128)(2,1)S(1)}, bf16[32,256]{1,0:T(8,128)(2,1)S(1)}, u32[]{:S(2)}, u32[]{:S(2)}) collective-permute-start(bf16[32,256]{1,0:T(8,128)(2,1)S(1)} %get-tuple-element.30), channel_id=1, source_target_pairs={{0,128},{64,192},{128,0},{192,64},{1,129},{65,193},{129,1},{193,65... | collective-permute-start | bytes 49160 | tf_op jit(solution)/shard_map/ppermute | solution.py:61
  201.5 5.8 %collective-permute-start.27 = (bf16[32,256]{1,0:T(8,128)(2,1)S(1)}, bf16[32,256]{1,0:T(8,128)(2,1)S(1)}, u32[]{:S(2)}, u32[]{:S(2)}) collective-permute-start(bf16[32,256]{1,0:T(8,128)(2,1)S(1)} %get-tuple-element.31), channel_id=1, source_target_pairs={{0,192},{64,0},{128,64},{192,128},{1,193},{65,1},{129,65},{193,129... | collective-permute-start | bytes 49160 | tf_op jit(solution)/shard_map/ppermute | solution.py:61

commit v13 on v12

--- a/solution.py
+++ b/solution.py
@@ -146,6 +146,46 @@
     shape = jax.ShapeDtypeStruct((rows.shape[0] * CAP, weights[0].shape[1]), BF)
     scratch = [pltpu.VMEM(shape.shape, F32)] * 2
     return call(hidden_kernel, shape, [rows] + weights, scratch=scratch)
+
+
+def late_hidden_kernel(rows, w_gate, w_up, out, gate_s, up_s, up_v, sems):
+    count, steps = out.shape[0], sems.shape[0]
+    span = w_up.shape[0] // steps
+    parts = [slice(c * span, (c + 1) * span) for c in range(steps)]
+    copies = [
+        pltpu.make_async_copy(w_up.at[pl.ds(c * span, span), :], up_v.at[c], sems.at[c])
+        for c in range(steps)
+    ]
+    for copy in copies:
+        copy.start()
+    for c, cols in enumerate(parts):
+        got = rows[:, :, cols].reshape(count, span)
+        gate = mm(got, w_gate[cols, :])
+        copies[c].wait()
+        up = mm(got, up_v[c])
+        gate_s[...] = gate if c == 0 else gate_s[...] + gate
+        up_s[...] = up if c == 0 else up_s[...] + up
+    gate = gate_s[...]
+    out[...] = (gate / (1.0 + jnp.exp(-gate)) * up_s[...]).astype(BF)
+
+
+def late_hidden_of(rows, w_gate, w_up):
+    height, units = w_up.shape
+    shape = (rows.shape[0] * CAP, units)
+    near = [pltpu.with_memory_space_constraint(a, pltpu.VMEM) for a in (rows, w_gate)]
+    return pl.pallas_call(
+        late_hidden_kernel,
+        in_specs=[VMEM_SPEC] * 2 + [pl.BlockSpec(memory_space=pl.ANY)],
+        out_specs=VMEM_SPEC,
+        out_shape=pltpu.VMEM(shape, BF),
+        scratch_shapes=[
+            pltpu.VMEM(shape, F32),
+            pltpu.VMEM(shape, F32),
+            pltpu.VMEM((4, height // 4, units), BF),
+            pltpu.SemaphoreType.DMA((4,)),
+        ],
+        compiler_params=pltpu.CompilerParams(vmem_limit_bytes=8 << 20),
+    )(*near, pltpu.with_memory_space_constraint(w_up, pltpu.HBM))
 
 
 def copy_kernel(value, out):
@@ -200,7 +240,7 @@
     parts = attend(where, queries, pair)
     own_a = hidden_of(arrived, set_a)
     mate_a = paired(hidden_of(mate_rows, set_a), row_mate)
-    mate_b = paired(hidden_of(mate_rows, set_b), row_mate)
+    mate_b = paired(late_hidden_of(mate_rows, *set_b), row_mate)
     own_b = hidden_of(arrived, set_b)
     shape = jax.ShapeDtypeStruct((4, *w_down.shape), BF)
     down = call(stage_kernel, shape, [w_down, down_w, down_r, down_rw], unplaced=range(4))

time: 216 us -> 216 us (level)
  waiting for transfers between devices: 123 us -> 120 us
  local copies, waits for them, and re-layouts: 1.09 us -> 3.27 us
    ppermute x8, waiting for transfers between devices: 56.4 us -> 53.3 us  [paired(): return lax.ppermute(value, 'x', [(i, mate(i)) for i in range(n)])]
    unnamed x10 -> x14, local copies, waits for them, and re-layouts: 1 us -> 3.19 us
    pallas_call x13 -> x12, Pallas kernels: 21.5 us -> 20.5 us  [call(): pl.pallas_call(kernel, in_specs=specs, out_specs=VMEM_SPEC if single else...]
  transfers between devices with their start and end apart: 30 -> 30, of which waited for: 22 -> 21; matrix products, arithmetic and copies ran while one was open for 0% -> 0% of each run, Pallas kernels for 8% -> 8%
where the time goes in v13:
time: 216 us; the launch traced here: 211 us
  waiting for transfers between devices  120 us (56%)
  starting transfers between devices  60.8 us (28%)
  Pallas kernels  26.3 us (12%)
  local copies, waits for them, and re-layouts  3.27 us (2%)
    ppermute x8, waiting for transfers between devices, paired(): return lax.ppermute(value, 'x', [(i, mate(i)) for i in range(n)])  53.3 us
    ppermute x20, waiting for transfers between devices, shifted(): return lax.ppermute(value, axis, [(i, (i + amount) % n) for i in range(n)])  41.5 us
    ppermute x20, starting transfers between devices, shifted(): return lax.ppermute(value, axis, [(i, (i + amount) % n) for i in range(n)])  30.3 us
    all_to_all x1, waiting for transfers between devices, both_halves(): lax.all_to_all(outgoing, EP, split_axis=0, concat_axis=0, tiled=True)  24.8 us
    pallas_call x12, Pallas kernels, call(): pl.pallas_call(kernel, in_specs=specs, out_specs=VMEM_SPEC if single else...  20.5 us
    ppermute x8, starting transfers between devices, paired(): return lax.ppermute(value, 'x', [(i, mate(i)) for i in range(n)])  14 us
    all_to_all x1, starting transfers between devices, both_halves(): lax.all_to_all(outgoing, EP, split_axis=0, concat_axis=0, tiled=True)  9.29 us
    all_to_all x1, starting transfers between devices, both_halves(): lax.all_to_all(result, EP, split_axis=0, concat_axis=0, tiled=True)  7.23 us
  transfers between devices with their start and end apart: 30, of which 21 were waited for; matrix products, arithmetic and copies ran while one was open for 0% of the time, Pallas kernels for 8%

profile of v13, /device:TPU:224, one launch (start us, length us, event | category | flops | bytes accessed | tf_op | source)
XLA Modules:
  0.0 211.5 jit_solution(4304477810535431400)
XLA Ops:
  0.7 2.8 %shard_map.158 = (bf16[64,4,2048]{2,1,0:T(4,128)(2,1)}, bf16[256,128]{1,0:T(8,128)(2,1)}) custom-call(bf16[64,2048]{1,0:T(8,128)(2,1)} %tokens.1, f32[1,2048]{1,0:T(1,128)} %bitcast.22, s32[2,64]{1,0:T(2,128)} %bitcast.24, f32[1,64]{1,0:T(1,128)} %bitcast.26, f32[2,64]{1,0:T(2,128)} %bitcast.25), custom_call_target="tpu_custom_call" | custom-call | tf_op jit(solution)/shard_map/pallas_call | solution.py:45
  3.4 9.3 %all-to-all-start = ((bf16[64,4,2048]{2,1,0:T(4,128)(2,1)}), bf16[64,4,2048]{2,1,0:T(4,128)(2,1)S(1)}, u32[]{:S(2)}, u32[]{:S(2)}) async-start(bf16[64,4,2048]{2,1,0:T(4,128)(2,1)} %get-tuple-element.18), calls=%async_computation | async-start | bytes 2097152 | tf_op jit(solution)/shard_map/all_to_all | solution.py:237
  12.7 1.6 collective-permute-start.5
  14.3 0.5 collective-permute-start
  14.8 24.8 %all-to-all-done.rows = bf16[64,4,2048]{2,1,0:T(4,128)(2,1)S(1)} async-done(((bf16[64,4,2048]{2,1,0:T(4,128)(2,1)}), bf16[64,4,2048]{2,1,0:T(4,128)(2,1)S(1)}, u32[]{:S(2)}, u32[]{:S(2)}) %all-to-all-start) | async-done | bytes 1048608 | tf_op jit(solution)/shard_map/all_to_all | solution.py:237
  39.6 2.8 %collective-permute-start.2 = (bf16[64,4,2048]{2,1,0:T(4,128)(2,1)S(1)}, bf16[64,4,2048]{2,1,0:T(4,128)(2,1)S(1)}, u32[]{:S(2)}, u32[]{:S(2)}) collective-permute-start(bf16[64,4,2048]{2,1,0:T(4,128)(2,1)S(1)} %all-to-all-done.rows), channel_id=1, source_target_pairs={{0,3},{1,2},{2,1},{3,0},{4,7},{5,6},{6,5},{7,4},{8,11},{9,10},{10,... | collective-permute-start | bytes 3145736 | tf_op jit(solution)/shard_map/ppermute | solution.py:66
  42.4 0.2 collective-permute-start.1
  42.6 1.1 collective-permute-start.6
  43.8 2.1 collective-permute-start.7
  45.9 15.8 %collective-permute-done.value = bf16[2048,256]{1,0:T(8,128)(2,1)} collective-permute-done((bf16[2048,256]{1,0:T(8,128)(2,1)}, bf16[2048,256]{1,0:T(8,128)(2,1)}, u32[]{:S(2)}, u32[]{:S(2)}) %collective-permute-start) | collective-permute-done | bytes 1048608 | tf_op jit(solution)/shard_map/ppermute | solution.py:66
  61.6 1.3 shard_map.160.w_gate
  62.9 4.0 %collective-permute-done.2.rows = bf16[64,4,2048]{2,1,0:T(4,128)(2,1)S(1)} collective-permute-done((bf16[64,4,2048]{2,1,0:T(4,128)(2,1)S(1)}, bf16[64,4,2048]{2,1,0:T(4,128)(2,1)S(1)}, u32[]{:S(2)}, u32[]{:S(2)}) %collective-permute-start.2) | collective-permute-done | bytes 1048608 | tf_op jit(solution)/shard_map/ppermute | solution.py:66
  66.9 1.0 shard_map.162
  67.9 2.8 %collective-permute-start.3 = (bf16[256,256]{1,0:T(8,128)(2,1)S(1)}, bf16[256,256]{1,0:T(8,128)(2,1)S(1)}, u32[]{:S(2)}, u32[]{:S(2)}) collective-permute-start(bf16[256,256]{1,0:T(8,128)(2,1)S(1)} %shard_map.162), channel_id=1, source_target_pairs={{0,3},{1,2},{2,1},{3,0},{4,7},{5,6},{6,5},{7,4},{8,11},{9,10},{10,... | collective-permute-start | bytes 393224 | tf_op jit(solution)/shard_map/ppermute | solution.py:66
  70.7 12.4 %collective-permute-done.1.w_up = bf16[2048,256]{1,0:T(8,128)(2,1)S(1)} collective-permute-done((bf16[2048,256]{1,0:T(8,128)(2,1)}, bf16[2048,256]{1,0:T(8,128)(2,1)S(1)}, u32[]{:S(2)}, u32[]{:S(2)}) %collective-permute-start.1) | collective-permute-done | bytes 1048608 | tf_op jit(solution)/shard_map/ppermute | solution.py:66
  83.1 1.0 copy-done.2
  84.1 1.9 shard_map.163
  86.1 2.8 %collective-permute-start.4 = (bf16[256,256]{1,0:T(8,128)(2,1)S(1)}, bf16[256,256]{1,0:T(8,128)(2,1)S(1)}, u32[]{:S(2)}, u32[]{:S(2)}) collective-permute-start(bf16[256,256]{1,0:T(8,128)(2,1)S(1)} %shard_map.163), channel_id=1, source_target_pairs={{0,3},{1,2},{2,1},{3,0},{4,7},{5,6},{6,5},{7,4},{8,11},{9,10},{10,... | collective-permute-start | bytes 393224 | tf_op jit(solution)/shard_map/ppermute | solution.py:66
  88.9 1.0 shard_map.159.h0
  89.9 1.2 copy-done.3
  91.1 1.0 shard_map.161.h1
  92.2 19.7 %collective-permute-done.7.w3 = bf16[256,2048]{1,0:T(8,128)(2,1)S(1)} collective-permute-done((bf16[256,2048]{1,0:T(8,128)(2,1)}, bf16[256,2048]{1,0:T(8,128)(2,1)S(1)}, u32[]{:S(2)}, u32[]{:S(2)}) %collective-permute-start.7) | collective-permute-done | bytes 1048608 | tf_op jit(solution)/shard_map/ppermute | solution.py:66
  111.8 1.0 copy-done.6
  112.8 2.4 %shard_map.164.weights = bf16[4,256,2048]{2,1,0:T(8,128)(2,1)S(1)} custom-call(bf16[256,2048]{1,0:T(8,128)(2,1)} %bitcast.21, bf16[256,2048]{1,0:T(8,128)(2,1)} %collective-permute-done.5.w1, bf16[256,2048]{1,0:T(8,128)(2,1)} %copy-done.5, bf16[256,2048]{1,0:T(8,128)(2,1)} %copy-done.6), custom_call_target="tpu_custom_call" | custom-call | tf_op jit(solution)/shard_map/pallas_call | solution.py:45
  115.3 1.4 collective-permute-done.4.h3
  116.7 2.3 %shard_map.165 = bf16[64,4,2048]{2,1,0:T(4,128)(2,1)} custom-call(bf16[256,256]{1,0:T(8,128)(2,1)S(1)} %shard_map.159.h0, bf16[256,256]{1,0:T(8,128)(2,1)S(1)} %shard_map.161.h1, bf16[256,256]{1,0:T(8,128)(2,1)S(1)} %collective-permute-done.3.h2, bf16[256,256]{1,0:T(8,128)(2,1)S(1)} %collective-permute-done.4.h3, bf16[4,256,2048]{2,1,0:T(8,128)(2,1)S(1)} %shard_map.164.weights), custom_call_target="tpu_custom_call" | custom-call | tf_op jit(solution)/shard_map/pallas_call | solution.py:45
  119.0 7.2 %all-to-all-start.1 = ((bf16[64,4,2048]{2,1,0:T(4,128)(2,1)}), bf16[64,4,2048]{2,1,0:T(4,128)(2,1)S(1)}, u32[]{:S(2)}, u32[]{:S(2)}) async-start(bf16[64,4,2048]{2,1,0:T(4,128)(2,1)} %shard_map.165), calls=%async_computation.1 | async-start | bytes 2097152 | tf_op jit(solution)/shard_map/all_to_all | solution.py:250
  126.2 0.1 multiply_sine_fusion
  126.5 0.9 shard_map.166.l0
  127.4 0.4 collective-permute-start.8
  127.7 3.9 %collective-permute-start.9 = (bf16[32,544]{1,0:T(8,128)(2,1)S(1)}, bf16[32,544]{1,0:T(8,128)(2,1)S(1)}, u32[]{:S(2)}, u32[]{:S(2)}) collective-permute-start(bf16[32,544]{1,0:T(8,128)(2,1)S(1)} %shard_map.166.l0), channel_id=1, source_target_pairs={{0,2},{1,3},{2,0},{3,1},{4,6},{5,7},{6,4},{7,5},{8,10},{9,11},{10,... | collective-permute-start | bytes 104456 | tf_op jit(solution)/shard_map/ppermute | solution.py:61
  131.7 0.2 collective-permute-start.10
  132.1 0.6 collective-permute-done.8.l1
  132.6 1.5 collective-permute-done.9.l2
  134.1 1.6 collective-permute-done.10.l3
  135.7 1.4 shard_map.167
  137.1 1.3 collective-permute-start.11
  138.4 4.6 %collective-permute-start.12 = (bf16[256,128]{1,0:T(8,128)(2,1)S(1)}, bf16[256,128]{1,0:T(8,128)(2,1)S(1)}, u32[]{:S(2)}, u32[]{:S(2)}) collective-permute-start(bf16[256,128]{1,0:T(8,128)(2,1)S(1)} %get-tuple-element.22), channel_id=1, source_target_pairs={{0,128},{64,192},{128,0},{192,64},{1,129},{65,193},{129,1},{193,65... | collective-permute-start | bytes 196616 | tf_op jit(solution)/shard_map/ppermute | solution.py:61
  143.1 12.0 %collective-permute-done.11.b1.q1 = bf16[256,128]{1,0:T(8,128)(2,1)S(1)} collective-permute-done((bf16[256,128]{1,0:T(8,128)(2,1)S(1)}, bf16[256,128]{1,0:T(8,128)(2,1)S(1)}, u32[]{:S(2)}, u32[]{:S(2)}) %collective-permute-start.11) | collective-permute-done | bytes 65568 | tf_op jit(solution)/shard_map/ppermute | solution.py:61
  155.1 1.2 collective-permute-done.13.b3.q3
  156.3 2.5 %collective-permute-start.14 = (bf16[4,160,128]{2,1,0:T(8,128)(2,1)S(1)}, bf16[4,160,128]{2,1,0:T(8,128)(2,1)S(1)}, u32[]{:S(2)}, u32[]{:S(2)}) collective-permute-start(bf16[4,160,128]{2,1,0:T(8,128)(2,1)S(1)} %shard_map.168), channel_id=1, source_target_pairs={{0,32},{32,0},{1,33},{33,1},{2,34},{34,2},{3,35},{35,3},{4,36},{36... | collective-permute-start | bytes 491528 | tf_op jit(solution)/shard_map/ppermute | solution.py:61
  158.8 4.1 %collective-permute-done.14 = bf16[4,160,128]{2,1,0:T(8,128)(2,1)S(1)} collective-permute-done((bf16[4,160,128]{2,1,0:T(8,128)(2,1)S(1)}, bf16[4,160,128]{2,1,0:T(8,128)(2,1)S(1)}, u32[]{:S(2)}, u32[]{:S(2)}) %collective-permute-start.14) | collective-permute-done | bytes 163872 | tf_op jit(solution)/shard_map/ppermute | solution.py:61
  162.9 1.6 collective-permute-start.15
  164.5 2.8 %collective-permute-start.16 = (bf16[4,160,256]{2,1,0:T(8,128)(2,1)S(1)}, bf16[4,160,256]{2,1,0:T(8,128)(2,1)S(1)}, u32[]{:S(2)}, u32[]{:S(2)}) collective-permute-start(bf16[4,160,256]{2,1,0:T(8,128)(2,1)S(1)} %pad_maximum_fusion.refs_0_), channel_id=1, source_target_pairs={{0,16},{8,24},{16,0},{24,8},{1,17},{9,25},{17,1},{25,9},{2,18},{10... | collective-permute-start | bytes 983048 | tf_op jit(solution)/shard_map/ppermute | solution.py:61
  167.3 1.4 collective-permute-start.17
  168.7 4.8 %collective-permute-done.15.refs_1_ = bf16[4,160,256]{2,1,0:T(8,128)(2,1)S(1)} collective-permute-done((bf16[4,160,256]{2,1,0:T(8,128)(2,1)S(1)}, bf16[4,160,256]{2,1,0:T(8,128)(2,1)S(1)}, u32[]{:S(2)}, u32[]{:S(2)}) %collective-permute-start.15) | collective-permute-done | bytes 327712 | tf_op jit(solution)/shard_map/ppermute | solution.py:61
  173.5 7.7 %collective-permute-done.16.refs_2_ = bf16[4,160,256]{2,1,0:T(8,128)(2,1)S(1)} collective-permute-done((bf16[4,160,256]{2,1,0:T(8,128)(2,1)S(1)}, bf16[4,160,256]{2,1,0:T(8,128)(2,1)S(1)}, u32[]{:S(2)}, u32[]{:S(2)}) %collective-permute-start.16) | collective-permute-done | bytes 327712 | tf_op jit(solution)/shard_map/ppermute | solution.py:61
  181.2 0.5 collective-permute-start.21
  181.7 1.1 collective-permute-done.20.refs_6_
  182.8 0.5 collective-permute-done.21.refs_7_
  183.3 5.8 %shard_map.169 = (bf16[128,64]{1,0:T(8,128)(2,1)S(1)}, bf16[128,64]{1,0:T(8,128)(2,1)S(1)}, bf16[128,64]{1,0:T(8,128)(2,1)S(1)}, bf16[128,64]{1,0:T(8,128)(2,1)S(1)}) custom-call(s32[5]{0:T(128)S(1)} %stack.23.where, bf16[256,128]{1,0:T(8,128)(2,1)S(1)} %get-tuple-element.20.b0.q0, bf16[256,128]{1,0:T(8,128)(2,1)S(1)} %collective-permute-done.11.b1.q1, ...), custom_call_target="tpu_custom_call" | custom-call | tf_op jit(solution)/shard_map/pallas_call | solution.py:45
  189.1 0.4 collective-permute-start.22
  189.5 3.9 %collective-permute-start.23 = (bf16[128,64]{1,0:T(8,128)(2,1)S(1)}, bf16[128,64]{1,0:T(8,128)(2,1)S(1)}, u32[]{:S(2)}, u32[]{:S(2)}) collective-permute-start(bf16[128,64]{1,0:T(8,128)(2,1)S(1)} %get-tuple-element.26), channel_id=1, source_target_pairs={{0,2},{1,3},{2,0},{3,1},{4,6},{5,7},{6,4},{7,5},{8,10},{9,11},{10,... | collective-permute-start | bytes 49160 | tf_op jit(solution)/shard_map/ppermute | solution.py:61
  193.4 0.2 collective-permute-start.24
  193.6 0.7 collective-permute-done.22.a1
  194.3 1.3 collective-permute-done.23.a2
  195.6 1.7 collective-permute-done.24.a3
  197.3 0.7 shard_map.170
  198.0 1.2 collective-permute-start.25
  199.2 2.4 %collective-permute-start.26 = (bf16[32,256]{1,0:T(8,128)(2,1)S(1)}, bf16[32,256]{1,0:T(8,128)(2,1)S(1)}, u32[]{:S(2)}, u32[]{:S(2)}) collective-permute-start(bf16[32,256]{1,0:T(8,128)(2,1)S(1)} %get-tuple-element.30), channel_id=1, source_target_pairs={{0,128},{64,192},{128,0},{192,64},{1,129},{65,193},{129,1},{193,65... | collective-permute-start | bytes 49160 | tf_op jit(solution)/shard_map/ppermute | solution.py:61
  201.6 2.8 %collective-permute-start.27 = (bf16[32,256]{1,0:T(8,128)(2,1)S(1)}, bf16[32,256]{1,0:T(8,128)(2,1)S(1)}, u32[]{:S(2)}, u32[]{:S(2)}) collective-permute-start(bf16[32,256]{1,0:T(8,128)(2,1)S(1)} %get-tuple-element.31), channel_id=1, source_target_pairs={{0,192},{64,0},{128,64},{192,128},{1,193},{65,1},{129,65},{193,129... | collective-permute-start | bytes 49160 | tf_op jit(solution)/shard_map/ppermute | solution.py:61
  204.4 2.5 %collective-permute-done.26.a2 = bf16[32,256]{1,0:T(8,128)(2,1)S(1)} collective-permute-done((bf16[32,256]{1,0:T(8,128)(2,1)S(1)}, bf16[32,256]{1,0:T(8,128)(2,1)S(1)}, u32[]{:S(2)}, u32[]{:S(2)}) %collective-permute-start.26) | collective-permute-done | bytes 16416 | tf_op jit(solution)/shard_map/ppermute | solution.py:61
  206.8 0.6 collective-permute-done.27.a3
  207.4 3.9 %finish.1 = (bf16[64,2048]{1,0:T(8,128)(2,1)}, bf16[32,2048]{1,0:T(8,128)(2,1)}) custom-call(s32[5]{0:T(128)S(1)} %stack.23.where, bf16[64,4,2048]{2,1,0:T(4,128)(2,1)S(1)} %all-to-all-done.1.returned, bf16[256,128]{1,0:T(8,128)(2,1)S(1)} %copy-done.4, bf16[32,256]{1,0:T(8,128)(2,1)S(1)} %get-tuple-element.28.a0, ...), custom_call_target="tpu_custom_call" | custom-call | tf_op jit(solution)/shard_map/finish/pallas_call | solution.py:271
  (32 shorter events, 0.5 us)
Async XLA Ops:
  0.6 66.3 %copy-start = (bf16[1,2048,256]{2,1,0:T(8,128)(2,1)S(1)}, bf16[1,2048,256]{2,1,0:T(8,128)(2,1)}, u32[]{:S(2)}) copy-start(bf16[1,2048,256]{2,1,0:T(8,128)(2,1)} %param.27) | copy-start | bytes 3145732
  0.6 66.2 %copy-start.1 = (bf16[1,2048,256]{2,1,0:T(8,128)(2,1)S(1)}, bf16[1,2048,256]{2,1,0:T(8,128)(2,1)}, u32[]{:S(2)}) copy-start(bf16[1,2048,256]{2,1,0:T(8,128)(2,1)} %param.28) | copy-start | bytes 3145732
  3.4 36.2 %all-to-all-start = ((bf16[64,4,2048]{2,1,0:T(4,128)(2,1)}), bf16[64,4,2048]{2,1,0:T(4,128)(2,1)S(1)}, u32[]{:S(2)}, u32[]{:S(2)}) async-start(bf16[64,4,2048]{2,1,0:T(4,128)(2,1)} %get-tuple-element.18), calls=%async_computation | async-start | bytes 2097152 | tf_op jit(solution)/shard_map/all_to_all | solution.py:237
  12.7 31.1 %collective-permute-start.5 = (bf16[256,2048]{1,0:T(8,128)(2,1)}, bf16[256,2048]{1,0:T(8,128)(2,1)}, u32[]{:S(2)}, u32[]{:S(2)}) collective-permute-start(bf16[256,2048]{1,0:T(8,128)(2,1)} %bitcast.19), channel_id=1, source_target_pairs={{0,1},{1,0},{2,3},{3,2},{4,5},{5,4},{6,7},{7,6},{8,9},{9,8},{10,11... | collective-permute-start | bytes 3145736 | tf_op jit(solution)/shard_map/ppermute | solution.py:66
  14.3 47.3 %collective-permute-start = (bf16[2048,256]{1,0:T(8,128)(2,1)}, bf16[2048,256]{1,0:T(8,128)(2,1)}, u32[]{:S(2)}, u32[]{:S(2)}) collective-permute-start(bf16[2048,256]{1,0:T(8,128)(2,1)} %bitcast.13), channel_id=1, source_target_pairs={{0,1},{1,0},{2,3},{3,2},{4,5},{5,4},{6,7},{7,6},{8,9},{9,8},{10,11... | collective-permute-start | bytes 3145736 | tf_op jit(solution)/shard_map/ppermute | solution.py:66
  39.6 27.2 %collective-permute-start.2 = (bf16[64,4,2048]{2,1,0:T(4,128)(2,1)S(1)}, bf16[64,4,2048]{2,1,0:T(4,128)(2,1)S(1)}, u32[]{:S(2)}, u32[]{:S(2)}) collective-permute-start(bf16[64,4,2048]{2,1,0:T(4,128)(2,1)S(1)} %all-to-all-done.rows), channel_id=1, source_target_pairs={{0,3},{1,2},{2,1},{3,0},{4,7},{5,6},{6,5},{7,4},{8,11},{9,10},{10,... | collective-permute-start | bytes 3145736 | tf_op jit(solution)/shard_map/ppermute | solution.py:66
  42.4 40.7 %collective-permute-start.1 = (bf16[2048,256]{1,0:T(8,128)(2,1)}, bf16[2048,256]{1,0:T(8,128)(2,1)S(1)}, u32[]{:S(2)}, u32[]{:S(2)}) collective-permute-start(bf16[2048,256]{1,0:T(8,128)(2,1)} %bitcast.16), channel_id=1, source_target_pairs={{0,1},{1,0},{2,3},{3,2},{4,5},{5,4},{6,7},{7,6},{8,9},{9,8},{10,11... | collective-permute-start | bytes 3145736 | tf_op jit(solution)/shard_map/ppermute | solution.py:66
  42.6 49.5 %collective-permute-start.6 = (bf16[256,2048]{1,0:T(8,128)(2,1)}, bf16[256,2048]{1,0:T(8,128)(2,1)S(1)}, u32[]{:S(2)}, u32[]{:S(2)}) collective-permute-start(bf16[256,2048]{1,0:T(8,128)(2,1)} %bitcast.20), channel_id=1, source_target_pairs={{0,3},{1,2},{2,1},{3,0},{4,7},{5,6},{6,5},{7,4},{8,11},{9,10},{10,... | collective-permute-start | bytes 3145736 | tf_op jit(solution)/shard_map/ppermute | solution.py:66
  43.8 68.1 %collective-permute-start.7 = (bf16[256,2048]{1,0:T(8,128)(2,1)}, bf16[256,2048]{1,0:T(8,128)(2,1)S(1)}, u32[]{:S(2)}, u32[]{:S(2)}) collective-permute-start(bf16[256,2048]{1,0:T(8,128)(2,1)} %collective-permute-done.5.w1), channel_id=1, source_target_pairs={{0,3},{1,2},{2,1},{3,0},{4,7},{5,6},{6,5},{7,4},{8,11},{9,10},{10,... | collective-permute-start | bytes 3145736 | tf_op jit(solution)/shard_map/ppermute | solution.py:66
  67.9 47.4 %collective-permute-start.3 = (bf16[256,256]{1,0:T(8,128)(2,1)S(1)}, bf16[256,256]{1,0:T(8,128)(2,1)S(1)}, u32[]{:S(2)}, u32[]{:S(2)}) collective-permute-start(bf16[256,256]{1,0:T(8,128)(2,1)S(1)} %shard_map.162), channel_id=1, source_target_pairs={{0,3},{1,2},{2,1},{3,0},{4,7},{5,6},{6,5},{7,4},{8,11},{9,10},{10,... | collective-permute-start | bytes 393224 | tf_op jit(solution)/shard_map/ppermute | solution.py:66
  83.1 1.0 copy-start.2
  86.1 30.6 %collective-permute-start.4 = (bf16[256,256]{1,0:T(8,128)(2,1)S(1)}, bf16[256,256]{1,0:T(8,128)(2,1)S(1)}, u32[]{:S(2)}, u32[]{:S(2)}) collective-permute-start(bf16[256,256]{1,0:T(8,128)(2,1)S(1)} %shard_map.163), channel_id=1, source_target_pairs={{0,3},{1,2},{2,1},{3,0},{4,7},{5,6},{6,5},{7,4},{8,11},{9,10},{10,... | collective-permute-start | bytes 393224 | tf_op jit(solution)/shard_map/ppermute | solution.py:66
  89.9 1.2 copy-start.3
  92.1 19.7 %copy-start.5 = (bf16[256,2048]{1,0:T(8,128)(2,1)}, bf16[256,2048]{1,0:T(8,128)(2,1)S(1)}, u32[]{:S(2)}) copy-start(bf16[256,2048]{1,0:T(8,128)(2,1)S(1)} %collective-permute-done.6.w2) | copy-start | bytes 3145732
  111.8 1.0 copy-start.6
  119.0 88.4 %copy-start.4 = (bf16[256,128]{1,0:T(8,128)(2,1)S(1)}, bf16[256,128]{1,0:T(8,128)(2,1)}, u32[]{:S(2)}) copy-start(bf16[256,128]{1,0:T(8,128)(2,1)} %get-tuple-element.19.shares) | copy-start | bytes 196612
  119.0 88.4 %all-to-all-start.1 = ((bf16[64,4,2048]{2,1,0:T(4,128)(2,1)}), bf16[64,4,2048]{2,1,0:T(4,128)(2,1)S(1)}, u32[]{:S(2)}, u32[]{:S(2)}) async-start(bf16[64,4,2048]{2,1,0:T(4,128)(2,1)} %shard_map.165), calls=%async_computation.1 | async-start | bytes 2097152 | tf_op jit(solution)/shard_map/all_to_all | solution.py:250
  127.4 5.3 %collective-permute-start.8 = (bf16[32,544]{1,0:T(8,128)(2,1)S(1)}, bf16[32,544]{1,0:T(8,128)(2,1)S(1)}, u32[]{:S(2)}, u32[]{:S(2)}) collective-permute-start(bf16[32,544]{1,0:T(8,128)(2,1)S(1)} %shard_map.166.l0), channel_id=1, source_target_pairs={{0,1},{1,2},{2,3},{3,0},{4,5},{5,6},{6,7},{7,4},{8,9},{9,10},{10,1... | collective-permute-start | bytes 104456 | tf_op jit(solution)/shard_map/ppermute | solution.py:61
  127.7 6.4 %collective-permute-start.9 = (bf16[32,544]{1,0:T(8,128)(2,1)S(1)}, bf16[32,544]{1,0:T(8,128)(2,1)S(1)}, u32[]{:S(2)}, u32[]{:S(2)}) collective-permute-start(bf16[32,544]{1,0:T(8,128)(2,1)S(1)} %shard_map.166.l0), channel_id=1, source_target_pairs={{0,2},{1,3},{2,0},{3,1},{4,6},{5,7},{6,4},{7,5},{8,10},{9,11},{10,... | collective-permute-start | bytes 104456 | tf_op jit(solution)/shard_map/ppermute | solution.py:61
  131.7 4.0 %collective-permute-start.10 = (bf16[32,544]{1,0:T(8,128)(2,1)S(1)}, bf16[32,544]{1,0:T(8,128)(2,1)S(1)}, u32[]{:S(2)}, u32[]{:S(2)}) collective-permute-start(bf16[32,544]{1,0:T(8,128)(2,1)S(1)} %shard_map.166.l0), channel_id=1, source_target_pairs={{0,3},{1,0},{2,1},{3,2},{4,7},{5,4},{6,5},{7,6},{8,11},{9,8},{10,9... | collective-permute-start | bytes 104456 | tf_op jit(solution)/shard_map/ppermute | solution.py:61
  137.1 18.0 %collective-permute-start.11 = (bf16[256,128]{1,0:T(8,128)(2,1)S(1)}, bf16[256,128]{1,0:T(8,128)(2,1)S(1)}, u32[]{:S(2)}, u32[]{:S(2)}) collective-permute-start(bf16[256,128]{1,0:T(8,128)(2,1)S(1)} %get-tuple-element.21), channel_id=1, source_target_pairs={{0,64},{64,128},{128,192},{192,0},{1,65},{65,129},{129,193},{193,1... | collective-permute-start | bytes 196616 | tf_op jit(solution)/shard_map/ppermute | solution.py:61
  138.4 16.7 %collective-permute-start.12 = (bf16[256,128]{1,0:T(8,128)(2,1)S(1)}, bf16[256,128]{1,0:T(8,128)(2,1)S(1)}, u32[]{:S(2)}, u32[]{:S(2)}) collective-permute-start(bf16[256,128]{1,0:T(8,128)(2,1)S(1)} %get-tuple-element.22), channel_id=1, source_target_pairs={{0,128},{64,192},{128,0},{192,64},{1,129},{65,193},{129,1},{193,65... | collective-permute-start | bytes 196616 | tf_op jit(solution)/shard_map/ppermute | solution.py:61
  143.0 13.3 %collective-permute-start.13 = (bf16[256,128]{1,0:T(8,128)(2,1)S(1)}, bf16[256,128]{1,0:T(8,128)(2,1)S(1)}, u32[]{:S(2)}, u32[]{:S(2)}) collective-permute-start(bf16[256,128]{1,0:T(8,128)(2,1)S(1)} %get-tuple-element.23), channel_id=1, source_target_pairs={{0,192},{64,0},{128,64},{192,128},{1,193},{65,1},{129,65},{193,129... | collective-permute-start | bytes 196616 | tf_op jit(solution)/shard_map/ppermute | solution.py:61
  156.3 6.5 %collective-permute-start.14 = (bf16[4,160,128]{2,1,0:T(8,128)(2,1)S(1)}, bf16[4,160,128]{2,1,0:T(8,128)(2,1)S(1)}, u32[]{:S(2)}, u32[]{:S(2)}) collective-permute-start(bf16[4,160,128]{2,1,0:T(8,128)(2,1)S(1)} %shard_map.168), channel_id=1, source_target_pairs={{0,32},{32,0},{1,33},{33,1},{2,34},{34,2},{3,35},{35,3},{4,36},{36... | collective-permute-start | bytes 491528 | tf_op jit(solution)/shard_map/ppermute | solution.py:61
  162.9 10.6 %collective-permute-start.15 = (bf16[4,160,256]{2,1,0:T(8,128)(2,1)S(1)}, bf16[4,160,256]{2,1,0:T(8,128)(2,1)S(1)}, u32[]{:S(2)}, u32[]{:S(2)}) collective-permute-start(bf16[4,160,256]{2,1,0:T(8,128)(2,1)S(1)} %pad_maximum_fusion.refs_0_), channel_id=1, source_target_pairs={{0,8},{8,16},{16,24},{24,0},{1,9},{9,17},{17,25},{25,1},{2,10},{10... | collective-permute-start | bytes 983048 | tf_op jit(solution)/shard_map/ppermute | solution.py:61
  164.5 16.7 %collective-permute-start.16 = (bf16[4,160,256]{2,1,0:T(8,128)(2,1)S(1)}, bf16[4,160,256]{2,1,0:T(8,128)(2,1)S(1)}, u32[]{:S(2)}, u32[]{:S(2)}) collective-permute-start(bf16[4,160,256]{2,1,0:T(8,128)(2,1)S(1)} %pad_maximum_fusion.refs_0_), channel_id=1, source_target_pairs={{0,16},{8,24},{16,0},{24,8},{1,17},{9,25},{17,1},{25,9},{2,18},{10... | collective-permute-start | bytes 983048 | tf_op jit(solution)/shard_map/ppermute | solution.py:61
  167.3 13.9 %collective-permute-start.17 = (bf16[4,160,256]{2,1,0:T(8,128)(2,1)S(1)}, bf16[4,160,256]{2,1,0:T(8,128)(2,1)S(1)}, u32[]{:S(2)}, u32[]{:S(2)}) collective-permute-start(bf16[4,160,256]{2,1,0:T(8,128)(2,1)S(1)} %pad_maximum_fusion.refs_0_), channel_id=1, source_target_pairs={{0,24},{8,0},{16,8},{24,16},{1,25},{9,1},{17,9},{25,17},{2,26},{10... | collective-permute-start | bytes 983048 | tf_op jit(solution)/shard_map/ppermute | solution.py:61
  168.7 13.0 %collective-permute-start.18 = (bf16[4,160,256]{2,1,0:T(8,128)(2,1)S(1)}, bf16[4,160,256]{2,1,0:T(8,128)(2,1)S(1)}, u32[]{:S(2)}, u32[]{:S(2)}) collective-permute-start(bf16[4,160,256]{2,1,0:T(8,128)(2,1)S(1)} %pad_maximum_fusion.refs_0_), channel_id=1, source_target_pairs={{0,4},{4,0},{1,5},{5,1},{2,6},{6,2},{3,7},{7,3},{8,12},{12,8},{9,1... | collective-permute-start | bytes 983048 | tf_op jit(solution)/shard_map/ppermute | solution.py:61
  173.5 8.2 %collective-permute-start.19 = (bf16[4,160,256]{2,1,0:T(8,128)(2,1)S(1)}, bf16[4,160,256]{2,1,0:T(8,128)(2,1)S(1)}, u32[]{:S(2)}, u32[]{:S(2)}) collective-permute-start(bf16[4,160,256]{2,1,0:T(8,128)(2,1)S(1)} %collective-permute-done.15.refs_1_), channel_id=1, source_target_pairs={{0,4},{4,0},{1,5},{5,1},{2,6},{6,2},{3,7},{7,3},{8,12},{12,8},{9,1... | collective-permute-start | bytes 983048 | tf_op jit(solution)/shard_map/ppermute | solution.py:61
  181.2 1.6 collective-permute-start.20
  181.2 2.1 collective-permute-start.21
  189.1 5.2 %collective-permute-start.22 = (bf16[128,64]{1,0:T(8,128)(2,1)S(1)}, bf16[128,64]{1,0:T(8,128)(2,1)S(1)}, u32[]{:S(2)}, u32[]{:S(2)}) collective-permute-start(bf16[128,64]{1,0:T(8,128)(2,1)S(1)} %get-tuple-element.25), channel_id=1, source_target_pairs={{0,1},{1,2},{2,3},{3,0},{4,5},{5,6},{6,7},{7,4},{8,9},{9,10},{10,1... | collective-permute-start | bytes 49160 | tf_op jit(solution)/shard_map/ppermute | solution.py:61
  189.5 6.2 %collective-permute-start.23 = (bf16[128,64]{1,0:T(8,128)(2,1)S(1)}, bf16[128,64]{1,0:T(8,128)(2,1)S(1)}, u32[]{:S(2)}, u32[]{:S(2)}) collective-permute-start(bf16[128,64]{1,0:T(8,128)(2,1)S(1)} %get-tuple-element.26), channel_id=1, source_target_pairs={{0,2},{1,3},{2,0},{3,1},{4,6},{5,7},{6,4},{7,5},{8,10},{9,11},{10,... | collective-permute-start | bytes 49160 | tf_op jit(solution)/shard_map/ppermute | solution.py:61
  193.4 3.9 %collective-permute-start.24 = (bf16[128,64]{1,0:T(8,128)(2,1)S(1)}, bf16[128,64]{1,0:T(8,128)(2,1)S(1)}, u32[]{:S(2)}, u32[]{:S(2)}) collective-permute-start(bf16[128,64]{1,0:T(8,128)(2,1)S(1)} %get-tuple-element.27), channel_id=1, source_target_pairs={{0,3},{1,0},{2,1},{3,2},{4,7},{5,4},{6,5},{7,6},{8,11},{9,8},{10,9... | collective-permute-start | bytes 49160 | tf_op jit(solution)/shard_map/ppermute | solution.py:61
  198.0 6.4 %collective-permute-start.25 = (bf16[32,256]{1,0:T(8,128)(2,1)S(1)}, bf16[32,256]{1,0:T(8,128)(2,1)S(1)}, u32[]{:S(2)}, u32[]{:S(2)}) collective-permute-start(bf16[32,256]{1,0:T(8,128)(2,1)S(1)} %get-tuple-element.29), channel_id=1, source_target_pairs={{0,64},{64,128},{128,192},{192,0},{1,65},{65,129},{129,193},{193,1... | collective-permute-start | bytes 49160 | tf_op jit(solution)/shard_map/ppermute | solution.py:61
  199.2 7.6 %collective-permute-start.26 = (bf16[32,256]{1,0:T(8,128)(2,1)S(1)}, bf16[32,256]{1,0:T(8,128)(2,1)S(1)}, u32[]{:S(2)}, u32[]{:S(2)}) collective-permute-start(bf16[32,256]{1,0:T(8,128)(2,1)S(1)} %get-tuple-element.30), channel_id=1, source_target_pairs={{0,128},{64,192},{128,0},{192,64},{1,129},{65,193},{129,1},{193,65... | collective-permute-start | bytes 49160 | tf_op jit(solution)/shard_map/ppermute | solution.py:61
  201.6 5.8 %collective-permute-start.27 = (bf16[32,256]{1,0:T(8,128)(2,1)S(1)}, bf16[32,256]{1,0:T(8,128)(2,1)S(1)}, u32[]{:S(2)}, u32[]{:S(2)}) collective-permute-start(bf16[32,256]{1,0:T(8,128)(2,1)S(1)} %get-tuple-element.31), channel_id=1, source_target_pairs={{0,192},{64,0},{128,64},{192,128},{1,193},{65,1},{129,65},{193,129... | collective-permute-start | bytes 49160 | tf_op jit(solution)/shard_map/ppermute | solution.py:61

commit v14 on v13

--- a/solution.py
+++ b/solution.py
@@ -202,10 +202,40 @@
         out[k] = piece[...]
 
 
-def down_kernel(h0, h1, h2, h3, weights, out):
-    total = mm(h0[...], weights[0]) + mm(h1[...], weights[1])
-    total = total + mm(h2[...], weights[2]) + mm(h3[...], weights[3])
-    out[...] = total.astype(BF).reshape(out.shape)
+def down_kernel(h0, h1, h2, h3, weights, out, pieces, sems):
+    count, experts, cap, span = pieces.shape
+    hidden = [h[...] for h in (h0, h1, h2, h3)]
+    copies = []
+    for c in range(count):
+        cols = slice(c * span, (c + 1) * span)
+        total = mm(hidden[0], weights[0, :, cols])
+        for k in range(1, 4):
+            total = total + mm(hidden[k], weights[k, :, cols])
+        pieces[c] = total.astype(BF).reshape(experts, cap, span)
+        copies.append(
+            pltpu.make_async_copy(
+                pieces.at[c], out.at[:, :, pl.ds(c * span, span)], sems.at[c]
+            )
+        )
+        copies[c].start()
+    for copy in copies:
+        copy.wait()
+
+
+def down_of(arrays, experts, width):
+    near = [pltpu.with_memory_space_constraint(a, pltpu.VMEM) for a in arrays]
+    return pl.pallas_call(
+        down_kernel,
+        in_specs=[VMEM_SPEC] * len(near),
+        out_specs=pl.BlockSpec(memory_space=pl.ANY),
+        out_shape=pltpu.HBM((experts, CAP, width), BF),
+        scratch_shapes=[
+            pltpu.VMEM((4, experts, CAP, width // 4), BF),
+            pltpu.SemaphoreType.DMA((4,)),
+        ],
+        compiler_params=pltpu.CompilerParams(vmem_limit_bytes=8 << 20),
+        name="down",
+    )(*near)
 
 
 def both_halves(
@@ -244,9 +274,7 @@
     own_b = hidden_of(arrived, set_b)
     shape = jax.ShapeDtypeStruct((4, *w_down.shape), BF)
     down = call(stage_kernel, shape, [w_down, down_w, down_r, down_rw], unplaced=range(4))
-    shape = jax.ShapeDtypeStruct((experts, CAP, width), BF)
-    arrays = [own_a, own_b, mate_a, mate_b, down]
-    result = call(down_kernel, shape, arrays, place=pltpu.HBM)
+    result = down_of([own_a, own_b, mate_a, mate_b, down], experts, width)
     returned = lax.all_to_all(result, EP, split_axis=0, concat_axis=0, tiled=True)
     parts = out_parts(where, parts, latent.shape[0])
     height, span = out_proj.shape[0], width // 4

time: 216 us -> 216 us (level)
    pallas_call x12 -> x11, Pallas kernels: 20.5 us -> 18.2 us  [call(): pl.pallas_call(kernel, in_specs=specs, out_specs=VMEM_SPEC if single else...]
where the time goes in v14:
time: 216 us; the launch traced here: 211 us
  waiting for transfers between devices  120 us (56%)
  starting transfers between devices  60.8 us (28%)
  Pallas kernels  26.1 us (12%)
  local copies, waits for them, and re-layouts  3.28 us (2%)
    ppermute x8, waiting for transfers between devices, paired(): return lax.ppermute(value, 'x', [(i, mate(i)) for i in range(n)])  53.3 us
    ppermute x20, waiting for transfers between devices, shifted(): return lax.ppermute(value, axis, [(i, (i + amount) % n) for i in range(n)])  41.5 us
    ppermute x20, starting transfers between devices, shifted(): return lax.ppermute(value, axis, [(i, (i + amount) % n) for i in range(n)])  30.3 us
    all_to_all x1, waiting for transfers between devices, both_halves(): lax.all_to_all(outgoing, EP, split_axis=0, concat_axis=0, tiled=True)  24.8 us
    pallas_call x11, Pallas kernels, call(): pl.pallas_call(kernel, in_specs=specs, out_specs=VMEM_SPEC if single else...  18.2 us
    ppermute x8, starting transfers between devices, paired(): return lax.ppermute(value, 'x', [(i, mate(i)) for i in range(n)])  14 us
    all_to_all x1, starting transfers between devices, both_halves(): lax.all_to_all(outgoing, EP, split_axis=0, concat_axis=0, tiled=True)  9.29 us
    all_to_all x1, starting transfers between devices, both_halves(): lax.all_to_all(result, EP, split_axis=0, concat_axis=0, tiled=True)  7.24 us
  transfers between devices with their start and end apart: 30, of which 21 were waited for; matrix products, arithmetic and copies ran while one was open for 0% of the time, Pallas kernels for 8%

profile of v14, /device:TPU:224, one launch (start us, length us, event | category | flops | bytes accessed | tf_op | source)
XLA Modules:
  0.0 211.2 jit_solution(706858880547033008)
XLA Ops:
  0.7 2.8 %shard_map.158 = (bf16[64,4,2048]{2,1,0:T(4,128)(2,1)}, bf16[256,128]{1,0:T(8,128)(2,1)}) custom-call(bf16[64,2048]{1,0:T(8,128)(2,1)} %tokens.1, f32[1,2048]{1,0:T(1,128)} %bitcast.22, s32[2,64]{1,0:T(2,128)} %bitcast.24, f32[1,64]{1,0:T(1,128)} %bitcast.26, f32[2,64]{1,0:T(2,128)} %bitcast.25), custom_call_target="tpu_custom_call" | custom-call | tf_op jit(solution)/shard_map/pallas_call | solution.py:45
  3.4 9.3 %all-to-all-start = ((bf16[64,4,2048]{2,1,0:T(4,128)(2,1)}), bf16[64,4,2048]{2,1,0:T(4,128)(2,1)S(1)}, u32[]{:S(2)}, u32[]{:S(2)}) async-start(bf16[64,4,2048]{2,1,0:T(4,128)(2,1)} %get-tuple-element.18), calls=%async_computation | async-start | bytes 2097152 | tf_op jit(solution)/shard_map/all_to_all | solution.py:267
  12.7 1.6 collective-permute-start.5
  14.3 0.5 collective-permute-start
  14.8 24.8 %all-to-all-done.rows = bf16[64,4,2048]{2,1,0:T(4,128)(2,1)S(1)} async-done(((bf16[64,4,2048]{2,1,0:T(4,128)(2,1)}), bf16[64,4,2048]{2,1,0:T(4,128)(2,1)S(1)}, u32[]{:S(2)}, u32[]{:S(2)}) %all-to-all-start) | async-done | bytes 1048608 | tf_op jit(solution)/shard_map/all_to_all | solution.py:267
  39.6 2.8 %collective-permute-start.2 = (bf16[64,4,2048]{2,1,0:T(4,128)(2,1)S(1)}, bf16[64,4,2048]{2,1,0:T(4,128)(2,1)S(1)}, u32[]{:S(2)}, u32[]{:S(2)}) collective-permute-start(bf16[64,4,2048]{2,1,0:T(4,128)(2,1)S(1)} %all-to-all-done.rows), channel_id=1, source_target_pairs={{0,3},{1,2},{2,1},{3,0},{4,7},{5,6},{6,5},{7,4},{8,11},{9,10},{10,... | collective-permute-start | bytes 3145736 | tf_op jit(solution)/shard_map/ppermute | solution.py:66
  42.4 0.2 collective-permute-start.1
  42.6 1.1 collective-permute-start.6
  43.8 2.1 collective-permute-start.7
  45.9 15.8 %collective-permute-done.value = bf16[2048,256]{1,0:T(8,128)(2,1)} collective-permute-done((bf16[2048,256]{1,0:T(8,128)(2,1)}, bf16[2048,256]{1,0:T(8,128)(2,1)}, u32[]{:S(2)}, u32[]{:S(2)}) %collective-permute-start) | collective-permute-done | bytes 1048608 | tf_op jit(solution)/shard_map/ppermute | solution.py:66
  61.6 1.3 shard_map.160.w_gate
  62.9 4.0 %collective-permute-done.2.rows = bf16[64,4,2048]{2,1,0:T(4,128)(2,1)S(1)} collective-permute-done((bf16[64,4,2048]{2,1,0:T(4,128)(2,1)S(1)}, bf16[64,4,2048]{2,1,0:T(4,128)(2,1)S(1)}, u32[]{:S(2)}, u32[]{:S(2)}) %collective-permute-start.2) | collective-permute-done | bytes 1048608 | tf_op jit(solution)/shard_map/ppermute | solution.py:66
  66.9 1.0 shard_map.162
  67.9 2.8 %collective-permute-start.3 = (bf16[256,256]{1,0:T(8,128)(2,1)S(1)}, bf16[256,256]{1,0:T(8,128)(2,1)S(1)}, u32[]{:S(2)}, u32[]{:S(2)}) collective-permute-start(bf16[256,256]{1,0:T(8,128)(2,1)S(1)} %shard_map.162), channel_id=1, source_target_pairs={{0,3},{1,2},{2,1},{3,0},{4,7},{5,6},{6,5},{7,4},{8,11},{9,10},{10,... | collective-permute-start | bytes 393224 | tf_op jit(solution)/shard_map/ppermute | solution.py:66
  70.7 12.4 %collective-permute-done.1.w_up = bf16[2048,256]{1,0:T(8,128)(2,1)S(1)} collective-permute-done((bf16[2048,256]{1,0:T(8,128)(2,1)}, bf16[2048,256]{1,0:T(8,128)(2,1)S(1)}, u32[]{:S(2)}, u32[]{:S(2)}) %collective-permute-start.1) | collective-permute-done | bytes 1048608 | tf_op jit(solution)/shard_map/ppermute | solution.py:66
  83.1 1.0 copy-done.2
  84.1 1.9 shard_map.163
  86.1 2.8 %collective-permute-start.4 = (bf16[256,256]{1,0:T(8,128)(2,1)S(1)}, bf16[256,256]{1,0:T(8,128)(2,1)S(1)}, u32[]{:S(2)}, u32[]{:S(2)}) collective-permute-start(bf16[256,256]{1,0:T(8,128)(2,1)S(1)} %shard_map.163), channel_id=1, source_target_pairs={{0,3},{1,2},{2,1},{3,0},{4,7},{5,6},{6,5},{7,4},{8,11},{9,10},{10,... | collective-permute-start | bytes 393224 | tf_op jit(solution)/shard_map/ppermute | solution.py:66
  88.9 1.0 shard_map.159.h0
  89.9 1.2 copy-done.3
  91.1 1.0 shard_map.161.h1
  92.2 19.7 %collective-permute-done.7.w3 = bf16[256,2048]{1,0:T(8,128)(2,1)S(1)} collective-permute-done((bf16[256,2048]{1,0:T(8,128)(2,1)}, bf16[256,2048]{1,0:T(8,128)(2,1)S(1)}, u32[]{:S(2)}, u32[]{:S(2)}) %collective-permute-start.7) | collective-permute-done | bytes 1048608 | tf_op jit(solution)/shard_map/ppermute | solution.py:66
  111.8 1.0 copy-done.6
  112.8 2.4 %shard_map.164.weights = bf16[4,256,2048]{2,1,0:T(8,128)(2,1)S(1)} custom-call(bf16[256,2048]{1,0:T(8,128)(2,1)} %bitcast.21, bf16[256,2048]{1,0:T(8,128)(2,1)} %collective-permute-done.5.w1, bf16[256,2048]{1,0:T(8,128)(2,1)} %copy-done.5, bf16[256,2048]{1,0:T(8,128)(2,1)} %copy-done.6), custom_call_target="tpu_custom_call" | custom-call | tf_op jit(solution)/shard_map/pallas_call | solution.py:45
  115.3 1.4 collective-permute-done.4.h3
  116.7 2.0 down.1
  118.7 7.2 %all-to-all-start.1 = ((bf16[64,4,2048]{2,1,0:T(4,128)(2,1)}), bf16[64,4,2048]{2,1,0:T(4,128)(2,1)S(1)}, u32[]{:S(2)}, u32[]{:S(2)}) async-start(bf16[64,4,2048]{2,1,0:T(4,128)(2,1)} %down.1), calls=%async_computation.1 | async-start | bytes 2097152 | tf_op jit(solution)/shard_map/all_to_all | solution.py:278
  126.0 0.1 multiply_sine_fusion
  126.2 0.9 shard_map.165.l0
  127.1 0.4 collective-permute-start.8
  127.5 3.9 %collective-permute-start.9 = (bf16[32,544]{1,0:T(8,128)(2,1)S(1)}, bf16[32,544]{1,0:T(8,128)(2,1)S(1)}, u32[]{:S(2)}, u32[]{:S(2)}) collective-permute-start(bf16[32,544]{1,0:T(8,128)(2,1)S(1)} %shard_map.165.l0), channel_id=1, source_target_pairs={{0,2},{1,3},{2,0},{3,1},{4,6},{5,7},{6,4},{7,5},{8,10},{9,11},{10,... | collective-permute-start | bytes 104456 | tf_op jit(solution)/shard_map/ppermute | solution.py:61
  131.4 0.2 collective-permute-start.10
  131.9 0.6 collective-permute-done.8.l1
  132.4 1.5 collective-permute-done.9.l2
  133.9 1.6 collective-permute-done.10.l3
  135.4 1.4 shard_map.166
  136.9 1.3 collective-permute-start.11
  138.1 4.6 %collective-permute-start.12 = (bf16[256,128]{1,0:T(8,128)(2,1)S(1)}, bf16[256,128]{1,0:T(8,128)(2,1)S(1)}, u32[]{:S(2)}, u32[]{:S(2)}) collective-permute-start(bf16[256,128]{1,0:T(8,128)(2,1)S(1)} %get-tuple-element.22), channel_id=1, source_target_pairs={{0,128},{64,192},{128,0},{192,64},{1,129},{65,193},{129,1},{193,65... | collective-permute-start | bytes 196616 | tf_op jit(solution)/shard_map/ppermute | solution.py:61
  142.9 12.0 %collective-permute-done.11.b1.q1 = bf16[256,128]{1,0:T(8,128)(2,1)S(1)} collective-permute-done((bf16[256,128]{1,0:T(8,128)(2,1)S(1)}, bf16[256,128]{1,0:T(8,128)(2,1)S(1)}, u32[]{:S(2)}, u32[]{:S(2)}) %collective-permute-start.11) | collective-permute-done | bytes 65568 | tf_op jit(solution)/shard_map/ppermute | solution.py:61
  154.8 1.2 collective-permute-done.13.b3.q3
  156.1 2.5 %collective-permute-start.14 = (bf16[4,160,128]{2,1,0:T(8,128)(2,1)S(1)}, bf16[4,160,128]{2,1,0:T(8,128)(2,1)S(1)}, u32[]{:S(2)}, u32[]{:S(2)}) collective-permute-start(bf16[4,160,128]{2,1,0:T(8,128)(2,1)S(1)} %shard_map.167), channel_id=1, source_target_pairs={{0,32},{32,0},{1,33},{33,1},{2,34},{34,2},{3,35},{35,3},{4,36},{36... | collective-permute-start | bytes 491528 | tf_op jit(solution)/shard_map/ppermute | solution.py:61
  158.5 4.1 %collective-permute-done.14 = bf16[4,160,128]{2,1,0:T(8,128)(2,1)S(1)} collective-permute-done((bf16[4,160,128]{2,1,0:T(8,128)(2,1)S(1)}, bf16[4,160,128]{2,1,0:T(8,128)(2,1)S(1)}, u32[]{:S(2)}, u32[]{:S(2)}) %collective-permute-start.14) | collective-permute-done | bytes 163872 | tf_op jit(solution)/shard_map/ppermute | solution.py:61
  162.7 1.6 collective-permute-start.15
  164.3 2.8 %collective-permute-start.16 = (bf16[4,160,256]{2,1,0:T(8,128)(2,1)S(1)}, bf16[4,160,256]{2,1,0:T(8,128)(2,1)S(1)}, u32[]{:S(2)}, u32[]{:S(2)}) collective-permute-start(bf16[4,160,256]{2,1,0:T(8,128)(2,1)S(1)} %pad_maximum_fusion.refs_0_), channel_id=1, source_target_pairs={{0,16},{8,24},{16,0},{24,8},{1,17},{9,25},{17,1},{25,9},{2,18},{10... | collective-permute-start | bytes 983048 | tf_op jit(solution)/shard_map/ppermute | solution.py:61
  167.1 1.4 collective-permute-start.17
  168.5 4.8 %collective-permute-done.15.refs_1_ = bf16[4,160,256]{2,1,0:T(8,128)(2,1)S(1)} collective-permute-done((bf16[4,160,256]{2,1,0:T(8,128)(2,1)S(1)}, bf16[4,160,256]{2,1,0:T(8,128)(2,1)S(1)}, u32[]{:S(2)}, u32[]{:S(2)}) %collective-permute-start.15) | collective-permute-done | bytes 327712 | tf_op jit(solution)/shard_map/ppermute | solution.py:61
  173.3 7.7 %collective-permute-done.16.refs_2_ = bf16[4,160,256]{2,1,0:T(8,128)(2,1)S(1)} collective-permute-done((bf16[4,160,256]{2,1,0:T(8,128)(2,1)S(1)}, bf16[4,160,256]{2,1,0:T(8,128)(2,1)S(1)}, u32[]{:S(2)}, u32[]{:S(2)}) %collective-permute-start.16) | collective-permute-done | bytes 327712 | tf_op jit(solution)/shard_map/ppermute | solution.py:61
  181.0 0.5 collective-permute-start.21
  181.5 1.1 collective-permute-done.20.refs_6_
  182.6 0.5 collective-permute-done.21.refs_7_
  183.0 5.8 %shard_map.168 = (bf16[128,64]{1,0:T(8,128)(2,1)S(1)}, bf16[128,64]{1,0:T(8,128)(2,1)S(1)}, bf16[128,64]{1,0:T(8,128)(2,1)S(1)}, bf16[128,64]{1,0:T(8,128)(2,1)S(1)}) custom-call(s32[5]{0:T(128)S(1)} %stack.23.where, bf16[256,128]{1,0:T(8,128)(2,1)S(1)} %get-tuple-element.20.b0.q0, bf16[256,128]{1,0:T(8,128)(2,1)S(1)} %collective-permute-done.11.b1.q1, ...), custom_call_target="tpu_custom_call" | custom-call | tf_op jit(solution)/shard_map/pallas_call | solution.py:45
  188.9 0.4 collective-permute-start.22
  189.2 3.9 %collective-permute-start.23 = (bf16[128,64]{1,0:T(8,128)(2,1)S(1)}, bf16[128,64]{1,0:T(8,128)(2,1)S(1)}, u32[]{:S(2)}, u32[]{:S(2)}) collective-permute-start(bf16[128,64]{1,0:T(8,128)(2,1)S(1)} %get-tuple-element.26), channel_id=1, source_target_pairs={{0,2},{1,3},{2,0},{3,1},{4,6},{5,7},{6,4},{7,5},{8,10},{9,11},{10,... | collective-permute-start | bytes 49160 | tf_op jit(solution)/shard_map/ppermute | solution.py:61
  193.2 0.2 collective-permute-start.24
  193.4 0.7 collective-permute-done.22.a1
  194.1 1.3 collective-permute-done.23.a2
  195.4 1.7 collective-permute-done.24.a3
  197.1 0.7 shard_map.169
  197.7 1.2 collective-permute-start.25
  199.0 2.4 %collective-permute-start.26 = (bf16[32,256]{1,0:T(8,128)(2,1)S(1)}, bf16[32,256]{1,0:T(8,128)(2,1)S(1)}, u32[]{:S(2)}, u32[]{:S(2)}) collective-permute-start(bf16[32,256]{1,0:T(8,128)(2,1)S(1)} %get-tuple-element.30), channel_id=1, source_target_pairs={{0,128},{64,192},{128,0},{192,64},{1,129},{65,193},{129,1},{193,65... | collective-permute-start | bytes 49160 | tf_op jit(solution)/shard_map/ppermute | solution.py:61
  201.3 2.8 %collective-permute-start.27 = (bf16[32,256]{1,0:T(8,128)(2,1)S(1)}, bf16[32,256]{1,0:T(8,128)(2,1)S(1)}, u32[]{:S(2)}, u32[]{:S(2)}) collective-permute-start(bf16[32,256]{1,0:T(8,128)(2,1)S(1)} %get-tuple-element.31), channel_id=1, source_target_pairs={{0,192},{64,0},{128,64},{192,128},{1,193},{65,1},{129,65},{193,129... | collective-permute-start | bytes 49160 | tf_op jit(solution)/shard_map/ppermute | solution.py:61
  204.1 2.5 %collective-permute-done.26.a2 = bf16[32,256]{1,0:T(8,128)(2,1)S(1)} collective-permute-done((bf16[32,256]{1,0:T(8,128)(2,1)S(1)}, bf16[32,256]{1,0:T(8,128)(2,1)S(1)}, u32[]{:S(2)}, u32[]{:S(2)}) %collective-permute-start.26) | collective-permute-done | bytes 16416 | tf_op jit(solution)/shard_map/ppermute | solution.py:61
  206.6 0.6 collective-permute-done.27.a3
  207.2 3.9 %finish.1 = (bf16[64,2048]{1,0:T(8,128)(2,1)}, bf16[32,2048]{1,0:T(8,128)(2,1)}) custom-call(s32[5]{0:T(128)S(1)} %stack.23.where, bf16[64,4,2048]{2,1,0:T(4,128)(2,1)S(1)} %all-to-all-done.1.returned, bf16[256,128]{1,0:T(8,128)(2,1)S(1)} %copy-done.4, bf16[32,256]{1,0:T(8,128)(2,1)S(1)} %get-tuple-element.28.a0, ...), custom_call_target="tpu_custom_call" | custom-call | tf_op jit(solution)/shard_map/finish/pallas_call | solution.py:299
  (32 shorter events, 0.5 us)
Async XLA Ops:
  0.6 66.3 %copy-start = (bf16[1,2048,256]{2,1,0:T(8,128)(2,1)S(1)}, bf16[1,2048,256]{2,1,0:T(8,128)(2,1)}, u32[]{:S(2)}) copy-start(bf16[1,2048,256]{2,1,0:T(8,128)(2,1)} %param.27) | copy-start | bytes 3145732
  0.6 66.2 %copy-start.1 = (bf16[1,2048,256]{2,1,0:T(8,128)(2,1)S(1)}, bf16[1,2048,256]{2,1,0:T(8,128)(2,1)}, u32[]{:S(2)}) copy-start(bf16[1,2048,256]{2,1,0:T(8,128)(2,1)} %param.28) | copy-start | bytes 3145732
  3.4 36.2 %all-to-all-start = ((bf16[64,4,2048]{2,1,0:T(4,128)(2,1)}), bf16[64,4,2048]{2,1,0:T(4,128)(2,1)S(1)}, u32[]{:S(2)}, u32[]{:S(2)}) async-start(bf16[64,4,2048]{2,1,0:T(4,128)(2,1)} %get-tuple-element.18), calls=%async_computation | async-start | bytes 2097152 | tf_op jit(solution)/shard_map/all_to_all | solution.py:267
  12.7 31.1 %collective-permute-start.5 = (bf16[256,2048]{1,0:T(8,128)(2,1)}, bf16[256,2048]{1,0:T(8,128)(2,1)}, u32[]{:S(2)}, u32[]{:S(2)}) collective-permute-start(bf16[256,2048]{1,0:T(8,128)(2,1)} %bitcast.19), channel_id=1, source_target_pairs={{0,1},{1,0},{2,3},{3,2},{4,5},{5,4},{6,7},{7,6},{8,9},{9,8},{10,11... | collective-permute-start | bytes 3145736 | tf_op jit(solution)/shard_map/ppermute | solution.py:66
  14.3 47.3 %collective-permute-start = (bf16[2048,256]{1,0:T(8,128)(2,1)}, bf16[2048,256]{1,0:T(8,128)(2,1)}, u32[]{:S(2)}, u32[]{:S(2)}) collective-permute-start(bf16[2048,256]{1,0:T(8,128)(2,1)} %bitcast.13), channel_id=1, source_target_pairs={{0,1},{1,0},{2,3},{3,2},{4,5},{5,4},{6,7},{7,6},{8,9},{9,8},{10,11... | collective-permute-start | bytes 3145736 | tf_op jit(solution)/shard_map/ppermute | solution.py:66
  39.6 27.2 %collective-permute-start.2 = (bf16[64,4,2048]{2,1,0:T(4,128)(2,1)S(1)}, bf16[64,4,2048]{2,1,0:T(4,128)(2,1)S(1)}, u32[]{:S(2)}, u32[]{:S(2)}) collective-permute-start(bf16[64,4,2048]{2,1,0:T(4,128)(2,1)S(1)} %all-to-all-done.rows), channel_id=1, source_target_pairs={{0,3},{1,2},{2,1},{3,0},{4,7},{5,6},{6,5},{7,4},{8,11},{9,10},{10,... | collective-permute-start | bytes 3145736 | tf_op jit(solution)/shard_map/ppermute | solution.py:66
  42.4 40.7 %collective-permute-start.1 = (bf16[2048,256]{1,0:T(8,128)(2,1)}, bf16[2048,256]{1,0:T(8,128)(2,1)S(1)}, u32[]{:S(2)}, u32[]{:S(2)}) collective-permute-start(bf16[2048,256]{1,0:T(8,128)(2,1)} %bitcast.16), channel_id=1, source_target_pairs={{0,1},{1,0},{2,3},{3,2},{4,5},{5,4},{6,7},{7,6},{8,9},{9,8},{10,11... | collective-permute-start | bytes 3145736 | tf_op jit(solution)/shard_map/ppermute | solution.py:66
  42.6 49.5 %collective-permute-start.6 = (bf16[256,2048]{1,0:T(8,128)(2,1)}, bf16[256,2048]{1,0:T(8,128)(2,1)S(1)}, u32[]{:S(2)}, u32[]{:S(2)}) collective-permute-start(bf16[256,2048]{1,0:T(8,128)(2,1)} %bitcast.20), channel_id=1, source_target_pairs={{0,3},{1,2},{2,1},{3,0},{4,7},{5,6},{6,5},{7,4},{8,11},{9,10},{10,... | collective-permute-start | bytes 3145736 | tf_op jit(solution)/shard_map/ppermute | solution.py:66
  43.8 68.1 %collective-permute-start.7 = (bf16[256,2048]{1,0:T(8,128)(2,1)}, bf16[256,2048]{1,0:T(8,128)(2,1)S(1)}, u32[]{:S(2)}, u32[]{:S(2)}) collective-permute-start(bf16[256,2048]{1,0:T(8,128)(2,1)} %collective-permute-done.5.w1), channel_id=1, source_target_pairs={{0,3},{1,2},{2,1},{3,0},{4,7},{5,6},{6,5},{7,4},{8,11},{9,10},{10,... | collective-permute-start | bytes 3145736 | tf_op jit(solution)/shard_map/ppermute | solution.py:66
  67.9 47.4 %collective-permute-start.3 = (bf16[256,256]{1,0:T(8,128)(2,1)S(1)}, bf16[256,256]{1,0:T(8,128)(2,1)S(1)}, u32[]{:S(2)}, u32[]{:S(2)}) collective-permute-start(bf16[256,256]{1,0:T(8,128)(2,1)S(1)} %shard_map.162), channel_id=1, source_target_pairs={{0,3},{1,2},{2,1},{3,0},{4,7},{5,6},{6,5},{7,4},{8,11},{9,10},{10,... | collective-permute-start | bytes 393224 | tf_op jit(solution)/shard_map/ppermute | solution.py:66
  83.1 1.0 copy-start.2
  86.1 30.6 %collective-permute-start.4 = (bf16[256,256]{1,0:T(8,128)(2,1)S(1)}, bf16[256,256]{1,0:T(8,128)(2,1)S(1)}, u32[]{:S(2)}, u32[]{:S(2)}) collective-permute-start(bf16[256,256]{1,0:T(8,128)(2,1)S(1)} %shard_map.163), channel_id=1, source_target_pairs={{0,3},{1,2},{2,1},{3,0},{4,7},{5,6},{6,5},{7,4},{8,11},{9,10},{10,... | collective-permute-start | bytes 393224 | tf_op jit(solution)/shard_map/ppermute | solution.py:66
  89.9 1.2 copy-start.3
  92.1 19.7 %copy-start.5 = (bf16[256,2048]{1,0:T(8,128)(2,1)}, bf16[256,2048]{1,0:T(8,128)(2,1)S(1)}, u32[]{:S(2)}) copy-start(bf16[256,2048]{1,0:T(8,128)(2,1)S(1)} %collective-permute-done.6.w2) | copy-start | bytes 3145732
  111.8 1.0 copy-start.6
  118.7 88.5 %copy-start.4 = (bf16[256,128]{1,0:T(8,128)(2,1)S(1)}, bf16[256,128]{1,0:T(8,128)(2,1)}, u32[]{:S(2)}) copy-start(bf16[256,128]{1,0:T(8,128)(2,1)} %get-tuple-element.19.shares) | copy-start | bytes 196612
  118.7 88.4 %all-to-all-start.1 = ((bf16[64,4,2048]{2,1,0:T(4,128)(2,1)}), bf16[64,4,2048]{2,1,0:T(4,128)(2,1)S(1)}, u32[]{:S(2)}, u32[]{:S(2)}) async-start(bf16[64,4,2048]{2,1,0:T(4,128)(2,1)} %down.1), calls=%async_computation.1 | async-start | bytes 2097152 | tf_op jit(solution)/shard_map/all_to_all | solution.py:278
  127.1 5.3 %collective-permute-start.8 = (bf16[32,544]{1,0:T(8,128)(2,1)S(1)}, bf16[32,544]{1,0:T(8,128)(2,1)S(1)}, u32[]{:S(2)}, u32[]{:S(2)}) collective-permute-start(bf16[32,544]{1,0:T(8,128)(2,1)S(1)} %shard_map.165.l0), channel_id=1, source_target_pairs={{0,1},{1,2},{2,3},{3,0},{4,5},{5,6},{6,7},{7,4},{8,9},{9,10},{10,1... | collective-permute-start | bytes 104456 | tf_op jit(solution)/shard_map/ppermute | solution.py:61
  127.5 6.4 %collective-permute-start.9 = (bf16[32,544]{1,0:T(8,128)(2,1)S(1)}, bf16[32,544]{1,0:T(8,128)(2,1)S(1)}, u32[]{:S(2)}, u32[]{:S(2)}) collective-permute-start(bf16[32,544]{1,0:T(8,128)(2,1)S(1)} %shard_map.165.l0), channel_id=1, source_target_pairs={{0,2},{1,3},{2,0},{3,1},{4,6},{5,7},{6,4},{7,5},{8,10},{9,11},{10,... | collective-permute-start | bytes 104456 | tf_op jit(solution)/shard_map/ppermute | solution.py:61
  131.4 4.0 %collective-permute-start.10 = (bf16[32,544]{1,0:T(8,128)(2,1)S(1)}, bf16[32,544]{1,0:T(8,128)(2,1)S(1)}, u32[]{:S(2)}, u32[]{:S(2)}) collective-permute-start(bf16[32,544]{1,0:T(8,128)(2,1)S(1)} %shard_map.165.l0), channel_id=1, source_target_pairs={{0,3},{1,0},{2,1},{3,2},{4,7},{5,4},{6,5},{7,6},{8,11},{9,8},{10,9... | collective-permute-start | bytes 104456 | tf_op jit(solution)/shard_map/ppermute | solution.py:61
  136.9 18.0 %collective-permute-start.11 = (bf16[256,128]{1,0:T(8,128)(2,1)S(1)}, bf16[256,128]{1,0:T(8,128)(2,1)S(1)}, u32[]{:S(2)}, u32[]{:S(2)}) collective-permute-start(bf16[256,128]{1,0:T(8,128)(2,1)S(1)} %get-tuple-element.21), channel_id=1, source_target_pairs={{0,64},{64,128},{128,192},{192,0},{1,65},{65,129},{129,193},{193,1... | collective-permute-start | bytes 196616 | tf_op jit(solution)/shard_map/ppermute | solution.py:61
  138.1 16.7 %collective-permute-start.12 = (bf16[256,128]{1,0:T(8,128)(2,1)S(1)}, bf16[256,128]{1,0:T(8,128)(2,1)S(1)}, u32[]{:S(2)}, u32[]{:S(2)}) collective-permute-start(bf16[256,128]{1,0:T(8,128)(2,1)S(1)} %get-tuple-element.22), channel_id=1, source_target_pairs={{0,128},{64,192},{128,0},{192,64},{1,129},{65,193},{129,1},{193,65... | collective-permute-start | bytes 196616 | tf_op jit(solution)/shard_map/ppermute | solution.py:61
  142.8 13.3 %collective-permute-start.13 = (bf16[256,128]{1,0:T(8,128)(2,1)S(1)}, bf16[256,128]{1,0:T(8,128)(2,1)S(1)}, u32[]{:S(2)}, u32[]{:S(2)}) collective-permute-start(bf16[256,128]{1,0:T(8,128)(2,1)S(1)} %get-tuple-element.23), channel_id=1, source_target_pairs={{0,192},{64,0},{128,64},{192,128},{1,193},{65,1},{129,65},{193,129... | collective-permute-start | bytes 196616 | tf_op jit(solution)/shard_map/ppermute | solution.py:61
  156.1 6.5 %collective-permute-start.14 = (bf16[4,160,128]{2,1,0:T(8,128)(2,1)S(1)}, bf16[4,160,128]{2,1,0:T(8,128)(2,1)S(1)}, u32[]{:S(2)}, u32[]{:S(2)}) collective-permute-start(bf16[4,160,128]{2,1,0:T(8,128)(2,1)S(1)} %shard_map.167), channel_id=1, source_target_pairs={{0,32},{32,0},{1,33},{33,1},{2,34},{34,2},{3,35},{35,3},{4,36},{36... | collective-permute-start | bytes 491528 | tf_op jit(solution)/shard_map/ppermute | solution.py:61
  162.7 10.6 %collective-permute-start.15 = (bf16[4,160,256]{2,1,0:T(8,128)(2,1)S(1)}, bf16[4,160,256]{2,1,0:T(8,128)(2,1)S(1)}, u32[]{:S(2)}, u32[]{:S(2)}) collective-permute-start(bf16[4,160,256]{2,1,0:T(8,128)(2,1)S(1)} %pad_maximum_fusion.refs_0_), channel_id=1, source_target_pairs={{0,8},{8,16},{16,24},{24,0},{1,9},{9,17},{17,25},{25,1},{2,10},{10... | collective-permute-start | bytes 983048 | tf_op jit(solution)/shard_map/ppermute | solution.py:61
  164.3 16.7 %collective-permute-start.16 = (bf16[4,160,256]{2,1,0:T(8,128)(2,1)S(1)}, bf16[4,160,256]{2,1,0:T(8,128)(2,1)S(1)}, u32[]{:S(2)}, u32[]{:S(2)}) collective-permute-start(bf16[4,160,256]{2,1,0:T(8,128)(2,1)S(1)} %pad_maximum_fusion.refs_0_), channel_id=1, source_target_pairs={{0,16},{8,24},{16,0},{24,8},{1,17},{9,25},{17,1},{25,9},{2,18},{10... | collective-permute-start | bytes 983048 | tf_op jit(solution)/shard_map/ppermute | solution.py:61
  167.1 13.9 %collective-permute-start.17 = (bf16[4,160,256]{2,1,0:T(8,128)(2,1)S(1)}, bf16[4,160,256]{2,1,0:T(8,128)(2,1)S(1)}, u32[]{:S(2)}, u32[]{:S(2)}) collective-permute-start(bf16[4,160,256]{2,1,0:T(8,128)(2,1)S(1)} %pad_maximum_fusion.refs_0_), channel_id=1, source_target_pairs={{0,24},{8,0},{16,8},{24,16},{1,25},{9,1},{17,9},{25,17},{2,26},{10... | collective-permute-start | bytes 983048 | tf_op jit(solution)/shard_map/ppermute | solution.py:61
  168.5 13.0 %collective-permute-start.18 = (bf16[4,160,256]{2,1,0:T(8,128)(2,1)S(1)}, bf16[4,160,256]{2,1,0:T(8,128)(2,1)S(1)}, u32[]{:S(2)}, u32[]{:S(2)}) collective-permute-start(bf16[4,160,256]{2,1,0:T(8,128)(2,1)S(1)} %pad_maximum_fusion.refs_0_), channel_id=1, source_target_pairs={{0,4},{4,0},{1,5},{5,1},{2,6},{6,2},{3,7},{7,3},{8,12},{12,8},{9,1... | collective-permute-start | bytes 983048 | tf_op jit(solution)/shard_map/ppermute | solution.py:61
  173.2 8.2 %collective-permute-start.19 = (bf16[4,160,256]{2,1,0:T(8,128)(2,1)S(1)}, bf16[4,160,256]{2,1,0:T(8,128)(2,1)S(1)}, u32[]{:S(2)}, u32[]{:S(2)}) collective-permute-start(bf16[4,160,256]{2,1,0:T(8,128)(2,1)S(1)} %collective-permute-done.15.refs_1_), channel_id=1, source_target_pairs={{0,4},{4,0},{1,5},{5,1},{2,6},{6,2},{3,7},{7,3},{8,12},{12,8},{9,1... | collective-permute-start | bytes 983048 | tf_op jit(solution)/shard_map/ppermute | solution.py:61
  180.9 1.6 collective-permute-start.20
  181.0 2.1 collective-permute-start.21
  188.9 5.2 %collective-permute-start.22 = (bf16[128,64]{1,0:T(8,128)(2,1)S(1)}, bf16[128,64]{1,0:T(8,128)(2,1)S(1)}, u32[]{:S(2)}, u32[]{:S(2)}) collective-permute-start(bf16[128,64]{1,0:T(8,128)(2,1)S(1)} %get-tuple-element.25), channel_id=1, source_target_pairs={{0,1},{1,2},{2,3},{3,0},{4,5},{5,6},{6,7},{7,4},{8,9},{9,10},{10,1... | collective-permute-start | bytes 49160 | tf_op jit(solution)/shard_map/ppermute | solution.py:61
  189.2 6.2 %collective-permute-start.23 = (bf16[128,64]{1,0:T(8,128)(2,1)S(1)}, bf16[128,64]{1,0:T(8,128)(2,1)S(1)}, u32[]{:S(2)}, u32[]{:S(2)}) collective-permute-start(bf16[128,64]{1,0:T(8,128)(2,1)S(1)} %get-tuple-element.26), channel_id=1, source_target_pairs={{0,2},{1,3},{2,0},{3,1},{4,6},{5,7},{6,4},{7,5},{8,10},{9,11},{10,... | collective-permute-start | bytes 49160 | tf_op jit(solution)/shard_map/ppermute | solution.py:61
  193.2 3.9 %collective-permute-start.24 = (bf16[128,64]{1,0:T(8,128)(2,1)S(1)}, bf16[128,64]{1,0:T(8,128)(2,1)S(1)}, u32[]{:S(2)}, u32[]{:S(2)}) collective-permute-start(bf16[128,64]{1,0:T(8,128)(2,1)S(1)} %get-tuple-element.27), channel_id=1, source_target_pairs={{0,3},{1,0},{2,1},{3,2},{4,7},{5,4},{6,5},{7,6},{8,11},{9,8},{10,9... | collective-permute-start | bytes 49160 | tf_op jit(solution)/shard_map/ppermute | solution.py:61
  197.7 6.4 %collective-permute-start.25 = (bf16[32,256]{1,0:T(8,128)(2,1)S(1)}, bf16[32,256]{1,0:T(8,128)(2,1)S(1)}, u32[]{:S(2)}, u32[]{:S(2)}) collective-permute-start(bf16[32,256]{1,0:T(8,128)(2,1)S(1)} %get-tuple-element.29), channel_id=1, source_target_pairs={{0,64},{64,128},{128,192},{192,0},{1,65},{65,129},{129,193},{193,1... | collective-permute-start | bytes 49160 | tf_op jit(solution)/shard_map/ppermute | solution.py:61
  199.0 7.6 %collective-permute-start.26 = (bf16[32,256]{1,0:T(8,128)(2,1)S(1)}, bf16[32,256]{1,0:T(8,128)(2,1)S(1)}, u32[]{:S(2)}, u32[]{:S(2)}) collective-permute-start(bf16[32,256]{1,0:T(8,128)(2,1)S(1)} %get-tuple-element.30), channel_id=1, source_target_pairs={{0,128},{64,192},{128,0},{192,64},{1,129},{65,193},{129,1},{193,65... | collective-permute-start | bytes 49160 | tf_op jit(solution)/shard_map/ppermute | solution.py:61
  201.3 5.8 %collective-permute-start.27 = (bf16[32,256]{1,0:T(8,128)(2,1)S(1)}, bf16[32,256]{1,0:T(8,128)(2,1)S(1)}, u32[]{:S(2)}, u32[]{:S(2)}) collective-permute-start(bf16[32,256]{1,0:T(8,128)(2,1)S(1)} %get-tuple-element.31), channel_id=1, source_target_pairs={{0,192},{64,0},{128,64},{192,128},{1,193},{65,1},{129,65},{193,129... | collective-permute-start | bytes 49160 | tf_op jit(solution)/shard_map/ppermute | solution.py:61
